TPU v7x, 256 devices: a whole 4x4x8 slice. The times are simulated.
256 devices in a mesh: gr: 2 (over z_hi), sp: 16 (over z_lo, y), tp: 8 (over x, core).
Axes of the slice: x: 4, y: 4, z: 8 (z_hi: 2, z_lo: 4; z = z_hi * 4 + z_lo), core: 2. Of those that a mesh axis runs over, the one named last changes fastest.
Arguments:
- prompt: bfloat16 [256, 256, 1024], P('gr', 'sp'), parts along dimension 0, may hold values from -6 to 6
- w_key: bfloat16 [1024, 8, 128], P(None, 'tp'), may hold values from -0.1875 to 0.1875
- w_value: bfloat16 [1024, 8, 128], P(None, 'tp'), may hold values from -0.1875 to 0.1875
- w_in_gate: bfloat16 [2, 1024, 8], P(None, None, 'tp'), may hold values from -0.1875 to 0.1875
- w_forget_gate: bfloat16 [2, 1024, 8], P(None, None, 'tp'), may hold values from -0.1875 to 0.1875
- in_bias: float32 [2, 8], P(None, 'tp'), may hold values from -6 to 0, as said below
- forget_bias: float32 [2, 8], P(None, 'tp'), may hold values from 1 to 10, as said below
- query: bfloat16 [256, 8, 128], P(('gr', 'sp'), 'tp'), parts along dimension 0, may hold values from -6 to 6
- w_out: bfloat16 [8, 128, 1024], P('tp'), may hold values from -0.5 to 0.5
Outputs:
- memory: bfloat16 [2, 256, 8, 128, 128], P(None, ('gr', 'sp'), 'tp'), parts along dimension 1
- normalizer: float32 [2, 256, 8, 128], P(None, ('gr', 'sp'), 'tp'), parts along dimension 1
- stabilizer: float32 [2, 256, 8], P(None, ('gr', 'sp'), 'tp'), parts along dimension 1
- read: bfloat16 [256, 1024], P(('gr', 'sp'), 'tp'), parts along dimension 0
There are 2 independent parts, one for each index of `gr`. A program takes and returns all parts, laid end to end along the dimension named above; an argument that names none is the same for every part. Nothing has to cross between parts.
Inputs may be any that keep to these rules, and one draw needn't show every extreme that they name: forget_bias lies between 1 and 10; the per-head share of memory kept over the whole prompt is spread between a few and some ninety percent. in_bias lies between -6 and 0.
All inputs are finite; a program needn't handle non-finite values.
Results may differ from a plain program's by a relative error of at most 0.015.
Values may be sent and summed in bfloat16 or wider, within the bound.
No kernel may reach another device: no remote copies, remote signals or barrier semaphores. Data moves between devices by JAX's collectives and lax.ppermute only.
A program may use at most 64 MiB of HBM per device.

v0:
```python
import jax
import jax.numpy as jnp
from jax import lax
from jax.experimental import pallas as pl
from jax.experimental.pallas import tpu as pltpu
from jax.sharding import Mesh
from jax.sharding import PartitionSpec as P


TP = ("tp_0", "tp_1")
BF = jnp.bfloat16
F32 = jnp.float32
SP = 16
TPN = 8
OWN = 8
POS = 16
ROWS = OWN * POS
HD = 128
D = 1024
SEND = 2 * ROWS + 8
ROW = 4


def dot(a, b, dims=((1,), (0,))):
    return lax.dot_general(a, b, (dims, ((), ())), preferred_element_type=F32)


def here():
    at = lax.axis_index("sp")
    return at // ROW, at % ROW


def take(x_ref, buf_ref, sem_ref, blocks):
    z, y = here()
    copies = []
    for i, (dz, dy) in enumerate(blocks):
        dest = ((z + dz) % ROW) * ROW + (y + dy) % ROW
        copies.append(pltpu.make_async_copy(x_ref.at[pl.ds(dest * OWN, OWN)], buf_ref.at[i], sem_ref.at[i]))
    for copy in copies:
        copy.start()
    return copies


def project_blocks(buf_ref, first, w, gates, outs):
    rows = buf_ref[first : first + ROW].reshape(ROW * ROWS, D)
    both = dot(rows, w).astype(BF)
    pre = dot(gates, rows, ((1,), (1,)))[:4]
    high = pre.astype(BF).astype(F32)
    coded = jnp.concatenate((high, pre - high), axis=0).astype(BF)
    for k, out in enumerate(outs):
        at = slice(k * ROWS, (k + 1) * ROWS)
        out[:ROWS, :] = both[at, :HD]
        out[ROWS : 2 * ROWS, :] = both[at, HD:]
        out[2 * ROWS :, :] = coded[:, at]


def near_kernel(x_ref, wk_ref, wv_ref, wi_ref, wf_ref, up_ref, down_ref, w_ref, g_ref, buf_ref, sem_ref):
    copies = take(x_ref, buf_ref, sem_ref, [(dz, dy) for dz in (1, 3) for dy in range(ROW)])
    w_ref[:, :HD] = wk_ref[...]
    w_ref[:, HD:] = wv_ref[...]
    gates = jnp.concatenate((wi_ref[...].astype(F32), wf_ref[...].astype(F32), jnp.zeros((4, D), F32)), axis=0)
    g_ref[...] = gates.astype(BF)
    for half, out_ref in enumerate((up_ref, down_ref)):
        for copy in copies[half * ROW : (half + 1) * ROW]:
            copy.wait()
        project_blocks(buf_ref, half * ROW, w_ref[...], g_ref[...], [out_ref.at[k] for k in range(ROW)])


def far_kernel(x_ref, w_ref, g_ref, *refs):
    outs, (buf_ref, sem_ref) = refs[:ROW], refs[ROW:]
    for copy in take(x_ref, buf_ref, sem_ref, [(2, dy) for dy in range(ROW)]):
        copy.wait()
    project_blocks(buf_ref, 0, w_ref[...], g_ref[...], outs)


def own_kernel(x_ref, w_ref, g_ref, out_ref, buf_ref, sem_ref):
    for copy in take(x_ref, buf_ref, sem_ref, [(0, dy) for dy in range(ROW)]):
        copy.wait()
    project_blocks(buf_ref, 0, w_ref[...], g_ref[...], [out_ref.at[k] for k in range(ROW)])


ANY = pl.BlockSpec(memory_space=pl.ANY)
VM = pl.BlockSpec(memory_space=pltpu.VMEM)


def scratch(blocks):
    return [pltpu.VMEM((blocks, OWN, POS, D), BF), pltpu.SemaphoreType.DMA((blocks,))]


def block(*lead):
    return jax.ShapeDtypeStruct((*lead, SEND, HD), BF)


def project_near(*args):
    return pl.pallas_call(
        near_kernel,
        in_specs=[ANY, VM, VM, VM, VM],
        out_shape=(block(ROW), block(ROW), jax.ShapeDtypeStruct((D, 2 * HD), BF), jax.ShapeDtypeStruct((8, D), BF)),
        scratch_shapes=scratch(2 * ROW),
        name="near",
    )(*args)


def project_far(*args):
    return pl.pallas_call(
        far_kernel, in_specs=[ANY, VM, VM], out_shape=(block(),) * ROW, scratch_shapes=scratch(ROW), name="far"
    )(*args)


def project_own(*args):
    return pl.pallas_call(
        own_kernel, in_specs=[ANY, VM, VM], out_shape=block(ROW), scratch_shapes=scratch(ROW), name="own"
    )(*args)


def stack_kernel(a_ref, b_ref, c_ref, *outs):
    for k, out in enumerate(outs):
        for i, ref in enumerate((a_ref, b_ref, c_ref)):
            out[i] = ref[k + 1]


def stack(*args):
    return pl.pallas_call(stack_kernel, out_shape=(block(3),) * 3, name="stack")(*args)


def three_parts(a):
    first = a.astype(BF)
    rest = a - first.astype(F32)
    second = rest.astype(BF)
    return first, second, (rest - second.astype(F32)).astype(BF)


def group_max(a, lane):
    for k in (1, 2, 4, 8):
        inside = (lane % POS) + k < POS
        a = jnp.maximum(a, jnp.where(inside, pltpu.roll(a, HD - k, 1), pltpu.roll(a, POS - k, 1)))
    return a


def log_sigmoid(a):
    return jnp.minimum(a, 0.0) - jnp.log1p(jnp.exp(-jnp.abs(a)))


def memory_kernel(own_ref, up_ref, down_ref, y1_ref, y2_ref, y3_ref, f0_ref, f1_ref, f2_ref, f3_ref,
                  q_ref, wo_ref, ib_ref, fb_ref, mem_ref, norm_ref, stab_ref, term_ref, vw_ref, recv_ref):
    for i, (dz, ref) in enumerate(((0, own_ref), (1, up_ref), (3, down_ref))):
        recv_ref[dz * ROW] = ref[0]
        for dy, far_ref in ((1, y1_ref), (2, y2_ref), (3, y3_ref)):
            recv_ref[dz * ROW + dy] = far_ref[i]
    for dy, ref in enumerate((f0_ref, f1_ref, f2_ref, f3_ref)):
        recv_ref[2 * ROW + dy] = ref[...]
    z, y = here()
    place = lambda j: ((z - j // ROW) & 3) * ROW + ((y - j % ROW) & 3)
    scale = HD ** -0.5
    gates = recv_ref[:, 2 * ROWS :, :].astype(F32)
    part = lambda c: gates[:, c, :] + gates[:, c + 4, :]
    in_pre = [part(g) + ib_ref[0:1, g : g + 1] for g in range(2)]
    forget = [log_sigmoid(part(2 + g) + fb_ref[0:1, g : g + 1]) for g in range(2)]

    r = lax.broadcasted_iota(jnp.int32, (HD, HD), 0)
    c = lax.broadcasted_iota(jnp.int32, (HD, HD), 1)
    same = (r // POS) == (c // POS)
    ones = lambda m: jnp.where(m, 1.0, 0.0).astype(BF)
    jr = lax.broadcasted_iota(jnp.int32, (2 * SP, SP), 0)
    jc = lax.broadcasted_iota(jnp.int32, (2 * SP, SP), 1)
    lane = lax.broadcasted_iota(jnp.int32, (1, HD), 1)
    log_weight = []
    total = []
    for g in range(2):
        order = (r > c) if g == 0 else (r < c)
        inside = jnp.concatenate((ones(same & order), ones(same)), axis=1)
        sums = sum(dot(p, inside) for p in three_parts(forget[g]))
        block = sums[:, HD:]
        across = ones(((place(jc) > place(jr)) if g == 0 else (place(jc) < place(jr))) | (jr >= SP))
        outside = sum(dot(across, p) for p in three_parts(block))
        log_weight.append(in_pre[g] + sums[:, :HD] + outside[:SP])
        total.append(outside[SP : SP + 1])
    stab = [
        jnp.maximum(total[g], group_max(jnp.max(log_weight[g], axis=0, keepdims=True), lane)) for g in range(2)
    ]
    weight = [jnp.exp(log_weight[g] - stab[g]) for g in range(2)]

    row8 = lax.broadcasted_iota(jnp.int32, (OWN, HD), 0)
    lane8 = lax.broadcasted_iota(jnp.int32, (OWN, HD), 1)
    mine = (lane8 // POS) == row8
    norm = jnp.zeros((4 * OWN, HD), F32)
    for j in range(SP):
        spread = jnp.concatenate([jnp.where(mine, weight[g][j : j + 1], 0.0) for g in range(2)], axis=0)
        high = spread.astype(BF)
        low = (spread - high.astype(F32)).astype(BF)
        norm += dot(jnp.concatenate((high, low), axis=0), recv_ref[j, :ROWS, :])
    norm = (norm[: 2 * OWN] + norm[2 * OWN :]) * scale
    norm_ref[...] = norm

    turned = jnp.concatenate(weight, axis=0).T
    for j in range(SP):
        value = recv_ref[j, ROWS : 2 * ROWS, :].astype(F32)
        for g in range(2):
            k = g * SP + j
            vw_ref[j, :, g * HD : (g + 1) * HD] = (value * turned[:, k : k + 1]).astype(BF)

    query = q_ref[...]
    row16 = lax.broadcasted_iota(jnp.int32, (OWN, 2 * HD), 0)
    numerator = jnp.zeros((OWN, 2 * HD), F32)
    for s in range(OWN):
        at = slice(s * POS, (s + 1) * POS)
        keys = recv_ref[:, at, :].reshape(SP * POS, HD)
        values = vw_ref[:, at, :].reshape(SP * POS, 2 * HD)
        memory = (dot(keys, values, ((0,), (0,))) * scale).astype(BF)
        mem_ref[0, s] = memory[:, :HD]
        mem_ref[1, s] = memory[:, HD:]
        numerator = jnp.where(row16 == s, dot(query, memory), numerator)

    query_f = query.astype(F32)
    hidden = jnp.zeros((OWN, HD), F32)
    for g in range(2):
        column = jnp.max(jnp.where(mine, stab[g], -jnp.inf), axis=1, keepdims=True)
        stab_ref[g] = jnp.sum(jnp.where(lane8 == row8, column, 0.0), axis=0, keepdims=True)[:, :OWN]
        denominator = jnp.sum(query_f * norm[g * OWN : (g + 1) * OWN], axis=1, keepdims=True)
        floor = jnp.maximum(jnp.maximum(jnp.abs(denominator), jnp.exp(-column)), 1.0)
        hidden += numerator[:, g * HD : (g + 1) * HD] / floor
    hidden = hidden.astype(BF)
    for t in range(TPN):
        term_ref[t] = dot(hidden, wo_ref[:, t * HD : (t + 1) * HD])


def memories(own, up, down, *rest):
    first = pl.BlockSpec((1, SEND, HD), lambda i: (0, 0, 0))
    return pl.pallas_call(
        memory_kernel,
        grid=(1,),
        in_specs=[first] * 3 + [VM] * len(rest),
        out_shape=(
            jax.ShapeDtypeStruct((2, OWN, HD, HD), BF),
            jax.ShapeDtypeStruct((2 * OWN, HD), F32),
            jax.ShapeDtypeStruct((2, 1, OWN), F32),
            jax.ShapeDtypeStruct((TPN, OWN, HD), F32),
        ),
        scratch_shapes=[pltpu.VMEM((SP, ROWS, 2 * HD), BF), pltpu.VMEM((SP, SEND, HD), BF)],
        name="memories",
    )(own, up, down, *rest)


def shift(array, dz, dy):
    spots = [(z, y) for z in range(ROW) for y in range(ROW)]
    pairs = [(z * ROW + y, ((z + dz) % ROW) * ROW + (y + dy) % ROW) for z, y in spots]
    return lax.ppermute(array, "sp", pairs)


def step(prompt, w_key, w_value, w_in_gate, w_forget_gate, in_bias, forget_bias, query, w_out):
    up, down, w, gates = project_near(
        prompt, w_key.reshape(D, HD), w_value.reshape(D, HD), w_in_gate.reshape(2, D), w_forget_gate.reshape(2, D)
    )
    up = shift(up, 1, 0)
    down = shift(down, 3, 0)
    far = project_far(prompt, w, gates)
    far = [shift(block, 2, dy) for dy, block in enumerate(far)]
    own = project_own(prompt, w, gates)
    aside = stack(own, up, down)
    aside = [shift(blocks, 0, dy + 1) for dy, blocks in enumerate(aside)]
    memory, norm, stab, terms = memories(
        own, up, down, *aside, *far,
        query.reshape(OWN, HD), w_out.reshape(HD, D), in_bias.reshape(1, 2), forget_bias.reshape(1, 2),
    )
    terms = lax.all_to_all(terms, TP, 0, 0, tiled=True)
    read = jnp.sum(terms, axis=0).astype(BF)
    return (
        memory.reshape(2, OWN, 1, HD, HD),
        norm.reshape(2, OWN, 1, HD),
        stab.reshape(2, OWN, 1),
        read,
    )


def solution(mesh):
    torus = Mesh(
        mesh.devices.reshape(mesh.shape["gr"], mesh.shape["sp"], 4, 2), ("gr", "sp", "tp_0", "tp_1")
    )
    return jax.shard_map(
        step,
        mesh=torus,
        in_specs=(
            P("gr", "sp", None),
            P(None, TP, None),
            P(None, TP, None),
            P(None, None, TP),
            P(None, None, TP),
            P(None, TP),
            P(None, TP),
            P(("gr", "sp"), TP, None),
            P(TP, None, None),
        ),
        out_specs=(
            P(None, ("gr", "sp"), TP, None, None),
            P(None, ("gr", "sp"), TP, None),
            P(None, ("gr", "sp"), TP),
            P(("gr", "sp"), TP),
        ),
        check_vma=False,
    )
```

profile of v0, /device:TPU:1, one launch (start us, length us, event | category | flops | bytes accessed | tf_op | source)
XLA Modules:
  0.0 67.0 jit_solution(8747583458980102325)
XLA Ops:
  0.6 4.6 %near.1 = (bf16[4,264,128]{2,1,0:T(8,128)(2,1)}, bf16[4,264,128]{2,1,0:T(8,128)(2,1)}, bf16[1024,256]{1,0:T(8,128)(2,1)}, bf16[8,1024]{1,0:T(8,128)(2,1)}) custom-call(bf16[128,16,1024]{2,1,0:T(8,128)(2,1)} %x_ref.5, bf16[1024,128]{1,0:T(8,128)(2,1)} %bitcast.17, bf16[1024,128]{1,0:T(8,128)(2,1)} %bitcast.18, bf16[2,1024]{1,0:T(2,128)(2,1)} %bitcast.20, ...), custom_call_target="tpu_custom_call" | custom-call | tf_op jit(solution)/shard_map/near/pallas_call | solution.py:95
  5.3 2.5 %collective-permute-start = (bf16[4,264,128]{2,1,0:T(8,128)(2,1)}, bf16[4,264,128]{2,1,0:T(8,128)(2,1)S(1)}, u32[]{:S(2)}, u32[]{:S(2)}) collective-permute-start(bf16[4,264,128]{2,1,0:T(8,128)(2,1)} %get-tuple-element.21), channel_id=1, source_target_pairs={{0,32},{8,40},{16,48},{24,56},{32,64},{40,72},{48,80},{56,88},{64,... | collective-permute-start | bytes 811016 | tf_op jit(solution)/shard_map/ppermute | solution.py:247
  7.8 2.8 %collective-permute-start.1 = (bf16[4,264,128]{2,1,0:T(8,128)(2,1)}, bf16[4,264,128]{2,1,0:T(8,128)(2,1)S(1)}, u32[]{:S(2)}, u32[]{:S(2)}) collective-permute-start(bf16[4,264,128]{2,1,0:T(8,128)(2,1)} %get-tuple-element.22), channel_id=1, source_target_pairs={{0,96},{8,104},{16,112},{24,120},{32,0},{40,8},{48,16},{56,24},{64... | collective-permute-start | bytes 811016 | tf_op jit(solution)/shard_map/ppermute | solution.py:247
  10.6 3.7 %own.1.a_ref.own_ref = bf16[4,264,128]{2,1,0:T(8,128)(2,1)} custom-call(bf16[128,16,1024]{2,1,0:T(8,128)(2,1)} %x_ref.5, bf16[1024,256]{1,0:T(8,128)(2,1)} %get-tuple-element.19.w_ref, bf16[8,1024]{1,0:T(8,128)(2,1)} %get-tuple-element.20.g_ref), custom_call_target="tpu_custom_call" | custom-call | tf_op jit(solution)/shard_map/own/pallas_call | solution.py:111
  14.2 1.8 %collective-permute-done.b_ref.up_ref = bf16[4,264,128]{2,1,0:T(8,128)(2,1)S(1)} collective-permute-done((bf16[4,264,128]{2,1,0:T(8,128)(2,1)}, bf16[4,264,128]{2,1,0:T(8,128)(2,1)S(1)}, u32[]{:S(2)}, u32[]{:S(2)}) %collective-permute-start) | collective-permute-done | bytes 270368 | tf_op jit(solution)/shard_map/ppermute | solution.py:247
  16.0 5.3 %collective-permute-done.1.c_ref.down_ref = bf16[4,264,128]{2,1,0:T(8,128)(2,1)S(1)} collective-permute-done((bf16[4,264,128]{2,1,0:T(8,128)(2,1)}, bf16[4,264,128]{2,1,0:T(8,128)(2,1)S(1)}, u32[]{:S(2)}, u32[]{:S(2)}) %collective-permute-start.1) | collective-permute-done | bytes 270368 | tf_op jit(solution)/shard_map/ppermute | solution.py:247
  21.3 0.0 copy-done
  21.3 0.7 %copy-done.1 = bf16[4,264,128]{2,1,0:T(8,128)(2,1)} copy-done((bf16[4,264,128]{2,1,0:T(8,128)(2,1)}, bf16[4,264,128]{2,1,0:T(8,128)(2,1)S(1)}, u32[]{:S(2)}) %copy-start.1) | copy-done | bytes 270360
  22.0 2.0 %stack.1 = (bf16[3,264,128]{2,1,0:T(8,128)(2,1)}, bf16[3,264,128]{2,1,0:T(8,128)(2,1)}, bf16[3,264,128]{2,1,0:T(8,128)(2,1)}) custom-call(bf16[4,264,128]{2,1,0:T(8,128)(2,1)} %own.1.a_ref.own_ref, bf16[4,264,128]{2,1,0:T(8,128)(2,1)} %copy-done, bf16[4,264,128]{2,1,0:T(8,128)(2,1)} %copy-done.1), custom_call_target="tpu_custom_call" | custom-call | tf_op jit(solution)/shard_map/stack/pallas_call | solution.py:123
  24.0 1.3 %collective-permute-start.2 = (bf16[3,264,128]{2,1,0:T(8,128)(2,1)}, bf16[3,264,128]{2,1,0:T(8,128)(2,1)S(1)}, u32[]{:S(2)}, u32[]{:S(2)}) collective-permute-start(bf16[3,264,128]{2,1,0:T(8,128)(2,1)} %get-tuple-element.23), channel_id=1, source_target_pairs={{0,8},{8,16},{16,24},{24,0},{32,40},{40,48},{48,56},{56,32},{64,72... | collective-permute-start | bytes 608264 | tf_op jit(solution)/shard_map/ppermute | solution.py:247
  25.3 2.6 %collective-permute-start.3 = (bf16[3,264,128]{2,1,0:T(8,128)(2,1)}, bf16[3,264,128]{2,1,0:T(8,128)(2,1)S(1)}, u32[]{:S(2)}, u32[]{:S(2)}) collective-permute-start(bf16[3,264,128]{2,1,0:T(8,128)(2,1)} %get-tuple-element.24), channel_id=1, source_target_pairs={{0,16},{8,24},{16,0},{24,8},{32,48},{40,56},{48,32},{56,40},{64,80... | collective-permute-start | bytes 608264 | tf_op jit(solution)/shard_map/ppermute | solution.py:247
  27.9 1.1 %collective-permute-start.4 = (bf16[3,264,128]{2,1,0:T(8,128)(2,1)}, bf16[3,264,128]{2,1,0:T(8,128)(2,1)S(1)}, u32[]{:S(2)}, u32[]{:S(2)}) collective-permute-start(bf16[3,264,128]{2,1,0:T(8,128)(2,1)} %get-tuple-element.25), channel_id=1, source_target_pairs={{0,24},{8,0},{16,8},{24,16},{32,56},{40,32},{48,40},{56,48},{64,88... | collective-permute-start | bytes 608264 | tf_op jit(solution)/shard_map/ppermute | solution.py:247
  29.0 3.6 %far.1 = (bf16[264,128]{1,0:T(8,128)(2,1)}, bf16[264,128]{1,0:T(8,128)(2,1)}, bf16[264,128]{1,0:T(8,128)(2,1)}, bf16[264,128]{1,0:T(8,128)(2,1)}) custom-call(bf16[128,16,1024]{2,1,0:T(8,128)(2,1)} %x_ref.5, bf16[1024,256]{1,0:T(8,128)(2,1)} %get-tuple-element.19.w_ref, bf16[8,1024]{1,0:T(8,128)(2,1)} %get-tuple-element.20.g_ref), custom_call_target="tpu_custom_call" | custom-call | tf_op jit(solution)/shard_map/far/pallas_call | solution.py:105
  32.6 1.8 %collective-permute-start.5 = (bf16[264,128]{1,0:T(8,128)(2,1)}, bf16[264,128]{1,0:T(8,128)(2,1)S(1)}, u32[]{:S(2)}, u32[]{:S(2)}) collective-permute-start(bf16[264,128]{1,0:T(8,128)(2,1)} %get-tuple-element.26), channel_id=1, source_target_pairs={{0,64},{8,72},{16,80},{24,88},{32,96},{40,104},{48,112},{56,120},{... | collective-permute-start | bytes 202760 | tf_op jit(solution)/shard_map/ppermute | solution.py:247
  34.4 0.8 %collective-permute-start.6 = (bf16[264,128]{1,0:T(8,128)(2,1)}, bf16[264,128]{1,0:T(8,128)(2,1)S(1)}, u32[]{:S(2)}, u32[]{:S(2)}) collective-permute-start(bf16[264,128]{1,0:T(8,128)(2,1)} %get-tuple-element.27), channel_id=1, source_target_pairs={{0,72},{8,80},{16,88},{24,64},{32,104},{40,112},{48,120},{56,96},{... | collective-permute-start | bytes 202760 | tf_op jit(solution)/shard_map/ppermute | solution.py:247
  35.1 2.1 %collective-permute-done.5.f0_ref = bf16[264,128]{1,0:T(8,128)(2,1)S(1)} collective-permute-done((bf16[264,128]{1,0:T(8,128)(2,1)}, bf16[264,128]{1,0:T(8,128)(2,1)S(1)}, u32[]{:S(2)}, u32[]{:S(2)}) %collective-permute-start.5) | collective-permute-done | bytes 67616 | tf_op jit(solution)/shard_map/ppermute | solution.py:247
  37.2 1.5 %collective-permute-start.7 = (bf16[264,128]{1,0:T(8,128)(2,1)}, bf16[264,128]{1,0:T(8,128)(2,1)S(1)}, u32[]{:S(2)}, u32[]{:S(2)}) collective-permute-start(bf16[264,128]{1,0:T(8,128)(2,1)} %get-tuple-element.28), channel_id=1, source_target_pairs={{0,80},{8,88},{16,64},{24,72},{32,112},{40,120},{48,96},{56,104},{... | collective-permute-start | bytes 202760 | tf_op jit(solution)/shard_map/ppermute | solution.py:247
  38.7 3.0 %collective-permute-done.6.f1_ref = bf16[264,128]{1,0:T(8,128)(2,1)S(1)} collective-permute-done((bf16[264,128]{1,0:T(8,128)(2,1)}, bf16[264,128]{1,0:T(8,128)(2,1)S(1)}, u32[]{:S(2)}, u32[]{:S(2)}) %collective-permute-start.6) | collective-permute-done | bytes 67616 | tf_op jit(solution)/shard_map/ppermute | solution.py:247
  41.7 0.0 collective-permute-start.8
  41.8 3.1 %collective-permute-done.7.f2_ref = bf16[264,128]{1,0:T(8,128)(2,1)S(1)} collective-permute-done((bf16[264,128]{1,0:T(8,128)(2,1)}, bf16[264,128]{1,0:T(8,128)(2,1)S(1)}, u32[]{:S(2)}, u32[]{:S(2)}) %collective-permute-start.7) | collective-permute-done | bytes 67616 | tf_op jit(solution)/shard_map/ppermute | solution.py:247
  44.9 2.3 %collective-permute-done.8.f3_ref = bf16[264,128]{1,0:T(8,128)(2,1)S(1)} collective-permute-done((bf16[264,128]{1,0:T(8,128)(2,1)}, bf16[264,128]{1,0:T(8,128)(2,1)S(1)}, u32[]{:S(2)}, u32[]{:S(2)}) %collective-permute-start.8) | collective-permute-done | bytes 67616 | tf_op jit(solution)/shard_map/ppermute | solution.py:247
  47.2 0.0 collective-permute-done.2.y1_ref
  47.2 0.0 collective-permute-done.3.y2_ref
  47.2 0.0 copy-start.3
  47.2 0.0 collective-permute-done.4.y3_ref
  47.3 0.5 copy-done.8
  47.8 0.1 copy-done.2
  47.9 0.1 copy-done.3
  48.0 0.1 copy-done.4
  48.1 4.7 %memories.1 = (bf16[2,8,128,128]{3,2,1,0:T(8,128)(2,1)}, f32[16,128]{1,0:T(8,128)}, f32[2,1,8]{2,1,0:T(1,128)}, f32[8,8,128]{2,1,0:T(8,128)}) custom-call(bf16[4,264,128]{2,1,0:T(8,128)(2,1)} %own.1.a_ref.own_ref, bf16[4,264,128]{2,1,0:T(8,128)(2,1)} %copy-done, bf16[4,264,128]{2,1,0:T(8,128)(2,1)} %copy-done.1, bf16[3,264,128]{2,1,0:T(8,128)(2,1)} %copy-done.2, ...), custom_call_target="tpu_custom_call" | custom-call | tf_op jit(solution)/shard_map/memories/pallas_call | solution.py:229
  52.8 13.7 %all_to_all.5 = f32[8,8,128]{2,1,0:T(8,128)S(1)} all-to-all(f32[8,8,128]{2,1,0:T(8,128)} %get-tuple-element.33), channel_id=1, replica_groups=mesh['gr'=2,'sp'=16,'tp_0'=4,'tp_1'=2] {'tp_0','tp_1'}, dimensions={0} | all-to-all | bytes 65536 | tf_op jit(solution)/shard_map/all_to_all | solution.py:265
  66.5 0.6 reduce_sum.9
  (11 shorter events, 0.0 us)
Async XLA Ops:
  5.3 10.8 %collective-permute-start = (bf16[4,264,128]{2,1,0:T(8,128)(2,1)}, bf16[4,264,128]{2,1,0:T(8,128)(2,1)S(1)}, u32[]{:S(2)}, u32[]{:S(2)}) collective-permute-start(bf16[4,264,128]{2,1,0:T(8,128)(2,1)} %get-tuple-element.21), channel_id=1, source_target_pairs={{0,32},{8,40},{16,48},{24,56},{32,64},{40,72},{48,80},{56,88},{64,... | collective-permute-start | bytes 811016 | tf_op jit(solution)/shard_map/ppermute | solution.py:247
  7.8 13.5 %collective-permute-start.1 = (bf16[4,264,128]{2,1,0:T(8,128)(2,1)}, bf16[4,264,128]{2,1,0:T(8,128)(2,1)S(1)}, u32[]{:S(2)}, u32[]{:S(2)}) collective-permute-start(bf16[4,264,128]{2,1,0:T(8,128)(2,1)} %get-tuple-element.22), channel_id=1, source_target_pairs={{0,96},{8,104},{16,112},{24,120},{32,0},{40,8},{48,16},{56,24},{64... | collective-permute-start | bytes 811016 | tf_op jit(solution)/shard_map/ppermute | solution.py:247
  16.0 5.3 %copy-start = (bf16[4,264,128]{2,1,0:T(8,128)(2,1)}, bf16[4,264,128]{2,1,0:T(8,128)(2,1)S(1)}, u32[]{:S(2)}) copy-start(bf16[4,264,128]{2,1,0:T(8,128)(2,1)S(1)} %collective-permute-done.b_ref.up_ref) | copy-start | bytes 811012
  21.3 0.7 %copy-start.1 = (bf16[4,264,128]{2,1,0:T(8,128)(2,1)}, bf16[4,264,128]{2,1,0:T(8,128)(2,1)S(1)}, u32[]{:S(2)}) copy-start(bf16[4,264,128]{2,1,0:T(8,128)(2,1)S(1)} %collective-permute-done.1.c_ref.down_ref) | copy-start | bytes 811012
  24.0 23.2 %collective-permute-start.2 = (bf16[3,264,128]{2,1,0:T(8,128)(2,1)}, bf16[3,264,128]{2,1,0:T(8,128)(2,1)S(1)}, u32[]{:S(2)}, u32[]{:S(2)}) collective-permute-start(bf16[3,264,128]{2,1,0:T(8,128)(2,1)} %get-tuple-element.23), channel_id=1, source_target_pairs={{0,8},{8,16},{16,24},{24,0},{32,40},{40,48},{48,56},{56,32},{64,72... | collective-permute-start | bytes 608264 | tf_op jit(solution)/shard_map/ppermute | solution.py:247
  25.3 21.9 %collective-permute-start.3 = (bf16[3,264,128]{2,1,0:T(8,128)(2,1)}, bf16[3,264,128]{2,1,0:T(8,128)(2,1)S(1)}, u32[]{:S(2)}, u32[]{:S(2)}) collective-permute-start(bf16[3,264,128]{2,1,0:T(8,128)(2,1)} %get-tuple-element.24), channel_id=1, source_target_pairs={{0,16},{8,24},{16,0},{24,8},{32,48},{40,56},{48,32},{56,40},{64,80... | collective-permute-start | bytes 608264 | tf_op jit(solution)/shard_map/ppermute | solution.py:247
  27.9 19.3 %collective-permute-start.4 = (bf16[3,264,128]{2,1,0:T(8,128)(2,1)}, bf16[3,264,128]{2,1,0:T(8,128)(2,1)S(1)}, u32[]{:S(2)}, u32[]{:S(2)}) collective-permute-start(bf16[3,264,128]{2,1,0:T(8,128)(2,1)} %get-tuple-element.25), channel_id=1, source_target_pairs={{0,24},{8,0},{16,8},{24,16},{32,56},{40,32},{48,40},{56,48},{64,88... | collective-permute-start | bytes 608264 | tf_op jit(solution)/shard_map/ppermute | solution.py:247
  32.6 4.6 %collective-permute-start.5 = (bf16[264,128]{1,0:T(8,128)(2,1)}, bf16[264,128]{1,0:T(8,128)(2,1)S(1)}, u32[]{:S(2)}, u32[]{:S(2)}) collective-permute-start(bf16[264,128]{1,0:T(8,128)(2,1)} %get-tuple-element.26), channel_id=1, source_target_pairs={{0,64},{8,72},{16,80},{24,88},{32,96},{40,104},{48,112},{56,120},{... | collective-permute-start | bytes 202760 | tf_op jit(solution)/shard_map/ppermute | solution.py:247
  34.4 7.4 %collective-permute-start.6 = (bf16[264,128]{1,0:T(8,128)(2,1)}, bf16[264,128]{1,0:T(8,128)(2,1)S(1)}, u32[]{:S(2)}, u32[]{:S(2)}) collective-permute-start(bf16[264,128]{1,0:T(8,128)(2,1)} %get-tuple-element.27), channel_id=1, source_target_pairs={{0,72},{8,80},{16,88},{24,64},{32,104},{40,112},{48,120},{56,96},{... | collective-permute-start | bytes 202760 | tf_op jit(solution)/shard_map/ppermute | solution.py:247
  37.2 10.1 %copy-start.5 = (bf16[264,128]{1,0:T(8,128)(2,1)}, bf16[264,128]{1,0:T(8,128)(2,1)S(1)}, u32[]{:S(2)}) copy-start(bf16[264,128]{1,0:T(8,128)(2,1)S(1)} %collective-permute-done.5.f0_ref) | copy-start | bytes 202756
  37.2 7.7 %collective-permute-start.7 = (bf16[264,128]{1,0:T(8,128)(2,1)}, bf16[264,128]{1,0:T(8,128)(2,1)S(1)}, u32[]{:S(2)}, u32[]{:S(2)}) collective-permute-start(bf16[264,128]{1,0:T(8,128)(2,1)} %get-tuple-element.28), channel_id=1, source_target_pairs={{0,80},{8,88},{16,64},{24,72},{32,112},{40,120},{48,96},{56,104},{... | collective-permute-start | bytes 202760 | tf_op jit(solution)/shard_map/ppermute | solution.py:247
  41.7 5.5 %copy-start.6 = (bf16[264,128]{1,0:T(8,128)(2,1)}, bf16[264,128]{1,0:T(8,128)(2,1)S(1)}, u32[]{:S(2)}) copy-start(bf16[264,128]{1,0:T(8,128)(2,1)S(1)} %collective-permute-done.6.f1_ref) | copy-start | bytes 202756
  41.7 5.5 %collective-permute-start.8 = (bf16[264,128]{1,0:T(8,128)(2,1)}, bf16[264,128]{1,0:T(8,128)(2,1)S(1)}, u32[]{:S(2)}, u32[]{:S(2)}) collective-permute-start(bf16[264,128]{1,0:T(8,128)(2,1)} %get-tuple-element.29), channel_id=1, source_target_pairs={{0,88},{8,64},{16,72},{24,80},{32,120},{40,96},{48,104},{56,112},{... | collective-permute-start | bytes 202760 | tf_op jit(solution)/shard_map/ppermute | solution.py:247
  44.9 2.4 %copy-start.7 = (bf16[264,128]{1,0:T(8,128)(2,1)}, bf16[264,128]{1,0:T(8,128)(2,1)S(1)}, u32[]{:S(2)}) copy-start(bf16[264,128]{1,0:T(8,128)(2,1)S(1)} %collective-permute-done.7.f2_ref) | copy-start | bytes 202756
  47.2 0.6 copy-start.8
  47.2 0.7 %copy-start.2 = (bf16[3,264,128]{2,1,0:T(8,128)(2,1)}, bf16[3,264,128]{2,1,0:T(8,128)(2,1)S(1)}, u32[]{:S(2)}) copy-start(bf16[3,264,128]{2,1,0:T(8,128)(2,1)S(1)} %collective-permute-done.2.y1_ref) | copy-start | bytes 608260
  47.2 0.8 %copy-start.3 = (bf16[3,264,128]{2,1,0:T(8,128)(2,1)}, bf16[3,264,128]{2,1,0:T(8,128)(2,1)S(1)}, u32[]{:S(2)}) copy-start(bf16[3,264,128]{2,1,0:T(8,128)(2,1)S(1)} %collective-permute-done.3.y2_ref) | copy-start | bytes 608260
  47.3 0.9 %copy-start.4 = (bf16[3,264,128]{2,1,0:T(8,128)(2,1)}, bf16[3,264,128]{2,1,0:T(8,128)(2,1)S(1)}, u32[]{:S(2)}) copy-start(bf16[3,264,128]{2,1,0:T(8,128)(2,1)S(1)} %collective-permute-done.4.y3_ref) | copy-start | bytes 608260
where the time goes:
time: 67.4 us; the launch traced here: 67 us
  Pallas kernels  18.5 us (27%)
  waiting for transfers between devices  17.5 us (26%)
  starting transfers between devices  14.4 us (21%)
  blocking collectives  13.7 us (20%)
  local copies, waits for them, and re-layouts  1.55 us (2%)
  between operations  0.72 us (1%)
    ppermute x9, waiting for transfers between devices, shift(): return lax.ppermute(array, 'sp', pairs)  17.5 us
    ppermute x9, starting transfers between devices, shift(): return lax.ppermute(array, 'sp', pairs)  14.4 us
    all_to_all x1, blocking collectives, step(): terms = lax.all_to_all(terms, TP, 0, 0, tiled=True)  13.7 us
    pallas_call x1, Pallas kernels, memories(): pl.pallas_call(memory_kernel, grid=(1,), in_specs=[first] * 3 + [VM] * le...  4.67 us
    pallas_call x1, Pallas kernels, project_near(): pl.pallas_call(near_kernel, in_specs=[ANY, VM, VM, VM, VM], out_shape=(bl...  4.61 us
    pallas_call x1, Pallas kernels, project_own(): pl.pallas_call(own_kernel, in_specs=[ANY, VM, VM], out_shape=block(ROW),...  3.66 us
    pallas_call x1, Pallas kernels, project_far(): pl.pallas_call(far_kernel, in_specs=[ANY, VM, VM], out_shape=(block(),) *...  3.6 us
    pallas_call x1, Pallas kernels, stack(): pl.pallas_call(stack_kernel, out_shape=(block(3),) * 3, name='stack')(*args)  1.99 us
  transfers between devices with their start and end apart: 9, of which 6 were waited for; matrix products, arithmetic and copies ran while one was open for 0% of the time, Pallas kernels for 11%

commit v1 on v0

--- a/solution.py
+++ b/solution.py
@@ -30,12 +30,12 @@
     return at // ROW, at % ROW
 
 
-def take(x_ref, buf_ref, sem_ref, blocks):
+def take(x_ref, buf_ref, sem_ref, sem, blocks):
     z, y = here()
     copies = []
     for i, (dz, dy) in enumerate(blocks):
         dest = ((z + dz) % ROW) * ROW + (y + dy) % ROW
-        copies.append(pltpu.make_async_copy(x_ref.at[pl.ds(dest * OWN, OWN)], buf_ref.at[i], sem_ref.at[i]))
+        copies.append(pltpu.make_async_copy(x_ref.at[pl.ds(dest * OWN, OWN)], buf_ref.at[i], sem_ref.at[sem + i]))
     for copy in copies:
         copy.start()
     return copies
@@ -54,73 +54,97 @@
         out[2 * ROWS :, :] = coded[:, at]
 
 
-def near_kernel(x_ref, wk_ref, wv_ref, wi_ref, wf_ref, up_ref, down_ref, w_ref, g_ref, buf_ref, sem_ref):
-    copies = take(x_ref, buf_ref, sem_ref, [(dz, dy) for dz in (1, 3) for dy in range(ROW)])
-    w_ref[:, :HD] = wk_ref[...]
-    w_ref[:, HD:] = wv_ref[...]
-    gates = jnp.concatenate((wi_ref[...].astype(F32), wf_ref[...].astype(F32), jnp.zeros((4, D), F32)), axis=0)
+def near_kernel(x_ref, wk_ref, wv_ref, wi_ref, wf_ref, up_ref, down_ref, w_ref, g_ref, rest_ref, buf_ref, wi_buf, wf_buf, sem_ref):
+    key_copy = pltpu.make_async_copy(wk_ref, w_ref.at[:, :HD], sem_ref.at[SP])
+    value_copy = pltpu.make_async_copy(wv_ref, w_ref.at[:, HD:], sem_ref.at[SP + 1])
+    gate_copies = [
+        pltpu.make_async_copy(wi_ref, wi_buf, sem_ref.at[SP + 2]),
+        pltpu.make_async_copy(wf_ref, wf_buf, sem_ref.at[SP + 3]),
+    ]
+    for copy in (*gate_copies, key_copy, value_copy):
+        copy.start()
+    copies = take(x_ref, buf_ref, sem_ref, 0, [(dz, dy) for dz in (1, 3) for dy in range(ROW)])
+    later = take(x_ref, rest_ref, sem_ref, 2 * ROW, [(dz, dy) for dz in (2, 0) for dy in range(ROW)])
+    for copy in gate_copies:
+        copy.wait()
+    gates = jnp.concatenate((wi_buf[...].astype(F32), wf_buf[...].astype(F32), jnp.zeros((4, D), F32)), axis=0)
     g_ref[...] = gates.astype(BF)
+    key_copy.wait()
+    value_copy.wait()
     for half, out_ref in enumerate((up_ref, down_ref)):
         for copy in copies[half * ROW : (half + 1) * ROW]:
             copy.wait()
         project_blocks(buf_ref, half * ROW, w_ref[...], g_ref[...], [out_ref.at[k] for k in range(ROW)])
-
-
-def far_kernel(x_ref, w_ref, g_ref, *refs):
-    outs, (buf_ref, sem_ref) = refs[:ROW], refs[ROW:]
-    for copy in take(x_ref, buf_ref, sem_ref, [(2, dy) for dy in range(ROW)]):
+    for copy in later:
         copy.wait()
-    project_blocks(buf_ref, 0, w_ref[...], g_ref[...], outs)
-
-
-def own_kernel(x_ref, w_ref, g_ref, out_ref, buf_ref, sem_ref):
-    for copy in take(x_ref, buf_ref, sem_ref, [(0, dy) for dy in range(ROW)]):
-        copy.wait()
-    project_blocks(buf_ref, 0, w_ref[...], g_ref[...], [out_ref.at[k] for k in range(ROW)])
+
+
+def rest_kernel(rest_ref, w_ref, g_ref, *outs):
+    for half in range(2):
+        project_blocks(rest_ref, half * ROW, w_ref[...], g_ref[...], outs[half * ROW : (half + 1) * ROW])
 
 
 ANY = pl.BlockSpec(memory_space=pl.ANY)
 VM = pl.BlockSpec(memory_space=pltpu.VMEM)
 
 
-def scratch(blocks):
-    return [pltpu.VMEM((blocks, OWN, POS, D), BF), pltpu.SemaphoreType.DMA((blocks,))]
+def vm(array):
+    return pltpu.with_memory_space_constraint(array, pltpu.VMEM)
+
+
+def grant(mib):
+    return pltpu.CompilerParams(vmem_limit_bytes=mib << 20)
 
 
 def block(*lead):
-    return jax.ShapeDtypeStruct((*lead, SEND, HD), BF)
+    return pltpu.VMEM((*lead, SEND, HD), BF)
 
 
 def project_near(*args):
     return pl.pallas_call(
         near_kernel,
-        in_specs=[ANY, VM, VM, VM, VM],
-        out_shape=(block(ROW), block(ROW), jax.ShapeDtypeStruct((D, 2 * HD), BF), jax.ShapeDtypeStruct((8, D), BF)),
-        scratch_shapes=scratch(2 * ROW),
+        in_specs=[ANY] * 5,
+        out_specs=[VM] * 5,
+        out_shape=(
+            block(ROW), block(ROW), pltpu.VMEM((D, 2 * HD), BF), pltpu.VMEM((8, D), BF),
+            pltpu.VMEM((2 * ROW, OWN, POS, D), BF),
+        ),
+        scratch_shapes=[
+            pltpu.VMEM((2 * ROW, OWN, POS, D), BF), pltpu.VMEM((2, D), BF), pltpu.VMEM((2, D), BF),
+            pltpu.SemaphoreType.DMA((SP + 4,)),
+        ],
+        compiler_params=grant(16),
         name="near",
-    )(*args)
-
-
-def project_far(*args):
-    return pl.pallas_call(
-        far_kernel, in_specs=[ANY, VM, VM], out_shape=(block(),) * ROW, scratch_shapes=scratch(ROW), name="far"
-    )(*args)
-
-
-def project_own(*args):
-    return pl.pallas_call(
-        own_kernel, in_specs=[ANY, VM, VM], out_shape=block(ROW), scratch_shapes=scratch(ROW), name="own"
-    )(*args)
-
-
-def stack_kernel(a_ref, b_ref, c_ref, *outs):
+    )(*[pltpu.with_memory_space_constraint(a, pltpu.HBM) for a in args])
+
+
+def project_rest(*args):
+    return pl.pallas_call(
+        rest_kernel, in_specs=[VM] * 3, out_specs=[VM] * 8, out_shape=(block(),) * 8, compiler_params=grant(16), name="rest"
+    )(*[vm(a) for a in args])
+
+
+def gather_kernel(*refs):
+    for i in range(ROW):
+        refs[ROW][i] = refs[i][...]
+
+
+def gather(*args):
+    return pl.pallas_call(
+        gather_kernel, in_specs=[VM] * ROW, out_specs=VM, out_shape=block(ROW), compiler_params=grant(4), name="gather"
+    )(*[vm(a) for a in args])
+
+
+def pair_kernel(a_ref, b_ref, *outs):
     for k, out in enumerate(outs):
-        for i, ref in enumerate((a_ref, b_ref, c_ref)):
-            out[i] = ref[k + 1]
-
-
-def stack(*args):
-    return pl.pallas_call(stack_kernel, out_shape=(block(3),) * 3, name="stack")(*args)
+        out[0] = a_ref[k + 1]
+        out[1] = b_ref[k + 1]
+
+
+def pair(*args):
+    return pl.pallas_call(
+        pair_kernel, in_specs=[VM] * 2, out_specs=[VM] * 3, out_shape=(block(2),) * 3, compiler_params=grant(4), name="pair"
+    )(*[vm(a) for a in args])
 
 
 def three_parts(a):
@@ -141,14 +165,17 @@
     return jnp.minimum(a, 0.0) - jnp.log1p(jnp.exp(-jnp.abs(a)))
 
 
-def memory_kernel(own_ref, up_ref, down_ref, y1_ref, y2_ref, y3_ref, f0_ref, f1_ref, f2_ref, f3_ref,
-                  q_ref, wo_ref, ib_ref, fb_ref, mem_ref, norm_ref, stab_ref, term_ref, vw_ref, recv_ref):
-    for i, (dz, ref) in enumerate(((0, own_ref), (1, up_ref), (3, down_ref))):
+def memory_kernel(
+    o0_ref, o1_ref, o2_ref, o3_ref, up_ref, down_ref, y1_ref, y2_ref, y3_ref, far_ref,
+    q_ref, wo_ref, ib_ref, fb_ref, mem_ref, norm_ref, stab_ref, term_ref, vw_ref, recv_ref,
+):
+    for dy, ref in enumerate((o0_ref, o1_ref, o2_ref, o3_ref)):
+        recv_ref[dy] = ref[...]
+        recv_ref[2 * ROW + dy] = far_ref[dy]
+    for i, (dz, ref) in enumerate(((1, up_ref), (3, down_ref))):
         recv_ref[dz * ROW] = ref[0]
-        for dy, far_ref in ((1, y1_ref), (2, y2_ref), (3, y3_ref)):
-            recv_ref[dz * ROW + dy] = far_ref[i]
-    for dy, ref in enumerate((f0_ref, f1_ref, f2_ref, f3_ref)):
-        recv_ref[2 * ROW + dy] = ref[...]
+        for dy, side_ref in ((1, y1_ref), (2, y2_ref), (3, y3_ref)):
+            recv_ref[dz * ROW + dy] = side_ref[i]
     z, y = here()
     place = lambda j: ((z - j // ROW) & 3) * ROW + ((y - j % ROW) & 3)
     scale = HD ** -0.5
@@ -224,12 +251,10 @@
         term_ref[t] = dot(hidden, wo_ref[:, t * HD : (t + 1) * HD])
 
 
-def memories(own, up, down, *rest):
-    first = pl.BlockSpec((1, SEND, HD), lambda i: (0, 0, 0))
+def memories(blocks, rest):
     return pl.pallas_call(
         memory_kernel,
-        grid=(1,),
-        in_specs=[first] * 3 + [VM] * len(rest),
+        in_specs=[VM] * (len(blocks) + len(rest)),
         out_shape=(
             jax.ShapeDtypeStruct((2, OWN, HD, HD), BF),
             jax.ShapeDtypeStruct((2 * OWN, HD), F32),
@@ -237,8 +262,9 @@
             jax.ShapeDtypeStruct((TPN, OWN, HD), F32),
         ),
         scratch_shapes=[pltpu.VMEM((SP, ROWS, 2 * HD), BF), pltpu.VMEM((SP, SEND, HD), BF)],
+        compiler_params=grant(16),
         name="memories",
-    )(own, up, down, *rest)
+    )(*[vm(a) for a in blocks], *rest)
 
 
 def shift(array, dz, dy):
@@ -248,19 +274,21 @@
 
 
 def step(prompt, w_key, w_value, w_in_gate, w_forget_gate, in_bias, forget_bias, query, w_out):
-    up, down, w, gates = project_near(
+    up, down, w, gates, later = project_near(
         prompt, w_key.reshape(D, HD), w_value.reshape(D, HD), w_in_gate.reshape(2, D), w_forget_gate.reshape(2, D)
     )
     up = shift(up, 1, 0)
     down = shift(down, 3, 0)
-    far = project_far(prompt, w, gates)
-    far = [shift(block, 2, dy) for dy, block in enumerate(far)]
-    own = project_own(prompt, w, gates)
-    aside = stack(own, up, down)
-    aside = [shift(blocks, 0, dy + 1) for dy, blocks in enumerate(aside)]
+    made = project_rest(later, w, gates)
+    far = [made[0]] + [shift(made[k], 0, k) for k in range(1, ROW)]
+    own = [made[ROW]] + [shift(made[ROW + k], 0, k) for k in range(1, ROW)]
+    far = gather(*far)
+    far = shift(far, 2, 0)
+    side = pair(up, down)
+    side = [shift(blocks, 0, k + 1) for k, blocks in enumerate(side)]
     memory, norm, stab, terms = memories(
-        own, up, down, *aside, *far,
-        query.reshape(OWN, HD), w_out.reshape(HD, D), in_bias.reshape(1, 2), forget_bias.reshape(1, 2),
+        (*own, up, down, *side, far),
+        (query.reshape(OWN, HD), w_out.reshape(HD, D), in_bias.reshape(1, 2), forget_bias.reshape(1, 2)),
     )
     terms = lax.all_to_all(terms, TP, 0, 0, tiled=True)
     read = jnp.sum(terms, axis=0).astype(BF)

time: 67.4 us -> 47.7 us (0.71)
  Pallas kernels: 18.5 us -> 7.47 us
  waiting for transfers between devices: 17.5 us -> 10.2 us
  blocking collectives: 13.7 us -> 10 us
  starting transfers between devices: 14.4 us -> 18 us
  local copies, waits for them, and re-layouts: 1.55 us -> 0.02 us
    pallas_call x5, Pallas kernels: 18.5 us -> 7.47 us  [the longest x1 3.2 us: memories(): pl.pallas_call(memory_kernel, in_specs=[VM] * (len(blocks) + len(rest)),...]
    ppermute x9 -> x12, waiting for transfers between devices: 17.5 us -> 10.2 us  [shift(): return lax.ppermute(array, 'sp', pairs)]
    all_to_all x1, blocking collectives: 13.7 us -> 10 us  [step(): terms = lax.all_to_all(terms, TP, 0, 0, tiled=True)]
    ppermute x9 -> x12, starting transfers between devices: 14.4 us -> 18 us  [shift(): return lax.ppermute(array, 'sp', pairs)]
    unnamed x18 -> x8, local copies, waits for them, and re-layouts: 1.55 us -> 0.02 us
  transfers between devices with their start and end apart: 9 -> 12, of which waited for: 6 -> 4; matrix products, arithmetic and copies ran while one was open for 0% -> 0% of each run, Pallas kernels for 11% -> 3%
where the time goes in v1:
time: 47.7 us; the launch traced here: 47.1 us
  starting transfers between devices  18 us (38%)
  waiting for transfers between devices  10.2 us (21%)
  blocking collectives  10 us (21%)
  Pallas kernels  7.47 us (16%)
  between operations  0.75 us (2%)
  other arithmetic  0.59 us (1%)
    ppermute x12, starting transfers between devices, shift(): return lax.ppermute(array, 'sp', pairs)  18 us
    ppermute x12, waiting for transfers between devices, shift(): return lax.ppermute(array, 'sp', pairs)  10.2 us
    all_to_all x1, blocking collectives, step(): terms = lax.all_to_all(terms, TP, 0, 0, tiled=True)  10 us
    pallas_call x1, Pallas kernels, memories(): pl.pallas_call(memory_kernel, in_specs=[VM] * (len(blocks) + len(rest)),...  3.2 us
    pallas_call x1, Pallas kernels, project_near(): pl.pallas_call(near_kernel, in_specs=[ANY] * 5, out_specs=[VM] * 5, out_s...  3 us
    pallas_call x1, Pallas kernels, project_rest(): pl.pallas_call(rest_kernel, in_specs=[VM] * 3, out_specs=[VM] * 8, out_sh...  1.23 us
  transfers between devices with their start and end apart: 12, of which 4 were waited for; matrix products, arithmetic and copies ran while one was open for 0% of the time, Pallas kernels for 3%

profile of v1, /device:TPU:1, one launch (start us, length us, event | category | flops | bytes accessed | tf_op | source)
XLA Modules:
  0.0 47.1 jit_solution(14090058487520349789)
XLA Ops:
  0.6 0.0 copy-start
  0.6 0.0 copy-start.1
  0.7 0.0 copy-start.2
  0.7 3.0 %near.1 = (bf16[4,264,128]{2,1,0:T(8,128)(2,1)S(1)}, bf16[4,264,128]{2,1,0:T(8,128)(2,1)S(1)}, bf16[1024,256]{1,0:T(8,128)(2,1)S(1)}, bf16[8,1024]{1,0:T(8,128)(2,1)S(1)}, bf16[8,8,16,1024]{3,2,1,0:T(8,128)(2,1)S(1)}) custom-call(bf16[128,16,1024]{2,1,0:T(8,128)(2,1)} %x_ref.1, bf16[1024,128]{1,0:T(8,128)(2,1)} %bitcast.21, bf16[1024,128]{1,0:T(8,128)(2,1)} %bitcast.22, ...), custom_call_target="tpu_custom_call" | custom-call | tf_op jit(solution)/shard_map/near/pallas_call | solution.py:104
  3.7 2.5 %collective-permute-start.3 = (bf16[4,264,128]{2,1,0:T(8,128)(2,1)S(1)}, bf16[4,264,128]{2,1,0:T(8,128)(2,1)S(1)}, u32[]{:S(2)}, u32[]{:S(2)}) collective-permute-start(bf16[4,264,128]{2,1,0:T(8,128)(2,1)S(1)} %get-tuple-element.31), channel_id=1, source_target_pairs={{0,32},{8,40},{16,48},{24,56},{32,64},{40,72},{48,80},{56,88},{64,... | collective-permute-start | bytes 811016 | tf_op jit(solution)/shard_map/ppermute | solution.py:273
  6.2 2.8 %collective-permute-start.4 = (bf16[4,264,128]{2,1,0:T(8,128)(2,1)S(1)}, bf16[4,264,128]{2,1,0:T(8,128)(2,1)S(1)}, u32[]{:S(2)}, u32[]{:S(2)}) collective-permute-start(bf16[4,264,128]{2,1,0:T(8,128)(2,1)S(1)} %get-tuple-element.32), channel_id=1, source_target_pairs={{0,96},{8,104},{16,112},{24,120},{32,0},{40,8},{48,16},{56,24},{64... | collective-permute-start | bytes 811016 | tf_op jit(solution)/shard_map/ppermute | solution.py:273
  9.0 1.2 %rest.1 = (bf16[264,128]{1,0:T(8,128)(2,1)S(1)}, bf16[264,128]{1,0:T(8,128)(2,1)S(1)}, bf16[264,128]{1,0:T(8,128)(2,1)S(1)}, bf16[264,128]{1,0:T(8,128)(2,1)S(1)...) custom-call(bf16[8,8,16,1024]{3,2,1,0:T(8,128)(2,1)S(1)} %get-tuple-, ...), custom_call_target="tpu_custom_call" | custom-call | tf_op jit(solution)/shard_map/rest/pallas_call | solution.py:122
  10.2 1.4 %collective-permute-start.8 = (bf16[264,128]{1,0:T(8,128)(2,1)S(1)}, bf16[264,128]{1,0:T(8,128)(2,1)S(1)}, u32[]{:S(2)}, u32[]{:S(2)}) collective-permute-start(bf16[264,128]{1,0:T(8,128)(2,1)S(1)} %get-tuple-element.37), channel_id=1, source_target_pairs={{0,8},{8,16},{16,24},{24,0},{32,40},{40,48},{48,56},{56,32},{64,72... | collective-permute-start | bytes 202760 | tf_op jit(solution)/shard_map/ppermute | solution.py:273
  11.6 2.6 %collective-permute-start.9 = (bf16[264,128]{1,0:T(8,128)(2,1)S(1)}, bf16[264,128]{1,0:T(8,128)(2,1)S(1)}, u32[]{:S(2)}, u32[]{:S(2)}) collective-permute-start(bf16[264,128]{1,0:T(8,128)(2,1)S(1)} %get-tuple-element.38), channel_id=1, source_target_pairs={{0,16},{8,24},{16,0},{24,8},{32,48},{40,56},{48,32},{56,40},{64,80... | collective-permute-start | bytes 202760 | tf_op jit(solution)/shard_map/ppermute | solution.py:273
  14.2 1.1 %collective-permute-start.10 = (bf16[264,128]{1,0:T(8,128)(2,1)S(1)}, bf16[264,128]{1,0:T(8,128)(2,1)S(1)}, u32[]{:S(2)}, u32[]{:S(2)}) collective-permute-start(bf16[264,128]{1,0:T(8,128)(2,1)S(1)} %get-tuple-element.39), channel_id=1, source_target_pairs={{0,24},{8,0},{16,8},{24,16},{32,56},{40,32},{48,40},{56,48},{64,88... | collective-permute-start | bytes 202760 | tf_op jit(solution)/shard_map/ppermute | solution.py:273
  15.3 0.0 collective-permute-done.8.refs_1_
  15.3 1.5 %collective-permute-done.9.refs_2_ = bf16[264,128]{1,0:T(8,128)(2,1)S(1)} collective-permute-done((bf16[264,128]{1,0:T(8,128)(2,1)S(1)}, bf16[264,128]{1,0:T(8,128)(2,1)S(1)}, u32[]{:S(2)}, u32[]{:S(2)}) %collective-permute-start.9) | collective-permute-done | bytes 67616 | tf_op jit(solution)/shard_map/ppermute | solution.py:273
  16.8 1.2 %collective-permute-done.10.refs_3_ = bf16[264,128]{1,0:T(8,128)(2,1)S(1)} collective-permute-done((bf16[264,128]{1,0:T(8,128)(2,1)S(1)}, bf16[264,128]{1,0:T(8,128)(2,1)S(1)}, u32[]{:S(2)}, u32[]{:S(2)}) %collective-permute-start.10) | collective-permute-done | bytes 67616 | tf_op jit(solution)/shard_map/ppermute | solution.py:273
  18.0 0.3 collective-permute-start.11
  18.4 0.0 collective-permute-start
  18.4 3.3 %collective-permute-start.1 = (bf16[264,128]{1,0:T(8,128)(2,1)S(1)}, bf16[264,128]{1,0:T(8,128)(2,1)S(1)}, u32[]{:S(2)}, u32[]{:S(2)}) collective-permute-start(bf16[264,128]{1,0:T(8,128)(2,1)S(1)} %get-tuple-element.29), channel_id=1, source_target_pairs={{0,16},{8,24},{16,0},{24,8},{32,48},{40,56},{48,32},{56,40},{64,80... | collective-permute-start | bytes 202760 | tf_op jit(solution)/shard_map/ppermute | solution.py:273
  21.7 0.0 collective-permute-done.3.a_ref.up_ref
  21.7 0.0 collective-permute-done.4.b_ref.down_ref
  21.7 0.1 collective-permute-start.5
  21.8 1.7 %collective-permute-start.6 = (bf16[2,264,128]{2,1,0:T(8,128)(2,1)S(1)}, bf16[2,264,128]{2,1,0:T(8,128)(2,1)S(1)}, u32[]{:S(2)}, u32[]{:S(2)}) collective-permute-start(bf16[2,264,128]{2,1,0:T(8,128)(2,1)S(1)} %get-tuple-element.34), channel_id=1, source_target_pairs={{0,16},{8,24},{16,0},{24,8},{32,48},{40,56},{48,32},{56,40},{64,80... | collective-permute-start | bytes 405512 | tf_op jit(solution)/shard_map/ppermute | solution.py:273
  23.5 0.0 collective-permute-done.o1_ref
  23.5 1.1 %collective-permute-start.7 = (bf16[2,264,128]{2,1,0:T(8,128)(2,1)S(1)}, bf16[2,264,128]{2,1,0:T(8,128)(2,1)S(1)}, u32[]{:S(2)}, u32[]{:S(2)}) collective-permute-start(bf16[2,264,128]{2,1,0:T(8,128)(2,1)S(1)} %get-tuple-element.35), channel_id=1, source_target_pairs={{0,24},{8,0},{16,8},{24,16},{32,56},{40,32},{48,40},{56,48},{64,88... | collective-permute-start | bytes 405512 | tf_op jit(solution)/shard_map/ppermute | solution.py:273
  24.6 0.0 collective-permute-done.1.o2_ref
  24.6 1.1 %collective-permute-start.2 = (bf16[264,128]{1,0:T(8,128)(2,1)S(1)}, bf16[264,128]{1,0:T(8,128)(2,1)S(1)}, u32[]{:S(2)}, u32[]{:S(2)}) collective-permute-start(bf16[264,128]{1,0:T(8,128)(2,1)S(1)} %get-tuple-element.30), channel_id=1, source_target_pairs={{0,24},{8,0},{16,8},{24,16},{32,56},{40,32},{48,40},{56,48},{64,88... | collective-permute-start | bytes 202760 | tf_op jit(solution)/shard_map/ppermute | solution.py:273
  25.7 4.9 %collective-permute-done.2.o3_ref = bf16[264,128]{1,0:T(8,128)(2,1)S(1)} collective-permute-done((bf16[264,128]{1,0:T(8,128)(2,1)S(1)}, bf16[264,128]{1,0:T(8,128)(2,1)S(1)}, u32[]{:S(2)}, u32[]{:S(2)}) %collective-permute-start.2) | collective-permute-done | bytes 67616 | tf_op jit(solution)/shard_map/ppermute | solution.py:273
  30.6 2.6 %collective-permute-done.11.far_ref = bf16[4,264,128]{2,1,0:T(8,128)(2,1)S(1)} collective-permute-done((bf16[4,264,128]{2,1,0:T(8,128)(2,1)S(1)}, bf16[4,264,128]{2,1,0:T(8,128)(2,1)S(1)}, u32[]{:S(2)}, u32[]{:S(2)}) %collective-permute-start.11) | collective-permute-done | bytes 270368 | tf_op jit(solution)/shard_map/ppermute | solution.py:273
  33.2 0.0 collective-permute-done.5.y1_ref
  33.2 0.0 collective-permute-done.6.y2_ref
  33.2 0.0 collective-permute-done.7.y3_ref
  33.3 3.2 %memories.1 = (bf16[2,8,128,128]{3,2,1,0:T(8,128)(2,1)}, f32[16,128]{1,0:T(8,128)}, f32[2,1,8]{2,1,0:T(1,128)}, f32[8,8,128]{2,1,0:T(8,128)S(1)}) custom-call(bf16[264,128]{1,0:T(8,128)(2,1)S(1)} %get-tuple-element.27.o0_ref, bf16[264,128]{1,0:T(8,128)(2,1)S(1)} %collective-permute-done.o1_ref, bf16[264,128]{1,0:T(8,128)(2,1)S(1)} %collective-permute-done.1.o2_ref, ...), custom_call_target="tpu_custom_call" | custom-call | tf_op jit(solution)/shard_map/memories/pallas_call | solution.py:255
  36.5 10.0 %all_to_all.5 = f32[8,8,128]{2,1,0:T(8,128)S(1)} all-to-all(f32[8,8,128]{2,1,0:T(8,128)S(1)} %get-tuple-element.43), channel_id=1, replica_groups=mesh['gr'=2,'sp'=16,'tp_0'=4,'tp_1'=2] {'tp_0','tp_1'}, dimensions={0} | all-to-all | bytes 65536 | tf_op jit(solution)/shard_map/all_to_all | solution.py:293
  46.5 0.6 %reduce_sum.9 = bf16[8,128]{1,0:T(8,128)(2,1)} reduce(f32[8,8,128]{2,1,0:T(8,128)S(1)} %all_to_all.5, f32[]{:T(128)} %constant.0.clone.1), dimensions={0}, to_apply=%region_0.0 | reduce | flops 7168 | bytes 34820 | tf_op jit(solution)/shard_map/reduce_sum | solution.py:294
  (7 shorter events, 0.1 us)
Async XLA Ops:
  0.6 32.6 %copy-start = (bf16[1,128,1024]{2,1,0:T(8,128)(2,1)S(1)}, bf16[1,128,1024]{2,1,0:T(8,128)(2,1)}, u32[]{:S(2)}) copy-start(bf16[1,128,1024]{2,1,0:T(8,128)(2,1)} %param.17) | copy-start | bytes 786436
  0.6 32.6 %copy-start.1 = (bf16[8,1,128]{2,0,1:T(8,128)(2,1)S(1)}, bf16[8,1,128]{2,0,1:T(8,128)(2,1)}, u32[]{:S(2)}) copy-start(bf16[8,1,128]{2,0,1:T(8,128)(2,1)} %param.16) | copy-start | bytes 6148
  0.7 32.6 %copy-start.2 = (f32[2,1]{0,1:T(1,128)S(1)}, f32[2,1]{0,1:T(1,128)}, u32[]{:S(2)}) copy-start(f32[2,1]{0,1:T(1,128)} %param.14) | copy-start | bytes 28
  0.7 32.6 %copy-start.3 = (f32[2,1]{0,1:T(1,128)S(1)}, f32[2,1]{0,1:T(1,128)}, u32[]{:S(2)}) copy-start(f32[2,1]{0,1:T(1,128)} %param.15) | copy-start | bytes 28
  3.7 18.0 %collective-permute-start.3 = (bf16[4,264,128]{2,1,0:T(8,128)(2,1)S(1)}, bf16[4,264,128]{2,1,0:T(8,128)(2,1)S(1)}, u32[]{:S(2)}, u32[]{:S(2)}) collective-permute-start(bf16[4,264,128]{2,1,0:T(8,128)(2,1)S(1)} %get-tuple-element.31), channel_id=1, source_target_pairs={{0,32},{8,40},{16,48},{24,56},{32,64},{40,72},{48,80},{56,88},{64,... | collective-permute-start | bytes 811016 | tf_op jit(solution)/shard_map/ppermute | solution.py:273
  6.2 15.5 %collective-permute-start.4 = (bf16[4,264,128]{2,1,0:T(8,128)(2,1)S(1)}, bf16[4,264,128]{2,1,0:T(8,128)(2,1)S(1)}, u32[]{:S(2)}, u32[]{:S(2)}) collective-permute-start(bf16[4,264,128]{2,1,0:T(8,128)(2,1)S(1)} %get-tuple-element.32), channel_id=1, source_target_pairs={{0,96},{8,104},{16,112},{24,120},{32,0},{40,8},{48,16},{56,24},{64... | collective-permute-start | bytes 811016 | tf_op jit(solution)/shard_map/ppermute | solution.py:273
  10.2 5.1 %collective-permute-start.8 = (bf16[264,128]{1,0:T(8,128)(2,1)S(1)}, bf16[264,128]{1,0:T(8,128)(2,1)S(1)}, u32[]{:S(2)}, u32[]{:S(2)}) collective-permute-start(bf16[264,128]{1,0:T(8,128)(2,1)S(1)} %get-tuple-element.37), channel_id=1, source_target_pairs={{0,8},{8,16},{16,24},{24,0},{32,40},{40,48},{48,56},{56,32},{64,72... | collective-permute-start | bytes 202760 | tf_op jit(solution)/shard_map/ppermute | solution.py:273
  11.6 5.2 %collective-permute-start.9 = (bf16[264,128]{1,0:T(8,128)(2,1)S(1)}, bf16[264,128]{1,0:T(8,128)(2,1)S(1)}, u32[]{:S(2)}, u32[]{:S(2)}) collective-permute-start(bf16[264,128]{1,0:T(8,128)(2,1)S(1)} %get-tuple-element.38), channel_id=1, source_target_pairs={{0,16},{8,24},{16,0},{24,8},{32,48},{40,56},{48,32},{56,40},{64,80... | collective-permute-start | bytes 202760 | tf_op jit(solution)/shard_map/ppermute | solution.py:273
  14.2 3.8 %collective-permute-start.10 = (bf16[264,128]{1,0:T(8,128)(2,1)S(1)}, bf16[264,128]{1,0:T(8,128)(2,1)S(1)}, u32[]{:S(2)}, u32[]{:S(2)}) collective-permute-start(bf16[264,128]{1,0:T(8,128)(2,1)S(1)} %get-tuple-element.39), channel_id=1, source_target_pairs={{0,24},{8,0},{16,8},{24,16},{32,56},{40,32},{48,40},{56,48},{64,88... | collective-permute-start | bytes 202760 | tf_op jit(solution)/shard_map/ppermute | solution.py:273
  18.0 15.2 %collective-permute-start.11 = (bf16[4,264,128]{2,1,0:T(8,128)(2,1)S(1)}, bf16[4,264,128]{2,1,0:T(8,128)(2,1)S(1)}, u32[]{:S(2)}, u32[]{:S(2)}) collective-permute-start(bf16[4,264,128]{2,1,0:T(8,128)(2,1)S(1)} %gather.1), channel_id=1, source_target_pairs={{0,64},{8,72},{16,80},{24,88},{32,96},{40,104},{48,112},{56,120},{... | collective-permute-start | bytes 811016 | tf_op jit(solution)/shard_map/ppermute | solution.py:273
  18.4 5.2 %collective-permute-start = (bf16[264,128]{1,0:T(8,128)(2,1)S(1)}, bf16[264,128]{1,0:T(8,128)(2,1)S(1)}, u32[]{:S(2)}, u32[]{:S(2)}) collective-permute-start(bf16[264,128]{1,0:T(8,128)(2,1)S(1)} %get-tuple-element.28), channel_id=1, source_target_pairs={{0,8},{8,16},{16,24},{24,0},{32,40},{40,48},{48,56},{56,32},{64,72... | collective-permute-start | bytes 202760 | tf_op jit(solution)/shard_map/ppermute | solution.py:273
  18.4 6.2 %collective-permute-start.1 = (bf16[264,128]{1,0:T(8,128)(2,1)S(1)}, bf16[264,128]{1,0:T(8,128)(2,1)S(1)}, u32[]{:S(2)}, u32[]{:S(2)}) collective-permute-start(bf16[264,128]{1,0:T(8,128)(2,1)S(1)} %get-tuple-element.29), channel_id=1, source_target_pairs={{0,16},{8,24},{16,0},{24,8},{32,48},{40,56},{48,32},{56,40},{64,80... | collective-permute-start | bytes 202760 | tf_op jit(solution)/shard_map/ppermute | solution.py:273
  21.7 11.5 %collective-permute-start.5 = (bf16[2,264,128]{2,1,0:T(8,128)(2,1)S(1)}, bf16[2,264,128]{2,1,0:T(8,128)(2,1)S(1)}, u32[]{:S(2)}, u32[]{:S(2)}) collective-permute-start(bf16[2,264,128]{2,1,0:T(8,128)(2,1)S(1)} %get-tuple-element.33), channel_id=1, source_target_pairs={{0,8},{8,16},{16,24},{24,0},{32,40},{40,48},{48,56},{56,32},{64,72... | collective-permute-start | bytes 405512 | tf_op jit(solution)/shard_map/ppermute | solution.py:273
  21.8 11.4 %collective-permute-start.6 = (bf16[2,264,128]{2,1,0:T(8,128)(2,1)S(1)}, bf16[2,264,128]{2,1,0:T(8,128)(2,1)S(1)}, u32[]{:S(2)}, u32[]{:S(2)}) collective-permute-start(bf16[2,264,128]{2,1,0:T(8,128)(2,1)S(1)} %get-tuple-element.34), channel_id=1, source_target_pairs={{0,16},{8,24},{16,0},{24,8},{32,48},{40,56},{48,32},{56,40},{64,80... | collective-permute-start | bytes 405512 | tf_op jit(solution)/shard_map/ppermute | solution.py:273
  23.5 9.7 %collective-permute-start.7 = (bf16[2,264,128]{2,1,0:T(8,128)(2,1)S(1)}, bf16[2,264,128]{2,1,0:T(8,128)(2,1)S(1)}, u32[]{:S(2)}, u32[]{:S(2)}) collective-permute-start(bf16[2,264,128]{2,1,0:T(8,128)(2,1)S(1)} %get-tuple-element.35), channel_id=1, source_target_pairs={{0,24},{8,0},{16,8},{24,16},{32,56},{40,32},{48,40},{56,48},{64,88... | collective-permute-start | bytes 405512 | tf_op jit(solution)/shard_map/ppermute | solution.py:273
  24.6 6.0 %collective-permute-start.2 = (bf16[264,128]{1,0:T(8,128)(2,1)S(1)}, bf16[264,128]{1,0:T(8,128)(2,1)S(1)}, u32[]{:S(2)}, u32[]{:S(2)}) collective-permute-start(bf16[264,128]{1,0:T(8,128)(2,1)S(1)} %get-tuple-element.30), channel_id=1, source_target_pairs={{0,24},{8,0},{16,8},{24,16},{32,56},{40,32},{48,40},{56,48},{64,88... | collective-permute-start | bytes 202760 | tf_op jit(solution)/shard_map/ppermute | solution.py:273

commit v2 on v1

v2 whole, which is shorter than its diff:
```python
import jax
import jax.numpy as jnp
from jax import lax
from jax.experimental import pallas as pl
from jax.experimental.pallas import tpu as pltpu
from jax.sharding import Mesh
from jax.sharding import PartitionSpec as P


TP = ("tp_0", "tp_1")
BF = jnp.bfloat16
F32 = jnp.float32
SP = 16
OWN = 8
POS = 16
ROWS = OWN * POS
HD = 128
D = 1024
SEND = 2 * ROWS + 8
ROW = 4
TPX = 4


def dot(a, b, dims=((1,), (0,))):
    return lax.dot_general(a, b, (dims, ((), ())), preferred_element_type=F32)


def here():
    at = lax.axis_index("sp")
    return at // ROW, at % ROW


def take(x_ref, buf_ref, sem_ref, sem, blocks):
    z, y = here()
    copies = []
    for i, (dz, dy) in enumerate(blocks):
        dest = ((z + dz) % ROW) * ROW + (y + dy) % ROW
        copies.append(pltpu.make_async_copy(x_ref.at[pl.ds(dest * OWN, OWN)], buf_ref.at[i], sem_ref.at[sem + i]))
    for copy in copies:
        copy.start()
    return copies


def project_blocks(buf_ref, first, w, gates, outs):
    rows = buf_ref[first : first + ROW].reshape(ROW * ROWS, D)
    both = dot(rows, w).astype(BF)
    pre = dot(gates, rows, ((1,), (1,)))[:4]
    high = pre.astype(BF).astype(F32)
    coded = jnp.concatenate((high, pre - high), axis=0).astype(BF)
    for k, out in enumerate(outs):
        at = slice(k * ROWS, (k + 1) * ROWS)
        out[:ROWS, :] = both[at, :HD]
        out[ROWS : 2 * ROWS, :] = both[at, HD:]
        out[2 * ROWS :, :] = coded[:, at]


def near_kernel(x_ref, wk_ref, wv_ref, wi_ref, wf_ref, up_ref, w_ref, g_ref, rest_ref, buf_ref, wi_buf, wf_buf, sem_ref):
    key_copy = pltpu.make_async_copy(wk_ref, w_ref.at[:, :HD], sem_ref.at[SP])
    value_copy = pltpu.make_async_copy(wv_ref, w_ref.at[:, HD:], sem_ref.at[SP + 1])
    gate_copies = [
        pltpu.make_async_copy(wi_ref, wi_buf, sem_ref.at[SP + 2]),
        pltpu.make_async_copy(wf_ref, wf_buf, sem_ref.at[SP + 3]),
    ]
    for copy in (*gate_copies, key_copy, value_copy):
        copy.start()
    copies = take(x_ref, buf_ref, sem_ref, 0, [(1, dy) for dy in range(ROW)])
    later = take(x_ref, rest_ref, sem_ref, ROW, [(dz, dy) for dz in (3, 2, 0) for dy in range(ROW)])
    for copy in gate_copies:
        copy.wait()
    gates = jnp.concatenate((wi_buf[...].astype(F32), wf_buf[...].astype(F32), jnp.zeros((4, D), F32)), axis=0)
    g_ref[...] = gates.astype(BF)
    key_copy.wait()
    value_copy.wait()
    for copy in copies:
        copy.wait()
    project_blocks(buf_ref, 0, w_ref[...], g_ref[...], [up_ref.at[k] for k in range(ROW)])
    for copy in later:
        copy.wait()


def second_kernel(rest_ref, w_ref, g_ref, down_ref):
    project_blocks(rest_ref, 0, w_ref[...], g_ref[...], [down_ref.at[k] for k in range(ROW)])


def third_kernel(rest_ref, w_ref, g_ref, *outs):
    for half in range(2):
        project_blocks(rest_ref, (half + 1) * ROW, w_ref[...], g_ref[...], [out.at[half] for out in outs])


ANY = pl.BlockSpec(memory_space=pl.ANY)
VM = pl.BlockSpec(memory_space=pltpu.VMEM)


def vm(array):
    return pltpu.with_memory_space_constraint(array, pltpu.VMEM)


def grant(mib):
    return pltpu.CompilerParams(vmem_limit_bytes=mib << 20)


def block(*lead):
    return pltpu.VMEM((*lead, SEND, HD), BF)


def run(kernel, out_shape, args, mib=16, scratch=()):
    specs = jax.tree.map(lambda _: VM, out_shape, is_leaf=lambda s: hasattr(s, "shape"))
    return pl.pallas_call(
        kernel,
        in_specs=[VM] * len(args),
        out_specs=specs,
        out_shape=out_shape,
        scratch_shapes=list(scratch),
        compiler_params=grant(mib),
    )(*[vm(a) for a in args])


def project_near(*args):
    return pl.pallas_call(
        near_kernel,
        in_specs=[ANY] * 5,
        out_specs=[VM] * 4,
        out_shape=(
            block(ROW), pltpu.VMEM((D, 2 * HD), BF), pltpu.VMEM((8, D), BF), pltpu.VMEM((3 * ROW, OWN, POS, D), BF)
        ),
        scratch_shapes=[
            pltpu.VMEM((ROW, OWN, POS, D), BF), pltpu.VMEM((2, D), BF), pltpu.VMEM((2, D), BF),
            pltpu.SemaphoreType.DMA((SP + 4,)),
        ],
        compiler_params=grant(16),
        name="near",
    )(*[pltpu.with_memory_space_constraint(a, pltpu.HBM) for a in args])


def gather_kernel(*refs):
    for i in range(ROW):
        refs[ROW][i] = refs[i][0]


def pair_kernel(a_ref, b_ref, *outs):
    for k, out in enumerate(outs):
        out[0] = a_ref[k + 1]
        out[1] = b_ref[k + 1]


def three_parts(a):
    first = a.astype(BF)
    rest = a - first.astype(F32)
    second = rest.astype(BF)
    return first, second, (rest - second.astype(F32)).astype(BF)


def group_max(a, lane):
    for k in (1, 2, 4, 8):
        inside = (lane % POS) + k < POS
        a = jnp.maximum(a, jnp.where(inside, pltpu.roll(a, HD - k, 1), pltpu.roll(a, POS - k, 1)))
    return a


def log_sigmoid(a):
    return jnp.minimum(a, 0.0) - jnp.log1p(jnp.exp(-jnp.abs(a)))


def landed(refs):
    c0, c1, c2, c3, up, down, s1, s2, s3, far = refs
    own = [c.at[1] for c in (c0, c1, c2, c3)]
    from_up = [up.at[0]] + [s.at[0] for s in (s1, s2, s3)]
    from_down = [down.at[0]] + [s.at[1] for s in (s1, s2, s3)]
    return own + from_up + [far.at[k] for k in range(ROW)] + from_down


def rows_mine():
    row = lax.broadcasted_iota(jnp.int32, (OWN, HD), 0)
    lane = lax.broadcasted_iota(jnp.int32, (OWN, HD), 1)
    return row, lane, (lane // POS) == row


def two_parts(a):
    high = a.astype(BF)
    return jnp.concatenate((high, (a - high.astype(F32)).astype(BF)), axis=0)


def read_kernel(*refs):
    blocks = landed(refs[:10])
    q_ref, wo_ref, ib_ref, fb_ref, keep_ref, send_ref, weight_ref, turned_ref, stab_ref = refs[10:]
    scale = HD ** -0.5
    row, lane8, mine = rows_mine()
    query = q_ref[...]
    scores = [jnp.where(mine, dot(query, blk[:ROWS, :], ((1,), (1,))), 0.0) for blk in blocks]

    gates = jnp.stack([blk[2 * ROWS :, :].astype(F32) for blk in blocks])
    part = lambda c: gates[:, c, :] + gates[:, c + 4, :]
    in_pre = [part(g) + ib_ref[0:1, g : g + 1] for g in range(2)]
    forget = [log_sigmoid(part(2 + g) + fb_ref[0:1, g : g + 1]) for g in range(2)]

    z, y = here()
    place = lambda j: ((z - j // ROW) & 3) * ROW + ((y - j % ROW) & 3)
    r = lax.broadcasted_iota(jnp.int32, (HD, HD), 0)
    c = lax.broadcasted_iota(jnp.int32, (HD, HD), 1)
    same = (r // POS) == (c // POS)
    ones = lambda m: jnp.where(m, 1.0, 0.0).astype(BF)
    jr = lax.broadcasted_iota(jnp.int32, (2 * SP, SP), 0)
    jc = lax.broadcasted_iota(jnp.int32, (2 * SP, SP), 1)
    lane = lax.broadcasted_iota(jnp.int32, (1, HD), 1)
    log_weight = []
    total = []
    for g in range(2):
        order = (r > c) if g == 0 else (r < c)
        inside = jnp.concatenate((ones(same & order), ones(same)), axis=1)
        sums = sum(dot(p, inside) for p in three_parts(forget[g]))
        block = sums[:, HD:]
        across = ones(((place(jc) > place(jr)) if g == 0 else (place(jc) < place(jr))) | (jr >= SP))
        outside = sum(dot(across, p) for p in three_parts(block))
        log_weight.append(in_pre[g] + sums[:, :HD] + outside[:SP])
        total.append(outside[SP : SP + 1])
    stab = [
        jnp.maximum(total[g], group_max(jnp.max(log_weight[g], axis=0, keepdims=True), lane)) for g in range(2)
    ]
    weight = jnp.concatenate([jnp.exp(log_weight[g] - stab[g]) for g in range(2)], axis=0)
    weight_ref[...] = weight
    turned_ref[...] = weight.T

    shares = jnp.zeros((2 * OWN, HD), F32)
    numerator = jnp.zeros((4 * OWN, HD), F32)
    for j, blk in enumerate(blocks):
        share = jnp.concatenate([scores[j] * weight[g * SP + j : g * SP + j + 1] for g in range(2)], axis=0)
        shares += share
        numerator += dot(two_parts(share), blk[ROWS : 2 * ROWS, :])
    numerator = (numerator[: 2 * OWN] + numerator[2 * OWN :]) * scale
    denominator = jnp.sum(shares, axis=1, keepdims=True) * scale
    hidden = jnp.zeros((OWN, HD), F32)
    for g in range(2):
        at = slice(g * OWN, (g + 1) * OWN)
        column = jnp.max(jnp.where(mine, stab[g], -jnp.inf), axis=1, keepdims=True)
        stab_ref[g] = jnp.sum(jnp.where(lane8 == row, column, 0.0), axis=0, keepdims=True)[:, :OWN]
        hidden += numerator[at] / jnp.maximum(jnp.maximum(jnp.abs(denominator[at]), jnp.exp(-column)), 1.0)
    hidden = hidden.astype(BF)
    x = lax.axis_index("tp_0")
    core = lax.axis_index("tp_1")
    for k in range(TPX):
        first = ((x + k) % TPX) * 2
        for out_ref, which in ((keep_ref, core), (send_ref, 1 - core)):
            at = pl.multiple_of((first + which) * HD, HD)
            out_ref[k] = dot(hidden, wo_ref[:, pl.ds(at, HD)])


def weigh_kernel(*refs):
    blocks = landed(refs[:10])
    weight_ref, turned_ref, vw_ref, norm_ref = refs[10:]
    _, _, mine = rows_mine()
    norm = jnp.zeros((4 * OWN, HD), F32)
    for j, blk in enumerate(blocks):
        spread = [jnp.where(mine, weight_ref[g * SP + j : g * SP + j + 1, :], 0.0) for g in range(2)]
        norm += dot(two_parts(jnp.concatenate(spread, axis=0)), blk[:ROWS, :])
        value = blk[ROWS : 2 * ROWS, :].astype(F32)
        for g in range(2):
            k = g * SP + j
            vw_ref[j, :, g * HD : (g + 1) * HD] = (value * turned_ref[:, k : k + 1]).astype(BF)
    norm_ref[...] = (norm[: 2 * OWN] + norm[2 * OWN :]) * (HD ** -0.5)


def memory_kernel(*refs):
    blocks = landed(refs[:10])
    vw_ref, mem_ref = refs[10:]
    for s in range(OWN):
        at = slice(s * POS, (s + 1) * POS)
        keys = jnp.concatenate([blk[at, :] for blk in blocks], axis=0)
        values = vw_ref[:, at, :].reshape(SP * POS, 2 * HD)
        memory = (dot(keys, values, ((0,), (0,))) * (HD ** -0.5)).astype(BF)
        mem_ref[0, s] = memory[:, :HD]
        mem_ref[1, s] = memory[:, HD:]


def join_kernel(keep_ref, got_ref, *outs):
    for k, out in enumerate(outs):
        out[...] = keep_ref[k] + got_ref[k]


def sum_kernel(a_ref, b_ref, c_ref, d_ref, out_ref):
    out_ref[...] = ((a_ref[...] + b_ref[...]) + (c_ref[...] + d_ref[...])).astype(BF)


def shift(array, dz, dy):
    spots = [(z, y) for z in range(ROW) for y in range(ROW)]
    pairs = [(z * ROW + y, ((z + dz) % ROW) * ROW + (y + dy) % ROW) for z, y in spots]
    return lax.ppermute(array, "sp", pairs)


def across(array, axis, hop):
    size = lax.axis_size(axis)
    return lax.ppermute(array, axis, [(i, (i + hop) % size) for i in range(size)])


def step(prompt, w_key, w_value, w_in_gate, w_forget_gate, in_bias, forget_bias, query, w_out):
    hops = range(1, ROW)
    up, w, gates, later = project_near(
        prompt, w_key.reshape(D, HD), w_value.reshape(D, HD), w_in_gate.reshape(2, D), w_forget_gate.reshape(2, D)
    )
    up = shift(up, 1, 0)
    down = run(second_kernel, block(ROW), (later, w, gates))
    down = shift(down, 3, 0)
    cross = run(third_kernel, (block(2),) * ROW, (later, w, gates))
    cross = [cross[0]] + [shift(cross[k], 0, k) for k in hops]
    far = run(gather_kernel, block(ROW), cross, 4)
    far = shift(far, 2, 0)
    side = run(pair_kernel, (block(2),) * 3, (up, down), 4)
    side = [shift(blocks, 0, k) for k, blocks in zip(hops, side)]
    blocks = (*cross, up, down, *side, far)
    half = pltpu.VMEM((TPX, OWN, HD), F32)
    keep, send, weight, turned, stab = run(
        read_kernel,
        (half, half, pltpu.VMEM((2 * SP, HD), F32), pltpu.VMEM((HD, 2 * SP), F32),
         jax.ShapeDtypeStruct((2, 1, OWN), F32)),
        (*blocks, query.reshape(OWN, HD), w_out.reshape(HD, D), in_bias.reshape(1, 2), forget_bias.reshape(1, 2)),
    )
    got = across(send, "tp_1", 1)
    values, norm = run(
        weigh_kernel,
        (pltpu.VMEM((SP, ROWS, 2 * HD), BF), jax.ShapeDtypeStruct((2 * OWN, HD), F32)),
        (*blocks, weight, turned),
    )
    terms = run(join_kernel, (pltpu.VMEM((OWN, HD), F32),) * TPX, (keep, got), 4)
    terms = [terms[0]] + [across(terms[k], "tp_0", k) for k in range(1, TPX)]
    memory = run(memory_kernel, jax.ShapeDtypeStruct((2, OWN, HD, HD), BF), (*blocks, values))
    read = run(sum_kernel, jax.ShapeDtypeStruct((OWN, HD), BF), terms, 4)
    return (
        memory.reshape(2, OWN, 1, HD, HD),
        norm.reshape(2, OWN, 1, HD),
        stab.reshape(2, OWN, 1),
        read,
    )


def solution(mesh):
    torus = Mesh(
        mesh.devices.reshape(mesh.shape["gr"], mesh.shape["sp"], 4, 2), ("gr", "sp", "tp_0", "tp_1")
    )
    return jax.shard_map(
        step,
        mesh=torus,
        in_specs=(
            P("gr", "sp", None),
            P(None, TP, None),
            P(None, TP, None),
            P(None, None, TP),
            P(None, None, TP),
            P(None, TP),
            P(None, TP),
            P(("gr", "sp"), TP, None),
            P(TP, None, None),
        ),
        out_specs=(
            P(None, ("gr", "sp"), TP, None, None),
            P(None, ("gr", "sp"), TP, None),
            P(None, ("gr", "sp"), TP),
            P(("gr", "sp"), TP),
        ),
        check_vma=False,
    )
```

time: 47.7 us -> 49.3 us (1.034); the launches traced: 47.1 us -> 49.2 us
  blocking collectives: 10 us -> 0 us
  waiting for transfers between devices: 10.2 us -> 20.2 us
  Pallas kernels: 7.47 us -> 9.09 us
  starting transfers between devices: 18 us -> 19.2 us
  other arithmetic: 0.59 us -> 0 us
    all_to_all x1 -> x0, blocking collectives: 10 us -> none  [step(): terms = lax.all_to_all(terms, TP, 0, 0, tiled=True)]
    ppermute x12 -> x9, waiting for transfers between devices: 10.2 us -> 19.3 us  [shift(): return lax.ppermute(array, 'sp', pairs)]
    ppermute x0 -> x4, starting transfers between devices: none -> 5.65 us  [across(): lax.ppermute(array, axis, [(i, (i + hop) % size) for i in range(size)])]
    ppermute x12 -> x9, starting transfers between devices: 18 us -> 13.5 us  [shift(): return lax.ppermute(array, 'sp', pairs)]
    pallas_call x5 -> x10, Pallas kernels: 7.47 us -> 9.09 us  [the longest x9 6.58 us: run(): pl.pallas_call(kernel, in_specs=[VM] * len(args), out_specs=specs, out_sh...]
    ppermute x0 -> x4, waiting for transfers between devices: none -> 0.85 us  [across(): lax.ppermute(array, axis, [(i, (i + hop) % size) for i in range(size)])]
    reduce_sum x1 -> x0, other arithmetic: 0.59 us -> none  [step(): read = jnp.sum(terms, axis=0).astype(BF)]
  transfers between devices with their start and end apart: 12 -> 13, of which waited for: 4 -> 5; matrix products, arithmetic and copies ran while one was open for 0% -> 0% of each run, Pallas kernels for 3% -> 6%
where the time goes in v2:
time: 49.3 us; the launch traced here: 49.2 us
  waiting for transfers between devices  20.2 us (41%)
  starting transfers between devices  19.2 us (39%)
  Pallas kernels  9.09 us (18%)
  between operations  0.75 us (2%)
    ppermute x9, waiting for transfers between devices, shift(): return lax.ppermute(array, 'sp', pairs)  19.3 us
    ppermute x9, starting transfers between devices, shift(): return lax.ppermute(array, 'sp', pairs)  13.5 us
    pallas_call x9, Pallas kernels, run(): pl.pallas_call(kernel, in_specs=[VM] * len(args), out_specs=specs, out_sh...  6.58 us
    ppermute x4, starting transfers between devices, across(): lax.ppermute(array, axis, [(i, (i + hop) % size) for i in range(size)])  5.65 us
    pallas_call x1, Pallas kernels, project_near(): pl.pallas_call(near_kernel, in_specs=[ANY] * 5, out_specs=[VM] * 4, out_s...  2.51 us
  transfers between devices with their start and end apart: 13, of which 5 were waited for; matrix products, arithmetic and copies ran while one was open for 0% of the time, Pallas kernels for 6%

profile of v2, /device:TPU:1, one launch (start us, length us, event | category | flops | bytes accessed | tf_op | source)
XLA Modules:
  0.0 49.2 jit_solution(14921494991079548311)
XLA Ops:
  0.6 2.5 %near.1 = (bf16[4,264,128]{2,1,0:T(8,128)(2,1)S(1)}, bf16[1024,256]{1,0:T(8,128)(2,1)S(1)}, bf16[8,1024]{1,0:T(8,128)(2,1)S(1)}, bf16[12,8,16,1024]{3,2,1,0:T(8,128)(2,1)S(1)}) custom-call(bf16[128,16,1024]{2,1,0:T(8,128)(2,1)} %x_ref.1, bf16[1024,128]{1,0:T(8,128)(2,1)} %bitcast.22, bf16[1024,128]{1,0:T(8,128)(2,1)} %bitcast.23, bf16[2,1024]{1,0:T(2,128)(2,1)} %bitcast.24, ...), custom_call_target="tpu_custom_call" | custom-call | tf_op jit(solution)/shard_map/near/pallas_call | solution.py:119
  3.1 0.0 copy-start
  3.2 0.0 copy-start.1
  3.2 0.0 copy-start.2
  3.2 0.0 copy-start.3
  3.2 1.2 %shard_map.120 = (bf16[2,264,128]{2,1,0:T(8,128)(2,1)S(1)}, bf16[2,264,128]{2,1,0:T(8,128)(2,1)S(1)}, bf16[2,264,128]{2,1,0:T(8,128)(2,1)S(1)}, bf16[2,264,128]{2,1,0:T(8,128)(2,1)S(1)}) custom-call(bf16[12,8,16,1024]{3,2,1,0:T(8,128)(2,1)S(1)} %get-tuple-element.26.rest_ref, bf16[1024,256]{1,0:T(8,128)(2,1)S(1)} %get-tuple-element.27.w_ref, ...), custom_call_target="tpu_custom_call" | custom-call | tf_op jit(solution)/shard_map/pallas_call | solution.py:108
  4.4 2.2 %collective-permute-start = (bf16[2,264,128]{2,1,0:T(8,128)(2,1)S(1)}, bf16[2,264,128]{2,1,0:T(8,128)(2,1)S(1)}, u32[]{:S(2)}, u32[]{:S(2)}) collective-permute-start(bf16[2,264,128]{2,1,0:T(8,128)(2,1)S(1)} %get-tuple-element.30), channel_id=1, source_target_pairs={{0,8},{8,16},{16,24},{24,0},{32,40},{40,48},{48,56},{56,32},{64,72... | collective-permute-start | bytes 405512 | tf_op jit(solution)/shard_map/ppermute | solution.py:286
  6.6 2.6 %collective-permute-start.1 = (bf16[2,264,128]{2,1,0:T(8,128)(2,1)S(1)}, bf16[2,264,128]{2,1,0:T(8,128)(2,1)S(1)}, u32[]{:S(2)}, u32[]{:S(2)}) collective-permute-start(bf16[2,264,128]{2,1,0:T(8,128)(2,1)S(1)} %get-tuple-element.31), channel_id=1, source_target_pairs={{0,16},{8,24},{16,0},{24,8},{32,48},{40,56},{48,32},{56,40},{64,80... | collective-permute-start | bytes 405512 | tf_op jit(solution)/shard_map/ppermute | solution.py:286
  9.3 0.7 %shard_map.121 = bf16[4,264,128]{2,1,0:T(8,128)(2,1)S(1)} custom-call(bf16[12,8,16,1024]{3,2,1,0:T(8,128)(2,1)S(1)} %get-tuple-element.26.rest_ref, bf16[1024,256]{1,0:T(8,128)(2,1)S(1)} %get-tuple-element.27.w_ref, bf16[8,1024]{1,0:T(8,128)(2,1)S(1)} %get-tuple-element.28.g_ref), custom_call_target="tpu_custom_call" | custom-call | tf_op jit(solution)/shard_map/pallas_call | solution.py:108
  10.0 4.4 %collective-permute-start.4 = (bf16[4,264,128]{2,1,0:T(8,128)(2,1)S(1)}, bf16[4,264,128]{2,1,0:T(8,128)(2,1)S(1)}, u32[]{:S(2)}, u32[]{:S(2)}) collective-permute-start(bf16[4,264,128]{2,1,0:T(8,128)(2,1)S(1)} %shard_map.121), channel_id=1, source_target_pairs={{0,96},{8,104},{16,112},{24,120},{32,0},{40,8},{48,16},{56,24},{64... | collective-permute-start | bytes 811016 | tf_op jit(solution)/shard_map/ppermute | solution.py:286
  14.4 0.0 collective-permute-start.3
  14.4 1.1 %collective-permute-start.2 = (bf16[2,264,128]{2,1,0:T(8,128)(2,1)S(1)}, bf16[2,264,128]{2,1,0:T(8,128)(2,1)S(1)}, u32[]{:S(2)}, u32[]{:S(2)}) collective-permute-start(bf16[2,264,128]{2,1,0:T(8,128)(2,1)S(1)} %get-tuple-element.32), channel_id=1, source_target_pairs={{0,24},{8,0},{16,8},{24,16},{32,56},{40,32},{48,40},{56,48},{64,88... | collective-permute-start | bytes 405512 | tf_op jit(solution)/shard_map/ppermute | solution.py:286
  15.4 0.0 collective-permute-done.refs_1_
  15.4 0.0 collective-permute-done.1.refs_2_
  15.4 3.1 %collective-permute-done.2.refs_3_ = bf16[2,264,128]{2,1,0:T(8,128)(2,1)S(1)} collective-permute-done((bf16[2,264,128]{2,1,0:T(8,128)(2,1)S(1)}, bf16[2,264,128]{2,1,0:T(8,128)(2,1)S(1)}, u32[]{:S(2)}, u32[]{:S(2)}) %collective-permute-start.2) | collective-permute-done | bytes 135200 | tf_op jit(solution)/shard_map/ppermute | solution.py:286
  18.6 0.5 collective-permute-start.8
  19.0 0.1 collective-permute-done.4.b_ref.refs_5_
  19.1 6.7 %collective-permute-done.3.a_ref.refs_4_ = bf16[4,264,128]{2,1,0:T(8,128)(2,1)S(1)} collective-permute-done((bf16[4,264,128]{2,1,0:T(8,128)(2,1)S(1)}, bf16[4,264,128]{2,1,0:T(8,128)(2,1)S(1)}, u32[]{:S(2)}, u32[]{:S(2)}) %collective-permute-start.3) | collective-permute-done | bytes 270368 | tf_op jit(solution)/shard_map/ppermute | solution.py:286
  25.8 0.1 collective-permute-start.5
  25.9 2.2 %collective-permute-start.6 = (bf16[2,264,128]{2,1,0:T(8,128)(2,1)S(1)}, bf16[2,264,128]{2,1,0:T(8,128)(2,1)S(1)}, u32[]{:S(2)}, u32[]{:S(2)}) collective-permute-start(bf16[2,264,128]{2,1,0:T(8,128)(2,1)S(1)} %get-tuple-element.35), channel_id=1, source_target_pairs={{0,16},{8,24},{16,0},{24,8},{32,48},{40,56},{48,32},{56,40},{64,80... | collective-permute-start | bytes 405512 | tf_op jit(solution)/shard_map/ppermute | solution.py:286
  28.1 0.4 collective-permute-start.7
  28.5 9.5 %collective-permute-done.8.refs_9_ = bf16[4,264,128]{2,1,0:T(8,128)(2,1)S(1)} collective-permute-done((bf16[4,264,128]{2,1,0:T(8,128)(2,1)S(1)}, bf16[4,264,128]{2,1,0:T(8,128)(2,1)S(1)}, u32[]{:S(2)}, u32[]{:S(2)}) %collective-permute-start.8) | collective-permute-done | bytes 270368 | tf_op jit(solution)/shard_map/ppermute | solution.py:286
  38.0 0.0 collective-permute-done.5.refs_6_
  38.1 1.8 %shard_map.124 = (f32[4,8,128]{2,1,0:T(8,128)S(1)}, f32[4,8,128]{2,1,0:T(8,128)S(1)}, f32[32,128]{1,0:T(8,128)S(1)}, f32[128,32]{1,0:T(8,128)S(1)}, f32[2,1,8]{2,1,0:T(1,128)}) custom-call(bf16[2,264,128]{2,1,0:T(8,128)(2,1)S(1)} %get-tuple-element.29.refs_0_, bf16[2,264,128]{2,1,0:T(8,128)(2,1)S(1)} %collective-permute-done.refs_1_, ...), custom_call_target="tpu_custom_call" | custom-call | tf_op jit(solution)/shard_map/pallas_call | solution.py:108
  39.8 0.8 %collective-permute-start.9 = (f32[4,8,128]{2,1,0:T(8,128)S(1)}, f32[4,8,128]{2,1,0:T(8,128)S(1)}, u32[]{:S(2)}, u32[]{:S(2)}) collective-permute-start(f32[4,8,128]{2,1,0:T(8,128)S(1)} %get-tuple-element.43), channel_id=1, source_target_pairs={{0,1},{1,0},{2,3},{3,2},{4,5},{5,4},{6,7},{7,6},{8,9},{9,8},{10,11... | collective-permute-start | bytes 49160 | tf_op jit(solution)/shard_map/ppermute | solution.py:291
  40.7 0.8 %collective-permute-done.9.got_ref = f32[4,8,128]{2,1,0:T(8,128)S(1)} collective-permute-done((f32[4,8,128]{2,1,0:T(8,128)S(1)}, f32[4,8,128]{2,1,0:T(8,128)S(1)}, u32[]{:S(2)}, u32[]{:S(2)}) %collective-permute-start.9) | collective-permute-done | bytes 16416 | tf_op jit(solution)/shard_map/ppermute | solution.py:291
  41.5 1.2 %collective-permute-start.10 = (f32[8,128]{1,0:T(8,128)S(1)}, f32[8,128]{1,0:T(8,128)S(1)}, u32[]{:S(2)}, u32[]{:S(2)}) collective-permute-start(f32[8,128]{1,0:T(8,128)S(1)} %get-tuple-element.45), channel_id=1, source_target_pairs={{0,2},{2,4},{4,6},{6,0},{1,3},{3,5},{5,7},{7,1},{8,10},{10,12},{12... | collective-permute-start | bytes 12296 | tf_op jit(solution)/shard_map/ppermute | solution.py:291
  42.7 2.4 %collective-permute-start.11 = (f32[8,128]{1,0:T(8,128)S(1)}, f32[8,128]{1,0:T(8,128)S(1)}, u32[]{:S(2)}, u32[]{:S(2)}) collective-permute-start(f32[8,128]{1,0:T(8,128)S(1)} %get-tuple-element.46), channel_id=1, source_target_pairs={{0,4},{2,6},{4,0},{6,2},{1,5},{3,7},{5,1},{7,3},{8,12},{10,14},{12... | collective-permute-start | bytes 12296 | tf_op jit(solution)/shard_map/ppermute | solution.py:291
  45.2 1.2 %collective-permute-start.12 = (f32[8,128]{1,0:T(8,128)S(1)}, f32[8,128]{1,0:T(8,128)S(1)}, u32[]{:S(2)}, u32[]{:S(2)}) collective-permute-start(f32[8,128]{1,0:T(8,128)S(1)} %get-tuple-element.47), channel_id=1, source_target_pairs={{0,6},{2,0},{4,2},{6,4},{1,7},{3,1},{5,3},{7,5},{8,14},{10,8},{12,... | collective-permute-start | bytes 12296 | tf_op jit(solution)/shard_map/ppermute | solution.py:291
  46.3 1.1 %shard_map.125 = (bf16[16,128,256]{2,1,0:T(8,128)(2,1)S(1)}, f32[16,128]{1,0:T(8,128)}) custom-call(bf16[2,264,128]{2,1,0:T(8,128)(2,1)S(1)} %get-tuple-element.29.refs_0_, bf16[2,264,128]{2,1,0:T(8,128)(2,1)S(1)} %collective-permute-done.refs_1_, bf16[2,264,128]{2,1,0:T(8,128)(2,1)S(1)} %collective-permute-done.1.refs_2_, ...), custom_call_target="tpu_custom_call" | custom-call | tf_op jit(solution)/shard_map/pallas_call | solution.py:108
  47.4 1.2 %shard_map.126 = bf16[2,8,128,128]{3,2,1,0:T(8,128)(2,1)} custom-call(bf16[2,264,128]{2,1,0:T(8,128)(2,1)S(1)} %get-tuple-element.29.refs_0_, bf16[2,264,128]{2,1,0:T(8,128)(2,1)S(1)} %collective-permute-done.refs_1_, bf16[2,264,128]{2,1,0:T(8,128)(2,1)S(1)} %collective-permute-done.1.refs_2_, bf16[2,264,128]{2,1,0:T(8,128)(2,1)S(1)} %collective-permute-done.2.refs_3_, ...), custom_call_target="tpu_custom_call" | custom-call | tf_op jit(solution)/shard_map/pallas_call | solution.py:108
  48.6 0.6 %shard_map.128 = bf16[8,128]{1,0:T(8,128)(2,1)} custom-call(f32[8,128]{1,0:T(8,128)S(1)} %get-tuple-element.44.a_ref, f32[8,128]{1,0:T(8,128)S(1)} %collective-permute-done.10.b_ref, f32[8,128]{1,0:T(8,128)S(1)} %collective-permute-done.11.c_ref, f32[8,128]{1,0:T(8,128)S(1)} %collective-permute-done.12.d_ref), custom_call_target="tpu_custom_call" | custom-call | tf_op jit(solution)/shard_map/pallas_call | solution.py:108
  (12 shorter events, 0.1 us)
Async XLA Ops:
  3.1 34.9 %copy-start = (bf16[1,128,1024]{2,1,0:T(8,128)(2,1)S(1)}, bf16[1,128,1024]{2,1,0:T(8,128)(2,1)}, u32[]{:S(2)}) copy-start(bf16[1,128,1024]{2,1,0:T(8,128)(2,1)} %param.17) | copy-start | bytes 786436
  3.2 34.9 %copy-start.1 = (bf16[8,1,128]{2,0,1:T(8,128)(2,1)S(1)}, bf16[8,1,128]{2,0,1:T(8,128)(2,1)}, u32[]{:S(2)}) copy-start(bf16[8,1,128]{2,0,1:T(8,128)(2,1)} %param.16) | copy-start | bytes 6148
  3.2 34.9 %copy-start.2 = (f32[2,1]{0,1:T(1,128)S(1)}, f32[2,1]{0,1:T(1,128)}, u32[]{:S(2)}) copy-start(f32[2,1]{0,1:T(1,128)} %param.14) | copy-start | bytes 28
  3.2 34.9 %copy-start.3 = (f32[2,1]{0,1:T(1,128)S(1)}, f32[2,1]{0,1:T(1,128)}, u32[]{:S(2)}) copy-start(f32[2,1]{0,1:T(1,128)} %param.15) | copy-start | bytes 28
  4.4 11.0 %collective-permute-start = (bf16[2,264,128]{2,1,0:T(8,128)(2,1)S(1)}, bf16[2,264,128]{2,1,0:T(8,128)(2,1)S(1)}, u32[]{:S(2)}, u32[]{:S(2)}) collective-permute-start(bf16[2,264,128]{2,1,0:T(8,128)(2,1)S(1)} %get-tuple-element.30), channel_id=1, source_target_pairs={{0,8},{8,16},{16,24},{24,0},{32,40},{40,48},{48,56},{56,32},{64,72... | collective-permute-start | bytes 405512 | tf_op jit(solution)/shard_map/ppermute | solution.py:286
  6.6 8.8 %collective-permute-start.1 = (bf16[2,264,128]{2,1,0:T(8,128)(2,1)S(1)}, bf16[2,264,128]{2,1,0:T(8,128)(2,1)S(1)}, u32[]{:S(2)}, u32[]{:S(2)}) collective-permute-start(bf16[2,264,128]{2,1,0:T(8,128)(2,1)S(1)} %get-tuple-element.31), channel_id=1, source_target_pairs={{0,16},{8,24},{16,0},{24,8},{32,48},{40,56},{48,32},{56,40},{64,80... | collective-permute-start | bytes 405512 | tf_op jit(solution)/shard_map/ppermute | solution.py:286
  10.0 9.1 %collective-permute-start.4 = (bf16[4,264,128]{2,1,0:T(8,128)(2,1)S(1)}, bf16[4,264,128]{2,1,0:T(8,128)(2,1)S(1)}, u32[]{:S(2)}, u32[]{:S(2)}) collective-permute-start(bf16[4,264,128]{2,1,0:T(8,128)(2,1)S(1)} %shard_map.121), channel_id=1, source_target_pairs={{0,96},{8,104},{16,112},{24,120},{32,0},{40,8},{48,16},{56,24},{64... | collective-permute-start | bytes 811016 | tf_op jit(solution)/shard_map/ppermute | solution.py:286
  14.4 11.4 %collective-permute-start.3 = (bf16[4,264,128]{2,1,0:T(8,128)(2,1)S(1)}, bf16[4,264,128]{2,1,0:T(8,128)(2,1)S(1)}, u32[]{:S(2)}, u32[]{:S(2)}) collective-permute-start(bf16[4,264,128]{2,1,0:T(8,128)(2,1)S(1)} %get-tuple-element.33), channel_id=1, source_target_pairs={{0,32},{8,40},{16,48},{24,56},{32,64},{40,72},{48,80},{56,88},{64,... | collective-permute-start | bytes 811016 | tf_op jit(solution)/shard_map/ppermute | solution.py:286
  14.4 4.2 %collective-permute-start.2 = (bf16[2,264,128]{2,1,0:T(8,128)(2,1)S(1)}, bf16[2,264,128]{2,1,0:T(8,128)(2,1)S(1)}, u32[]{:S(2)}, u32[]{:S(2)}) collective-permute-start(bf16[2,264,128]{2,1,0:T(8,128)(2,1)S(1)} %get-tuple-element.32), channel_id=1, source_target_pairs={{0,24},{8,0},{16,8},{24,16},{32,56},{40,32},{48,40},{56,48},{64,88... | collective-permute-start | bytes 405512 | tf_op jit(solution)/shard_map/ppermute | solution.py:286
  18.6 19.5 %collective-permute-start.8 = (bf16[4,264,128]{2,1,0:T(8,128)(2,1)S(1)}, bf16[4,264,128]{2,1,0:T(8,128)(2,1)S(1)}, u32[]{:S(2)}, u32[]{:S(2)}) collective-permute-start(bf16[4,264,128]{2,1,0:T(8,128)(2,1)S(1)} %shard_map.123), channel_id=1, source_target_pairs={{0,64},{8,72},{16,80},{24,88},{32,96},{40,104},{48,112},{56,120},{... | collective-permute-start | bytes 811016 | tf_op jit(solution)/shard_map/ppermute | solution.py:286
  25.8 12.3 %collective-permute-start.5 = (bf16[2,264,128]{2,1,0:T(8,128)(2,1)S(1)}, bf16[2,264,128]{2,1,0:T(8,128)(2,1)S(1)}, u32[]{:S(2)}, u32[]{:S(2)}) collective-permute-start(bf16[2,264,128]{2,1,0:T(8,128)(2,1)S(1)} %get-tuple-element.34), channel_id=1, source_target_pairs={{0,8},{8,16},{16,24},{24,0},{32,40},{40,48},{48,56},{56,32},{64,72... | collective-permute-start | bytes 405512 | tf_op jit(solution)/shard_map/ppermute | solution.py:286
  25.9 12.2 %collective-permute-start.6 = (bf16[2,264,128]{2,1,0:T(8,128)(2,1)S(1)}, bf16[2,264,128]{2,1,0:T(8,128)(2,1)S(1)}, u32[]{:S(2)}, u32[]{:S(2)}) collective-permute-start(bf16[2,264,128]{2,1,0:T(8,128)(2,1)S(1)} %get-tuple-element.35), channel_id=1, source_target_pairs={{0,16},{8,24},{16,0},{24,8},{32,48},{40,56},{48,32},{56,40},{64,80... | collective-permute-start | bytes 405512 | tf_op jit(solution)/shard_map/ppermute | solution.py:286
  28.1 9.9 %collective-permute-start.7 = (bf16[2,264,128]{2,1,0:T(8,128)(2,1)S(1)}, bf16[2,264,128]{2,1,0:T(8,128)(2,1)S(1)}, u32[]{:S(2)}, u32[]{:S(2)}) collective-permute-start(bf16[2,264,128]{2,1,0:T(8,128)(2,1)S(1)} %get-tuple-element.36), channel_id=1, source_target_pairs={{0,24},{8,0},{16,8},{24,16},{32,56},{40,32},{48,40},{56,48},{64,88... | collective-permute-start | bytes 405512 | tf_op jit(solution)/shard_map/ppermute | solution.py:286
  39.8 1.7 %collective-permute-start.9 = (f32[4,8,128]{2,1,0:T(8,128)S(1)}, f32[4,8,128]{2,1,0:T(8,128)S(1)}, u32[]{:S(2)}, u32[]{:S(2)}) collective-permute-start(f32[4,8,128]{2,1,0:T(8,128)S(1)} %get-tuple-element.43), channel_id=1, source_target_pairs={{0,1},{1,0},{2,3},{3,2},{4,5},{5,4},{6,7},{7,6},{8,9},{9,8},{10,11... | collective-permute-start | bytes 49160 | tf_op jit(solution)/shard_map/ppermute | solution.py:291
  41.5 7.1 %collective-permute-start.10 = (f32[8,128]{1,0:T(8,128)S(1)}, f32[8,128]{1,0:T(8,128)S(1)}, u32[]{:S(2)}, u32[]{:S(2)}) collective-permute-start(f32[8,128]{1,0:T(8,128)S(1)} %get-tuple-element.45), channel_id=1, source_target_pairs={{0,2},{2,4},{4,6},{6,0},{1,3},{3,5},{5,7},{7,1},{8,10},{10,12},{12... | collective-permute-start | bytes 12296 | tf_op jit(solution)/shard_map/ppermute | solution.py:291
  42.7 5.8 %collective-permute-start.11 = (f32[8,128]{1,0:T(8,128)S(1)}, f32[8,128]{1,0:T(8,128)S(1)}, u32[]{:S(2)}, u32[]{:S(2)}) collective-permute-start(f32[8,128]{1,0:T(8,128)S(1)} %get-tuple-element.46), channel_id=1, source_target_pairs={{0,4},{2,6},{4,0},{6,2},{1,5},{3,7},{5,1},{7,3},{8,12},{10,14},{12... | collective-permute-start | bytes 12296 | tf_op jit(solution)/shard_map/ppermute | solution.py:291
  45.2 3.4 %collective-permute-start.12 = (f32[8,128]{1,0:T(8,128)S(1)}, f32[8,128]{1,0:T(8,128)S(1)}, u32[]{:S(2)}, u32[]{:S(2)}) collective-permute-start(f32[8,128]{1,0:T(8,128)S(1)} %get-tuple-element.47), channel_id=1, source_target_pairs={{0,6},{2,0},{4,2},{6,4},{1,7},{3,1},{5,3},{7,5},{8,14},{10,8},{12,... | collective-permute-start | bytes 12296 | tf_op jit(solution)/shard_map/ppermute | solution.py:291

commit v3 on v2

--- a/solution.py
+++ b/solution.py
@@ -83,8 +83,11 @@
 
 
 def third_kernel(rest_ref, w_ref, g_ref, *outs):
-    for half in range(2):
-        project_blocks(rest_ref, (half + 1) * ROW, w_ref[...], g_ref[...], [out.at[half] for out in outs])
+    project_blocks(rest_ref, ROW, w_ref[...], g_ref[...], outs)
+
+
+def own_kernel(rest_ref, w_ref, g_ref, *outs):
+    project_blocks(rest_ref, 2 * ROW, w_ref[...], g_ref[...], outs)
 
 
 ANY = pl.BlockSpec(memory_space=pl.ANY)
@@ -134,7 +137,7 @@
 
 def gather_kernel(*refs):
     for i in range(ROW):
-        refs[ROW][i] = refs[i][0]
+        refs[ROW][i] = refs[i][...]
 
 
 def pair_kernel(a_ref, b_ref, *outs):
@@ -162,8 +165,7 @@
 
 
 def landed(refs):
-    c0, c1, c2, c3, up, down, s1, s2, s3, far = refs
-    own = [c.at[1] for c in (c0, c1, c2, c3)]
+    own, (up, down, s1, s2, s3, far) = list(refs[:ROW]), refs[ROW:]
     from_up = [up.at[0]] + [s.at[0] for s in (s1, s2, s3)]
     from_down = [down.at[0]] + [s.at[1] for s in (s1, s2, s3)]
     return own + from_up + [far.at[k] for k in range(ROW)] + from_down
@@ -299,13 +301,15 @@
     up = shift(up, 1, 0)
     down = run(second_kernel, block(ROW), (later, w, gates))
     down = shift(down, 3, 0)
-    cross = run(third_kernel, (block(2),) * ROW, (later, w, gates))
+    cross = run(third_kernel, (block(),) * ROW, (later, w, gates))
     cross = [cross[0]] + [shift(cross[k], 0, k) for k in hops]
     far = run(gather_kernel, block(ROW), cross, 4)
     far = shift(far, 2, 0)
+    own = run(own_kernel, (block(),) * ROW, (later, w, gates))
+    own = [own[0]] + [shift(own[k], 0, k) for k in hops]
     side = run(pair_kernel, (block(2),) * 3, (up, down), 4)
     side = [shift(blocks, 0, k) for k, blocks in zip(hops, side)]
-    blocks = (*cross, up, down, *side, far)
+    blocks = (*own, up, down, *side, far)
     half = pltpu.VMEM((TPX, OWN, HD), F32)
     keep, send, weight, turned, stab = run(
         read_kernel,

time: 49.3 us -> 46.9 us (0.951)
  the two profiles are of different devices: /device:TPU:1 before, /device:TPU:32 now
where the time goes in v3:
time: 46.9 us; the launch traced here: 46.8 us
  starting transfers between devices  27.4 us (58%)
  waiting for transfers between devices  9.32 us (20%)
  Pallas kernels  9.24 us (20%)
  between operations  0.74 us (2%)
    ppermute x12, starting transfers between devices, shift(): return lax.ppermute(array, 'sp', pairs)  21.8 us
    ppermute x12, waiting for transfers between devices, shift(): return lax.ppermute(array, 'sp', pairs)  8.13 us
    pallas_call x10, Pallas kernels, run(): pl.pallas_call(kernel, in_specs=[VM] * len(args), out_specs=specs, out_sh...  6.74 us
    ppermute x4, starting transfers between devices, across(): lax.ppermute(array, axis, [(i, (i + hop) % size) for i in range(size)])  5.66 us
    pallas_call x1, Pallas kernels, project_near(): pl.pallas_call(near_kernel, in_specs=[ANY] * 5, out_specs=[VM] * 4, out_s...  2.51 us
    ppermute x4, waiting for transfers between devices, across(): lax.ppermute(array, axis, [(i, (i + hop) % size) for i in range(size)])  1.19 us
  transfers between devices with their start and end apart: 16, of which 6 were waited for; matrix products, arithmetic and copies ran while one was open for 0% of the time, Pallas kernels for 8%

profile of v3, /device:TPU:32, one launch (start us, length us, event | category | flops | bytes accessed | tf_op | source)
XLA Modules:
  0.0 46.8 jit_solution(11169250926040399393)
XLA Ops:
  0.6 2.5 %near.1 = (bf16[4,264,128]{2,1,0:T(8,128)(2,1)S(1)}, bf16[1024,256]{1,0:T(8,128)(2,1)S(1)}, bf16[8,1024]{1,0:T(8,128)(2,1)S(1)}, bf16[12,8,16,1024]{3,2,1,0:T(8,128)(2,1)S(1)}) custom-call(bf16[128,16,1024]{2,1,0:T(8,128)(2,1)} %x_ref.1, bf16[1024,128]{1,0:T(8,128)(2,1)} %bitcast.22, bf16[1024,128]{1,0:T(8,128)(2,1)} %bitcast.23, bf16[2,1024]{1,0:T(2,128)(2,1)} %bitcast.24, ...), custom_call_target="tpu_custom_call" | custom-call | tf_op jit(solution)/shard_map/near/pallas_call | solution.py:122
  3.1 0.7 %shard_map.121 = bf16[4,264,128]{2,1,0:T(8,128)(2,1)S(1)} custom-call(bf16[12,8,16,1024]{3,2,1,0:T(8,128)(2,1)S(1)} %get-tuple-element.30.rest_ref, bf16[1024,256]{1,0:T(8,128)(2,1)S(1)} %get-tuple-element.31.w_ref, bf16[8,1024]{1,0:T(8,128)(2,1)S(1)} %get-tuple-element.32.g_ref), custom_call_target="tpu_custom_call" | custom-call | tf_op jit(solution)/shard_map/pallas_call | solution.py:111
  3.8 1.9 %collective-permute-start.4 = (bf16[4,264,128]{2,1,0:T(8,128)(2,1)S(1)}, bf16[4,264,128]{2,1,0:T(8,128)(2,1)S(1)}, u32[]{:S(2)}, u32[]{:S(2)}) collective-permute-start(bf16[4,264,128]{2,1,0:T(8,128)(2,1)S(1)} %shard_map.121), channel_id=1, source_target_pairs={{0,96},{8,104},{16,112},{24,120},{32,0},{40,8},{48,16},{56,24},{64... | collective-permute-start | bytes 811016 | tf_op jit(solution)/shard_map/ppermute | solution.py:288
  5.8 0.3 collective-permute-start.3
  6.0 0.7 %shard_map.123 = (bf16[264,128]{1,0:T(8,128)(2,1)S(1)}, bf16[264,128]{1,0:T(8,128)(2,1)S(1)}, bf16[264,128]{1,0:T(8,128)(2,1)S(1)}, bf16[264,128]{1,0:T(8,128)(2,1)S(1)}) custom-call(bf16[12,8,16,1024]{3,2,1,0:T(8,128)(2,1)S(1)} %get-tuple-element.30.rest_ref, bf16[1024,256]{1,0:T(8,128)(2,1)S(1)} %get-tuple-element.31.w_ref, ...), custom_call_target="tpu_custom_call" | custom-call | tf_op jit(solution)/shard_map/pallas_call | solution.py:111
  6.7 1.7 %collective-permute-start.8 = (bf16[264,128]{1,0:T(8,128)(2,1)S(1)}, bf16[264,128]{1,0:T(8,128)(2,1)S(1)}, u32[]{:S(2)}, u32[]{:S(2)}) collective-permute-start(bf16[264,128]{1,0:T(8,128)(2,1)S(1)} %get-tuple-element.42), channel_id=1, source_target_pairs={{0,8},{8,16},{16,24},{24,0},{32,40},{40,48},{48,56},{56,32},{64,72... | collective-permute-start | bytes 202760 | tf_op jit(solution)/shard_map/ppermute | solution.py:288
  8.4 2.9 %collective-permute-start.9 = (bf16[264,128]{1,0:T(8,128)(2,1)S(1)}, bf16[264,128]{1,0:T(8,128)(2,1)S(1)}, u32[]{:S(2)}, u32[]{:S(2)}) collective-permute-start(bf16[264,128]{1,0:T(8,128)(2,1)S(1)} %get-tuple-element.43), channel_id=1, source_target_pairs={{0,16},{8,24},{16,0},{24,8},{32,48},{40,56},{48,32},{56,40},{64,80... | collective-permute-start | bytes 202760 | tf_op jit(solution)/shard_map/ppermute | solution.py:288
  11.3 1.3 %collective-permute-start.10 = (bf16[264,128]{1,0:T(8,128)(2,1)S(1)}, bf16[264,128]{1,0:T(8,128)(2,1)S(1)}, u32[]{:S(2)}, u32[]{:S(2)}) collective-permute-start(bf16[264,128]{1,0:T(8,128)(2,1)S(1)} %get-tuple-element.44), channel_id=1, source_target_pairs={{0,24},{8,0},{16,8},{24,16},{32,56},{40,32},{48,40},{56,48},{64,88... | collective-permute-start | bytes 202760 | tf_op jit(solution)/shard_map/ppermute | solution.py:288
  12.6 0.4 collective-permute-done.8.refs_1_
  13.0 1.2 %collective-permute-done.9.refs_2_ = bf16[264,128]{1,0:T(8,128)(2,1)S(1)} collective-permute-done((bf16[264,128]{1,0:T(8,128)(2,1)S(1)}, bf16[264,128]{1,0:T(8,128)(2,1)S(1)}, u32[]{:S(2)}, u32[]{:S(2)}) %collective-permute-start.9) | collective-permute-done | bytes 67616 | tf_op jit(solution)/shard_map/ppermute | solution.py:288
  14.3 1.3 %collective-permute-done.10.refs_3_ = bf16[264,128]{1,0:T(8,128)(2,1)S(1)} collective-permute-done((bf16[264,128]{1,0:T(8,128)(2,1)S(1)}, bf16[264,128]{1,0:T(8,128)(2,1)S(1)}, u32[]{:S(2)}, u32[]{:S(2)}) %collective-permute-start.10) | collective-permute-done | bytes 67616 | tf_op jit(solution)/shard_map/ppermute | solution.py:288
  15.6 5.2 %collective-permute-start.11 = (bf16[4,264,128]{2,1,0:T(8,128)(2,1)S(1)}, bf16[4,264,128]{2,1,0:T(8,128)(2,1)S(1)}, u32[]{:S(2)}, u32[]{:S(2)}) collective-permute-start(bf16[4,264,128]{2,1,0:T(8,128)(2,1)S(1)} %shard_map.124), channel_id=1, source_target_pairs={{0,64},{8,72},{16,80},{24,88},{32,96},{40,104},{48,112},{56,120},{... | collective-permute-start | bytes 811016 | tf_op jit(solution)/shard_map/ppermute | solution.py:288
  20.8 0.7 %shard_map.120 = (bf16[264,128]{1,0:T(8,128)(2,1)S(1)}, bf16[264,128]{1,0:T(8,128)(2,1)S(1)}, bf16[264,128]{1,0:T(8,128)(2,1)S(1)}, bf16[264,128]{1,0:T(8,128)(2,1)S(1)}) custom-call(bf16[12,8,16,1024]{3,2,1,0:T(8,128)(2,1)S(1)} %get-tuple-element.30.rest_ref, bf16[1024,256]{1,0:T(8,128)(2,1)S(1)} %get-tuple-element.31.w_ref, ...), custom_call_target="tpu_custom_call" | custom-call | tf_op jit(solution)/shard_map/pallas_call | solution.py:111
  21.5 0.4 collective-permute-start
  21.9 3.7 %collective-permute-start.1 = (bf16[264,128]{1,0:T(8,128)(2,1)S(1)}, bf16[264,128]{1,0:T(8,128)(2,1)S(1)}, u32[]{:S(2)}, u32[]{:S(2)}) collective-permute-start(bf16[264,128]{1,0:T(8,128)(2,1)S(1)} %get-tuple-element.35), channel_id=1, source_target_pairs={{0,16},{8,24},{16,0},{24,8},{32,48},{40,56},{48,32},{56,40},{64,80... | collective-permute-start | bytes 202760 | tf_op jit(solution)/shard_map/ppermute | solution.py:288
  25.6 0.0 collective-permute-done.3.a_ref.refs_4_
  25.6 0.1 collective-permute-start.5
  25.8 1.5 %collective-permute-start.6 = (bf16[2,264,128]{2,1,0:T(8,128)(2,1)S(1)}, bf16[2,264,128]{2,1,0:T(8,128)(2,1)S(1)}, u32[]{:S(2)}, u32[]{:S(2)}) collective-permute-start(bf16[2,264,128]{2,1,0:T(8,128)(2,1)S(1)} %get-tuple-element.39), channel_id=1, source_target_pairs={{0,16},{8,24},{16,0},{24,8},{32,48},{40,56},{48,32},{56,40},{64,80... | collective-permute-start | bytes 405512 | tf_op jit(solution)/shard_map/ppermute | solution.py:288
  27.3 1.7 %collective-permute-start.7 = (bf16[2,264,128]{2,1,0:T(8,128)(2,1)S(1)}, bf16[2,264,128]{2,1,0:T(8,128)(2,1)S(1)}, u32[]{:S(2)}, u32[]{:S(2)}) collective-permute-start(bf16[2,264,128]{2,1,0:T(8,128)(2,1)S(1)} %get-tuple-element.40), channel_id=1, source_target_pairs={{0,24},{8,0},{16,8},{24,16},{32,56},{40,32},{48,40},{56,48},{64,88... | collective-permute-start | bytes 405512 | tf_op jit(solution)/shard_map/ppermute | solution.py:288
  28.9 0.9 %collective-permute-done.1.refs_2_ = bf16[264,128]{1,0:T(8,128)(2,1)S(1)} collective-permute-done((bf16[264,128]{1,0:T(8,128)(2,1)S(1)}, bf16[264,128]{1,0:T(8,128)(2,1)S(1)}, u32[]{:S(2)}, u32[]{:S(2)}) %collective-permute-start.1) | collective-permute-done | bytes 67616 | tf_op jit(solution)/shard_map/ppermute | solution.py:288
  29.8 1.1 %collective-permute-start.2 = (bf16[264,128]{1,0:T(8,128)(2,1)S(1)}, bf16[264,128]{1,0:T(8,128)(2,1)S(1)}, u32[]{:S(2)}, u32[]{:S(2)}) collective-permute-start(bf16[264,128]{1,0:T(8,128)(2,1)S(1)} %get-tuple-element.36), channel_id=1, source_target_pairs={{0,24},{8,0},{16,8},{24,16},{32,56},{40,32},{48,40},{56,48},{64,88... | collective-permute-start | bytes 202760 | tf_op jit(solution)/shard_map/ppermute | solution.py:288
  31.0 4.3 %collective-permute-done.2.refs_3_ = bf16[264,128]{1,0:T(8,128)(2,1)S(1)} collective-permute-done((bf16[264,128]{1,0:T(8,128)(2,1)S(1)}, bf16[264,128]{1,0:T(8,128)(2,1)S(1)}, u32[]{:S(2)}, u32[]{:S(2)}) %collective-permute-start.2) | collective-permute-done | bytes 67616 | tf_op jit(solution)/shard_map/ppermute | solution.py:288
  35.2 0.0 collective-permute-done.11.refs_9_
  35.2 0.0 collective-permute-done.5.refs_6_
  35.3 1.8 %shard_map.125 = (f32[4,8,128]{2,1,0:T(8,128)S(1)}, f32[4,8,128]{2,1,0:T(8,128)S(1)}, f32[32,128]{1,0:T(8,128)S(1)}, f32[128,32]{1,0:T(8,128)S(1)}, f32[2,1,8]{2,1,0:T(1,128)}) custom-call(bf16[264,128]{1,0:T(8,128)(2,1)S(1)} %get-tuple-element.33.refs_0_, bf16[264,128]{1,0:T(8,128)(2,1)S(1)} %collective-permute-done.refs_1_, ...), custom_call_target="tpu_custom_call" | custom-call | tf_op jit(solution)/shard_map/pallas_call | solution.py:111
  37.1 1.2 %collective-permute-done.12.got_ref = f32[4,8,128]{2,1,0:T(8,128)S(1)} collective-permute-done((f32[4,8,128]{2,1,0:T(8,128)S(1)}, f32[4,8,128]{2,1,0:T(8,128)S(1)}, u32[]{:S(2)}, u32[]{:S(2)}) %collective-permute-start.12) | collective-permute-done | bytes 16416 | tf_op jit(solution)/shard_map/ppermute | solution.py:293
  38.3 1.5 %collective-permute-start.13 = (f32[8,128]{1,0:T(8,128)S(1)}, f32[8,128]{1,0:T(8,128)S(1)}, u32[]{:S(2)}, u32[]{:S(2)}) collective-permute-start(f32[8,128]{1,0:T(8,128)S(1)} %get-tuple-element.53), channel_id=1, source_target_pairs={{0,2},{2,4},{4,6},{6,0},{1,3},{3,5},{5,7},{7,1},{8,10},{10,12},{12... | collective-permute-start | bytes 12296 | tf_op jit(solution)/shard_map/ppermute | solution.py:293
  39.7 2.7 %collective-permute-start.14 = (f32[8,128]{1,0:T(8,128)S(1)}, f32[8,128]{1,0:T(8,128)S(1)}, u32[]{:S(2)}, u32[]{:S(2)}) collective-permute-start(f32[8,128]{1,0:T(8,128)S(1)} %get-tuple-element.54), channel_id=1, source_target_pairs={{0,4},{2,6},{4,0},{6,2},{1,5},{3,7},{5,1},{7,3},{8,12},{10,14},{12... | collective-permute-start | bytes 12296 | tf_op jit(solution)/shard_map/ppermute | solution.py:293
  42.5 1.4 %collective-permute-start.15 = (f32[8,128]{1,0:T(8,128)S(1)}, f32[8,128]{1,0:T(8,128)S(1)}, u32[]{:S(2)}, u32[]{:S(2)}) collective-permute-start(f32[8,128]{1,0:T(8,128)S(1)} %get-tuple-element.55), channel_id=1, source_target_pairs={{0,6},{2,0},{4,2},{6,4},{1,7},{3,1},{5,3},{7,5},{8,14},{10,8},{12,... | collective-permute-start | bytes 12296 | tf_op jit(solution)/shard_map/ppermute | solution.py:293
  43.9 1.1 %shard_map.126 = (bf16[16,128,256]{2,1,0:T(8,128)(2,1)S(1)}, f32[16,128]{1,0:T(8,128)}) custom-call(bf16[264,128]{1,0:T(8,128)(2,1)S(1)} %get-tuple-element.33.refs_0_, bf16[264,128]{1,0:T(8,128)(2,1)S(1)} %collective-permute-done.refs_1_, bf16[264,128]{1,0:T(8,128)(2,1)S(1)} %collective-permute-done.1.refs_2_, ...), custom_call_target="tpu_custom_call" | custom-call | tf_op jit(solution)/shard_map/pallas_call | solution.py:111
  45.0 1.2 %shard_map.127 = bf16[2,8,128,128]{3,2,1,0:T(8,128)(2,1)} custom-call(bf16[264,128]{1,0:T(8,128)(2,1)S(1)} %get-tuple-element.33.refs_0_, bf16[264,128]{1,0:T(8,128)(2,1)S(1)} %collective-permute-done.refs_1_, bf16[264,128]{1,0:T(8,128)(2,1)S(1)} %collective-permute-done.1.refs_2_, bf16[264,128]{1,0:T(8,128)(2,1)S(1)} %collective-permute-done.2.refs_3_, ...), custom_call_target="tpu_custom_call" | custom-call | tf_op jit(solution)/shard_map/pallas_call | solution.py:111
  46.2 0.6 %shard_map.129 = bf16[8,128]{1,0:T(8,128)(2,1)} custom-call(f32[8,128]{1,0:T(8,128)S(1)} %get-tuple-element.52.a_ref, f32[8,128]{1,0:T(8,128)S(1)} %collective-permute-done.13.b_ref, f32[8,128]{1,0:T(8,128)S(1)} %collective-permute-done.14.c_ref, f32[8,128]{1,0:T(8,128)S(1)} %collective-permute-done.15.d_ref), custom_call_target="tpu_custom_call" | custom-call | tf_op jit(solution)/shard_map/pallas_call | solution.py:111
  (19 shorter events, 0.1 us)
Async XLA Ops:
  3.8 21.7 %collective-permute-start.4 = (bf16[4,264,128]{2,1,0:T(8,128)(2,1)S(1)}, bf16[4,264,128]{2,1,0:T(8,128)(2,1)S(1)}, u32[]{:S(2)}, u32[]{:S(2)}) collective-permute-start(bf16[4,264,128]{2,1,0:T(8,128)(2,1)S(1)} %shard_map.121), channel_id=1, source_target_pairs={{0,96},{8,104},{16,112},{24,120},{32,0},{40,8},{48,16},{56,24},{64... | collective-permute-start | bytes 811016 | tf_op jit(solution)/shard_map/ppermute | solution.py:288
  5.7 29.5 %copy-start = (bf16[1,128,1024]{2,1,0:T(8,128)(2,1)S(1)}, bf16[1,128,1024]{2,1,0:T(8,128)(2,1)}, u32[]{:S(2)}) copy-start(bf16[1,128,1024]{2,1,0:T(8,128)(2,1)} %param.17) | copy-start | bytes 786436
  5.7 29.5 %copy-start.1 = (bf16[8,1,128]{2,0,1:T(8,128)(2,1)S(1)}, bf16[8,1,128]{2,0,1:T(8,128)(2,1)}, u32[]{:S(2)}) copy-start(bf16[8,1,128]{2,0,1:T(8,128)(2,1)} %param.16) | copy-start | bytes 6148
  5.7 29.5 %copy-start.2 = (f32[2,1]{0,1:T(1,128)S(1)}, f32[2,1]{0,1:T(1,128)}, u32[]{:S(2)}) copy-start(f32[2,1]{0,1:T(1,128)} %param.14) | copy-start | bytes 28
  5.7 29.5 %copy-start.3 = (f32[2,1]{0,1:T(1,128)S(1)}, f32[2,1]{0,1:T(1,128)}, u32[]{:S(2)}) copy-start(f32[2,1]{0,1:T(1,128)} %param.15) | copy-start | bytes 28
  5.8 19.8 %collective-permute-start.3 = (bf16[4,264,128]{2,1,0:T(8,128)(2,1)S(1)}, bf16[4,264,128]{2,1,0:T(8,128)(2,1)S(1)}, u32[]{:S(2)}, u32[]{:S(2)}) collective-permute-start(bf16[4,264,128]{2,1,0:T(8,128)(2,1)S(1)} %get-tuple-element.37), channel_id=1, source_target_pairs={{0,32},{8,40},{16,48},{24,56},{32,64},{40,72},{48,80},{56,88},{64,... | collective-permute-start | bytes 811016 | tf_op jit(solution)/shard_map/ppermute | solution.py:288
  6.7 6.3 %collective-permute-start.8 = (bf16[264,128]{1,0:T(8,128)(2,1)S(1)}, bf16[264,128]{1,0:T(8,128)(2,1)S(1)}, u32[]{:S(2)}, u32[]{:S(2)}) collective-permute-start(bf16[264,128]{1,0:T(8,128)(2,1)S(1)} %get-tuple-element.42), channel_id=1, source_target_pairs={{0,8},{8,16},{16,24},{24,0},{32,40},{40,48},{48,56},{56,32},{64,72... | collective-permute-start | bytes 202760 | tf_op jit(solution)/shard_map/ppermute | solution.py:288
  8.4 5.9 %collective-permute-start.9 = (bf16[264,128]{1,0:T(8,128)(2,1)S(1)}, bf16[264,128]{1,0:T(8,128)(2,1)S(1)}, u32[]{:S(2)}, u32[]{:S(2)}) collective-permute-start(bf16[264,128]{1,0:T(8,128)(2,1)S(1)} %get-tuple-element.43), channel_id=1, source_target_pairs={{0,16},{8,24},{16,0},{24,8},{32,48},{40,56},{48,32},{56,40},{64,80... | collective-permute-start | bytes 202760 | tf_op jit(solution)/shard_map/ppermute | solution.py:288
  11.3 4.3 %collective-permute-start.10 = (bf16[264,128]{1,0:T(8,128)(2,1)S(1)}, bf16[264,128]{1,0:T(8,128)(2,1)S(1)}, u32[]{:S(2)}, u32[]{:S(2)}) collective-permute-start(bf16[264,128]{1,0:T(8,128)(2,1)S(1)} %get-tuple-element.44), channel_id=1, source_target_pairs={{0,24},{8,0},{16,8},{24,16},{32,56},{40,32},{48,40},{56,48},{64,88... | collective-permute-start | bytes 202760 | tf_op jit(solution)/shard_map/ppermute | solution.py:288
  15.6 19.6 %collective-permute-start.11 = (bf16[4,264,128]{2,1,0:T(8,128)(2,1)S(1)}, bf16[4,264,128]{2,1,0:T(8,128)(2,1)S(1)}, u32[]{:S(2)}, u32[]{:S(2)}) collective-permute-start(bf16[4,264,128]{2,1,0:T(8,128)(2,1)S(1)} %shard_map.124), channel_id=1, source_target_pairs={{0,64},{8,72},{16,80},{24,88},{32,96},{40,104},{48,112},{56,120},{... | collective-permute-start | bytes 811016 | tf_op jit(solution)/shard_map/ppermute | solution.py:288
  21.5 5.8 %collective-permute-start = (bf16[264,128]{1,0:T(8,128)(2,1)S(1)}, bf16[264,128]{1,0:T(8,128)(2,1)S(1)}, u32[]{:S(2)}, u32[]{:S(2)}) collective-permute-start(bf16[264,128]{1,0:T(8,128)(2,1)S(1)} %get-tuple-element.34), channel_id=1, source_target_pairs={{0,8},{8,16},{16,24},{24,0},{32,40},{40,48},{48,56},{56,32},{64,72... | collective-permute-start | bytes 202760 | tf_op jit(solution)/shard_map/ppermute | solution.py:288
  21.9 7.9 %collective-permute-start.1 = (bf16[264,128]{1,0:T(8,128)(2,1)S(1)}, bf16[264,128]{1,0:T(8,128)(2,1)S(1)}, u32[]{:S(2)}, u32[]{:S(2)}) collective-permute-start(bf16[264,128]{1,0:T(8,128)(2,1)S(1)} %get-tuple-element.35), channel_id=1, source_target_pairs={{0,16},{8,24},{16,0},{24,8},{32,48},{40,56},{48,32},{56,40},{64,80... | collective-permute-start | bytes 202760 | tf_op jit(solution)/shard_map/ppermute | solution.py:288
  25.6 9.6 %collective-permute-start.5 = (bf16[2,264,128]{2,1,0:T(8,128)(2,1)S(1)}, bf16[2,264,128]{2,1,0:T(8,128)(2,1)S(1)}, u32[]{:S(2)}, u32[]{:S(2)}) collective-permute-start(bf16[2,264,128]{2,1,0:T(8,128)(2,1)S(1)} %get-tuple-element.38), channel_id=1, source_target_pairs={{0,8},{8,16},{16,24},{24,0},{32,40},{40,48},{48,56},{56,32},{64,72... | collective-permute-start | bytes 405512 | tf_op jit(solution)/shard_map/ppermute | solution.py:288
  25.8 9.5 %collective-permute-start.6 = (bf16[2,264,128]{2,1,0:T(8,128)(2,1)S(1)}, bf16[2,264,128]{2,1,0:T(8,128)(2,1)S(1)}, u32[]{:S(2)}, u32[]{:S(2)}) collective-permute-start(bf16[2,264,128]{2,1,0:T(8,128)(2,1)S(1)} %get-tuple-element.39), channel_id=1, source_target_pairs={{0,16},{8,24},{16,0},{24,8},{32,48},{40,56},{48,32},{56,40},{64,80... | collective-permute-start | bytes 405512 | tf_op jit(solution)/shard_map/ppermute | solution.py:288
  27.3 8.0 %collective-permute-start.7 = (bf16[2,264,128]{2,1,0:T(8,128)(2,1)S(1)}, bf16[2,264,128]{2,1,0:T(8,128)(2,1)S(1)}, u32[]{:S(2)}, u32[]{:S(2)}) collective-permute-start(bf16[2,264,128]{2,1,0:T(8,128)(2,1)S(1)} %get-tuple-element.40), channel_id=1, source_target_pairs={{0,24},{8,0},{16,8},{24,16},{32,56},{40,32},{48,40},{56,48},{64,88... | collective-permute-start | bytes 405512 | tf_op jit(solution)/shard_map/ppermute | solution.py:288
  29.8 5.4 %collective-permute-start.2 = (bf16[264,128]{1,0:T(8,128)(2,1)S(1)}, bf16[264,128]{1,0:T(8,128)(2,1)S(1)}, u32[]{:S(2)}, u32[]{:S(2)}) collective-permute-start(bf16[264,128]{1,0:T(8,128)(2,1)S(1)} %get-tuple-element.36), channel_id=1, source_target_pairs={{0,24},{8,0},{16,8},{24,16},{32,56},{40,32},{48,40},{56,48},{64,88... | collective-permute-start | bytes 202760 | tf_op jit(solution)/shard_map/ppermute | solution.py:288
  37.1 1.2 %collective-permute-start.12 = (f32[4,8,128]{2,1,0:T(8,128)S(1)}, f32[4,8,128]{2,1,0:T(8,128)S(1)}, u32[]{:S(2)}, u32[]{:S(2)}) collective-permute-start(f32[4,8,128]{2,1,0:T(8,128)S(1)} %get-tuple-element.51), channel_id=1, source_target_pairs={{0,1},{1,0},{2,3},{3,2},{4,5},{5,4},{6,7},{7,6},{8,9},{9,8},{10,11... | collective-permute-start | bytes 49160 | tf_op jit(solution)/shard_map/ppermute | solution.py:293
  38.3 7.9 %collective-permute-start.13 = (f32[8,128]{1,0:T(8,128)S(1)}, f32[8,128]{1,0:T(8,128)S(1)}, u32[]{:S(2)}, u32[]{:S(2)}) collective-permute-start(f32[8,128]{1,0:T(8,128)S(1)} %get-tuple-element.53), channel_id=1, source_target_pairs={{0,2},{2,4},{4,6},{6,0},{1,3},{3,5},{5,7},{7,1},{8,10},{10,12},{12... | collective-permute-start | bytes 12296 | tf_op jit(solution)/shard_map/ppermute | solution.py:293
  39.7 6.4 %collective-permute-start.14 = (f32[8,128]{1,0:T(8,128)S(1)}, f32[8,128]{1,0:T(8,128)S(1)}, u32[]{:S(2)}, u32[]{:S(2)}) collective-permute-start(f32[8,128]{1,0:T(8,128)S(1)} %get-tuple-element.54), channel_id=1, source_target_pairs={{0,4},{2,6},{4,0},{6,2},{1,5},{3,7},{5,1},{7,3},{8,12},{10,14},{12... | collective-permute-start | bytes 12296 | tf_op jit(solution)/shard_map/ppermute | solution.py:293
  42.5 3.7 %collective-permute-start.15 = (f32[8,128]{1,0:T(8,128)S(1)}, f32[8,128]{1,0:T(8,128)S(1)}, u32[]{:S(2)}, u32[]{:S(2)}) collective-permute-start(f32[8,128]{1,0:T(8,128)S(1)} %get-tuple-element.55), channel_id=1, source_target_pairs={{0,6},{2,0},{4,2},{6,4},{1,7},{3,1},{5,3},{7,5},{8,14},{10,8},{12,... | collective-permute-start | bytes 12296 | tf_op jit(solution)/shard_map/ppermute | solution.py:293

commit v4 on v3

--- a/solution.py
+++ b/solution.py
@@ -34,7 +34,7 @@
     z, y = here()
     copies = []
     for i, (dz, dy) in enumerate(blocks):
-        dest = ((z + dz) % ROW) * ROW + (y + dy) % ROW
+        dest = (z ^ dz) * ROW + (y + dy) % ROW
         copies.append(pltpu.make_async_copy(x_ref.at[pl.ds(dest * OWN, OWN)], buf_ref.at[i], sem_ref.at[sem + i]))
     for copy in copies:
         copy.start()
@@ -54,7 +54,7 @@
         out[2 * ROWS :, :] = coded[:, at]
 
 
-def near_kernel(x_ref, wk_ref, wv_ref, wi_ref, wf_ref, up_ref, w_ref, g_ref, rest_ref, buf_ref, wi_buf, wf_buf, sem_ref):
+def near_kernel(x_ref, wk_ref, wv_ref, wi_ref, wf_ref, mirror_ref, w_ref, g_ref, rest_ref, buf_ref, wi_buf, wf_buf, sem_ref):
     key_copy = pltpu.make_async_copy(wk_ref, w_ref.at[:, :HD], sem_ref.at[SP])
     value_copy = pltpu.make_async_copy(wv_ref, w_ref.at[:, HD:], sem_ref.at[SP + 1])
     gate_copies = [
@@ -63,8 +63,8 @@
     ]
     for copy in (*gate_copies, key_copy, value_copy):
         copy.start()
-    copies = take(x_ref, buf_ref, sem_ref, 0, [(1, dy) for dy in range(ROW)])
-    later = take(x_ref, rest_ref, sem_ref, ROW, [(dz, dy) for dz in (3, 2, 0) for dy in range(ROW)])
+    copies = take(x_ref, buf_ref, sem_ref, 0, [(3, dy) for dy in range(ROW)])
+    later = take(x_ref, rest_ref, sem_ref, ROW, [(dz, dy) for dz in (1, 2, 0) for dy in range(ROW)])
     for copy in gate_copies:
         copy.wait()
     gates = jnp.concatenate((wi_buf[...].astype(F32), wf_buf[...].astype(F32), jnp.zeros((4, D), F32)), axis=0)
@@ -73,21 +73,21 @@
     value_copy.wait()
     for copy in copies:
         copy.wait()
-    project_blocks(buf_ref, 0, w_ref[...], g_ref[...], [up_ref.at[k] for k in range(ROW)])
+    project_blocks(buf_ref, 0, w_ref[...], g_ref[...], [mirror_ref.at[k] for k in range(ROW)])
     for copy in later:
         copy.wait()
 
 
-def second_kernel(rest_ref, w_ref, g_ref, down_ref):
-    project_blocks(rest_ref, 0, w_ref[...], g_ref[...], [down_ref.at[k] for k in range(ROW)])
+def second_kernel(rest_ref, w_ref, g_ref, twin_ref):
+    project_blocks(rest_ref, 0, w_ref[...], g_ref[...], [twin_ref.at[k] for k in range(ROW)])
 
 
 def third_kernel(rest_ref, w_ref, g_ref, *outs):
     project_blocks(rest_ref, ROW, w_ref[...], g_ref[...], outs)
 
 
-def own_kernel(rest_ref, w_ref, g_ref, *outs):
-    project_blocks(rest_ref, 2 * ROW, w_ref[...], g_ref[...], outs)
+def own_kernel(rest_ref, w_ref, g_ref, own_ref):
+    project_blocks(rest_ref, 2 * ROW, w_ref[...], g_ref[...], [own_ref.at[k] for k in range(ROW)])
 
 
 ANY = pl.BlockSpec(memory_space=pl.ANY)
@@ -140,10 +140,10 @@
         refs[ROW][i] = refs[i][...]
 
 
-def pair_kernel(a_ref, b_ref, *outs):
+def triple_kernel(a_ref, b_ref, c_ref, *outs):
     for k, out in enumerate(outs):
-        out[0] = a_ref[k + 1]
-        out[1] = b_ref[k + 1]
+        for i, ref in enumerate((a_ref, b_ref, c_ref)):
+            out[i] = ref[k + 1]
 
 
 def three_parts(a):
@@ -165,10 +165,9 @@
 
 
 def landed(refs):
-    own, (up, down, s1, s2, s3, far) = list(refs[:ROW]), refs[ROW:]
-    from_up = [up.at[0]] + [s.at[0] for s in (s1, s2, s3)]
-    from_down = [down.at[0]] + [s.at[1] for s in (s1, s2, s3)]
-    return own + from_up + [far.at[k] for k in range(ROW)] + from_down
+    own, mirror, twin, s1, s2, s3, far = refs
+    legs = [[kept.at[0]] + [s.at[i] for s in (s1, s2, s3)] for i, kept in enumerate((mirror, twin, own))]
+    return legs[2] + legs[1] + [far.at[k] for k in range(ROW)] + legs[0]
 
 
 def rows_mine():
@@ -183,8 +182,8 @@
 
 
 def read_kernel(*refs):
-    blocks = landed(refs[:10])
-    q_ref, wo_ref, ib_ref, fb_ref, keep_ref, send_ref, weight_ref, turned_ref, stab_ref = refs[10:]
+    blocks = landed(refs[:7])
+    q_ref, wo_ref, ib_ref, fb_ref, keep_ref, send_ref, weight_ref, turned_ref, stab_ref = refs[7:]
     scale = HD ** -0.5
     row, lane8, mine = rows_mine()
     query = q_ref[...]
@@ -196,7 +195,7 @@
     forget = [log_sigmoid(part(2 + g) + fb_ref[0:1, g : g + 1]) for g in range(2)]
 
     z, y = here()
-    place = lambda j: ((z - j // ROW) & 3) * ROW + ((y - j % ROW) & 3)
+    place = lambda j: (z ^ (j // ROW)) * ROW + ((y - j % ROW) & 3)
     r = lax.broadcasted_iota(jnp.int32, (HD, HD), 0)
     c = lax.broadcasted_iota(jnp.int32, (HD, HD), 1)
     same = (r // POS) == (c // POS)
@@ -209,10 +208,12 @@
     for g in range(2):
         order = (r > c) if g == 0 else (r < c)
         inside = jnp.concatenate((ones(same & order), ones(same)), axis=1)
-        sums = sum(dot(p, inside) for p in three_parts(forget[g]))
+        sums = dot(jnp.concatenate(three_parts(forget[g]), axis=0), inside)
+        sums = sums[:SP] + sums[SP : 2 * SP] + sums[2 * SP :]
         block = sums[:, HD:]
         across = ones(((place(jc) > place(jr)) if g == 0 else (place(jc) < place(jr))) | (jr >= SP))
-        outside = sum(dot(across, p) for p in three_parts(block))
+        outside = dot(across, jnp.concatenate(three_parts(block), axis=1))
+        outside = outside[:, :HD] + outside[:, HD : 2 * HD] + outside[:, 2 * HD :]
         log_weight.append(in_pre[g] + sums[:, :HD] + outside[:SP])
         total.append(outside[SP : SP + 1])
     stab = [
@@ -247,8 +248,8 @@
 
 
 def weigh_kernel(*refs):
-    blocks = landed(refs[:10])
-    weight_ref, turned_ref, vw_ref, norm_ref = refs[10:]
+    blocks = landed(refs[:7])
+    weight_ref, turned_ref, vw_ref, norm_ref = refs[7:]
     _, _, mine = rows_mine()
     norm = jnp.zeros((4 * OWN, HD), F32)
     for j, blk in enumerate(blocks):
@@ -262,8 +263,8 @@
 
 
 def memory_kernel(*refs):
-    blocks = landed(refs[:10])
-    vw_ref, mem_ref = refs[10:]
+    blocks = landed(refs[:7])
+    vw_ref, mem_ref = refs[7:]
     for s in range(OWN):
         at = slice(s * POS, (s + 1) * POS)
         keys = jnp.concatenate([blk[at, :] for blk in blocks], axis=0)
@@ -284,7 +285,7 @@
 
 def shift(array, dz, dy):
     spots = [(z, y) for z in range(ROW) for y in range(ROW)]
-    pairs = [(z * ROW + y, ((z + dz) % ROW) * ROW + (y + dy) % ROW) for z, y in spots]
+    pairs = [(z * ROW + y, (z ^ dz) * ROW + (y + dy) % ROW) for z, y in spots]
     return lax.ppermute(array, "sp", pairs)
 
 
@@ -295,21 +296,20 @@
 
 def step(prompt, w_key, w_value, w_in_gate, w_forget_gate, in_bias, forget_bias, query, w_out):
     hops = range(1, ROW)
-    up, w, gates, later = project_near(
+    mirror, w, gates, later = project_near(
         prompt, w_key.reshape(D, HD), w_value.reshape(D, HD), w_in_gate.reshape(2, D), w_forget_gate.reshape(2, D)
     )
-    up = shift(up, 1, 0)
-    down = run(second_kernel, block(ROW), (later, w, gates))
-    down = shift(down, 3, 0)
+    mirror = shift(mirror, 3, 0)
+    twin = run(second_kernel, block(ROW), (later, w, gates))
+    twin = shift(twin, 1, 0)
     cross = run(third_kernel, (block(),) * ROW, (later, w, gates))
     cross = [cross[0]] + [shift(cross[k], 0, k) for k in hops]
     far = run(gather_kernel, block(ROW), cross, 4)
     far = shift(far, 2, 0)
-    own = run(own_kernel, (block(),) * ROW, (later, w, gates))
-    own = [own[0]] + [shift(own[k], 0, k) for k in hops]
-    side = run(pair_kernel, (block(2),) * 3, (up, down), 4)
+    own = run(own_kernel, block(ROW), (later, w, gates))
+    side = run(triple_kernel, (block(3),) * 3, (mirror, twin, own), 4)
     side = [shift(blocks, 0, k) for k, blocks in zip(hops, side)]
-    blocks = (*own, up, down, *side, far)
+    blocks = (own, mirror, twin, *side, far)
     half = pltpu.VMEM((TPX, OWN, HD), F32)
     keep, send, weight, turned, stab = run(
         read_kernel,

time: 46.9 us -> 49.9 us (1.064)
  the two profiles are of different devices: /device:TPU:32 before, /device:TPU:64 now
where the time goes in v4:
time: 49.9 us; the launch traced here: 49.8 us
  starting transfers between devices  22.1 us (44%)
  waiting for transfers between devices  17.4 us (35%)
  Pallas kernels  9.55 us (19%)
  between operations  0.72 us (1%)
    ppermute x9, starting transfers between devices, shift(): return lax.ppermute(array, 'sp', pairs)  16.4 us
    ppermute x9, waiting for transfers between devices, shift(): return lax.ppermute(array, 'sp', pairs)  16.2 us
    pallas_call x10, Pallas kernels, run(): pl.pallas_call(kernel, in_specs=[VM] * len(args), out_specs=specs, out_sh...  7.05 us
    ppermute x4, starting transfers between devices, across(): lax.ppermute(array, axis, [(i, (i + hop) % size) for i in range(size)])  5.66 us
    pallas_call x1, Pallas kernels, project_near(): pl.pallas_call(near_kernel, in_specs=[ANY] * 5, out_specs=[VM] * 4, out_s...  2.5 us
    ppermute x4, waiting for transfers between devices, across(): lax.ppermute(array, axis, [(i, (i + hop) % size) for i in range(size)])  1.19 us
  transfers between devices with their start and end apart: 13, of which 7 were waited for; matrix products, arithmetic and copies ran while one was open for 0% of the time, Pallas kernels for 7%

profile of v4, /device:TPU:64, one launch (start us, length us, event | category | flops | bytes accessed | tf_op | source)
XLA Modules:
  0.0 49.8 jit_solution(11404631775092729860)
XLA Ops:
  0.6 2.5 %near.1 = (bf16[4,264,128]{2,1,0:T(8,128)(2,1)S(1)}, bf16[1024,256]{1,0:T(8,128)(2,1)S(1)}, bf16[8,1024]{1,0:T(8,128)(2,1)S(1)}, bf16[12,8,16,1024]{3,2,1,0:T(8,128)(2,1)S(1)}) custom-call(bf16[128,16,1024]{2,1,0:T(8,128)(2,1)} %x_ref.1, bf16[1024,128]{1,0:T(8,128)(2,1)} %bitcast.22, bf16[1024,128]{1,0:T(8,128)(2,1)} %bitcast.23, bf16[2,1024]{1,0:T(2,128)(2,1)} %bitcast.24, ...), custom_call_target="tpu_custom_call" | custom-call | tf_op jit(solution)/shard_map/near/pallas_call | solution.py:122
  3.1 0.7 %shard_map.121 = bf16[4,264,128]{2,1,0:T(8,128)(2,1)S(1)} custom-call(bf16[12,8,16,1024]{3,2,1,0:T(8,128)(2,1)S(1)} %get-tuple-element.26.rest_ref, bf16[1024,256]{1,0:T(8,128)(2,1)S(1)} %get-tuple-element.27.w_ref, bf16[8,1024]{1,0:T(8,128)(2,1)S(1)} %get-tuple-element.28.g_ref), custom_call_target="tpu_custom_call" | custom-call | tf_op jit(solution)/shard_map/pallas_call | solution.py:111
  3.8 2.0 %collective-permute-start.1 = (bf16[4,264,128]{2,1,0:T(8,128)(2,1)S(1)}, bf16[4,264,128]{2,1,0:T(8,128)(2,1)S(1)}, u32[]{:S(2)}, u32[]{:S(2)}) collective-permute-start(bf16[4,264,128]{2,1,0:T(8,128)(2,1)S(1)} %shard_map.121), channel_id=1, source_target_pairs={{0,32},{8,40},{16,48},{24,56},{32,0},{40,8},{48,16},{56,24},{64,96... | collective-permute-start | bytes 811016 | tf_op jit(solution)/shard_map/ppermute | solution.py:289
  5.8 0.1 collective-permute-start
  6.0 0.7 %shard_map.123 = (bf16[264,128]{1,0:T(8,128)(2,1)S(1)}, bf16[264,128]{1,0:T(8,128)(2,1)S(1)}, bf16[264,128]{1,0:T(8,128)(2,1)S(1)}, bf16[264,128]{1,0:T(8,128)(2,1)S(1)}) custom-call(bf16[12,8,16,1024]{3,2,1,0:T(8,128)(2,1)S(1)} %get-tuple-element.26.rest_ref, bf16[1024,256]{1,0:T(8,128)(2,1)S(1)} %get-tuple-element.27.w_ref, ...), custom_call_target="tpu_custom_call" | custom-call | tf_op jit(solution)/shard_map/pallas_call | solution.py:111
  6.6 1.7 %collective-permute-start.5 = (bf16[264,128]{1,0:T(8,128)(2,1)S(1)}, bf16[264,128]{1,0:T(8,128)(2,1)S(1)}, u32[]{:S(2)}, u32[]{:S(2)}) collective-permute-start(bf16[264,128]{1,0:T(8,128)(2,1)S(1)} %get-tuple-element.34), channel_id=1, source_target_pairs={{0,8},{8,16},{16,24},{24,0},{32,40},{40,48},{48,56},{56,32},{64,72... | collective-permute-start | bytes 202760 | tf_op jit(solution)/shard_map/ppermute | solution.py:289
  8.3 2.9 %collective-permute-start.6 = (bf16[264,128]{1,0:T(8,128)(2,1)S(1)}, bf16[264,128]{1,0:T(8,128)(2,1)S(1)}, u32[]{:S(2)}, u32[]{:S(2)}) collective-permute-start(bf16[264,128]{1,0:T(8,128)(2,1)S(1)} %get-tuple-element.35), channel_id=1, source_target_pairs={{0,16},{8,24},{16,0},{24,8},{32,48},{40,56},{48,32},{56,40},{64,80... | collective-permute-start | bytes 202760 | tf_op jit(solution)/shard_map/ppermute | solution.py:289
  11.2 1.3 %collective-permute-start.7 = (bf16[264,128]{1,0:T(8,128)(2,1)S(1)}, bf16[264,128]{1,0:T(8,128)(2,1)S(1)}, u32[]{:S(2)}, u32[]{:S(2)}) collective-permute-start(bf16[264,128]{1,0:T(8,128)(2,1)S(1)} %get-tuple-element.36), channel_id=1, source_target_pairs={{0,24},{8,0},{16,8},{24,16},{32,56},{40,32},{48,40},{56,48},{64,88... | collective-permute-start | bytes 202760 | tf_op jit(solution)/shard_map/ppermute | solution.py:289
  12.6 0.4 collective-permute-done.5.refs_1_
  12.9 1.3 %collective-permute-done.6.refs_2_ = bf16[264,128]{1,0:T(8,128)(2,1)S(1)} collective-permute-done((bf16[264,128]{1,0:T(8,128)(2,1)S(1)}, bf16[264,128]{1,0:T(8,128)(2,1)S(1)}, u32[]{:S(2)}, u32[]{:S(2)}) %collective-permute-start.6) | collective-permute-done | bytes 67616 | tf_op jit(solution)/shard_map/ppermute | solution.py:289
  14.2 1.3 %collective-permute-done.7.refs_3_ = bf16[264,128]{1,0:T(8,128)(2,1)S(1)} collective-permute-done((bf16[264,128]{1,0:T(8,128)(2,1)S(1)}, bf16[264,128]{1,0:T(8,128)(2,1)S(1)}, u32[]{:S(2)}, u32[]{:S(2)}) %collective-permute-start.7) | collective-permute-done | bytes 67616 | tf_op jit(solution)/shard_map/ppermute | solution.py:289
  15.5 2.5 %collective-permute-start.8 = (bf16[4,264,128]{2,1,0:T(8,128)(2,1)S(1)}, bf16[4,264,128]{2,1,0:T(8,128)(2,1)S(1)}, u32[]{:S(2)}, u32[]{:S(2)}) collective-permute-start(bf16[4,264,128]{2,1,0:T(8,128)(2,1)S(1)} %shard_map.124), channel_id=1, source_target_pairs={{0,64},{8,72},{16,80},{24,88},{32,96},{40,104},{48,112},{56,120},{... | collective-permute-start | bytes 811016 | tf_op jit(solution)/shard_map/ppermute | solution.py:289
  18.1 0.7 %shard_map.120.c_ref.refs_0_ = bf16[4,264,128]{2,1,0:T(8,128)(2,1)S(1)} custom-call(bf16[12,8,16,1024]{3,2,1,0:T(8,128)(2,1)S(1)} %get-tuple-element.26.rest_ref, bf16[1024,256]{1,0:T(8,128)(2,1)S(1)} %get-tuple-element.27.w_ref, bf16[8,1024]{1,0:T(8,128)(2,1)S(1)} %get-tuple-element.28.g_ref), custom_call_target="tpu_custom_call" | custom-call | tf_op jit(solution)/shard_map/pallas_call | solution.py:111
  18.7 0.0 collective-permute-done.1.b_ref.refs_2_
  18.8 8.1 %collective-permute-done.a_ref.refs_1_ = bf16[4,264,128]{2,1,0:T(8,128)(2,1)S(1)} collective-permute-done((bf16[4,264,128]{2,1,0:T(8,128)(2,1)S(1)}, bf16[4,264,128]{2,1,0:T(8,128)(2,1)S(1)}, u32[]{:S(2)}, u32[]{:S(2)}) %collective-permute-start) | collective-permute-done | bytes 270368 | tf_op jit(solution)/shard_map/ppermute | solution.py:289
  26.9 1.7 %collective-permute-start.2 = (bf16[3,264,128]{2,1,0:T(8,128)(2,1)S(1)}, bf16[3,264,128]{2,1,0:T(8,128)(2,1)S(1)}, u32[]{:S(2)}, u32[]{:S(2)}) collective-permute-start(bf16[3,264,128]{2,1,0:T(8,128)(2,1)S(1)} %get-tuple-element.30), channel_id=1, source_target_pairs={{0,8},{8,16},{16,24},{24,0},{32,40},{40,48},{48,56},{56,32},{64,72... | collective-permute-start | bytes 608264 | tf_op jit(solution)/shard_map/ppermute | solution.py:289
  28.6 2.9 %collective-permute-start.3 = (bf16[3,264,128]{2,1,0:T(8,128)(2,1)S(1)}, bf16[3,264,128]{2,1,0:T(8,128)(2,1)S(1)}, u32[]{:S(2)}, u32[]{:S(2)}) collective-permute-start(bf16[3,264,128]{2,1,0:T(8,128)(2,1)S(1)} %get-tuple-element.31), channel_id=1, source_target_pairs={{0,16},{8,24},{16,0},{24,8},{32,48},{40,56},{48,32},{56,40},{64,80... | collective-permute-start | bytes 608264 | tf_op jit(solution)/shard_map/ppermute | solution.py:289
  31.5 1.3 %collective-permute-start.4 = (bf16[3,264,128]{2,1,0:T(8,128)(2,1)S(1)}, bf16[3,264,128]{2,1,0:T(8,128)(2,1)S(1)}, u32[]{:S(2)}, u32[]{:S(2)}) collective-permute-start(bf16[3,264,128]{2,1,0:T(8,128)(2,1)S(1)} %get-tuple-element.32), channel_id=1, source_target_pairs={{0,24},{8,0},{16,8},{24,16},{32,56},{40,32},{48,40},{56,48},{64,88... | collective-permute-start | bytes 608264 | tf_op jit(solution)/shard_map/ppermute | solution.py:289
  32.8 0.0 collective-permute-done.8.refs_6_
  32.8 3.0 %collective-permute-done.2.refs_3_ = bf16[3,264,128]{2,1,0:T(8,128)(2,1)S(1)} collective-permute-done((bf16[3,264,128]{2,1,0:T(8,128)(2,1)S(1)}, bf16[3,264,128]{2,1,0:T(8,128)(2,1)S(1)}, u32[]{:S(2)}, u32[]{:S(2)}) %collective-permute-start.2) | collective-permute-done | bytes 202784 | tf_op jit(solution)/shard_map/ppermute | solution.py:289
  35.8 2.2 %collective-permute-done.3.refs_4_ = bf16[3,264,128]{2,1,0:T(8,128)(2,1)S(1)} collective-permute-done((bf16[3,264,128]{2,1,0:T(8,128)(2,1)S(1)}, bf16[3,264,128]{2,1,0:T(8,128)(2,1)S(1)}, u32[]{:S(2)}, u32[]{:S(2)}) %collective-permute-start.3) | collective-permute-done | bytes 202784 | tf_op jit(solution)/shard_map/ppermute | solution.py:289
  38.0 0.0 collective-permute-done.4.refs_5_
  38.0 2.1 %shard_map.125 = (f32[4,8,128]{2,1,0:T(8,128)S(1)}, f32[4,8,128]{2,1,0:T(8,128)S(1)}, f32[32,128]{1,0:T(8,128)S(1)}, f32[128,32]{1,0:T(8,128)S(1)}, f32[2,1,8]{2,1,0:T(1,128)}) custom-call(bf16[4,264,128]{2,1,0:T(8,128)(2,1)S(1)} %shard_map.120.c_ref.refs_0_, bf16[4,264,128]{2,1,0:T(8,128)(2,1)S(1)} %collective-permute-done.a_ref.refs_1_, ...), custom_call_target="tpu_custom_call" | custom-call | tf_op jit(solution)/shard_map/pallas_call | solution.py:111
  40.1 0.0 collective-permute-start.9
  40.1 1.2 %collective-permute-done.9.got_ref = f32[4,8,128]{2,1,0:T(8,128)S(1)} collective-permute-done((f32[4,8,128]{2,1,0:T(8,128)S(1)}, f32[4,8,128]{2,1,0:T(8,128)S(1)}, u32[]{:S(2)}, u32[]{:S(2)}) %collective-permute-start.9) | collective-permute-done | bytes 16416 | tf_op jit(solution)/shard_map/ppermute | solution.py:294
  41.3 1.5 %collective-permute-start.10 = (f32[8,128]{1,0:T(8,128)S(1)}, f32[8,128]{1,0:T(8,128)S(1)}, u32[]{:S(2)}, u32[]{:S(2)}) collective-permute-start(f32[8,128]{1,0:T(8,128)S(1)} %get-tuple-element.45), channel_id=1, source_target_pairs={{0,2},{2,4},{4,6},{6,0},{1,3},{3,5},{5,7},{7,1},{8,10},{10,12},{12... | collective-permute-start | bytes 12296 | tf_op jit(solution)/shard_map/ppermute | solution.py:294
  42.8 2.7 %collective-permute-start.11 = (f32[8,128]{1,0:T(8,128)S(1)}, f32[8,128]{1,0:T(8,128)S(1)}, u32[]{:S(2)}, u32[]{:S(2)}) collective-permute-start(f32[8,128]{1,0:T(8,128)S(1)} %get-tuple-element.46), channel_id=1, source_target_pairs={{0,4},{2,6},{4,0},{6,2},{1,5},{3,7},{5,1},{7,3},{8,12},{10,14},{12... | collective-permute-start | bytes 12296 | tf_op jit(solution)/shard_map/ppermute | solution.py:294
  45.6 1.4 %collective-permute-start.12 = (f32[8,128]{1,0:T(8,128)S(1)}, f32[8,128]{1,0:T(8,128)S(1)}, u32[]{:S(2)}, u32[]{:S(2)}) collective-permute-start(f32[8,128]{1,0:T(8,128)S(1)} %get-tuple-element.47), channel_id=1, source_target_pairs={{0,6},{2,0},{4,2},{6,4},{1,7},{3,1},{5,3},{7,5},{8,14},{10,8},{12,... | collective-permute-start | bytes 12296 | tf_op jit(solution)/shard_map/ppermute | solution.py:294
  47.0 1.1 %shard_map.126 = (bf16[16,128,256]{2,1,0:T(8,128)(2,1)S(1)}, f32[16,128]{1,0:T(8,128)}) custom-call(bf16[4,264,128]{2,1,0:T(8,128)(2,1)S(1)} %shard_map.120.c_ref.refs_0_, bf16[4,264,128]{2,1,0:T(8,128)(2,1)S(1)} %collective-permute-done.a_ref.refs_1_, bf16[4,264,128]{2,1,0:T(8,128)(2,1)S(1)} %collective-permute-done.1.b_ref.refs_2_, ...), custom_call_target="tpu_custom_call" | custom-call | tf_op jit(solution)/shard_map/pallas_call | solution.py:111
  48.1 1.2 %shard_map.127 = bf16[2,8,128,128]{3,2,1,0:T(8,128)(2,1)} custom-call(bf16[4,264,128]{2,1,0:T(8,128)(2,1)S(1)} %shard_map.120.c_ref.refs_0_, bf16[4,264,128]{2,1,0:T(8,128)(2,1)S(1)} %collective-permute-done.a_ref.refs_1_, bf16[4,264,128]{2,1,0:T(8,128)(2,1)S(1)} %collective-permute-done.1.b_ref.refs_2_, ...), custom_call_target="tpu_custom_call" | custom-call | tf_op jit(solution)/shard_map/pallas_call | solution.py:111
  49.2 0.0 collective-permute-done.10.b_ref
  49.2 0.6 %shard_map.129 = bf16[8,128]{1,0:T(8,128)(2,1)} custom-call(f32[8,128]{1,0:T(8,128)S(1)} %get-tuple-element.44.a_ref, f32[8,128]{1,0:T(8,128)S(1)} %collective-permute-done.10.b_ref, f32[8,128]{1,0:T(8,128)S(1)} %collective-permute-done.11.c_ref, f32[8,128]{1,0:T(8,128)S(1)} %collective-permute-done.12.d_ref), custom_call_target="tpu_custom_call" | custom-call | tf_op jit(solution)/shard_map/pallas_call | solution.py:111
  (13 shorter events, 0.1 us)
Async XLA Ops:
  3.8 14.9 %collective-permute-start.1 = (bf16[4,264,128]{2,1,0:T(8,128)(2,1)S(1)}, bf16[4,264,128]{2,1,0:T(8,128)(2,1)S(1)}, u32[]{:S(2)}, u32[]{:S(2)}) collective-permute-start(bf16[4,264,128]{2,1,0:T(8,128)(2,1)S(1)} %shard_map.121), channel_id=1, source_target_pairs={{0,32},{8,40},{16,48},{24,56},{32,0},{40,8},{48,16},{56,24},{64,96... | collective-permute-start | bytes 811016 | tf_op jit(solution)/shard_map/ppermute | solution.py:289
  5.8 32.2 %copy-start = (bf16[1,128,1024]{2,1,0:T(8,128)(2,1)S(1)}, bf16[1,128,1024]{2,1,0:T(8,128)(2,1)}, u32[]{:S(2)}) copy-start(bf16[1,128,1024]{2,1,0:T(8,128)(2,1)} %param.17) | copy-start | bytes 786436
  5.8 32.2 %copy-start.1 = (bf16[8,1,128]{2,0,1:T(8,128)(2,1)S(1)}, bf16[8,1,128]{2,0,1:T(8,128)(2,1)}, u32[]{:S(2)}) copy-start(bf16[8,1,128]{2,0,1:T(8,128)(2,1)} %param.16) | copy-start | bytes 6148
  5.8 32.2 %copy-start.2 = (f32[2,1]{0,1:T(1,128)S(1)}, f32[2,1]{0,1:T(1,128)}, u32[]{:S(2)}) copy-start(f32[2,1]{0,1:T(1,128)} %param.14) | copy-start | bytes 28
  5.8 32.2 %copy-start.3 = (f32[2,1]{0,1:T(1,128)S(1)}, f32[2,1]{0,1:T(1,128)}, u32[]{:S(2)}) copy-start(f32[2,1]{0,1:T(1,128)} %param.15) | copy-start | bytes 28
  5.8 21.0 %collective-permute-start = (bf16[4,264,128]{2,1,0:T(8,128)(2,1)S(1)}, bf16[4,264,128]{2,1,0:T(8,128)(2,1)S(1)}, u32[]{:S(2)}, u32[]{:S(2)}) collective-permute-start(bf16[4,264,128]{2,1,0:T(8,128)(2,1)S(1)} %get-tuple-element.29), channel_id=1, source_target_pairs={{0,96},{8,104},{16,112},{24,120},{32,64},{40,72},{48,80},{56,88},{... | collective-permute-start | bytes 811016 | tf_op jit(solution)/shard_map/ppermute | solution.py:289
  6.6 6.3 %collective-permute-start.5 = (bf16[264,128]{1,0:T(8,128)(2,1)S(1)}, bf16[264,128]{1,0:T(8,128)(2,1)S(1)}, u32[]{:S(2)}, u32[]{:S(2)}) collective-permute-start(bf16[264,128]{1,0:T(8,128)(2,1)S(1)} %get-tuple-element.34), channel_id=1, source_target_pairs={{0,8},{8,16},{16,24},{24,0},{32,40},{40,48},{48,56},{56,32},{64,72... | collective-permute-start | bytes 202760 | tf_op jit(solution)/shard_map/ppermute | solution.py:289
  8.3 5.9 %collective-permute-start.6 = (bf16[264,128]{1,0:T(8,128)(2,1)S(1)}, bf16[264,128]{1,0:T(8,128)(2,1)S(1)}, u32[]{:S(2)}, u32[]{:S(2)}) collective-permute-start(bf16[264,128]{1,0:T(8,128)(2,1)S(1)} %get-tuple-element.35), channel_id=1, source_target_pairs={{0,16},{8,24},{16,0},{24,8},{32,48},{40,56},{48,32},{56,40},{64,80... | collective-permute-start | bytes 202760 | tf_op jit(solution)/shard_map/ppermute | solution.py:289
  11.2 4.3 %collective-permute-start.7 = (bf16[264,128]{1,0:T(8,128)(2,1)S(1)}, bf16[264,128]{1,0:T(8,128)(2,1)S(1)}, u32[]{:S(2)}, u32[]{:S(2)}) collective-permute-start(bf16[264,128]{1,0:T(8,128)(2,1)S(1)} %get-tuple-element.36), channel_id=1, source_target_pairs={{0,24},{8,0},{16,8},{24,16},{32,56},{40,32},{48,40},{56,48},{64,88... | collective-permute-start | bytes 202760 | tf_op jit(solution)/shard_map/ppermute | solution.py:289
  15.5 17.3 %collective-permute-start.8 = (bf16[4,264,128]{2,1,0:T(8,128)(2,1)S(1)}, bf16[4,264,128]{2,1,0:T(8,128)(2,1)S(1)}, u32[]{:S(2)}, u32[]{:S(2)}) collective-permute-start(bf16[4,264,128]{2,1,0:T(8,128)(2,1)S(1)} %shard_map.124), channel_id=1, source_target_pairs={{0,64},{8,72},{16,80},{24,88},{32,96},{40,104},{48,112},{56,120},{... | collective-permute-start | bytes 811016 | tf_op jit(solution)/shard_map/ppermute | solution.py:289
  26.9 8.9 %collective-permute-start.2 = (bf16[3,264,128]{2,1,0:T(8,128)(2,1)S(1)}, bf16[3,264,128]{2,1,0:T(8,128)(2,1)S(1)}, u32[]{:S(2)}, u32[]{:S(2)}) collective-permute-start(bf16[3,264,128]{2,1,0:T(8,128)(2,1)S(1)} %get-tuple-element.30), channel_id=1, source_target_pairs={{0,8},{8,16},{16,24},{24,0},{32,40},{40,48},{48,56},{56,32},{64,72... | collective-permute-start | bytes 608264 | tf_op jit(solution)/shard_map/ppermute | solution.py:289
  28.6 9.4 %collective-permute-start.3 = (bf16[3,264,128]{2,1,0:T(8,128)(2,1)S(1)}, bf16[3,264,128]{2,1,0:T(8,128)(2,1)S(1)}, u32[]{:S(2)}, u32[]{:S(2)}) collective-permute-start(bf16[3,264,128]{2,1,0:T(8,128)(2,1)S(1)} %get-tuple-element.31), channel_id=1, source_target_pairs={{0,16},{8,24},{16,0},{24,8},{32,48},{40,56},{48,32},{56,40},{64,80... | collective-permute-start | bytes 608264 | tf_op jit(solution)/shard_map/ppermute | solution.py:289
  31.5 6.5 %collective-permute-start.4 = (bf16[3,264,128]{2,1,0:T(8,128)(2,1)S(1)}, bf16[3,264,128]{2,1,0:T(8,128)(2,1)S(1)}, u32[]{:S(2)}, u32[]{:S(2)}) collective-permute-start(bf16[3,264,128]{2,1,0:T(8,128)(2,1)S(1)} %get-tuple-element.32), channel_id=1, source_target_pairs={{0,24},{8,0},{16,8},{24,16},{32,56},{40,32},{48,40},{56,48},{64,88... | collective-permute-start | bytes 608264 | tf_op jit(solution)/shard_map/ppermute | solution.py:289
  40.1 1.2 %collective-permute-start.9 = (f32[4,8,128]{2,1,0:T(8,128)S(1)}, f32[4,8,128]{2,1,0:T(8,128)S(1)}, u32[]{:S(2)}, u32[]{:S(2)}) collective-permute-start(f32[4,8,128]{2,1,0:T(8,128)S(1)} %get-tuple-element.43), channel_id=1, source_target_pairs={{0,1},{1,0},{2,3},{3,2},{4,5},{5,4},{6,7},{7,6},{8,9},{9,8},{10,11... | collective-permute-start | bytes 49160 | tf_op jit(solution)/shard_map/ppermute | solution.py:294
  41.3 7.9 %collective-permute-start.10 = (f32[8,128]{1,0:T(8,128)S(1)}, f32[8,128]{1,0:T(8,128)S(1)}, u32[]{:S(2)}, u32[]{:S(2)}) collective-permute-start(f32[8,128]{1,0:T(8,128)S(1)} %get-tuple-element.45), channel_id=1, source_target_pairs={{0,2},{2,4},{4,6},{6,0},{1,3},{3,5},{5,7},{7,1},{8,10},{10,12},{12... | collective-permute-start | bytes 12296 | tf_op jit(solution)/shard_map/ppermute | solution.py:294
  42.8 6.4 %collective-permute-start.11 = (f32[8,128]{1,0:T(8,128)S(1)}, f32[8,128]{1,0:T(8,128)S(1)}, u32[]{:S(2)}, u32[]{:S(2)}) collective-permute-start(f32[8,128]{1,0:T(8,128)S(1)} %get-tuple-element.46), channel_id=1, source_target_pairs={{0,4},{2,6},{4,0},{6,2},{1,5},{3,7},{5,1},{7,3},{8,12},{10,14},{12... | collective-permute-start | bytes 12296 | tf_op jit(solution)/shard_map/ppermute | solution.py:294
  45.6 3.7 %collective-permute-start.12 = (f32[8,128]{1,0:T(8,128)S(1)}, f32[8,128]{1,0:T(8,128)S(1)}, u32[]{:S(2)}, u32[]{:S(2)}) collective-permute-start(f32[8,128]{1,0:T(8,128)S(1)} %get-tuple-element.47), channel_id=1, source_target_pairs={{0,6},{2,0},{4,2},{6,4},{1,7},{3,1},{5,3},{7,5},{8,14},{10,8},{12,... | collective-permute-start | bytes 12296 | tf_op jit(solution)/shard_map/ppermute | solution.py:294

commit v5 on v4

--- a/solution.py
+++ b/solution.py
@@ -82,12 +82,9 @@
     project_blocks(rest_ref, 0, w_ref[...], g_ref[...], [twin_ref.at[k] for k in range(ROW)])
 
 
-def third_kernel(rest_ref, w_ref, g_ref, *outs):
-    project_blocks(rest_ref, ROW, w_ref[...], g_ref[...], outs)
-
-
-def own_kernel(rest_ref, w_ref, g_ref, own_ref):
-    project_blocks(rest_ref, 2 * ROW, w_ref[...], g_ref[...], [own_ref.at[k] for k in range(ROW)])
+def third_kernel(rest_ref, w_ref, g_ref, c1_ref, c2_ref, c3_ref, far_ref, own0_ref, own3_ref):
+    project_blocks(rest_ref, ROW, w_ref[...], g_ref[...], [far_ref, c1_ref.at[0], c2_ref.at[0], c3_ref])
+    project_blocks(rest_ref, 2 * ROW, w_ref[...], g_ref[...], [own0_ref, c1_ref.at[1], c2_ref.at[1], own3_ref])
 
 
 ANY = pl.BlockSpec(memory_space=pl.ANY)
@@ -135,15 +132,18 @@
     )(*[pltpu.with_memory_space_constraint(a, pltpu.HBM) for a in args])
 
 
-def gather_kernel(*refs):
-    for i in range(ROW):
-        refs[ROW][i] = refs[i][...]
-
-
-def triple_kernel(a_ref, b_ref, c_ref, *outs):
+def gather_kernel(a_ref, b_ref, c_ref, d_ref, out_ref):
+    out_ref[0] = a_ref[...]
+    out_ref[1] = b_ref[0]
+    out_ref[2] = c_ref[0]
+    out_ref[3] = d_ref[...]
+
+
+def legs_kernel(a_ref, b_ref, own3_ref, *outs):
     for k, out in enumerate(outs):
-        for i, ref in enumerate((a_ref, b_ref, c_ref)):
-            out[i] = ref[k + 1]
+        out[0] = a_ref[k + 1]
+        out[1] = b_ref[k + 1]
+    outs[2][2] = own3_ref[...]
 
 
 def three_parts(a):
@@ -165,9 +165,12 @@
 
 
 def landed(refs):
-    own, mirror, twin, s1, s2, s3, far = refs
-    legs = [[kept.at[0]] + [s.at[i] for s in (s1, s2, s3)] for i, kept in enumerate((mirror, twin, own))]
-    return legs[2] + legs[1] + [far.at[k] for k in range(ROW)] + legs[0]
+    own0, c1, c2, mirror, twin, s1, s2, s3, far = refs
+    own = [own0, c1.at[1], c2.at[1], s3.at[2]]
+    from_mirror, from_twin = [
+        [kept.at[0]] + [s.at[i] for s in (s1, s2, s3)] for i, kept in enumerate((mirror, twin))
+    ]
+    return own + from_twin + [far.at[k] for k in range(ROW)] + from_mirror
 
 
 def rows_mine():
@@ -182,8 +185,8 @@
 
 
 def read_kernel(*refs):
-    blocks = landed(refs[:7])
-    q_ref, wo_ref, ib_ref, fb_ref, keep_ref, send_ref, weight_ref, turned_ref, stab_ref = refs[7:]
+    blocks = landed(refs[:9])
+    q_ref, wo_ref, ib_ref, fb_ref, keep_ref, send_ref, weight_ref, turned_ref, stab_ref = refs[9:]
     scale = HD ** -0.5
     row, lane8, mine = rows_mine()
     query = q_ref[...]
@@ -208,12 +211,10 @@
     for g in range(2):
         order = (r > c) if g == 0 else (r < c)
         inside = jnp.concatenate((ones(same & order), ones(same)), axis=1)
-        sums = dot(jnp.concatenate(three_parts(forget[g]), axis=0), inside)
-        sums = sums[:SP] + sums[SP : 2 * SP] + sums[2 * SP :]
+        sums = sum(dot(p, inside) for p in three_parts(forget[g]))
         block = sums[:, HD:]
         across = ones(((place(jc) > place(jr)) if g == 0 else (place(jc) < place(jr))) | (jr >= SP))
-        outside = dot(across, jnp.concatenate(three_parts(block), axis=1))
-        outside = outside[:, :HD] + outside[:, HD : 2 * HD] + outside[:, 2 * HD :]
+        outside = sum(dot(across, p) for p in three_parts(block))
         log_weight.append(in_pre[g] + sums[:, :HD] + outside[:SP])
         total.append(outside[SP : SP + 1])
     stab = [
@@ -248,8 +249,8 @@
 
 
 def weigh_kernel(*refs):
-    blocks = landed(refs[:7])
-    weight_ref, turned_ref, vw_ref, norm_ref = refs[7:]
+    blocks = landed(refs[:9])
+    weight_ref, turned_ref, vw_ref, norm_ref = refs[9:]
     _, _, mine = rows_mine()
     norm = jnp.zeros((4 * OWN, HD), F32)
     for j, blk in enumerate(blocks):
@@ -263,8 +264,8 @@
 
 
 def memory_kernel(*refs):
-    blocks = landed(refs[:7])
-    vw_ref, mem_ref = refs[7:]
+    blocks = landed(refs[:9])
+    vw_ref, mem_ref = refs[9:]
     for s in range(OWN):
         at = slice(s * POS, (s + 1) * POS)
         keys = jnp.concatenate([blk[at, :] for blk in blocks], axis=0)
@@ -302,14 +303,15 @@
     mirror = shift(mirror, 3, 0)
     twin = run(second_kernel, block(ROW), (later, w, gates))
     twin = shift(twin, 1, 0)
-    cross = run(third_kernel, (block(),) * ROW, (later, w, gates))
-    cross = [cross[0]] + [shift(cross[k], 0, k) for k in hops]
-    far = run(gather_kernel, block(ROW), cross, 4)
+    *cross, far, own0, own3 = run(
+        third_kernel, (block(2), block(2), block(), block(), block(), block()), (later, w, gates)
+    )
+    cross = [shift(blocks, 0, k) for k, blocks in zip(hops, cross)]
+    far = run(gather_kernel, block(ROW), (far, *cross), 4)
     far = shift(far, 2, 0)
-    own = run(own_kernel, block(ROW), (later, w, gates))
-    side = run(triple_kernel, (block(3),) * 3, (mirror, twin, own), 4)
+    side = run(legs_kernel, (block(2), block(2), block(3)), (mirror, twin, own3), 4)
     side = [shift(blocks, 0, k) for k, blocks in zip(hops, side)]
-    blocks = (own, mirror, twin, *side, far)
+    blocks = (own0, cross[0], cross[1], mirror, twin, *side, far)
     half = pltpu.VMEM((TPX, OWN, HD), F32)
     keep, send, weight, turned, stab = run(
         read_kernel,

time: 49.9 us -> 49.2 us (0.986)
    pallas_call x10 -> x9, Pallas kernels: 7.05 us -> 6.57 us  [run(): pl.pallas_call(kernel, in_specs=[VM] * len(args), out_specs=specs, out_sh...]
  transfers between devices with their start and end apart: 13 -> 13, of which waited for: 7 -> 5; matrix products, arithmetic and copies ran while one was open for 0% -> 0% of each run, Pallas kernels for 7% -> 7%
where the time goes in v5:
time: 49.2 us; the launch traced here: 49.1 us
  starting transfers between devices  22 us (45%)
  waiting for transfers between devices  17.3 us (35%)
  Pallas kernels  9.07 us (18%)
  between operations  0.74 us (2%)
    ppermute x9, starting transfers between devices, shift(): return lax.ppermute(array, 'sp', pairs)  16.4 us
    ppermute x9, waiting for transfers between devices, shift(): return lax.ppermute(array, 'sp', pairs)  16.1 us
    pallas_call x9, Pallas kernels, run(): pl.pallas_call(kernel, in_specs=[VM] * len(args), out_specs=specs, out_sh...  6.57 us
    ppermute x4, starting transfers between devices, across(): lax.ppermute(array, axis, [(i, (i + hop) % size) for i in range(size)])  5.66 us
    pallas_call x1, Pallas kernels, project_near(): pl.pallas_call(near_kernel, in_specs=[ANY] * 5, out_specs=[VM] * 4, out_s...  2.5 us
    ppermute x4, waiting for transfers between devices, across(): lax.ppermute(array, axis, [(i, (i + hop) % size) for i in range(size)])  1.19 us
  transfers between devices with their start and end apart: 13, of which 5 were waited for; matrix products, arithmetic and copies ran while one was open for 0% of the time, Pallas kernels for 7%

profile of v5, /device:TPU:64, one launch (start us, length us, event | category | flops | bytes accessed | tf_op | source)
XLA Modules:
  0.0 49.1 jit_solution(14065748731833901294)
XLA Ops:
  0.6 2.5 %near.1 = (bf16[4,264,128]{2,1,0:T(8,128)(2,1)S(1)}, bf16[1024,256]{1,0:T(8,128)(2,1)S(1)}, bf16[8,1024]{1,0:T(8,128)(2,1)S(1)}, bf16[12,8,16,1024]{3,2,1,0:T(8,128)(2,1)S(1)}) custom-call(bf16[128,16,1024]{2,1,0:T(8,128)(2,1)} %x_ref.1, bf16[1024,128]{1,0:T(8,128)(2,1)} %bitcast.22, bf16[1024,128]{1,0:T(8,128)(2,1)} %bitcast.23, bf16[2,1024]{1,0:T(2,128)(2,1)} %bitcast.24, ...), custom_call_target="tpu_custom_call" | custom-call | tf_op jit(solution)/shard_map/near/pallas_call | solution.py:119
  3.1 0.0 copy-start
  3.2 0.0 copy-start.1
  3.2 0.0 copy-start.2
  3.2 0.0 copy-start.3
  3.2 0.7 %shard_map.121 = bf16[4,264,128]{2,1,0:T(8,128)(2,1)S(1)} custom-call(bf16[12,8,16,1024]{3,2,1,0:T(8,128)(2,1)S(1)} %get-tuple-element.28.rest_ref, bf16[1024,256]{1,0:T(8,128)(2,1)S(1)} %get-tuple-element.29.w_ref, bf16[8,1024]{1,0:T(8,128)(2,1)S(1)} %get-tuple-element.30.g_ref), custom_call_target="tpu_custom_call" | custom-call | tf_op jit(solution)/shard_map/pallas_call | solution.py:108
  3.9 2.0 %collective-permute-start.3 = (bf16[4,264,128]{2,1,0:T(8,128)(2,1)S(1)}, bf16[4,264,128]{2,1,0:T(8,128)(2,1)S(1)}, u32[]{:S(2)}, u32[]{:S(2)}) collective-permute-start(bf16[4,264,128]{2,1,0:T(8,128)(2,1)S(1)} %shard_map.121), channel_id=1, source_target_pairs={{0,32},{8,40},{16,48},{24,56},{32,0},{40,8},{48,16},{56,24},{64,96... | collective-permute-start | bytes 811016 | tf_op jit(solution)/shard_map/ppermute | solution.py:290
  5.9 0.0 collective-permute-start.2
  5.9 1.2 %shard_map.120 = (bf16[2,264,128]{2,1,0:T(8,128)(2,1)S(1)}, bf16[2,264,128]{2,1,0:T(8,128)(2,1)S(1)}, bf16[264,128]{1,0:T(8,128)(2,1)S(1)}, bf16[264,128]{1,0:T(...) custom-call(bf16[12,8,16,1024]{3,2,1,0:T(8,128)(2,1)S(1)} %get-tuple-element.28.rest_ref, ...), custom_call_target="tpu_custom_call" | custom-call | tf_op jit(solution)/shard_map/pallas_call | solution.py:108
  7.1 1.6 %collective-permute-start = (bf16[2,264,128]{2,1,0:T(8,128)(2,1)S(1)}, bf16[2,264,128]{2,1,0:T(8,128)(2,1)S(1)}, u32[]{:S(2)}, u32[]{:S(2)}) collective-permute-start(bf16[2,264,128]{2,1,0:T(8,128)(2,1)S(1)} %get-tuple-element.32), channel_id=1, source_target_pairs={{0,8},{8,16},{16,24},{24,0},{32,40},{40,48},{48,56},{56,32},{64,72... | collective-permute-start | bytes 405512 | tf_op jit(solution)/shard_map/ppermute | solution.py:290
  8.8 2.9 %collective-permute-start.1 = (bf16[2,264,128]{2,1,0:T(8,128)(2,1)S(1)}, bf16[2,264,128]{2,1,0:T(8,128)(2,1)S(1)}, u32[]{:S(2)}, u32[]{:S(2)}) collective-permute-start(bf16[2,264,128]{2,1,0:T(8,128)(2,1)S(1)} %get-tuple-element.33), channel_id=1, source_target_pairs={{0,16},{8,24},{16,0},{24,8},{32,48},{40,56},{48,32},{56,40},{64,80... | collective-permute-start | bytes 405512 | tf_op jit(solution)/shard_map/ppermute | solution.py:290
  11.7 1.3 %collective-permute-start.7 = (bf16[264,128]{1,0:T(8,128)(2,1)S(1)}, bf16[264,128]{1,0:T(8,128)(2,1)S(1)}, u32[]{:S(2)}, u32[]{:S(2)}) collective-permute-start(bf16[264,128]{1,0:T(8,128)(2,1)S(1)} %get-tuple-element.40), channel_id=1, source_target_pairs={{0,24},{8,0},{16,8},{24,16},{32,56},{40,32},{48,40},{56,48},{64,88... | collective-permute-start | bytes 202760 | tf_op jit(solution)/shard_map/ppermute | solution.py:290
  13.0 2.9 %collective-permute-done.7.d_ref = bf16[264,128]{1,0:T(8,128)(2,1)S(1)} collective-permute-done((bf16[264,128]{1,0:T(8,128)(2,1)S(1)}, bf16[264,128]{1,0:T(8,128)(2,1)S(1)}, u32[]{:S(2)}, u32[]{:S(2)}) %collective-permute-start.7) | collective-permute-done | bytes 67616 | tf_op jit(solution)/shard_map/ppermute | solution.py:290
  16.0 0.0 collective-permute-done.b_ref.refs_1_
  16.0 1.6 %collective-permute-done.1.c_ref.refs_2_ = bf16[2,264,128]{2,1,0:T(8,128)(2,1)S(1)} collective-permute-done((bf16[2,264,128]{2,1,0:T(8,128)(2,1)S(1)}, bf16[2,264,128]{2,1,0:T(8,128)(2,1)S(1)}, u32[]{:S(2)}, u32[]{:S(2)}) %collective-permute-start.1) | collective-permute-done | bytes 135200 | tf_op jit(solution)/shard_map/ppermute | solution.py:290
  17.6 2.5 %collective-permute-start.8 = (bf16[4,264,128]{2,1,0:T(8,128)(2,1)S(1)}, bf16[4,264,128]{2,1,0:T(8,128)(2,1)S(1)}, u32[]{:S(2)}, u32[]{:S(2)}) collective-permute-start(bf16[4,264,128]{2,1,0:T(8,128)(2,1)S(1)} %shard_map.123), channel_id=1, source_target_pairs={{0,64},{8,72},{16,80},{24,88},{32,96},{40,104},{48,112},{56,120},{... | collective-permute-start | bytes 811016 | tf_op jit(solution)/shard_map/ppermute | solution.py:290
  20.2 6.0 %collective-permute-done.2.a_ref.refs_3_ = bf16[4,264,128]{2,1,0:T(8,128)(2,1)S(1)} collective-permute-done((bf16[4,264,128]{2,1,0:T(8,128)(2,1)S(1)}, bf16[4,264,128]{2,1,0:T(8,128)(2,1)S(1)}, u32[]{:S(2)}, u32[]{:S(2)}) %collective-permute-start.2) | collective-permute-done | bytes 270368 | tf_op jit(solution)/shard_map/ppermute | solution.py:290
  26.2 3.7 %collective-permute-start.6 = (bf16[3,264,128]{2,1,0:T(8,128)(2,1)S(1)}, bf16[3,264,128]{2,1,0:T(8,128)(2,1)S(1)}, u32[]{:S(2)}, u32[]{:S(2)}) collective-permute-start(bf16[3,264,128]{2,1,0:T(8,128)(2,1)S(1)} %get-tuple-element.38), channel_id=1, source_target_pairs={{0,24},{8,0},{16,8},{24,16},{32,56},{40,32},{48,40},{56,48},{64,88... | collective-permute-start | bytes 608264 | tf_op jit(solution)/shard_map/ppermute | solution.py:290
  30.0 0.0 collective-permute-start.4
  30.0 2.2 %collective-permute-start.5 = (bf16[2,264,128]{2,1,0:T(8,128)(2,1)S(1)}, bf16[2,264,128]{2,1,0:T(8,128)(2,1)S(1)}, u32[]{:S(2)}, u32[]{:S(2)}) collective-permute-start(bf16[2,264,128]{2,1,0:T(8,128)(2,1)S(1)} %get-tuple-element.37), channel_id=1, source_target_pairs={{0,16},{8,24},{16,0},{24,8},{32,48},{40,56},{48,32},{56,40},{64,80... | collective-permute-start | bytes 405512 | tf_op jit(solution)/shard_map/ppermute | solution.py:290
  32.2 0.0 collective-permute-done.8.refs_8_
  32.2 5.5 %collective-permute-done.4.refs_5_ = bf16[2,264,128]{2,1,0:T(8,128)(2,1)S(1)} collective-permute-done((bf16[2,264,128]{2,1,0:T(8,128)(2,1)S(1)}, bf16[2,264,128]{2,1,0:T(8,128)(2,1)S(1)}, u32[]{:S(2)}, u32[]{:S(2)}) %collective-permute-start.4) | collective-permute-done | bytes 135200 | tf_op jit(solution)/shard_map/ppermute | solution.py:290
  37.7 1.8 %shard_map.124 = (f32[4,8,128]{2,1,0:T(8,128)S(1)}, f32[4,8,128]{2,1,0:T(8,128)S(1)}, f32[32,128]{1,0:T(8,128)S(1)}, f32[128,32]{1,0:T(8,128)S(1)}, f32[2,1,8]{2,1,0:T(1,128)}) custom-call(bf16[264,128]{1,0:T(8,128)(2,1)S(1)} %get-tuple-element.31.refs_0_, bf16[2,264,128]{2,1,0:T(8,128)(2,1)S(1)} %collective-permute-done.b_ref.refs_1_, ...), custom_call_target="tpu_custom_call" | custom-call | tf_op jit(solution)/shard_map/pallas_call | solution.py:108
  39.4 1.2 %collective-permute-done.9.got_ref = f32[4,8,128]{2,1,0:T(8,128)S(1)} collective-permute-done((f32[4,8,128]{2,1,0:T(8,128)S(1)}, f32[4,8,128]{2,1,0:T(8,128)S(1)}, u32[]{:S(2)}, u32[]{:S(2)}) %collective-permute-start.9) | collective-permute-done | bytes 16416 | tf_op jit(solution)/shard_map/ppermute | solution.py:295
  40.6 1.5 %collective-permute-start.10 = (f32[8,128]{1,0:T(8,128)S(1)}, f32[8,128]{1,0:T(8,128)S(1)}, u32[]{:S(2)}, u32[]{:S(2)}) collective-permute-start(f32[8,128]{1,0:T(8,128)S(1)} %get-tuple-element.49), channel_id=1, source_target_pairs={{0,2},{2,4},{4,6},{6,0},{1,3},{3,5},{5,7},{7,1},{8,10},{10,12},{12... | collective-permute-start | bytes 12296 | tf_op jit(solution)/shard_map/ppermute | solution.py:295
  42.1 2.7 %collective-permute-start.11 = (f32[8,128]{1,0:T(8,128)S(1)}, f32[8,128]{1,0:T(8,128)S(1)}, u32[]{:S(2)}, u32[]{:S(2)}) collective-permute-start(f32[8,128]{1,0:T(8,128)S(1)} %get-tuple-element.50), channel_id=1, source_target_pairs={{0,4},{2,6},{4,0},{6,2},{1,5},{3,7},{5,1},{7,3},{8,12},{10,14},{12... | collective-permute-start | bytes 12296 | tf_op jit(solution)/shard_map/ppermute | solution.py:295
  44.9 1.4 %collective-permute-start.12 = (f32[8,128]{1,0:T(8,128)S(1)}, f32[8,128]{1,0:T(8,128)S(1)}, u32[]{:S(2)}, u32[]{:S(2)}) collective-permute-start(f32[8,128]{1,0:T(8,128)S(1)} %get-tuple-element.51), channel_id=1, source_target_pairs={{0,6},{2,0},{4,2},{6,4},{1,7},{3,1},{5,3},{7,5},{8,14},{10,8},{12,... | collective-permute-start | bytes 12296 | tf_op jit(solution)/shard_map/ppermute | solution.py:295
  46.3 1.1 %shard_map.125 = (bf16[16,128,256]{2,1,0:T(8,128)(2,1)S(1)}, f32[16,128]{1,0:T(8,128)}) custom-call(bf16[264,128]{1,0:T(8,128)(2,1)S(1)} %get-tuple-element.31.refs_0_, bf16[2,264,128]{2,1,0:T(8,128)(2,1)S(1)} %collective-permute-done.b_ref.refs_1_, bf16[2,264,128]{2,1,0:T(8,128)(2,1)S(1)} %collective-permute-done.1.c_ref.refs_2_, ...), custom_call_target="tpu_custom_call" | custom-call | tf_op jit(solution)/shard_map/pallas_call | solution.py:108
  47.4 1.2 %shard_map.126 = bf16[2,8,128,128]{3,2,1,0:T(8,128)(2,1)} custom-call(bf16[264,128]{1,0:T(8,128)(2,1)S(1)} %get-tuple-element.31.refs_0_, bf16[2,264,128]{2,1,0:T(8,128)(2,1)S(1)} %collective-permute-done.b_ref.refs_1_, bf16[2,264,128]{2,1,0:T(8,128)(2,1)S(1)} %collective-permute-done.1.c_ref.refs_2_, ...), custom_call_target="tpu_custom_call" | custom-call | tf_op jit(solution)/shard_map/pallas_call | solution.py:108
  48.5 0.0 collective-permute-done.11.c_ref
  48.5 0.0 collective-permute-done.12.d_ref
  48.5 0.6 %shard_map.128 = bf16[8,128]{1,0:T(8,128)(2,1)} custom-call(f32[8,128]{1,0:T(8,128)S(1)} %get-tuple-element.48.a_ref, f32[8,128]{1,0:T(8,128)S(1)} %collective-permute-done.10.b_ref, f32[8,128]{1,0:T(8,128)S(1)} %collective-permute-done.11.c_ref, f32[8,128]{1,0:T(8,128)S(1)} %collective-permute-done.12.d_ref), custom_call_target="tpu_custom_call" | custom-call | tf_op jit(solution)/shard_map/pallas_call | solution.py:108
  (12 shorter events, 0.1 us)
Async XLA Ops:
  3.1 34.5 %copy-start = (bf16[1,128,1024]{2,1,0:T(8,128)(2,1)S(1)}, bf16[1,128,1024]{2,1,0:T(8,128)(2,1)}, u32[]{:S(2)}) copy-start(bf16[1,128,1024]{2,1,0:T(8,128)(2,1)} %param.17) | copy-start | bytes 786436
  3.2 34.5 %copy-start.1 = (bf16[8,1,128]{2,0,1:T(8,128)(2,1)S(1)}, bf16[8,1,128]{2,0,1:T(8,128)(2,1)}, u32[]{:S(2)}) copy-start(bf16[8,1,128]{2,0,1:T(8,128)(2,1)} %param.16) | copy-start | bytes 6148
  3.2 34.5 %copy-start.2 = (f32[2,1]{0,1:T(1,128)S(1)}, f32[2,1]{0,1:T(1,128)}, u32[]{:S(2)}) copy-start(f32[2,1]{0,1:T(1,128)} %param.14) | copy-start | bytes 28
  3.2 34.5 %copy-start.3 = (f32[2,1]{0,1:T(1,128)S(1)}, f32[2,1]{0,1:T(1,128)}, u32[]{:S(2)}) copy-start(f32[2,1]{0,1:T(1,128)} %param.15) | copy-start | bytes 28
  3.9 16.3 %collective-permute-start.3 = (bf16[4,264,128]{2,1,0:T(8,128)(2,1)S(1)}, bf16[4,264,128]{2,1,0:T(8,128)(2,1)S(1)}, u32[]{:S(2)}, u32[]{:S(2)}) collective-permute-start(bf16[4,264,128]{2,1,0:T(8,128)(2,1)S(1)} %shard_map.121), channel_id=1, source_target_pairs={{0,32},{8,40},{16,48},{24,56},{32,0},{40,8},{48,16},{56,24},{64,96... | collective-permute-start | bytes 811016 | tf_op jit(solution)/shard_map/ppermute | solution.py:290
  5.9 20.3 %collective-permute-start.2 = (bf16[4,264,128]{2,1,0:T(8,128)(2,1)S(1)}, bf16[4,264,128]{2,1,0:T(8,128)(2,1)S(1)}, u32[]{:S(2)}, u32[]{:S(2)}) collective-permute-start(bf16[4,264,128]{2,1,0:T(8,128)(2,1)S(1)} %get-tuple-element.34), channel_id=1, source_target_pairs={{0,96},{8,104},{16,112},{24,120},{32,64},{40,72},{48,80},{56,88},{... | collective-permute-start | bytes 811016 | tf_op jit(solution)/shard_map/ppermute | solution.py:290
  7.1 8.8 %collective-permute-start = (bf16[2,264,128]{2,1,0:T(8,128)(2,1)S(1)}, bf16[2,264,128]{2,1,0:T(8,128)(2,1)S(1)}, u32[]{:S(2)}, u32[]{:S(2)}) collective-permute-start(bf16[2,264,128]{2,1,0:T(8,128)(2,1)S(1)} %get-tuple-element.32), channel_id=1, source_target_pairs={{0,8},{8,16},{16,24},{24,0},{32,40},{40,48},{48,56},{56,32},{64,72... | collective-permute-start | bytes 405512 | tf_op jit(solution)/shard_map/ppermute | solution.py:290
  8.8 8.8 %collective-permute-start.1 = (bf16[2,264,128]{2,1,0:T(8,128)(2,1)S(1)}, bf16[2,264,128]{2,1,0:T(8,128)(2,1)S(1)}, u32[]{:S(2)}, u32[]{:S(2)}) collective-permute-start(bf16[2,264,128]{2,1,0:T(8,128)(2,1)S(1)} %get-tuple-element.33), channel_id=1, source_target_pairs={{0,16},{8,24},{16,0},{24,8},{32,48},{40,56},{48,32},{56,40},{64,80... | collective-permute-start | bytes 405512 | tf_op jit(solution)/shard_map/ppermute | solution.py:290
  11.7 4.3 %collective-permute-start.7 = (bf16[264,128]{1,0:T(8,128)(2,1)S(1)}, bf16[264,128]{1,0:T(8,128)(2,1)S(1)}, u32[]{:S(2)}, u32[]{:S(2)}) collective-permute-start(bf16[264,128]{1,0:T(8,128)(2,1)S(1)} %get-tuple-element.40), channel_id=1, source_target_pairs={{0,24},{8,0},{16,8},{24,16},{32,56},{40,32},{48,40},{56,48},{64,88... | collective-permute-start | bytes 202760 | tf_op jit(solution)/shard_map/ppermute | solution.py:290
  17.6 14.5 %collective-permute-start.8 = (bf16[4,264,128]{2,1,0:T(8,128)(2,1)S(1)}, bf16[4,264,128]{2,1,0:T(8,128)(2,1)S(1)}, u32[]{:S(2)}, u32[]{:S(2)}) collective-permute-start(bf16[4,264,128]{2,1,0:T(8,128)(2,1)S(1)} %shard_map.123), channel_id=1, source_target_pairs={{0,64},{8,72},{16,80},{24,88},{32,96},{40,104},{48,112},{56,120},{... | collective-permute-start | bytes 811016 | tf_op jit(solution)/shard_map/ppermute | solution.py:290
  26.2 11.4 %collective-permute-start.6 = (bf16[3,264,128]{2,1,0:T(8,128)(2,1)S(1)}, bf16[3,264,128]{2,1,0:T(8,128)(2,1)S(1)}, u32[]{:S(2)}, u32[]{:S(2)}) collective-permute-start(bf16[3,264,128]{2,1,0:T(8,128)(2,1)S(1)} %get-tuple-element.38), channel_id=1, source_target_pairs={{0,24},{8,0},{16,8},{24,16},{32,56},{40,32},{48,40},{56,48},{64,88... | collective-permute-start | bytes 608264 | tf_op jit(solution)/shard_map/ppermute | solution.py:290
  30.0 7.7 %collective-permute-start.4 = (bf16[2,264,128]{2,1,0:T(8,128)(2,1)S(1)}, bf16[2,264,128]{2,1,0:T(8,128)(2,1)S(1)}, u32[]{:S(2)}, u32[]{:S(2)}) collective-permute-start(bf16[2,264,128]{2,1,0:T(8,128)(2,1)S(1)} %get-tuple-element.36), channel_id=1, source_target_pairs={{0,8},{8,16},{16,24},{24,0},{32,40},{40,48},{48,56},{56,32},{64,72... | collective-permute-start | bytes 405512 | tf_op jit(solution)/shard_map/ppermute | solution.py:290
  30.0 7.7 %collective-permute-start.5 = (bf16[2,264,128]{2,1,0:T(8,128)(2,1)S(1)}, bf16[2,264,128]{2,1,0:T(8,128)(2,1)S(1)}, u32[]{:S(2)}, u32[]{:S(2)}) collective-permute-start(bf16[2,264,128]{2,1,0:T(8,128)(2,1)S(1)} %get-tuple-element.37), channel_id=1, source_target_pairs={{0,16},{8,24},{16,0},{24,8},{32,48},{40,56},{48,32},{56,40},{64,80... | collective-permute-start | bytes 405512 | tf_op jit(solution)/shard_map/ppermute | solution.py:290
  39.4 1.2 %collective-permute-start.9 = (f32[4,8,128]{2,1,0:T(8,128)S(1)}, f32[4,8,128]{2,1,0:T(8,128)S(1)}, u32[]{:S(2)}, u32[]{:S(2)}) collective-permute-start(f32[4,8,128]{2,1,0:T(8,128)S(1)} %get-tuple-element.47), channel_id=1, source_target_pairs={{0,1},{1,0},{2,3},{3,2},{4,5},{5,4},{6,7},{7,6},{8,9},{9,8},{10,11... | collective-permute-start | bytes 49160 | tf_op jit(solution)/shard_map/ppermute | solution.py:295
  40.6 7.9 %collective-permute-start.10 = (f32[8,128]{1,0:T(8,128)S(1)}, f32[8,128]{1,0:T(8,128)S(1)}, u32[]{:S(2)}, u32[]{:S(2)}) collective-permute-start(f32[8,128]{1,0:T(8,128)S(1)} %get-tuple-element.49), channel_id=1, source_target_pairs={{0,2},{2,4},{4,6},{6,0},{1,3},{3,5},{5,7},{7,1},{8,10},{10,12},{12... | collective-permute-start | bytes 12296 | tf_op jit(solution)/shard_map/ppermute | solution.py:295
  42.1 6.4 %collective-permute-start.11 = (f32[8,128]{1,0:T(8,128)S(1)}, f32[8,128]{1,0:T(8,128)S(1)}, u32[]{:S(2)}, u32[]{:S(2)}) collective-permute-start(f32[8,128]{1,0:T(8,128)S(1)} %get-tuple-element.50), channel_id=1, source_target_pairs={{0,4},{2,6},{4,0},{6,2},{1,5},{3,7},{5,1},{7,3},{8,12},{10,14},{12... | collective-permute-start | bytes 12296 | tf_op jit(solution)/shard_map/ppermute | solution.py:295
  44.9 3.7 %collective-permute-start.12 = (f32[8,128]{1,0:T(8,128)S(1)}, f32[8,128]{1,0:T(8,128)S(1)}, u32[]{:S(2)}, u32[]{:S(2)}) collective-permute-start(f32[8,128]{1,0:T(8,128)S(1)} %get-tuple-element.51), channel_id=1, source_target_pairs={{0,6},{2,0},{4,2},{6,4},{1,7},{3,1},{5,3},{7,5},{8,14},{10,8},{12,... | collective-permute-start | bytes 12296 | tf_op jit(solution)/shard_map/ppermute | solution.py:295

commit v6 on v5

--- a/solution.py
+++ b/solution.py
@@ -82,9 +82,9 @@
     project_blocks(rest_ref, 0, w_ref[...], g_ref[...], [twin_ref.at[k] for k in range(ROW)])
 
 
-def third_kernel(rest_ref, w_ref, g_ref, c1_ref, c2_ref, c3_ref, far_ref, own0_ref, own3_ref):
-    project_blocks(rest_ref, ROW, w_ref[...], g_ref[...], [far_ref, c1_ref.at[0], c2_ref.at[0], c3_ref])
-    project_blocks(rest_ref, 2 * ROW, w_ref[...], g_ref[...], [own0_ref, c1_ref.at[1], c2_ref.at[1], own3_ref])
+def third_kernel(rest_ref, w_ref, g_ref, *outs):
+    project_blocks(rest_ref, ROW, w_ref[...], g_ref[...], outs[:ROW])
+    project_blocks(rest_ref, 2 * ROW, w_ref[...], g_ref[...], outs[ROW:])
 
 
 ANY = pl.BlockSpec(memory_space=pl.ANY)
@@ -132,18 +132,15 @@
     )(*[pltpu.with_memory_space_constraint(a, pltpu.HBM) for a in args])
 
 
-def gather_kernel(a_ref, b_ref, c_ref, d_ref, out_ref):
-    out_ref[0] = a_ref[...]
-    out_ref[1] = b_ref[0]
-    out_ref[2] = c_ref[0]
-    out_ref[3] = d_ref[...]
-
-
-def legs_kernel(a_ref, b_ref, own3_ref, *outs):
+def gather_kernel(*refs):
+    for i in range(ROW):
+        refs[ROW][i] = refs[i][...]
+
+
+def legs_kernel(a_ref, b_ref, *outs):
     for k, out in enumerate(outs):
         out[0] = a_ref[k + 1]
         out[1] = b_ref[k + 1]
-    outs[2][2] = own3_ref[...]
 
 
 def three_parts(a):
@@ -165,8 +162,7 @@
 
 
 def landed(refs):
-    own0, c1, c2, mirror, twin, s1, s2, s3, far = refs
-    own = [own0, c1.at[1], c2.at[1], s3.at[2]]
+    own, (mirror, twin, s1, s2, s3, far) = list(refs[:ROW]), refs[ROW:]
     from_mirror, from_twin = [
         [kept.at[0]] + [s.at[i] for s in (s1, s2, s3)] for i, kept in enumerate((mirror, twin))
     ]
@@ -185,8 +181,8 @@
 
 
 def read_kernel(*refs):
-    blocks = landed(refs[:9])
-    q_ref, wo_ref, ib_ref, fb_ref, keep_ref, send_ref, weight_ref, turned_ref, stab_ref = refs[9:]
+    blocks = landed(refs[:10])
+    q_ref, wo_ref, ib_ref, fb_ref, keep_ref, send_ref, weight_ref, turned_ref, stab_ref = refs[10:]
     scale = HD ** -0.5
     row, lane8, mine = rows_mine()
     query = q_ref[...]
@@ -249,8 +245,8 @@
 
 
 def weigh_kernel(*refs):
-    blocks = landed(refs[:9])
-    weight_ref, turned_ref, vw_ref, norm_ref = refs[9:]
+    blocks = landed(refs[:10])
+    weight_ref, turned_ref, vw_ref, norm_ref = refs[10:]
     _, _, mine = rows_mine()
     norm = jnp.zeros((4 * OWN, HD), F32)
     for j, blk in enumerate(blocks):
@@ -264,8 +260,8 @@
 
 
 def memory_kernel(*refs):
-    blocks = landed(refs[:9])
-    vw_ref, mem_ref = refs[9:]
+    blocks = landed(refs[:10])
+    vw_ref, mem_ref = refs[10:]
     for s in range(OWN):
         at = slice(s * POS, (s + 1) * POS)
         keys = jnp.concatenate([blk[at, :] for blk in blocks], axis=0)
@@ -303,15 +299,14 @@
     mirror = shift(mirror, 3, 0)
     twin = run(second_kernel, block(ROW), (later, w, gates))
     twin = shift(twin, 1, 0)
-    *cross, far, own0, own3 = run(
-        third_kernel, (block(2), block(2), block(), block(), block(), block()), (later, w, gates)
-    )
-    cross = [shift(blocks, 0, k) for k, blocks in zip(hops, cross)]
-    far = run(gather_kernel, block(ROW), (far, *cross), 4)
+    made = run(third_kernel, (block(),) * (2 * ROW), (later, w, gates))
+    cross = [made[0]] + [shift(made[k], 0, k) for k in hops]
+    own = [made[ROW]] + [shift(made[ROW + k], 0, k) for k in hops]
+    far = run(gather_kernel, block(ROW), cross, 4)
     far = shift(far, 2, 0)
-    side = run(legs_kernel, (block(2), block(2), block(3)), (mirror, twin, own3), 4)
+    side = run(legs_kernel, (block(2),) * 3, (mirror, twin), 4)
     side = [shift(blocks, 0, k) for k, blocks in zip(hops, side)]
-    blocks = (own0, cross[0], cross[1], mirror, twin, *side, far)
+    blocks = (*own, mirror, twin, *side, far)
     half = pltpu.VMEM((TPX, OWN, HD), F32)
     keep, send, weight, turned, stab = run(
         read_kernel,

time: 49.2 us -> 48.8 us (level)
  waiting for transfers between devices: 17.3 us -> 12.7 us
  starting transfers between devices: 22 us -> 26.1 us
    ppermute x9 -> x12, waiting for transfers between devices: 16.1 us -> 11.5 us  [shift(): return lax.ppermute(array, 'sp', pairs)]
    ppermute x9 -> x12, starting transfers between devices: 16.4 us -> 20.5 us  [shift(): return lax.ppermute(array, 'sp', pairs)]
  transfers between devices with their start and end apart: 13 -> 16, of which waited for: 5 -> 6; matrix products, arithmetic and copies ran while one was open for 0% -> 0% of each run, Pallas kernels for 7% -> 7%
where the time goes in v6:
time: 48.8 us; the launch traced here: 48.7 us
  starting transfers between devices  26.1 us (53%)
  waiting for transfers between devices  12.7 us (26%)
  Pallas kernels  9.08 us (19%)
  between operations  0.76 us (2%)
    ppermute x12, starting transfers between devices, shift(): return lax.ppermute(array, 'sp', pairs)  20.5 us
    ppermute x12, waiting for transfers between devices, shift(): return lax.ppermute(array, 'sp', pairs)  11.5 us
    pallas_call x9, Pallas kernels, run(): pl.pallas_call(kernel, in_specs=[VM] * len(args), out_specs=specs, out_sh...  6.58 us
    ppermute x4, starting transfers between devices, across(): lax.ppermute(array, axis, [(i, (i + hop) % size) for i in range(size)])  5.66 us
    pallas_call x1, Pallas kernels, project_near(): pl.pallas_call(near_kernel, in_specs=[ANY] * 5, out_specs=[VM] * 4, out_s...  2.5 us
    ppermute x4, waiting for transfers between devices, across(): lax.ppermute(array, axis, [(i, (i + hop) % size) for i in range(size)])  1.19 us
  transfers between devices with their start and end apart: 16, of which 6 were waited for; matrix products, arithmetic and copies ran while one was open for 0% of the time, Pallas kernels for 7%

profile of v6, /device:TPU:64, one launch (start us, length us, event | category | flops | bytes accessed | tf_op | source)
XLA Modules:
  0.0 48.7 jit_solution(17569902999715699378)
XLA Ops:
  0.6 2.5 %near.1 = (bf16[4,264,128]{2,1,0:T(8,128)(2,1)S(1)}, bf16[1024,256]{1,0:T(8,128)(2,1)S(1)}, bf16[8,1024]{1,0:T(8,128)(2,1)S(1)}, bf16[12,8,16,1024]{3,2,1,0:T(8,128)(2,1)S(1)}) custom-call(bf16[128,16,1024]{2,1,0:T(8,128)(2,1)} %x_ref.1, bf16[1024,128]{1,0:T(8,128)(2,1)} %bitcast.22, bf16[1024,128]{1,0:T(8,128)(2,1)} %bitcast.23, bf16[2,1024]{1,0:T(2,128)(2,1)} %bitcast.24, ...), custom_call_target="tpu_custom_call" | custom-call | tf_op jit(solution)/shard_map/near/pallas_call | solution.py:119
  3.1 0.0 copy-start
  3.2 0.0 copy-start.1
  3.2 0.0 copy-start.2
  3.2 0.0 copy-start.3
  3.2 0.7 %shard_map.121 = bf16[4,264,128]{2,1,0:T(8,128)(2,1)S(1)} custom-call(bf16[12,8,16,1024]{3,2,1,0:T(8,128)(2,1)S(1)} %get-tuple-element.30.rest_ref, bf16[1024,256]{1,0:T(8,128)(2,1)S(1)} %get-tuple-element.31.w_ref, bf16[8,1024]{1,0:T(8,128)(2,1)S(1)} %get-tuple-element.32.g_ref), custom_call_target="tpu_custom_call" | custom-call | tf_op jit(solution)/shard_map/pallas_call | solution.py:108
  3.9 2.0 %collective-permute-start.4 = (bf16[4,264,128]{2,1,0:T(8,128)(2,1)S(1)}, bf16[4,264,128]{2,1,0:T(8,128)(2,1)S(1)}, u32[]{:S(2)}, u32[]{:S(2)}) collective-permute-start(bf16[4,264,128]{2,1,0:T(8,128)(2,1)S(1)} %shard_map.121), channel_id=1, source_target_pairs={{0,32},{8,40},{16,48},{24,56},{32,0},{40,8},{48,16},{56,24},{64,96... | collective-permute-start | bytes 811016 | tf_op jit(solution)/shard_map/ppermute | solution.py:286
  5.9 0.0 collective-permute-start.3
  5.9 1.2 %shard_map.120 = (bf16[264,128]{1,0:T(8,128)(2,1)S(1)}, bf16[264,128]{1,0:T(8,128)(2,1)S(1)}, bf16[264,128]{1,0:T(8,128)(2,1)S(1)}, bf16[264,128]{1,0:T(8,128)(2...) custom-call(bf16[12,8,16,1024]{3,2,1,0:T(8,128)(2,1)S(1)} %get-tuple, ...), custom_call_target="tpu_custom_call" | custom-call | tf_op jit(solution)/shard_map/pallas_call | solution.py:108
  7.2 1.6 %collective-permute-start.8 = (bf16[264,128]{1,0:T(8,128)(2,1)S(1)}, bf16[264,128]{1,0:T(8,128)(2,1)S(1)}, u32[]{:S(2)}, u32[]{:S(2)}) collective-permute-start(bf16[264,128]{1,0:T(8,128)(2,1)S(1)} %get-tuple-element.42), channel_id=1, source_target_pairs={{0,8},{8,16},{16,24},{24,0},{32,40},{40,48},{48,56},{56,32},{64,72... | collective-permute-start | bytes 202760 | tf_op jit(solution)/shard_map/ppermute | solution.py:286
  8.8 2.9 %collective-permute-start.9 = (bf16[264,128]{1,0:T(8,128)(2,1)S(1)}, bf16[264,128]{1,0:T(8,128)(2,1)S(1)}, u32[]{:S(2)}, u32[]{:S(2)}) collective-permute-start(bf16[264,128]{1,0:T(8,128)(2,1)S(1)} %get-tuple-element.43), channel_id=1, source_target_pairs={{0,16},{8,24},{16,0},{24,8},{32,48},{40,56},{48,32},{56,40},{64,80... | collective-permute-start | bytes 202760 | tf_op jit(solution)/shard_map/ppermute | solution.py:286
  11.7 1.3 %collective-permute-start.10 = (bf16[264,128]{1,0:T(8,128)(2,1)S(1)}, bf16[264,128]{1,0:T(8,128)(2,1)S(1)}, u32[]{:S(2)}, u32[]{:S(2)}) collective-permute-start(bf16[264,128]{1,0:T(8,128)(2,1)S(1)} %get-tuple-element.44), channel_id=1, source_target_pairs={{0,24},{8,0},{16,8},{24,16},{32,56},{40,32},{48,40},{56,48},{64,88... | collective-permute-start | bytes 202760 | tf_op jit(solution)/shard_map/ppermute | solution.py:286
  13.0 0.4 collective-permute-done.8.refs_1_
  13.5 1.3 %collective-permute-done.9.refs_2_ = bf16[264,128]{1,0:T(8,128)(2,1)S(1)} collective-permute-done((bf16[264,128]{1,0:T(8,128)(2,1)S(1)}, bf16[264,128]{1,0:T(8,128)(2,1)S(1)}, u32[]{:S(2)}, u32[]{:S(2)}) %collective-permute-start.9) | collective-permute-done | bytes 67616 | tf_op jit(solution)/shard_map/ppermute | solution.py:286
  14.7 1.3 %collective-permute-done.10.refs_3_ = bf16[264,128]{1,0:T(8,128)(2,1)S(1)} collective-permute-done((bf16[264,128]{1,0:T(8,128)(2,1)S(1)}, bf16[264,128]{1,0:T(8,128)(2,1)S(1)}, u32[]{:S(2)}, u32[]{:S(2)}) %collective-permute-start.10) | collective-permute-done | bytes 67616 | tf_op jit(solution)/shard_map/ppermute | solution.py:286
  16.0 2.6 %collective-permute-start.11 = (bf16[4,264,128]{2,1,0:T(8,128)(2,1)S(1)}, bf16[4,264,128]{2,1,0:T(8,128)(2,1)S(1)}, u32[]{:S(2)}, u32[]{:S(2)}) collective-permute-start(bf16[4,264,128]{2,1,0:T(8,128)(2,1)S(1)} %shard_map.123), channel_id=1, source_target_pairs={{0,64},{8,72},{16,80},{24,88},{32,96},{40,104},{48,112},{56,120},{... | collective-permute-start | bytes 811016 | tf_op jit(solution)/shard_map/ppermute | solution.py:286
  18.6 0.3 collective-permute-start
  18.9 3.7 %collective-permute-start.1 = (bf16[264,128]{1,0:T(8,128)(2,1)S(1)}, bf16[264,128]{1,0:T(8,128)(2,1)S(1)}, u32[]{:S(2)}, u32[]{:S(2)}) collective-permute-start(bf16[264,128]{1,0:T(8,128)(2,1)S(1)} %get-tuple-element.35), channel_id=1, source_target_pairs={{0,16},{8,24},{16,0},{24,8},{32,48},{40,56},{48,32},{56,40},{64,80... | collective-permute-start | bytes 202760 | tf_op jit(solution)/shard_map/ppermute | solution.py:286
  22.6 4.2 %collective-permute-done.3.a_ref.refs_4_ = bf16[4,264,128]{2,1,0:T(8,128)(2,1)S(1)} collective-permute-done((bf16[4,264,128]{2,1,0:T(8,128)(2,1)S(1)}, bf16[4,264,128]{2,1,0:T(8,128)(2,1)S(1)}, u32[]{:S(2)}, u32[]{:S(2)}) %collective-permute-start.3) | collective-permute-done | bytes 270368 | tf_op jit(solution)/shard_map/ppermute | solution.py:286
  26.9 1.7 %collective-permute-start.5 = (bf16[2,264,128]{2,1,0:T(8,128)(2,1)S(1)}, bf16[2,264,128]{2,1,0:T(8,128)(2,1)S(1)}, u32[]{:S(2)}, u32[]{:S(2)}) collective-permute-start(bf16[2,264,128]{2,1,0:T(8,128)(2,1)S(1)} %get-tuple-element.38), channel_id=1, source_target_pairs={{0,8},{8,16},{16,24},{24,0},{32,40},{40,48},{48,56},{56,32},{64,72... | collective-permute-start | bytes 405512 | tf_op jit(solution)/shard_map/ppermute | solution.py:286
  28.5 2.9 %collective-permute-start.6 = (bf16[2,264,128]{2,1,0:T(8,128)(2,1)S(1)}, bf16[2,264,128]{2,1,0:T(8,128)(2,1)S(1)}, u32[]{:S(2)}, u32[]{:S(2)}) collective-permute-start(bf16[2,264,128]{2,1,0:T(8,128)(2,1)S(1)} %get-tuple-element.39), channel_id=1, source_target_pairs={{0,16},{8,24},{16,0},{24,8},{32,48},{40,56},{48,32},{56,40},{64,80... | collective-permute-start | bytes 405512 | tf_op jit(solution)/shard_map/ppermute | solution.py:286
  31.4 1.3 %collective-permute-start.7 = (bf16[2,264,128]{2,1,0:T(8,128)(2,1)S(1)}, bf16[2,264,128]{2,1,0:T(8,128)(2,1)S(1)}, u32[]{:S(2)}, u32[]{:S(2)}) collective-permute-start(bf16[2,264,128]{2,1,0:T(8,128)(2,1)S(1)} %get-tuple-element.40), channel_id=1, source_target_pairs={{0,24},{8,0},{16,8},{24,16},{32,56},{40,32},{48,40},{56,48},{64,88... | collective-permute-start | bytes 405512 | tf_op jit(solution)/shard_map/ppermute | solution.py:286
  32.8 0.1 collective-permute-start.2
  32.9 4.3 %collective-permute-done.2.refs_3_ = bf16[264,128]{1,0:T(8,128)(2,1)S(1)} collective-permute-done((bf16[264,128]{1,0:T(8,128)(2,1)S(1)}, bf16[264,128]{1,0:T(8,128)(2,1)S(1)}, u32[]{:S(2)}, u32[]{:S(2)}) %collective-permute-start.2) | collective-permute-done | bytes 67616 | tf_op jit(solution)/shard_map/ppermute | solution.py:286
  37.2 1.8 %shard_map.124 = (f32[4,8,128]{2,1,0:T(8,128)S(1)}, f32[4,8,128]{2,1,0:T(8,128)S(1)}, f32[32,128]{1,0:T(8,128)S(1)}, f32[128,32]{1,0:T(8,128)S(1)}, f32[2,1,8]{2,1,0:T(1,128)}) custom-call(bf16[264,128]{1,0:T(8,128)(2,1)S(1)} %get-tuple-element.33.refs_0_, bf16[264,128]{1,0:T(8,128)(2,1)S(1)} %collective-permute-done.refs_1_, ...), custom_call_target="tpu_custom_call" | custom-call | tf_op jit(solution)/shard_map/pallas_call | solution.py:108
  39.0 1.2 %collective-permute-done.12.got_ref = f32[4,8,128]{2,1,0:T(8,128)S(1)} collective-permute-done((f32[4,8,128]{2,1,0:T(8,128)S(1)}, f32[4,8,128]{2,1,0:T(8,128)S(1)}, u32[]{:S(2)}, u32[]{:S(2)}) %collective-permute-start.12) | collective-permute-done | bytes 16416 | tf_op jit(solution)/shard_map/ppermute | solution.py:291
  40.2 1.5 %collective-permute-start.13 = (f32[8,128]{1,0:T(8,128)S(1)}, f32[8,128]{1,0:T(8,128)S(1)}, u32[]{:S(2)}, u32[]{:S(2)}) collective-permute-start(f32[8,128]{1,0:T(8,128)S(1)} %get-tuple-element.53), channel_id=1, source_target_pairs={{0,2},{2,4},{4,6},{6,0},{1,3},{3,5},{5,7},{7,1},{8,10},{10,12},{12... | collective-permute-start | bytes 12296 | tf_op jit(solution)/shard_map/ppermute | solution.py:291
  41.7 2.7 %collective-permute-start.14 = (f32[8,128]{1,0:T(8,128)S(1)}, f32[8,128]{1,0:T(8,128)S(1)}, u32[]{:S(2)}, u32[]{:S(2)}) collective-permute-start(f32[8,128]{1,0:T(8,128)S(1)} %get-tuple-element.54), channel_id=1, source_target_pairs={{0,4},{2,6},{4,0},{6,2},{1,5},{3,7},{5,1},{7,3},{8,12},{10,14},{12... | collective-permute-start | bytes 12296 | tf_op jit(solution)/shard_map/ppermute | solution.py:291
  44.4 1.4 %collective-permute-start.15 = (f32[8,128]{1,0:T(8,128)S(1)}, f32[8,128]{1,0:T(8,128)S(1)}, u32[]{:S(2)}, u32[]{:S(2)}) collective-permute-start(f32[8,128]{1,0:T(8,128)S(1)} %get-tuple-element.55), channel_id=1, source_target_pairs={{0,6},{2,0},{4,2},{6,4},{1,7},{3,1},{5,3},{7,5},{8,14},{10,8},{12,... | collective-permute-start | bytes 12296 | tf_op jit(solution)/shard_map/ppermute | solution.py:291
  45.8 1.1 %shard_map.125 = (bf16[16,128,256]{2,1,0:T(8,128)(2,1)S(1)}, f32[16,128]{1,0:T(8,128)}) custom-call(bf16[264,128]{1,0:T(8,128)(2,1)S(1)} %get-tuple-element.33.refs_0_, bf16[264,128]{1,0:T(8,128)(2,1)S(1)} %collective-permute-done.refs_1_, bf16[264,128]{1,0:T(8,128)(2,1)S(1)} %collective-permute-done.1.refs_2_, ...), custom_call_target="tpu_custom_call" | custom-call | tf_op jit(solution)/shard_map/pallas_call | solution.py:108
  46.9 1.2 %shard_map.126 = bf16[2,8,128,128]{3,2,1,0:T(8,128)(2,1)} custom-call(bf16[264,128]{1,0:T(8,128)(2,1)S(1)} %get-tuple-element.33.refs_0_, bf16[264,128]{1,0:T(8,128)(2,1)S(1)} %collective-permute-done.refs_1_, bf16[264,128]{1,0:T(8,128)(2,1)S(1)} %collective-permute-done.1.refs_2_, bf16[264,128]{1,0:T(8,128)(2,1)S(1)} %collective-permute-done.2.refs_3_, ...), custom_call_target="tpu_custom_call" | custom-call | tf_op jit(solution)/shard_map/pallas_call | solution.py:108
  48.1 0.6 %shard_map.128 = bf16[8,128]{1,0:T(8,128)(2,1)} custom-call(f32[8,128]{1,0:T(8,128)S(1)} %get-tuple-element.52.a_ref, f32[8,128]{1,0:T(8,128)S(1)} %collective-permute-done.13.b_ref, f32[8,128]{1,0:T(8,128)S(1)} %collective-permute-done.14.c_ref, f32[8,128]{1,0:T(8,128)S(1)} %collective-permute-done.15.d_ref), custom_call_target="tpu_custom_call" | custom-call | tf_op jit(solution)/shard_map/pallas_call | solution.py:108
  (18 shorter events, 0.1 us)
Async XLA Ops:
  3.1 34.0 %copy-start = (bf16[1,128,1024]{2,1,0:T(8,128)(2,1)S(1)}, bf16[1,128,1024]{2,1,0:T(8,128)(2,1)}, u32[]{:S(2)}) copy-start(bf16[1,128,1024]{2,1,0:T(8,128)(2,1)} %param.17) | copy-start | bytes 786436
  3.2 34.0 %copy-start.1 = (bf16[8,1,128]{2,0,1:T(8,128)(2,1)S(1)}, bf16[8,1,128]{2,0,1:T(8,128)(2,1)}, u32[]{:S(2)}) copy-start(bf16[8,1,128]{2,0,1:T(8,128)(2,1)} %param.16) | copy-start | bytes 6148
  3.2 34.0 %copy-start.2 = (f32[2,1]{0,1:T(1,128)S(1)}, f32[2,1]{0,1:T(1,128)}, u32[]{:S(2)}) copy-start(f32[2,1]{0,1:T(1,128)} %param.14) | copy-start | bytes 28
  3.2 34.0 %copy-start.3 = (f32[2,1]{0,1:T(1,128)S(1)}, f32[2,1]{0,1:T(1,128)}, u32[]{:S(2)}) copy-start(f32[2,1]{0,1:T(1,128)} %param.15) | copy-start | bytes 28
  3.9 18.7 %collective-permute-start.4 = (bf16[4,264,128]{2,1,0:T(8,128)(2,1)S(1)}, bf16[4,264,128]{2,1,0:T(8,128)(2,1)S(1)}, u32[]{:S(2)}, u32[]{:S(2)}) collective-permute-start(bf16[4,264,128]{2,1,0:T(8,128)(2,1)S(1)} %shard_map.121), channel_id=1, source_target_pairs={{0,32},{8,40},{16,48},{24,56},{32,0},{40,8},{48,16},{56,24},{64,96... | collective-permute-start | bytes 811016 | tf_op jit(solution)/shard_map/ppermute | solution.py:286
  5.9 20.9 %collective-permute-start.3 = (bf16[4,264,128]{2,1,0:T(8,128)(2,1)S(1)}, bf16[4,264,128]{2,1,0:T(8,128)(2,1)S(1)}, u32[]{:S(2)}, u32[]{:S(2)}) collective-permute-start(bf16[4,264,128]{2,1,0:T(8,128)(2,1)S(1)} %get-tuple-element.37), channel_id=1, source_target_pairs={{0,96},{8,104},{16,112},{24,120},{32,64},{40,72},{48,80},{56,88},{... | collective-permute-start | bytes 811016 | tf_op jit(solution)/shard_map/ppermute | solution.py:286
  7.2 6.3 %collective-permute-start.8 = (bf16[264,128]{1,0:T(8,128)(2,1)S(1)}, bf16[264,128]{1,0:T(8,128)(2,1)S(1)}, u32[]{:S(2)}, u32[]{:S(2)}) collective-permute-start(bf16[264,128]{1,0:T(8,128)(2,1)S(1)} %get-tuple-element.42), channel_id=1, source_target_pairs={{0,8},{8,16},{16,24},{24,0},{32,40},{40,48},{48,56},{56,32},{64,72... | collective-permute-start | bytes 202760 | tf_op jit(solution)/shard_map/ppermute | solution.py:286
  8.8 5.9 %collective-permute-start.9 = (bf16[264,128]{1,0:T(8,128)(2,1)S(1)}, bf16[264,128]{1,0:T(8,128)(2,1)S(1)}, u32[]{:S(2)}, u32[]{:S(2)}) collective-permute-start(bf16[264,128]{1,0:T(8,128)(2,1)S(1)} %get-tuple-element.43), channel_id=1, source_target_pairs={{0,16},{8,24},{16,0},{24,8},{32,48},{40,56},{48,32},{56,40},{64,80... | collective-permute-start | bytes 202760 | tf_op jit(solution)/shard_map/ppermute | solution.py:286
  11.7 4.3 %collective-permute-start.10 = (bf16[264,128]{1,0:T(8,128)(2,1)S(1)}, bf16[264,128]{1,0:T(8,128)(2,1)S(1)}, u32[]{:S(2)}, u32[]{:S(2)}) collective-permute-start(bf16[264,128]{1,0:T(8,128)(2,1)S(1)} %get-tuple-element.44), channel_id=1, source_target_pairs={{0,24},{8,0},{16,8},{24,16},{32,56},{40,32},{48,40},{56,48},{64,88... | collective-permute-start | bytes 202760 | tf_op jit(solution)/shard_map/ppermute | solution.py:286
  16.0 21.2 %collective-permute-start.11 = (bf16[4,264,128]{2,1,0:T(8,128)(2,1)S(1)}, bf16[4,264,128]{2,1,0:T(8,128)(2,1)S(1)}, u32[]{:S(2)}, u32[]{:S(2)}) collective-permute-start(bf16[4,264,128]{2,1,0:T(8,128)(2,1)S(1)} %shard_map.123), channel_id=1, source_target_pairs={{0,64},{8,72},{16,80},{24,88},{32,96},{40,104},{48,112},{56,120},{... | collective-permute-start | bytes 811016 | tf_op jit(solution)/shard_map/ppermute | solution.py:286
  18.6 12.9 %collective-permute-start = (bf16[264,128]{1,0:T(8,128)(2,1)S(1)}, bf16[264,128]{1,0:T(8,128)(2,1)S(1)}, u32[]{:S(2)}, u32[]{:S(2)}) collective-permute-start(bf16[264,128]{1,0:T(8,128)(2,1)S(1)} %get-tuple-element.34), channel_id=1, source_target_pairs={{0,8},{8,16},{16,24},{24,0},{32,40},{40,48},{48,56},{56,32},{64,72... | collective-permute-start | bytes 202760 | tf_op jit(solution)/shard_map/ppermute | solution.py:286
  18.9 13.9 %collective-permute-start.1 = (bf16[264,128]{1,0:T(8,128)(2,1)S(1)}, bf16[264,128]{1,0:T(8,128)(2,1)S(1)}, u32[]{:S(2)}, u32[]{:S(2)}) collective-permute-start(bf16[264,128]{1,0:T(8,128)(2,1)S(1)} %get-tuple-element.35), channel_id=1, source_target_pairs={{0,16},{8,24},{16,0},{24,8},{32,48},{40,56},{48,32},{56,40},{64,80... | collective-permute-start | bytes 202760 | tf_op jit(solution)/shard_map/ppermute | solution.py:286
  26.9 10.3 %collective-permute-start.5 = (bf16[2,264,128]{2,1,0:T(8,128)(2,1)S(1)}, bf16[2,264,128]{2,1,0:T(8,128)(2,1)S(1)}, u32[]{:S(2)}, u32[]{:S(2)}) collective-permute-start(bf16[2,264,128]{2,1,0:T(8,128)(2,1)S(1)} %get-tuple-element.38), channel_id=1, source_target_pairs={{0,8},{8,16},{16,24},{24,0},{32,40},{40,48},{48,56},{56,32},{64,72... | collective-permute-start | bytes 405512 | tf_op jit(solution)/shard_map/ppermute | solution.py:286
  28.5 8.6 %collective-permute-start.6 = (bf16[2,264,128]{2,1,0:T(8,128)(2,1)S(1)}, bf16[2,264,128]{2,1,0:T(8,128)(2,1)S(1)}, u32[]{:S(2)}, u32[]{:S(2)}) collective-permute-start(bf16[2,264,128]{2,1,0:T(8,128)(2,1)S(1)} %get-tuple-element.39), channel_id=1, source_target_pairs={{0,16},{8,24},{16,0},{24,8},{32,48},{40,56},{48,32},{56,40},{64,80... | collective-permute-start | bytes 405512 | tf_op jit(solution)/shard_map/ppermute | solution.py:286
  31.4 5.8 %collective-permute-start.7 = (bf16[2,264,128]{2,1,0:T(8,128)(2,1)S(1)}, bf16[2,264,128]{2,1,0:T(8,128)(2,1)S(1)}, u32[]{:S(2)}, u32[]{:S(2)}) collective-permute-start(bf16[2,264,128]{2,1,0:T(8,128)(2,1)S(1)} %get-tuple-element.40), channel_id=1, source_target_pairs={{0,24},{8,0},{16,8},{24,16},{32,56},{40,32},{48,40},{56,48},{64,88... | collective-permute-start | bytes 405512 | tf_op jit(solution)/shard_map/ppermute | solution.py:286
  32.8 4.4 %collective-permute-start.2 = (bf16[264,128]{1,0:T(8,128)(2,1)S(1)}, bf16[264,128]{1,0:T(8,128)(2,1)S(1)}, u32[]{:S(2)}, u32[]{:S(2)}) collective-permute-start(bf16[264,128]{1,0:T(8,128)(2,1)S(1)} %get-tuple-element.36), channel_id=1, source_target_pairs={{0,24},{8,0},{16,8},{24,16},{32,56},{40,32},{48,40},{56,48},{64,88... | collective-permute-start | bytes 202760 | tf_op jit(solution)/shard_map/ppermute | solution.py:286
  39.0 1.2 %collective-permute-start.12 = (f32[4,8,128]{2,1,0:T(8,128)S(1)}, f32[4,8,128]{2,1,0:T(8,128)S(1)}, u32[]{:S(2)}, u32[]{:S(2)}) collective-permute-start(f32[4,8,128]{2,1,0:T(8,128)S(1)} %get-tuple-element.51), channel_id=1, source_target_pairs={{0,1},{1,0},{2,3},{3,2},{4,5},{5,4},{6,7},{7,6},{8,9},{9,8},{10,11... | collective-permute-start | bytes 49160 | tf_op jit(solution)/shard_map/ppermute | solution.py:291
  40.2 7.9 %collective-permute-start.13 = (f32[8,128]{1,0:T(8,128)S(1)}, f32[8,128]{1,0:T(8,128)S(1)}, u32[]{:S(2)}, u32[]{:S(2)}) collective-permute-start(f32[8,128]{1,0:T(8,128)S(1)} %get-tuple-element.53), channel_id=1, source_target_pairs={{0,2},{2,4},{4,6},{6,0},{1,3},{3,5},{5,7},{7,1},{8,10},{10,12},{12... | collective-permute-start | bytes 12296 | tf_op jit(solution)/shard_map/ppermute | solution.py:291
  41.7 6.4 %collective-permute-start.14 = (f32[8,128]{1,0:T(8,128)S(1)}, f32[8,128]{1,0:T(8,128)S(1)}, u32[]{:S(2)}, u32[]{:S(2)}) collective-permute-start(f32[8,128]{1,0:T(8,128)S(1)} %get-tuple-element.54), channel_id=1, source_target_pairs={{0,4},{2,6},{4,0},{6,2},{1,5},{3,7},{5,1},{7,3},{8,12},{10,14},{12... | collective-permute-start | bytes 12296 | tf_op jit(solution)/shard_map/ppermute | solution.py:291
  44.4 3.7 %collective-permute-start.15 = (f32[8,128]{1,0:T(8,128)S(1)}, f32[8,128]{1,0:T(8,128)S(1)}, u32[]{:S(2)}, u32[]{:S(2)}) collective-permute-start(f32[8,128]{1,0:T(8,128)S(1)} %get-tuple-element.55), channel_id=1, source_target_pairs={{0,6},{2,0},{4,2},{6,4},{1,7},{3,1},{5,3},{7,5},{8,14},{10,8},{12,... | collective-permute-start | bytes 12296 | tf_op jit(solution)/shard_map/ppermute | solution.py:291

commit v7 on v6

--- a/solution.py
+++ b/solution.py
@@ -54,17 +54,16 @@
         out[2 * ROWS :, :] = coded[:, at]
 
 
-def near_kernel(x_ref, wk_ref, wv_ref, wi_ref, wf_ref, mirror_ref, w_ref, g_ref, rest_ref, buf_ref, wi_buf, wf_buf, sem_ref):
-    key_copy = pltpu.make_async_copy(wk_ref, w_ref.at[:, :HD], sem_ref.at[SP])
-    value_copy = pltpu.make_async_copy(wv_ref, w_ref.at[:, HD:], sem_ref.at[SP + 1])
+def near_kernel(x_ref, wk_ref, wv_ref, wi_ref, wf_ref, mirror_ref, w_ref, g_ref, buf_ref, wi_buf, wf_buf, sem_ref):
+    key_copy = pltpu.make_async_copy(wk_ref, w_ref.at[:, :HD], sem_ref.at[ROW])
+    value_copy = pltpu.make_async_copy(wv_ref, w_ref.at[:, HD:], sem_ref.at[ROW + 1])
     gate_copies = [
-        pltpu.make_async_copy(wi_ref, wi_buf, sem_ref.at[SP + 2]),
-        pltpu.make_async_copy(wf_ref, wf_buf, sem_ref.at[SP + 3]),
+        pltpu.make_async_copy(wi_ref, wi_buf, sem_ref.at[ROW + 2]),
+        pltpu.make_async_copy(wf_ref, wf_buf, sem_ref.at[ROW + 3]),
     ]
     for copy in (*gate_copies, key_copy, value_copy):
         copy.start()
     copies = take(x_ref, buf_ref, sem_ref, 0, [(3, dy) for dy in range(ROW)])
-    later = take(x_ref, rest_ref, sem_ref, ROW, [(dz, dy) for dz in (1, 2, 0) for dy in range(ROW)])
     for copy in gate_copies:
         copy.wait()
     gates = jnp.concatenate((wi_buf[...].astype(F32), wf_buf[...].astype(F32), jnp.zeros((4, D), F32)), axis=0)
@@ -74,17 +73,25 @@
     for copy in copies:
         copy.wait()
     project_blocks(buf_ref, 0, w_ref[...], g_ref[...], [mirror_ref.at[k] for k in range(ROW)])
+
+
+def cross_kernel(x_ref, w_ref, g_ref, *refs):
+    outs, (rest_ref, buf_ref, sem_ref) = refs[:ROW], refs[ROW:]
+    copies = take(x_ref, buf_ref, sem_ref, 0, [(2, dy) for dy in range(ROW)])
+    later = take(x_ref, rest_ref, sem_ref, ROW, [(dz, dy) for dz in (1, 0) for dy in range(ROW)])
+    for copy in copies:
+        copy.wait()
+    project_blocks(buf_ref, 0, w_ref[...], g_ref[...], outs)
     for copy in later:
         copy.wait()
 
 
-def second_kernel(rest_ref, w_ref, g_ref, twin_ref):
+def twin_kernel(rest_ref, w_ref, g_ref, twin_ref):
     project_blocks(rest_ref, 0, w_ref[...], g_ref[...], [twin_ref.at[k] for k in range(ROW)])
 
 
-def third_kernel(rest_ref, w_ref, g_ref, *outs):
-    project_blocks(rest_ref, ROW, w_ref[...], g_ref[...], outs[:ROW])
-    project_blocks(rest_ref, 2 * ROW, w_ref[...], g_ref[...], outs[ROW:])
+def own_kernel(rest_ref, w_ref, g_ref, *outs):
+    project_blocks(rest_ref, ROW, w_ref[...], g_ref[...], outs)
 
 
 ANY = pl.BlockSpec(memory_space=pl.ANY)
@@ -119,17 +126,29 @@
     return pl.pallas_call(
         near_kernel,
         in_specs=[ANY] * 5,
-        out_specs=[VM] * 4,
+        out_specs=[VM] * 3,
         out_shape=(
-            block(ROW), pltpu.VMEM((D, 2 * HD), BF), pltpu.VMEM((8, D), BF), pltpu.VMEM((3 * ROW, OWN, POS, D), BF)
+            block(ROW), pltpu.VMEM((D, 2 * HD), BF), pltpu.VMEM((8, D), BF)
         ),
         scratch_shapes=[
             pltpu.VMEM((ROW, OWN, POS, D), BF), pltpu.VMEM((2, D), BF), pltpu.VMEM((2, D), BF),
-            pltpu.SemaphoreType.DMA((SP + 4,)),
+            pltpu.SemaphoreType.DMA((ROW + 4,)),
         ],
         compiler_params=grant(16),
         name="near",
     )(*[pltpu.with_memory_space_constraint(a, pltpu.HBM) for a in args])
+
+
+def project_cross(prompt, w, gates):
+    return pl.pallas_call(
+        cross_kernel,
+        in_specs=[ANY, VM, VM],
+        out_specs=[VM] * (ROW + 1),
+        out_shape=(block(),) * ROW + (pltpu.VMEM((2 * ROW, OWN, POS, D), BF),),
+        scratch_shapes=[pltpu.VMEM((ROW, OWN, POS, D), BF), pltpu.SemaphoreType.DMA((3 * ROW,))],
+        compiler_params=grant(16),
+        name="cross",
+    )(pltpu.with_memory_space_constraint(prompt, pltpu.HBM), vm(w), vm(gates))
 
 
 def gather_kernel(*refs):
@@ -293,17 +312,18 @@
 
 def step(prompt, w_key, w_value, w_in_gate, w_forget_gate, in_bias, forget_bias, query, w_out):
     hops = range(1, ROW)
-    mirror, w, gates, later = project_near(
+    mirror, w, gates = project_near(
         prompt, w_key.reshape(D, HD), w_value.reshape(D, HD), w_in_gate.reshape(2, D), w_forget_gate.reshape(2, D)
     )
     mirror = shift(mirror, 3, 0)
-    twin = run(second_kernel, block(ROW), (later, w, gates))
+    *cross, later = project_cross(prompt, w, gates)
+    cross = [cross[0]] + [shift(cross[k], 0, k) for k in hops]
+    twin = run(twin_kernel, block(ROW), (later, w, gates))
     twin = shift(twin, 1, 0)
-    made = run(third_kernel, (block(),) * (2 * ROW), (later, w, gates))
-    cross = [made[0]] + [shift(made[k], 0, k) for k in hops]
-    own = [made[ROW]] + [shift(made[ROW + k], 0, k) for k in hops]
     far = run(gather_kernel, block(ROW), cross, 4)
     far = shift(far, 2, 0)
+    own = run(own_kernel, (block(),) * ROW, (later, w, gates))
+    own = [own[0]] + [shift(own[k], 0, k) for k in hops]
     side = run(legs_kernel, (block(2),) * 3, (mirror, twin), 4)
     side = [shift(blocks, 0, k) for k, blocks in zip(hops, side)]
     blocks = (*own, mirror, twin, *side, far)

time: 48.8 us -> 46.2 us (0.947)
  the two profiles are of different devices: /device:TPU:64 before, /device:TPU:1 now
where the time goes in v7:
time: 46.2 us; the launch traced here: 46.1 us
  starting transfers between devices  26.2 us (57%)
  Pallas kernels  10.2 us (22%)
  waiting for transfers between devices  8.93 us (19%)
  between operations  0.78 us (2%)
    ppermute x12, starting transfers between devices, shift(): return lax.ppermute(array, 'sp', pairs)  18 us
    ppermute x4, starting transfers between devices, across(): lax.ppermute(array, axis, [(i, (i + hop) % size) for i in range(size)])  8.14 us
    ppermute x12, waiting for transfers between devices, shift(): return lax.ppermute(array, 'sp', pairs)  8.08 us
    pallas_call x9, Pallas kernels, run(): pl.pallas_call(kernel, in_specs=[VM] * len(args), out_specs=specs, out_sh...  6.03 us
    pallas_call x1, Pallas kernels, project_near(): pl.pallas_call(near_kernel, in_specs=[ANY] * 5, out_specs=[VM] * 3, out_s...  2.14 us
    pallas_call x1, Pallas kernels, project_cross(): pl.pallas_call(cross_kernel, in_specs=[ANY, VM, VM], out_specs=[VM] * (RO...  2.02 us
  transfers between devices with their start and end apart: 16, of which 5 were waited for; matrix products, arithmetic and copies ran while one was open for 0% of the time, Pallas kernels for 12%

profile of v7, /device:TPU:1, one launch (start us, length us, event | category | flops | bytes accessed | tf_op | source)
XLA Modules:
  0.0 46.1 jit_solution(13395206860518507640)
XLA Ops:
  0.6 2.1 %near.1 = (bf16[4,264,128]{2,1,0:T(8,128)(2,1)S(1)}, bf16[1024,256]{1,0:T(8,128)(2,1)S(1)}, bf16[8,1024]{1,0:T(8,128)(2,1)S(1)}) custom-call(bf16[128,16,1024]{2,1,0:T(8,128)(2,1)} %x_ref.3, bf16[1024,128]{1,0:T(8,128)(2,1)} %bitcast.22, bf16[1024,128]{1,0:T(8,128)(2,1)} %bitcast.23, bf16[2,1024]{1,0:T(2,128)(2,1)} %bitcast.24, bf16[2,1024]{1,0:T(2,128)(2,1)} %bitcast.25), custom_call_target="tpu_custom_call" | custom-call | tf_op jit(solution)/shard_map/near/pallas_call | solution.py:126
  2.8 5.2 %collective-permute-start.3 = (bf16[4,264,128]{2,1,0:T(8,128)(2,1)S(1)}, bf16[4,264,128]{2,1,0:T(8,128)(2,1)S(1)}, u32[]{:S(2)}, u32[]{:S(2)}) collective-permute-start(bf16[4,264,128]{2,1,0:T(8,128)(2,1)S(1)} %get-tuple-element.37), channel_id=1, source_target_pairs={{0,96},{8,104},{16,112},{24,120},{32,64},{40,72},{48,80},{56,88},{... | collective-permute-start | bytes 811016 | tf_op jit(solution)/shard_map/ppermute | solution.py:305
  8.0 2.0 %cross.1 = (bf16[264,128]{1,0:T(8,128)(2,1)S(1)}, bf16[264,128]{1,0:T(8,128)(2,1)S(1)}, bf16[264,128]{1,0:T(8,128)(2,1)S(1)}, bf16[264,128]{1,0:T(8,128)(2,1)S(1)}, bf16[8,8,16,1024]{3,2,1,0:T(8,128)(2,1)S(1)}) custom-call(bf16[128,16,1024]{2,1,0:T(8,128)(2,1)} %x_ref.3, bf16[1024,256]{1,0:T(8,128)(2,1)S(1)} %get-tuple-element.30.w_ref, ...), custom_call_target="tpu_custom_call" | custom-call | tf_op jit(solution)/shard_map/cross/pallas_call | solution.py:143
  10.1 0.0 copy-start
  10.1 0.0 copy-start.1
  10.1 0.0 copy-start.3
  10.1 0.7 %shard_map.121 = bf16[4,264,128]{2,1,0:T(8,128)(2,1)S(1)} custom-call(bf16[8,8,16,1024]{3,2,1,0:T(8,128)(2,1)S(1)} %get-tuple-element.32.rest_ref, bf16[1024,256]{1,0:T(8,128)(2,1)S(1)} %get-tuple-element.30.w_ref, bf16[8,1024]{1,0:T(8,128)(2,1)S(1)} %get-tuple-element.31.g_ref), custom_call_target="tpu_custom_call" | custom-call | tf_op jit(solution)/shard_map/pallas_call | solution.py:115
  10.8 0.1 collective-permute-start.4
  10.9 1.4 %collective-permute-start.8 = (bf16[264,128]{1,0:T(8,128)(2,1)S(1)}, bf16[264,128]{1,0:T(8,128)(2,1)S(1)}, u32[]{:S(2)}, u32[]{:S(2)}) collective-permute-start(bf16[264,128]{1,0:T(8,128)(2,1)S(1)} %get-tuple-element.42), channel_id=1, source_target_pairs={{0,8},{8,16},{16,24},{24,0},{32,40},{40,48},{48,56},{56,32},{64,72... | collective-permute-start | bytes 202760 | tf_op jit(solution)/shard_map/ppermute | solution.py:305
  12.3 2.6 %collective-permute-start.9 = (bf16[264,128]{1,0:T(8,128)(2,1)S(1)}, bf16[264,128]{1,0:T(8,128)(2,1)S(1)}, u32[]{:S(2)}, u32[]{:S(2)}) collective-permute-start(bf16[264,128]{1,0:T(8,128)(2,1)S(1)} %get-tuple-element.43), channel_id=1, source_target_pairs={{0,16},{8,24},{16,0},{24,8},{32,48},{40,56},{48,32},{56,40},{64,80... | collective-permute-start | bytes 202760 | tf_op jit(solution)/shard_map/ppermute | solution.py:305
  14.9 1.1 %collective-permute-start.10 = (bf16[264,128]{1,0:T(8,128)(2,1)S(1)}, bf16[264,128]{1,0:T(8,128)(2,1)S(1)}, u32[]{:S(2)}, u32[]{:S(2)}) collective-permute-start(bf16[264,128]{1,0:T(8,128)(2,1)S(1)} %get-tuple-element.44), channel_id=1, source_target_pairs={{0,24},{8,0},{16,8},{24,16},{32,56},{40,32},{48,40},{56,48},{64,88... | collective-permute-start | bytes 202760 | tf_op jit(solution)/shard_map/ppermute | solution.py:305
  16.0 1.4 %collective-permute-done.9.refs_2_ = bf16[264,128]{1,0:T(8,128)(2,1)S(1)} collective-permute-done((bf16[264,128]{1,0:T(8,128)(2,1)S(1)}, bf16[264,128]{1,0:T(8,128)(2,1)S(1)}, u32[]{:S(2)}, u32[]{:S(2)}) %collective-permute-start.9) | collective-permute-done | bytes 67616 | tf_op jit(solution)/shard_map/ppermute | solution.py:305
  17.4 1.2 %collective-permute-done.10.refs_3_ = bf16[264,128]{1,0:T(8,128)(2,1)S(1)} collective-permute-done((bf16[264,128]{1,0:T(8,128)(2,1)S(1)}, bf16[264,128]{1,0:T(8,128)(2,1)S(1)}, u32[]{:S(2)}, u32[]{:S(2)}) %collective-permute-start.10) | collective-permute-done | bytes 67616 | tf_op jit(solution)/shard_map/ppermute | solution.py:305
  18.6 0.3 collective-permute-start.11
  18.9 0.7 %shard_map.120 = (bf16[264,128]{1,0:T(8,128)(2,1)S(1)}, bf16[264,128]{1,0:T(8,128)(2,1)S(1)}, bf16[264,128]{1,0:T(8,128)(2,1)S(1)}, bf16[264,128]{1,0:T(8,128)(2,1)S(1)}) custom-call(bf16[8,8,16,1024]{3,2,1,0:T(8,128)(2,1)S(1)} %get-tuple-element.32.rest_ref, bf16[1024,256]{1,0:T(8,128)(2,1)S(1)} %get-tuple-element.30.w_ref, ...), custom_call_target="tpu_custom_call" | custom-call | tf_op jit(solution)/shard_map/pallas_call | solution.py:115
  19.6 0.1 collective-permute-start
  19.7 3.3 %collective-permute-start.1 = (bf16[264,128]{1,0:T(8,128)(2,1)S(1)}, bf16[264,128]{1,0:T(8,128)(2,1)S(1)}, u32[]{:S(2)}, u32[]{:S(2)}) collective-permute-start(bf16[264,128]{1,0:T(8,128)(2,1)S(1)} %get-tuple-element.35), channel_id=1, source_target_pairs={{0,16},{8,24},{16,0},{24,8},{32,48},{40,56},{48,32},{56,40},{64,80... | collective-permute-start | bytes 202760 | tf_op jit(solution)/shard_map/ppermute | solution.py:305
  23.1 0.1 collective-permute-start.5
  23.2 1.5 %collective-permute-start.6 = (bf16[2,264,128]{2,1,0:T(8,128)(2,1)S(1)}, bf16[2,264,128]{2,1,0:T(8,128)(2,1)S(1)}, u32[]{:S(2)}, u32[]{:S(2)}) collective-permute-start(bf16[2,264,128]{2,1,0:T(8,128)(2,1)S(1)} %get-tuple-element.39), channel_id=1, source_target_pairs={{0,16},{8,24},{16,0},{24,8},{32,48},{40,56},{48,32},{56,40},{64,80... | collective-permute-start | bytes 405512 | tf_op jit(solution)/shard_map/ppermute | solution.py:305
  24.7 1.2 %collective-permute-start.7 = (bf16[2,264,128]{2,1,0:T(8,128)(2,1)S(1)}, bf16[2,264,128]{2,1,0:T(8,128)(2,1)S(1)}, u32[]{:S(2)}, u32[]{:S(2)}) collective-permute-start(bf16[2,264,128]{2,1,0:T(8,128)(2,1)S(1)} %get-tuple-element.40), channel_id=1, source_target_pairs={{0,24},{8,0},{16,8},{24,16},{32,56},{40,32},{48,40},{56,48},{64,88... | collective-permute-start | bytes 405512 | tf_op jit(solution)/shard_map/ppermute | solution.py:305
  25.9 1.2 %collective-permute-start.2 = (bf16[264,128]{1,0:T(8,128)(2,1)S(1)}, bf16[264,128]{1,0:T(8,128)(2,1)S(1)}, u32[]{:S(2)}, u32[]{:S(2)}) collective-permute-start(bf16[264,128]{1,0:T(8,128)(2,1)S(1)} %get-tuple-element.36), channel_id=1, source_target_pairs={{0,24},{8,0},{16,8},{24,16},{32,56},{40,32},{48,40},{56,48},{64,88... | collective-permute-start | bytes 202760 | tf_op jit(solution)/shard_map/ppermute | solution.py:305
  27.0 4.9 %collective-permute-done.2.refs_3_ = bf16[264,128]{1,0:T(8,128)(2,1)S(1)} collective-permute-done((bf16[264,128]{1,0:T(8,128)(2,1)S(1)}, bf16[264,128]{1,0:T(8,128)(2,1)S(1)}, u32[]{:S(2)}, u32[]{:S(2)}) %collective-permute-start.2) | collective-permute-done | bytes 67616 | tf_op jit(solution)/shard_map/ppermute | solution.py:305
  31.9 0.5 %collective-permute-done.11.refs_9_ = bf16[4,264,128]{2,1,0:T(8,128)(2,1)S(1)} collective-permute-done((bf16[4,264,128]{2,1,0:T(8,128)(2,1)S(1)}, bf16[4,264,128]{2,1,0:T(8,128)(2,1)S(1)}, u32[]{:S(2)}, u32[]{:S(2)}) %collective-permute-start.11) | collective-permute-done | bytes 270368 | tf_op jit(solution)/shard_map/ppermute | solution.py:305
  32.5 1.8 %shard_map.124 = (f32[4,8,128]{2,1,0:T(8,128)S(1)}, f32[4,8,128]{2,1,0:T(8,128)S(1)}, f32[32,128]{1,0:T(8,128)S(1)}, f32[128,32]{1,0:T(8,128)S(1)}, f32[2,1,8]{2,1,0:T(1,128)}) custom-call(bf16[264,128]{1,0:T(8,128)(2,1)S(1)} %get-tuple-element.33.refs_0_, bf16[264,128]{1,0:T(8,128)(2,1)S(1)} %collective-permute-done.refs_1_, ...), custom_call_target="tpu_custom_call" | custom-call | tf_op jit(solution)/shard_map/pallas_call | solution.py:115
  34.3 3.3 %collective-permute-start.12 = (f32[4,8,128]{2,1,0:T(8,128)S(1)}, f32[4,8,128]{2,1,0:T(8,128)S(1)}, u32[]{:S(2)}, u32[]{:S(2)}) collective-permute-start(f32[4,8,128]{2,1,0:T(8,128)S(1)} %get-tuple-element.51), channel_id=1, source_target_pairs={{0,1},{1,0},{2,3},{3,2},{4,5},{5,4},{6,7},{7,6},{8,9},{9,8},{10,11... | collective-permute-start | bytes 49160 | tf_op jit(solution)/shard_map/ppermute | solution.py:310
  37.6 0.8 %collective-permute-done.12.got_ref = f32[4,8,128]{2,1,0:T(8,128)S(1)} collective-permute-done((f32[4,8,128]{2,1,0:T(8,128)S(1)}, f32[4,8,128]{2,1,0:T(8,128)S(1)}, u32[]{:S(2)}, u32[]{:S(2)}) %collective-permute-start.12) | collective-permute-done | bytes 16416 | tf_op jit(solution)/shard_map/ppermute | solution.py:310
  38.4 1.2 %collective-permute-start.13 = (f32[8,128]{1,0:T(8,128)S(1)}, f32[8,128]{1,0:T(8,128)S(1)}, u32[]{:S(2)}, u32[]{:S(2)}) collective-permute-start(f32[8,128]{1,0:T(8,128)S(1)} %get-tuple-element.53), channel_id=1, source_target_pairs={{0,2},{2,4},{4,6},{6,0},{1,3},{3,5},{5,7},{7,1},{8,10},{10,12},{12... | collective-permute-start | bytes 12296 | tf_op jit(solution)/shard_map/ppermute | solution.py:310
  39.7 2.5 %collective-permute-start.14 = (f32[8,128]{1,0:T(8,128)S(1)}, f32[8,128]{1,0:T(8,128)S(1)}, u32[]{:S(2)}, u32[]{:S(2)}) collective-permute-start(f32[8,128]{1,0:T(8,128)S(1)} %get-tuple-element.54), channel_id=1, source_target_pairs={{0,4},{2,6},{4,0},{6,2},{1,5},{3,7},{5,1},{7,3},{8,12},{10,14},{12... | collective-permute-start | bytes 12296 | tf_op jit(solution)/shard_map/ppermute | solution.py:310
  42.1 1.2 %collective-permute-start.15 = (f32[8,128]{1,0:T(8,128)S(1)}, f32[8,128]{1,0:T(8,128)S(1)}, u32[]{:S(2)}, u32[]{:S(2)}) collective-permute-start(f32[8,128]{1,0:T(8,128)S(1)} %get-tuple-element.55), channel_id=1, source_target_pairs={{0,6},{2,0},{4,2},{6,4},{1,7},{3,1},{5,3},{7,5},{8,14},{10,8},{12,... | collective-permute-start | bytes 12296 | tf_op jit(solution)/shard_map/ppermute | solution.py:310
  43.3 1.1 %shard_map.125 = (bf16[16,128,256]{2,1,0:T(8,128)(2,1)S(1)}, f32[16,128]{1,0:T(8,128)}) custom-call(bf16[264,128]{1,0:T(8,128)(2,1)S(1)} %get-tuple-element.33.refs_0_, bf16[264,128]{1,0:T(8,128)(2,1)S(1)} %collective-permute-done.refs_1_, bf16[264,128]{1,0:T(8,128)(2,1)S(1)} %collective-permute-done.1.refs_2_, ...), custom_call_target="tpu_custom_call" | custom-call | tf_op jit(solution)/shard_map/pallas_call | solution.py:115
  44.3 1.2 %shard_map.126 = bf16[2,8,128,128]{3,2,1,0:T(8,128)(2,1)} custom-call(bf16[264,128]{1,0:T(8,128)(2,1)S(1)} %get-tuple-element.33.refs_0_, bf16[264,128]{1,0:T(8,128)(2,1)S(1)} %collective-permute-done.refs_1_, bf16[264,128]{1,0:T(8,128)(2,1)S(1)} %collective-permute-done.1.refs_2_, bf16[264,128]{1,0:T(8,128)(2,1)S(1)} %collective-permute-done.2.refs_3_, ...), custom_call_target="tpu_custom_call" | custom-call | tf_op jit(solution)/shard_map/pallas_call | solution.py:115
  45.5 0.6 %shard_map.128 = bf16[8,128]{1,0:T(8,128)(2,1)} custom-call(f32[8,128]{1,0:T(8,128)S(1)} %get-tuple-element.52.a_ref, f32[8,128]{1,0:T(8,128)S(1)} %collective-permute-done.13.b_ref, f32[8,128]{1,0:T(8,128)S(1)} %collective-permute-done.14.c_ref, f32[8,128]{1,0:T(8,128)S(1)} %collective-permute-done.15.d_ref), custom_call_target="tpu_custom_call" | custom-call | tf_op jit(solution)/shard_map/pallas_call | solution.py:115
  (19 shorter events, 0.1 us)
Async XLA Ops:
  2.8 20.3 %collective-permute-start.3 = (bf16[4,264,128]{2,1,0:T(8,128)(2,1)S(1)}, bf16[4,264,128]{2,1,0:T(8,128)(2,1)S(1)}, u32[]{:S(2)}, u32[]{:S(2)}) collective-permute-start(bf16[4,264,128]{2,1,0:T(8,128)(2,1)S(1)} %get-tuple-element.37), channel_id=1, source_target_pairs={{0,96},{8,104},{16,112},{24,120},{32,64},{40,72},{48,80},{56,88},{... | collective-permute-start | bytes 811016 | tf_op jit(solution)/shard_map/ppermute | solution.py:305
  10.1 22.4 %copy-start = (bf16[1,128,1024]{2,1,0:T(8,128)(2,1)S(1)}, bf16[1,128,1024]{2,1,0:T(8,128)(2,1)}, u32[]{:S(2)}) copy-start(bf16[1,128,1024]{2,1,0:T(8,128)(2,1)} %param.17) | copy-start | bytes 786436
  10.1 22.4 %copy-start.1 = (bf16[8,1,128]{2,0,1:T(8,128)(2,1)S(1)}, bf16[8,1,128]{2,0,1:T(8,128)(2,1)}, u32[]{:S(2)}) copy-start(bf16[8,1,128]{2,0,1:T(8,128)(2,1)} %param.16) | copy-start | bytes 6148
  10.1 22.4 %copy-start.2 = (f32[2,1]{0,1:T(1,128)S(1)}, f32[2,1]{0,1:T(1,128)}, u32[]{:S(2)}) copy-start(f32[2,1]{0,1:T(1,128)} %param.14) | copy-start | bytes 28
  10.1 22.4 %copy-start.3 = (f32[2,1]{0,1:T(1,128)S(1)}, f32[2,1]{0,1:T(1,128)}, u32[]{:S(2)}) copy-start(f32[2,1]{0,1:T(1,128)} %param.15) | copy-start | bytes 28
  10.8 12.3 %collective-permute-start.4 = (bf16[4,264,128]{2,1,0:T(8,128)(2,1)S(1)}, bf16[4,264,128]{2,1,0:T(8,128)(2,1)S(1)}, u32[]{:S(2)}, u32[]{:S(2)}) collective-permute-start(bf16[4,264,128]{2,1,0:T(8,128)(2,1)S(1)} %shard_map.121), channel_id=1, source_target_pairs={{0,32},{8,40},{16,48},{24,56},{32,0},{40,8},{48,16},{56,24},{64,96... | collective-permute-start | bytes 811016 | tf_op jit(solution)/shard_map/ppermute | solution.py:305
  10.9 5.1 %collective-permute-start.8 = (bf16[264,128]{1,0:T(8,128)(2,1)S(1)}, bf16[264,128]{1,0:T(8,128)(2,1)S(1)}, u32[]{:S(2)}, u32[]{:S(2)}) collective-permute-start(bf16[264,128]{1,0:T(8,128)(2,1)S(1)} %get-tuple-element.42), channel_id=1, source_target_pairs={{0,8},{8,16},{16,24},{24,0},{32,40},{40,48},{48,56},{56,32},{64,72... | collective-permute-start | bytes 202760 | tf_op jit(solution)/shard_map/ppermute | solution.py:305
  12.3 5.1 %collective-permute-start.9 = (bf16[264,128]{1,0:T(8,128)(2,1)S(1)}, bf16[264,128]{1,0:T(8,128)(2,1)S(1)}, u32[]{:S(2)}, u32[]{:S(2)}) collective-permute-start(bf16[264,128]{1,0:T(8,128)(2,1)S(1)} %get-tuple-element.43), channel_id=1, source_target_pairs={{0,16},{8,24},{16,0},{24,8},{32,48},{40,56},{48,32},{56,40},{64,80... | collective-permute-start | bytes 202760 | tf_op jit(solution)/shard_map/ppermute | solution.py:305
  14.9 3.7 %collective-permute-start.10 = (bf16[264,128]{1,0:T(8,128)(2,1)S(1)}, bf16[264,128]{1,0:T(8,128)(2,1)S(1)}, u32[]{:S(2)}, u32[]{:S(2)}) collective-permute-start(bf16[264,128]{1,0:T(8,128)(2,1)S(1)} %get-tuple-element.44), channel_id=1, source_target_pairs={{0,24},{8,0},{16,8},{24,16},{32,56},{40,32},{48,40},{56,48},{64,88... | collective-permute-start | bytes 202760 | tf_op jit(solution)/shard_map/ppermute | solution.py:305
  18.6 13.8 %collective-permute-start.11 = (bf16[4,264,128]{2,1,0:T(8,128)(2,1)S(1)}, bf16[4,264,128]{2,1,0:T(8,128)(2,1)S(1)}, u32[]{:S(2)}, u32[]{:S(2)}) collective-permute-start(bf16[4,264,128]{2,1,0:T(8,128)(2,1)S(1)} %shard_map.123), channel_id=1, source_target_pairs={{0,64},{8,72},{16,80},{24,88},{32,96},{40,104},{48,112},{56,120},{... | collective-permute-start | bytes 811016 | tf_op jit(solution)/shard_map/ppermute | solution.py:305
  19.6 5.0 %collective-permute-start = (bf16[264,128]{1,0:T(8,128)(2,1)S(1)}, bf16[264,128]{1,0:T(8,128)(2,1)S(1)}, u32[]{:S(2)}, u32[]{:S(2)}) collective-permute-start(bf16[264,128]{1,0:T(8,128)(2,1)S(1)} %get-tuple-element.34), channel_id=1, source_target_pairs={{0,8},{8,16},{16,24},{24,0},{32,40},{40,48},{48,56},{56,32},{64,72... | collective-permute-start | bytes 202760 | tf_op jit(solution)/shard_map/ppermute | solution.py:305
  19.7 6.1 %collective-permute-start.1 = (bf16[264,128]{1,0:T(8,128)(2,1)S(1)}, bf16[264,128]{1,0:T(8,128)(2,1)S(1)}, u32[]{:S(2)}, u32[]{:S(2)}) collective-permute-start(bf16[264,128]{1,0:T(8,128)(2,1)S(1)} %get-tuple-element.35), channel_id=1, source_target_pairs={{0,16},{8,24},{16,0},{24,8},{32,48},{40,56},{48,32},{56,40},{64,80... | collective-permute-start | bytes 202760 | tf_op jit(solution)/shard_map/ppermute | solution.py:305
  23.1 9.3 %collective-permute-start.5 = (bf16[2,264,128]{2,1,0:T(8,128)(2,1)S(1)}, bf16[2,264,128]{2,1,0:T(8,128)(2,1)S(1)}, u32[]{:S(2)}, u32[]{:S(2)}) collective-permute-start(bf16[2,264,128]{2,1,0:T(8,128)(2,1)S(1)} %get-tuple-element.38), channel_id=1, source_target_pairs={{0,8},{8,16},{16,24},{24,0},{32,40},{40,48},{48,56},{56,32},{64,72... | collective-permute-start | bytes 405512 | tf_op jit(solution)/shard_map/ppermute | solution.py:305
  23.2 9.3 %collective-permute-start.6 = (bf16[2,264,128]{2,1,0:T(8,128)(2,1)S(1)}, bf16[2,264,128]{2,1,0:T(8,128)(2,1)S(1)}, u32[]{:S(2)}, u32[]{:S(2)}) collective-permute-start(bf16[2,264,128]{2,1,0:T(8,128)(2,1)S(1)} %get-tuple-element.39), channel_id=1, source_target_pairs={{0,16},{8,24},{16,0},{24,8},{32,48},{40,56},{48,32},{56,40},{64,80... | collective-permute-start | bytes 405512 | tf_op jit(solution)/shard_map/ppermute | solution.py:305
  24.7 7.8 %collective-permute-start.7 = (bf16[2,264,128]{2,1,0:T(8,128)(2,1)S(1)}, bf16[2,264,128]{2,1,0:T(8,128)(2,1)S(1)}, u32[]{:S(2)}, u32[]{:S(2)}) collective-permute-start(bf16[2,264,128]{2,1,0:T(8,128)(2,1)S(1)} %get-tuple-element.40), channel_id=1, source_target_pairs={{0,24},{8,0},{16,8},{24,16},{32,56},{40,32},{48,40},{56,48},{64,88... | collective-permute-start | bytes 405512 | tf_op jit(solution)/shard_map/ppermute | solution.py:305
  25.9 6.1 %collective-permute-start.2 = (bf16[264,128]{1,0:T(8,128)(2,1)S(1)}, bf16[264,128]{1,0:T(8,128)(2,1)S(1)}, u32[]{:S(2)}, u32[]{:S(2)}) collective-permute-start(bf16[264,128]{1,0:T(8,128)(2,1)S(1)} %get-tuple-element.36), channel_id=1, source_target_pairs={{0,24},{8,0},{16,8},{24,16},{32,56},{40,32},{48,40},{56,48},{64,88... | collective-permute-start | bytes 202760 | tf_op jit(solution)/shard_map/ppermute | solution.py:305
  34.3 4.2 %collective-permute-start.12 = (f32[4,8,128]{2,1,0:T(8,128)S(1)}, f32[4,8,128]{2,1,0:T(8,128)S(1)}, u32[]{:S(2)}, u32[]{:S(2)}) collective-permute-start(f32[4,8,128]{2,1,0:T(8,128)S(1)} %get-tuple-element.51), channel_id=1, source_target_pairs={{0,1},{1,0},{2,3},{3,2},{4,5},{5,4},{6,7},{7,6},{8,9},{9,8},{10,11... | collective-permute-start | bytes 49160 | tf_op jit(solution)/shard_map/ppermute | solution.py:310
  38.4 7.1 %collective-permute-start.13 = (f32[8,128]{1,0:T(8,128)S(1)}, f32[8,128]{1,0:T(8,128)S(1)}, u32[]{:S(2)}, u32[]{:S(2)}) collective-permute-start(f32[8,128]{1,0:T(8,128)S(1)} %get-tuple-element.53), channel_id=1, source_target_pairs={{0,2},{2,4},{4,6},{6,0},{1,3},{3,5},{5,7},{7,1},{8,10},{10,12},{12... | collective-permute-start | bytes 12296 | tf_op jit(solution)/shard_map/ppermute | solution.py:310
  39.7 5.9 %collective-permute-start.14 = (f32[8,128]{1,0:T(8,128)S(1)}, f32[8,128]{1,0:T(8,128)S(1)}, u32[]{:S(2)}, u32[]{:S(2)}) collective-permute-start(f32[8,128]{1,0:T(8,128)S(1)} %get-tuple-element.54), channel_id=1, source_target_pairs={{0,4},{2,6},{4,0},{6,2},{1,5},{3,7},{5,1},{7,3},{8,12},{10,14},{12... | collective-permute-start | bytes 12296 | tf_op jit(solution)/shard_map/ppermute | solution.py:310
  42.1 3.4 %collective-permute-start.15 = (f32[8,128]{1,0:T(8,128)S(1)}, f32[8,128]{1,0:T(8,128)S(1)}, u32[]{:S(2)}, u32[]{:S(2)}) collective-permute-start(f32[8,128]{1,0:T(8,128)S(1)} %get-tuple-element.55), channel_id=1, source_target_pairs={{0,6},{2,0},{4,2},{6,4},{1,7},{3,1},{5,3},{7,5},{8,14},{10,8},{12,... | collective-permute-start | bytes 12296 | tf_op jit(solution)/shard_map/ppermute | solution.py:310

commit v8 on v6

--- a/solution.py
+++ b/solution.py
@@ -83,8 +83,11 @@
 
 
 def third_kernel(rest_ref, w_ref, g_ref, *outs):
-    project_blocks(rest_ref, ROW, w_ref[...], g_ref[...], outs[:ROW])
-    project_blocks(rest_ref, 2 * ROW, w_ref[...], g_ref[...], outs[ROW:])
+    project_blocks(rest_ref, ROW, w_ref[...], g_ref[...], outs)
+
+
+def own_kernel(rest_ref, w_ref, g_ref, *outs):
+    project_blocks(rest_ref, 2 * ROW, w_ref[...], g_ref[...], outs)
 
 
 ANY = pl.BlockSpec(memory_space=pl.ANY)
@@ -137,10 +140,23 @@
         refs[ROW][i] = refs[i][...]
 
 
-def legs_kernel(a_ref, b_ref, *outs):
-    for k, out in enumerate(outs):
-        out[0] = a_ref[k + 1]
-        out[1] = b_ref[k + 1]
+def legs_kernel(inner_ref, outer_ref, twin_ref, mirror0_ref, *outs):
+    z, _ = here()
+    edge = (z == 0) | (z == ROW - 1)
+
+    def fill(mirror_ref):
+        mirror0_ref[...] = mirror_ref[0]
+        for k, out in enumerate(outs):
+            out[0] = mirror_ref[k + 1]
+            out[1] = twin_ref[k + 1]
+
+    @pl.when(edge)
+    def _():
+        fill(outer_ref)
+
+    @pl.when(jnp.logical_not(edge))
+    def _():
+        fill(inner_ref)
 
 
 def three_parts(a):
@@ -163,9 +179,9 @@
 
 def landed(refs):
     own, (mirror, twin, s1, s2, s3, far) = list(refs[:ROW]), refs[ROW:]
-    from_mirror, from_twin = [
-        [kept.at[0]] + [s.at[i] for s in (s1, s2, s3)] for i, kept in enumerate((mirror, twin))
-    ]
+    sides = (s1, s2, s3)
+    from_mirror = [mirror] + [s.at[0] for s in sides]
+    from_twin = [twin.at[0]] + [s.at[1] for s in sides]
     return own + from_twin + [far.at[k] for k in range(ROW)] + from_mirror
 
 
@@ -280,8 +296,8 @@
     out_ref[...] = ((a_ref[...] + b_ref[...]) + (c_ref[...] + d_ref[...])).astype(BF)
 
 
-def shift(array, dz, dy):
-    spots = [(z, y) for z in range(ROW) for y in range(ROW)]
+def shift(array, dz, dy, rows=range(ROW)):
+    spots = [(z, y) for z in rows for y in range(ROW)]
     pairs = [(z * ROW + y, (z ^ dz) * ROW + (y + dy) % ROW) for z, y in spots]
     return lax.ppermute(array, "sp", pairs)
 
@@ -296,15 +312,17 @@
     mirror, w, gates, later = project_near(
         prompt, w_key.reshape(D, HD), w_value.reshape(D, HD), w_in_gate.reshape(2, D), w_forget_gate.reshape(2, D)
     )
-    mirror = shift(mirror, 3, 0)
+    inner = shift(mirror, 3, 0, (1, 2))
+    outer = shift(mirror, 3, 0, (0, 3))
     twin = run(second_kernel, block(ROW), (later, w, gates))
     twin = shift(twin, 1, 0)
-    made = run(third_kernel, (block(),) * (2 * ROW), (later, w, gates))
-    cross = [made[0]] + [shift(made[k], 0, k) for k in hops]
-    own = [made[ROW]] + [shift(made[ROW + k], 0, k) for k in hops]
+    cross = run(third_kernel, (block(),) * ROW, (later, w, gates))
+    cross = [cross[0]] + [shift(cross[k], 0, k) for k in hops]
+    own = run(own_kernel, (block(),) * ROW, (later, w, gates))
+    own = [own[0]] + [shift(own[k], 0, k) for k in hops]
     far = run(gather_kernel, block(ROW), cross, 4)
     far = shift(far, 2, 0)
-    side = run(legs_kernel, (block(2),) * 3, (mirror, twin), 4)
+    mirror, *side = run(legs_kernel, (block(),) + (block(2),) * 3, (inner, outer, twin), 4)
     side = [shift(blocks, 0, k) for k, blocks in zip(hops, side)]
     blocks = (*own, mirror, twin, *side, far)
     half = pltpu.VMEM((TPX, OWN, HD), F32)

time: 48.8 us -> 51.6 us (1.057)
  starting transfers between devices: 26.1 us -> 28.4 us
    ppermute x12 -> x13, starting transfers between devices: 20.5 us -> 22.7 us  [shift(): return lax.ppermute(array, 'sp', pairs)]
    ppermute x12 -> x13, waiting for transfers between devices: 11.5 us -> 11.8 us  [shift(): return lax.ppermute(array, 'sp', pairs)]
    pallas_call x9 -> x10, Pallas kernels: 6.58 us -> 6.74 us  [run(): pl.pallas_call(kernel, in_specs=[VM] * len(args), out_specs=specs, out_sh...]
  transfers between devices with their start and end apart: 16 -> 17, of which waited for: 6 -> 6; matrix products, arithmetic and copies ran while one was open for 0% -> 0% of each run, Pallas kernels for 7% -> 7%
where the time goes in v8:
time: 51.6 us; the launch traced here: 51.4 us
  starting transfers between devices  28.4 us (55%)
  waiting for transfers between devices  13 us (25%)
  Pallas kernels  9.25 us (18%)
  between operations  0.77 us (1%)
    ppermute x13, starting transfers between devices, shift(): return lax.ppermute(array, 'sp', pairs)  22.7 us
    ppermute x13, waiting for transfers between devices, shift(): return lax.ppermute(array, 'sp', pairs)  11.8 us
    pallas_call x10, Pallas kernels, run(): pl.pallas_call(kernel, in_specs=[VM] * len(args), out_specs=specs, out_sh...  6.74 us
    ppermute x4, starting transfers between devices, across(): lax.ppermute(array, axis, [(i, (i + hop) % size) for i in range(size)])  5.66 us
    pallas_call x1, Pallas kernels, project_near(): pl.pallas_call(near_kernel, in_specs=[ANY] * 5, out_specs=[VM] * 4, out_s...  2.5 us
    ppermute x4, waiting for transfers between devices, across(): lax.ppermute(array, axis, [(i, (i + hop) % size) for i in range(size)])  1.19 us
  transfers between devices with their start and end apart: 17, of which 6 were waited for; matrix products, arithmetic and copies ran while one was open for 0% of the time, Pallas kernels for 7%

profile of v8, /device:TPU:64, one launch (start us, length us, event | category | flops | bytes accessed | tf_op | source)
XLA Modules:
  0.0 51.4 jit_solution(1799974109983986263)
XLA Ops:
  0.6 2.5 %near.1 = (bf16[4,264,128]{2,1,0:T(8,128)(2,1)S(1)}, bf16[1024,256]{1,0:T(8,128)(2,1)S(1)}, bf16[8,1024]{1,0:T(8,128)(2,1)S(1)}, bf16[12,8,16,1024]{3,2,1,0:T(8,128)(2,1)S(1)}) custom-call(bf16[128,16,1024]{2,1,0:T(8,128)(2,1)} %x_ref.1, bf16[1024,128]{1,0:T(8,128)(2,1)} %bitcast.22, bf16[1024,128]{1,0:T(8,128)(2,1)} %bitcast.23, bf16[2,1024]{1,0:T(2,128)(2,1)} %bitcast.24, ...), custom_call_target="tpu_custom_call" | custom-call | tf_op jit(solution)/shard_map/near/pallas_call | solution.py:122
  3.1 0.7 %shard_map.121 = bf16[4,264,128]{2,1,0:T(8,128)(2,1)S(1)} custom-call(bf16[12,8,16,1024]{3,2,1,0:T(8,128)(2,1)S(1)} %get-tuple-element.31.rest_ref, bf16[1024,256]{1,0:T(8,128)(2,1)S(1)} %get-tuple-element.32.w_ref, bf16[8,1024]{1,0:T(8,128)(2,1)S(1)} %get-tuple-element.33.g_ref), custom_call_target="tpu_custom_call" | custom-call | tf_op jit(solution)/shard_map/pallas_call | solution.py:111
  3.8 2.0 %collective-permute-start.5 = (bf16[4,264,128]{2,1,0:T(8,128)(2,1)S(1)}, bf16[4,264,128]{2,1,0:T(8,128)(2,1)S(1)}, u32[]{:S(2)}, u32[]{:S(2)}) collective-permute-start(bf16[4,264,128]{2,1,0:T(8,128)(2,1)S(1)} %shard_map.121), channel_id=1, source_target_pairs={{0,32},{8,40},{16,48},{24,56},{32,0},{40,8},{48,16},{56,24},{64,96... | collective-permute-start | bytes 811016 | tf_op jit(solution)/shard_map/ppermute | solution.py:302
  5.9 0.8 %collective-permute-start.4 = (bf16[4,264,128]{2,1,0:T(8,128)(2,1)S(1)}, bf16[4,264,128]{2,1,0:T(8,128)(2,1)S(1)}, u32[]{:S(2)}, u32[]{:S(2)}) collective-permute-start(bf16[4,264,128]{2,1,0:T(8,128)(2,1)S(1)} %get-tuple-element.38), channel_id=1, source_target_pairs={{0,96},{8,104},{16,112},{24,120},{96,0},{104,8},{112,16},{120,24},... | collective-permute-start | bytes 811016 | tf_op jit(solution)/shard_map/ppermute | solution.py:302
  6.7 1.9 %collective-permute-start.3 = (bf16[4,264,128]{2,1,0:T(8,128)(2,1)S(1)}, bf16[4,264,128]{2,1,0:T(8,128)(2,1)S(1)}, u32[]{:S(2)}, u32[]{:S(2)}) collective-permute-start(bf16[4,264,128]{2,1,0:T(8,128)(2,1)S(1)} %get-tuple-element.38), channel_id=1, source_target_pairs={{32,64},{40,72},{48,80},{56,88},{64,32},{72,40},{80,48},{88,56},{3... | collective-permute-start | bytes 811016 | tf_op jit(solution)/shard_map/ppermute | solution.py:302
  8.6 0.7 %shard_map.123 = (bf16[264,128]{1,0:T(8,128)(2,1)S(1)}, bf16[264,128]{1,0:T(8,128)(2,1)S(1)}, bf16[264,128]{1,0:T(8,128)(2,1)S(1)}, bf16[264,128]{1,0:T(8,128)(2,1)S(1)}) custom-call(bf16[12,8,16,1024]{3,2,1,0:T(8,128)(2,1)S(1)} %get-tuple-element.31.rest_ref, bf16[1024,256]{1,0:T(8,128)(2,1)S(1)} %get-tuple-element.32.w_ref, ...), custom_call_target="tpu_custom_call" | custom-call | tf_op jit(solution)/shard_map/pallas_call | solution.py:111
  9.3 1.7 %collective-permute-start.9 = (bf16[264,128]{1,0:T(8,128)(2,1)S(1)}, bf16[264,128]{1,0:T(8,128)(2,1)S(1)}, u32[]{:S(2)}, u32[]{:S(2)}) collective-permute-start(bf16[264,128]{1,0:T(8,128)(2,1)S(1)} %get-tuple-element.44), channel_id=1, source_target_pairs={{0,8},{8,16},{16,24},{24,0},{32,40},{40,48},{48,56},{56,32},{64,72... | collective-permute-start | bytes 202760 | tf_op jit(solution)/shard_map/ppermute | solution.py:302
  11.0 2.9 %collective-permute-start.10 = (bf16[264,128]{1,0:T(8,128)(2,1)S(1)}, bf16[264,128]{1,0:T(8,128)(2,1)S(1)}, u32[]{:S(2)}, u32[]{:S(2)}) collective-permute-start(bf16[264,128]{1,0:T(8,128)(2,1)S(1)} %get-tuple-element.45), channel_id=1, source_target_pairs={{0,16},{8,24},{16,0},{24,8},{32,48},{40,56},{48,32},{56,40},{64,80... | collective-permute-start | bytes 202760 | tf_op jit(solution)/shard_map/ppermute | solution.py:302
  13.9 1.7 %collective-permute-done.9.refs_1_ = bf16[264,128]{1,0:T(8,128)(2,1)S(1)} collective-permute-done((bf16[264,128]{1,0:T(8,128)(2,1)S(1)}, bf16[264,128]{1,0:T(8,128)(2,1)S(1)}, u32[]{:S(2)}, u32[]{:S(2)}) %collective-permute-start.9) | collective-permute-done | bytes 67616 | tf_op jit(solution)/shard_map/ppermute | solution.py:302
  15.6 1.1 %collective-permute-start.11 = (bf16[264,128]{1,0:T(8,128)(2,1)S(1)}, bf16[264,128]{1,0:T(8,128)(2,1)S(1)}, u32[]{:S(2)}, u32[]{:S(2)}) collective-permute-start(bf16[264,128]{1,0:T(8,128)(2,1)S(1)} %get-tuple-element.46), channel_id=1, source_target_pairs={{0,24},{8,0},{16,8},{24,16},{32,56},{40,32},{48,40},{56,48},{64,88... | collective-permute-start | bytes 202760 | tf_op jit(solution)/shard_map/ppermute | solution.py:302
  16.7 0.2 collective-permute-done.10.refs_2_
  16.9 3.0 %collective-permute-done.11.refs_3_ = bf16[264,128]{1,0:T(8,128)(2,1)S(1)} collective-permute-done((bf16[264,128]{1,0:T(8,128)(2,1)S(1)}, bf16[264,128]{1,0:T(8,128)(2,1)S(1)}, u32[]{:S(2)}, u32[]{:S(2)}) %collective-permute-start.11) | collective-permute-done | bytes 67616 | tf_op jit(solution)/shard_map/ppermute | solution.py:302
  19.9 2.5 %collective-permute-start.12 = (bf16[4,264,128]{2,1,0:T(8,128)(2,1)S(1)}, bf16[4,264,128]{2,1,0:T(8,128)(2,1)S(1)}, u32[]{:S(2)}, u32[]{:S(2)}) collective-permute-start(bf16[4,264,128]{2,1,0:T(8,128)(2,1)S(1)} %shard_map.124), channel_id=1, source_target_pairs={{0,64},{8,72},{16,80},{24,88},{32,96},{40,104},{48,112},{56,120},{... | collective-permute-start | bytes 811016 | tf_op jit(solution)/shard_map/ppermute | solution.py:302
  22.5 0.7 %shard_map.120 = (bf16[264,128]{1,0:T(8,128)(2,1)S(1)}, bf16[264,128]{1,0:T(8,128)(2,1)S(1)}, bf16[264,128]{1,0:T(8,128)(2,1)S(1)}, bf16[264,128]{1,0:T(8,128)(2,1)S(1)}) custom-call(bf16[12,8,16,1024]{3,2,1,0:T(8,128)(2,1)S(1)} %get-tuple-element.31.rest_ref, bf16[1024,256]{1,0:T(8,128)(2,1)S(1)} %get-tuple-element.32.w_ref, ...), custom_call_target="tpu_custom_call" | custom-call | tf_op jit(solution)/shard_map/pallas_call | solution.py:111
  23.2 0.1 collective-permute-start
  23.3 0.0 collective-permute-done.5.twin_ref.refs_5_
  23.3 3.7 %collective-permute-start.1 = (bf16[264,128]{1,0:T(8,128)(2,1)S(1)}, bf16[264,128]{1,0:T(8,128)(2,1)S(1)}, u32[]{:S(2)}, u32[]{:S(2)}) collective-permute-start(bf16[264,128]{1,0:T(8,128)(2,1)S(1)} %get-tuple-element.36), channel_id=1, source_target_pairs={{0,16},{8,24},{16,0},{24,8},{32,48},{40,56},{48,32},{56,40},{64,80... | collective-permute-start | bytes 202760 | tf_op jit(solution)/shard_map/ppermute | solution.py:302
  27.0 1.8 %collective-permute-done.3.inner_ref = bf16[4,264,128]{2,1,0:T(8,128)(2,1)S(1)} collective-permute-done((bf16[4,264,128]{2,1,0:T(8,128)(2,1)S(1)}, bf16[4,264,128]{2,1,0:T(8,128)(2,1)S(1)}, u32[]{:S(2)}, u32[]{:S(2)}) %collective-permute-start.3) | collective-permute-done | bytes 270368 | tf_op jit(solution)/shard_map/ppermute | solution.py:302
  28.8 1.7 %collective-permute-start.6 = (bf16[2,264,128]{2,1,0:T(8,128)(2,1)S(1)}, bf16[2,264,128]{2,1,0:T(8,128)(2,1)S(1)}, u32[]{:S(2)}, u32[]{:S(2)}) collective-permute-start(bf16[2,264,128]{2,1,0:T(8,128)(2,1)S(1)} %get-tuple-element.40), channel_id=1, source_target_pairs={{0,8},{8,16},{16,24},{24,0},{32,40},{40,48},{48,56},{56,32},{64,72... | collective-permute-start | bytes 405512 | tf_op jit(solution)/shard_map/ppermute | solution.py:302
  30.5 2.9 %collective-permute-start.7 = (bf16[2,264,128]{2,1,0:T(8,128)(2,1)S(1)}, bf16[2,264,128]{2,1,0:T(8,128)(2,1)S(1)}, u32[]{:S(2)}, u32[]{:S(2)}) collective-permute-start(bf16[2,264,128]{2,1,0:T(8,128)(2,1)S(1)} %get-tuple-element.41), channel_id=1, source_target_pairs={{0,16},{8,24},{16,0},{24,8},{32,48},{40,56},{48,32},{56,40},{64,80... | collective-permute-start | bytes 405512 | tf_op jit(solution)/shard_map/ppermute | solution.py:302
  33.4 0.0 collective-permute-done.refs_1_
  33.4 1.3 %collective-permute-start.8 = (bf16[2,264,128]{2,1,0:T(8,128)(2,1)S(1)}, bf16[2,264,128]{2,1,0:T(8,128)(2,1)S(1)}, u32[]{:S(2)}, u32[]{:S(2)}) collective-permute-start(bf16[2,264,128]{2,1,0:T(8,128)(2,1)S(1)} %get-tuple-element.42), channel_id=1, source_target_pairs={{0,24},{8,0},{16,8},{24,16},{32,56},{40,32},{48,40},{56,48},{64,88... | collective-permute-start | bytes 405512 | tf_op jit(solution)/shard_map/ppermute | solution.py:302
  34.7 0.1 collective-permute-start.2
  34.8 5.1 %collective-permute-done.2.refs_3_ = bf16[264,128]{1,0:T(8,128)(2,1)S(1)} collective-permute-done((bf16[264,128]{1,0:T(8,128)(2,1)S(1)}, bf16[264,128]{1,0:T(8,128)(2,1)S(1)}, u32[]{:S(2)}, u32[]{:S(2)}) %collective-permute-start.2) | collective-permute-done | bytes 67616 | tf_op jit(solution)/shard_map/ppermute | solution.py:302
  40.0 1.8 %shard_map.125 = (f32[4,8,128]{2,1,0:T(8,128)S(1)}, f32[4,8,128]{2,1,0:T(8,128)S(1)}, f32[32,128]{1,0:T(8,128)S(1)}, f32[128,32]{1,0:T(8,128)S(1)}, f32[2,1,8]{2,1,0:T(1,128)}) custom-call(bf16[264,128]{1,0:T(8,128)(2,1)S(1)} %get-tuple-element.34.refs_0_, bf16[264,128]{1,0:T(8,128)(2,1)S(1)} %collective-permute-done.refs_1_, ...), custom_call_target="tpu_custom_call" | custom-call | tf_op jit(solution)/shard_map/pallas_call | solution.py:111
  41.8 1.2 %collective-permute-done.13.got_ref = f32[4,8,128]{2,1,0:T(8,128)S(1)} collective-permute-done((f32[4,8,128]{2,1,0:T(8,128)S(1)}, f32[4,8,128]{2,1,0:T(8,128)S(1)}, u32[]{:S(2)}, u32[]{:S(2)}) %collective-permute-start.13) | collective-permute-done | bytes 16416 | tf_op jit(solution)/shard_map/ppermute | solution.py:307
  42.9 1.5 %collective-permute-start.14 = (f32[8,128]{1,0:T(8,128)S(1)}, f32[8,128]{1,0:T(8,128)S(1)}, u32[]{:S(2)}, u32[]{:S(2)}) collective-permute-start(f32[8,128]{1,0:T(8,128)S(1)} %get-tuple-element.55), channel_id=1, source_target_pairs={{0,2},{2,4},{4,6},{6,0},{1,3},{3,5},{5,7},{7,1},{8,10},{10,12},{12... | collective-permute-start | bytes 12296 | tf_op jit(solution)/shard_map/ppermute | solution.py:307
  44.4 2.7 %collective-permute-start.15 = (f32[8,128]{1,0:T(8,128)S(1)}, f32[8,128]{1,0:T(8,128)S(1)}, u32[]{:S(2)}, u32[]{:S(2)}) collective-permute-start(f32[8,128]{1,0:T(8,128)S(1)} %get-tuple-element.56), channel_id=1, source_target_pairs={{0,4},{2,6},{4,0},{6,2},{1,5},{3,7},{5,1},{7,3},{8,12},{10,14},{12... | collective-permute-start | bytes 12296 | tf_op jit(solution)/shard_map/ppermute | solution.py:307
  47.2 1.4 %collective-permute-start.16 = (f32[8,128]{1,0:T(8,128)S(1)}, f32[8,128]{1,0:T(8,128)S(1)}, u32[]{:S(2)}, u32[]{:S(2)}) collective-permute-start(f32[8,128]{1,0:T(8,128)S(1)} %get-tuple-element.57), channel_id=1, source_target_pairs={{0,6},{2,0},{4,2},{6,4},{1,7},{3,1},{5,3},{7,5},{8,14},{10,8},{12,... | collective-permute-start | bytes 12296 | tf_op jit(solution)/shard_map/ppermute | solution.py:307
  48.6 1.1 %shard_map.126 = (bf16[16,128,256]{2,1,0:T(8,128)(2,1)S(1)}, f32[16,128]{1,0:T(8,128)}) custom-call(bf16[264,128]{1,0:T(8,128)(2,1)S(1)} %get-tuple-element.34.refs_0_, bf16[264,128]{1,0:T(8,128)(2,1)S(1)} %collective-permute-done.refs_1_, bf16[264,128]{1,0:T(8,128)(2,1)S(1)} %collective-permute-done.1.refs_2_, ...), custom_call_target="tpu_custom_call" | custom-call | tf_op jit(solution)/shard_map/pallas_call | solution.py:111
  49.7 1.2 %shard_map.127 = bf16[2,8,128,128]{3,2,1,0:T(8,128)(2,1)} custom-call(bf16[264,128]{1,0:T(8,128)(2,1)S(1)} %get-tuple-element.34.refs_0_, bf16[264,128]{1,0:T(8,128)(2,1)S(1)} %collective-permute-done.refs_1_, bf16[264,128]{1,0:T(8,128)(2,1)S(1)} %collective-permute-done.1.refs_2_, bf16[264,128]{1,0:T(8,128)(2,1)S(1)} %collective-permute-done.2.refs_3_, ...), custom_call_target="tpu_custom_call" | custom-call | tf_op jit(solution)/shard_map/pallas_call | solution.py:111
  50.9 0.6 %shard_map.129 = bf16[8,128]{1,0:T(8,128)(2,1)} custom-call(f32[8,128]{1,0:T(8,128)S(1)} %get-tuple-element.54.a_ref, f32[8,128]{1,0:T(8,128)S(1)} %collective-permute-done.14.b_ref, f32[8,128]{1,0:T(8,128)S(1)} %collective-permute-done.15.c_ref, f32[8,128]{1,0:T(8,128)S(1)} %collective-permute-done.16.d_ref), custom_call_target="tpu_custom_call" | custom-call | tf_op jit(solution)/shard_map/pallas_call | solution.py:111
  (21 shorter events, 0.1 us)
Async XLA Ops:
  3.8 19.4 %collective-permute-start.5 = (bf16[4,264,128]{2,1,0:T(8,128)(2,1)S(1)}, bf16[4,264,128]{2,1,0:T(8,128)(2,1)S(1)}, u32[]{:S(2)}, u32[]{:S(2)}) collective-permute-start(bf16[4,264,128]{2,1,0:T(8,128)(2,1)S(1)} %shard_map.121), channel_id=1, source_target_pairs={{0,32},{8,40},{16,48},{24,56},{32,0},{40,8},{48,16},{56,24},{64,96... | collective-permute-start | bytes 811016 | tf_op jit(solution)/shard_map/ppermute | solution.py:302
  5.8 34.1 %copy-start = (bf16[1,128,1024]{2,1,0:T(8,128)(2,1)S(1)}, bf16[1,128,1024]{2,1,0:T(8,128)(2,1)}, u32[]{:S(2)}) copy-start(bf16[1,128,1024]{2,1,0:T(8,128)(2,1)} %param.17) | copy-start | bytes 786436
  5.8 34.1 %copy-start.1 = (bf16[8,1,128]{2,0,1:T(8,128)(2,1)S(1)}, bf16[8,1,128]{2,0,1:T(8,128)(2,1)}, u32[]{:S(2)}) copy-start(bf16[8,1,128]{2,0,1:T(8,128)(2,1)} %param.16) | copy-start | bytes 6148
  5.8 34.1 %copy-start.2 = (f32[2,1]{0,1:T(1,128)S(1)}, f32[2,1]{0,1:T(1,128)}, u32[]{:S(2)}) copy-start(f32[2,1]{0,1:T(1,128)} %param.14) | copy-start | bytes 28
  5.9 34.1 %copy-start.3 = (f32[2,1]{0,1:T(1,128)S(1)}, f32[2,1]{0,1:T(1,128)}, u32[]{:S(2)}) copy-start(f32[2,1]{0,1:T(1,128)} %param.15) | copy-start | bytes 28
  5.9 21.1 %collective-permute-start.4 = (bf16[4,264,128]{2,1,0:T(8,128)(2,1)S(1)}, bf16[4,264,128]{2,1,0:T(8,128)(2,1)S(1)}, u32[]{:S(2)}, u32[]{:S(2)}) collective-permute-start(bf16[4,264,128]{2,1,0:T(8,128)(2,1)S(1)} %get-tuple-element.38), channel_id=1, source_target_pairs={{0,96},{8,104},{16,112},{24,120},{96,0},{104,8},{112,16},{120,24},... | collective-permute-start | bytes 811016 | tf_op jit(solution)/shard_map/ppermute | solution.py:302
  6.7 22.1 %collective-permute-start.3 = (bf16[4,264,128]{2,1,0:T(8,128)(2,1)S(1)}, bf16[4,264,128]{2,1,0:T(8,128)(2,1)S(1)}, u32[]{:S(2)}, u32[]{:S(2)}) collective-permute-start(bf16[4,264,128]{2,1,0:T(8,128)(2,1)S(1)} %get-tuple-element.38), channel_id=1, source_target_pairs={{32,64},{40,72},{48,80},{56,88},{64,32},{72,40},{80,48},{88,56},{3... | collective-permute-start | bytes 811016 | tf_op jit(solution)/shard_map/ppermute | solution.py:302
  9.3 6.3 %collective-permute-start.9 = (bf16[264,128]{1,0:T(8,128)(2,1)S(1)}, bf16[264,128]{1,0:T(8,128)(2,1)S(1)}, u32[]{:S(2)}, u32[]{:S(2)}) collective-permute-start(bf16[264,128]{1,0:T(8,128)(2,1)S(1)} %get-tuple-element.44), channel_id=1, source_target_pairs={{0,8},{8,16},{16,24},{24,0},{32,40},{40,48},{48,56},{56,32},{64,72... | collective-permute-start | bytes 202760 | tf_op jit(solution)/shard_map/ppermute | solution.py:302
  11.0 5.9 %collective-permute-start.10 = (bf16[264,128]{1,0:T(8,128)(2,1)S(1)}, bf16[264,128]{1,0:T(8,128)(2,1)S(1)}, u32[]{:S(2)}, u32[]{:S(2)}) collective-permute-start(bf16[264,128]{1,0:T(8,128)(2,1)S(1)} %get-tuple-element.45), channel_id=1, source_target_pairs={{0,16},{8,24},{16,0},{24,8},{32,48},{40,56},{48,32},{56,40},{64,80... | collective-permute-start | bytes 202760 | tf_op jit(solution)/shard_map/ppermute | solution.py:302
  15.6 4.3 %collective-permute-start.11 = (bf16[264,128]{1,0:T(8,128)(2,1)S(1)}, bf16[264,128]{1,0:T(8,128)(2,1)S(1)}, u32[]{:S(2)}, u32[]{:S(2)}) collective-permute-start(bf16[264,128]{1,0:T(8,128)(2,1)S(1)} %get-tuple-element.46), channel_id=1, source_target_pairs={{0,24},{8,0},{16,8},{24,16},{32,56},{40,32},{48,40},{56,48},{64,88... | collective-permute-start | bytes 202760 | tf_op jit(solution)/shard_map/ppermute | solution.py:302
  19.9 20.0 %collective-permute-start.12 = (bf16[4,264,128]{2,1,0:T(8,128)(2,1)S(1)}, bf16[4,264,128]{2,1,0:T(8,128)(2,1)S(1)}, u32[]{:S(2)}, u32[]{:S(2)}) collective-permute-start(bf16[4,264,128]{2,1,0:T(8,128)(2,1)S(1)} %shard_map.124), channel_id=1, source_target_pairs={{0,64},{8,72},{16,80},{24,88},{32,96},{40,104},{48,112},{56,120},{... | collective-permute-start | bytes 811016 | tf_op jit(solution)/shard_map/ppermute | solution.py:302
  23.2 10.2 %collective-permute-start = (bf16[264,128]{1,0:T(8,128)(2,1)S(1)}, bf16[264,128]{1,0:T(8,128)(2,1)S(1)}, u32[]{:S(2)}, u32[]{:S(2)}) collective-permute-start(bf16[264,128]{1,0:T(8,128)(2,1)S(1)} %get-tuple-element.35), channel_id=1, source_target_pairs={{0,8},{8,16},{16,24},{24,0},{32,40},{40,48},{48,56},{56,32},{64,72... | collective-permute-start | bytes 202760 | tf_op jit(solution)/shard_map/ppermute | solution.py:302
  23.3 11.5 %collective-permute-start.1 = (bf16[264,128]{1,0:T(8,128)(2,1)S(1)}, bf16[264,128]{1,0:T(8,128)(2,1)S(1)}, u32[]{:S(2)}, u32[]{:S(2)}) collective-permute-start(bf16[264,128]{1,0:T(8,128)(2,1)S(1)} %get-tuple-element.36), channel_id=1, source_target_pairs={{0,16},{8,24},{16,0},{24,8},{32,48},{40,56},{48,32},{56,40},{64,80... | collective-permute-start | bytes 202760 | tf_op jit(solution)/shard_map/ppermute | solution.py:302
  28.8 11.1 %collective-permute-start.6 = (bf16[2,264,128]{2,1,0:T(8,128)(2,1)S(1)}, bf16[2,264,128]{2,1,0:T(8,128)(2,1)S(1)}, u32[]{:S(2)}, u32[]{:S(2)}) collective-permute-start(bf16[2,264,128]{2,1,0:T(8,128)(2,1)S(1)} %get-tuple-element.40), channel_id=1, source_target_pairs={{0,8},{8,16},{16,24},{24,0},{32,40},{40,48},{48,56},{56,32},{64,72... | collective-permute-start | bytes 405512 | tf_op jit(solution)/shard_map/ppermute | solution.py:302
  30.5 9.4 %collective-permute-start.7 = (bf16[2,264,128]{2,1,0:T(8,128)(2,1)S(1)}, bf16[2,264,128]{2,1,0:T(8,128)(2,1)S(1)}, u32[]{:S(2)}, u32[]{:S(2)}) collective-permute-start(bf16[2,264,128]{2,1,0:T(8,128)(2,1)S(1)} %get-tuple-element.41), channel_id=1, source_target_pairs={{0,16},{8,24},{16,0},{24,8},{32,48},{40,56},{48,32},{56,40},{64,80... | collective-permute-start | bytes 405512 | tf_op jit(solution)/shard_map/ppermute | solution.py:302
  33.4 6.5 %collective-permute-start.8 = (bf16[2,264,128]{2,1,0:T(8,128)(2,1)S(1)}, bf16[2,264,128]{2,1,0:T(8,128)(2,1)S(1)}, u32[]{:S(2)}, u32[]{:S(2)}) collective-permute-start(bf16[2,264,128]{2,1,0:T(8,128)(2,1)S(1)} %get-tuple-element.42), channel_id=1, source_target_pairs={{0,24},{8,0},{16,8},{24,16},{32,56},{40,32},{48,40},{56,48},{64,88... | collective-permute-start | bytes 405512 | tf_op jit(solution)/shard_map/ppermute | solution.py:302
  34.7 5.2 %collective-permute-start.2 = (bf16[264,128]{1,0:T(8,128)(2,1)S(1)}, bf16[264,128]{1,0:T(8,128)(2,1)S(1)}, u32[]{:S(2)}, u32[]{:S(2)}) collective-permute-start(bf16[264,128]{1,0:T(8,128)(2,1)S(1)} %get-tuple-element.37), channel_id=1, source_target_pairs={{0,24},{8,0},{16,8},{24,16},{32,56},{40,32},{48,40},{56,48},{64,88... | collective-permute-start | bytes 202760 | tf_op jit(solution)/shard_map/ppermute | solution.py:302
  41.8 1.2 %collective-permute-start.13 = (f32[4,8,128]{2,1,0:T(8,128)S(1)}, f32[4,8,128]{2,1,0:T(8,128)S(1)}, u32[]{:S(2)}, u32[]{:S(2)}) collective-permute-start(f32[4,8,128]{2,1,0:T(8,128)S(1)} %get-tuple-element.53), channel_id=1, source_target_pairs={{0,1},{1,0},{2,3},{3,2},{4,5},{5,4},{6,7},{7,6},{8,9},{9,8},{10,11... | collective-permute-start | bytes 49160 | tf_op jit(solution)/shard_map/ppermute | solution.py:307
  42.9 7.9 %collective-permute-start.14 = (f32[8,128]{1,0:T(8,128)S(1)}, f32[8,128]{1,0:T(8,128)S(1)}, u32[]{:S(2)}, u32[]{:S(2)}) collective-permute-start(f32[8,128]{1,0:T(8,128)S(1)} %get-tuple-element.55), channel_id=1, source_target_pairs={{0,2},{2,4},{4,6},{6,0},{1,3},{3,5},{5,7},{7,1},{8,10},{10,12},{12... | collective-permute-start | bytes 12296 | tf_op jit(solution)/shard_map/ppermute | solution.py:307
  44.4 6.4 %collective-permute-start.15 = (f32[8,128]{1,0:T(8,128)S(1)}, f32[8,128]{1,0:T(8,128)S(1)}, u32[]{:S(2)}, u32[]{:S(2)}) collective-permute-start(f32[8,128]{1,0:T(8,128)S(1)} %get-tuple-element.56), channel_id=1, source_target_pairs={{0,4},{2,6},{4,0},{6,2},{1,5},{3,7},{5,1},{7,3},{8,12},{10,14},{12... | collective-permute-start | bytes 12296 | tf_op jit(solution)/shard_map/ppermute | solution.py:307
  47.2 3.7 %collective-permute-start.16 = (f32[8,128]{1,0:T(8,128)S(1)}, f32[8,128]{1,0:T(8,128)S(1)}, u32[]{:S(2)}, u32[]{:S(2)}) collective-permute-start(f32[8,128]{1,0:T(8,128)S(1)} %get-tuple-element.57), channel_id=1, source_target_pairs={{0,6},{2,0},{4,2},{6,4},{1,7},{3,1},{5,3},{7,5},{8,14},{10,8},{12,... | collective-permute-start | bytes 12296 | tf_op jit(solution)/shard_map/ppermute | solution.py:307

commit v9 on v6

--- a/solution.py
+++ b/solution.py
@@ -64,7 +64,7 @@
     for copy in (*gate_copies, key_copy, value_copy):
         copy.start()
     copies = take(x_ref, buf_ref, sem_ref, 0, [(3, dy) for dy in range(ROW)])
-    later = take(x_ref, rest_ref, sem_ref, ROW, [(dz, dy) for dz in (1, 2, 0) for dy in range(ROW)])
+    later = take(x_ref, rest_ref, sem_ref, ROW, [(dz, dy) for dz in (2, 1, 0) for dy in range(ROW)])
     for copy in gate_copies:
         copy.wait()
     gates = jnp.concatenate((wi_buf[...].astype(F32), wf_buf[...].astype(F32), jnp.zeros((4, D), F32)), axis=0)
@@ -78,13 +78,17 @@
         copy.wait()
 
 
-def second_kernel(rest_ref, w_ref, g_ref, twin_ref):
-    project_blocks(rest_ref, 0, w_ref[...], g_ref[...], [twin_ref.at[k] for k in range(ROW)])
-
-
 def third_kernel(rest_ref, w_ref, g_ref, *outs):
-    project_blocks(rest_ref, ROW, w_ref[...], g_ref[...], outs[:ROW])
-    project_blocks(rest_ref, 2 * ROW, w_ref[...], g_ref[...], outs[ROW:])
+    project_blocks(rest_ref, 0, w_ref[...], g_ref[...], outs)
+
+
+def twin_kernel(rest_ref, w_ref, g_ref, twin_ref):
+    project_blocks(rest_ref, ROW, w_ref[...], g_ref[...], [twin_ref.at[k] for k in range(ROW)])
+
+
+def own_kernel(rest_ref, w_ref, g_ref, *refs):
+    project_blocks(rest_ref, 2 * ROW, w_ref[...], g_ref[...], refs[:ROW])
+    fill_masks(*refs[ROW:])
 
 
 ANY = pl.BlockSpec(memory_space=pl.ANY)
@@ -143,56 +147,7 @@
         out[1] = b_ref[k + 1]
 
 
-def three_parts(a):
-    first = a.astype(BF)
-    rest = a - first.astype(F32)
-    second = rest.astype(BF)
-    return first, second, (rest - second.astype(F32)).astype(BF)
-
-
-def group_max(a, lane):
-    for k in (1, 2, 4, 8):
-        inside = (lane % POS) + k < POS
-        a = jnp.maximum(a, jnp.where(inside, pltpu.roll(a, HD - k, 1), pltpu.roll(a, POS - k, 1)))
-    return a
-
-
-def log_sigmoid(a):
-    return jnp.minimum(a, 0.0) - jnp.log1p(jnp.exp(-jnp.abs(a)))
-
-
-def landed(refs):
-    own, (mirror, twin, s1, s2, s3, far) = list(refs[:ROW]), refs[ROW:]
-    from_mirror, from_twin = [
-        [kept.at[0]] + [s.at[i] for s in (s1, s2, s3)] for i, kept in enumerate((mirror, twin))
-    ]
-    return own + from_twin + [far.at[k] for k in range(ROW)] + from_mirror
-
-
-def rows_mine():
-    row = lax.broadcasted_iota(jnp.int32, (OWN, HD), 0)
-    lane = lax.broadcasted_iota(jnp.int32, (OWN, HD), 1)
-    return row, lane, (lane // POS) == row
-
-
-def two_parts(a):
-    high = a.astype(BF)
-    return jnp.concatenate((high, (a - high.astype(F32)).astype(BF)), axis=0)
-
-
-def read_kernel(*refs):
-    blocks = landed(refs[:10])
-    q_ref, wo_ref, ib_ref, fb_ref, keep_ref, send_ref, weight_ref, turned_ref, stab_ref = refs[10:]
-    scale = HD ** -0.5
-    row, lane8, mine = rows_mine()
-    query = q_ref[...]
-    scores = [jnp.where(mine, dot(query, blk[:ROWS, :], ((1,), (1,))), 0.0) for blk in blocks]
-
-    gates = jnp.stack([blk[2 * ROWS :, :].astype(F32) for blk in blocks])
-    part = lambda c: gates[:, c, :] + gates[:, c + 4, :]
-    in_pre = [part(g) + ib_ref[0:1, g : g + 1] for g in range(2)]
-    forget = [log_sigmoid(part(2 + g) + fb_ref[0:1, g : g + 1]) for g in range(2)]
-
+def fill_masks(inside_ref, across_ref):
     z, y = here()
     place = lambda j: (z ^ (j // ROW)) * ROW + ((y - j % ROW) & 3)
     r = lax.broadcasted_iota(jnp.int32, (HD, HD), 0)
@@ -201,16 +156,69 @@
     ones = lambda m: jnp.where(m, 1.0, 0.0).astype(BF)
     jr = lax.broadcasted_iota(jnp.int32, (2 * SP, SP), 0)
     jc = lax.broadcasted_iota(jnp.int32, (2 * SP, SP), 1)
+    for g in range(2):
+        inside_ref[g, :, :HD] = ones(same & ((r > c) if g == 0 else (r < c)))
+        inside_ref[g, :, HD:] = ones(same)
+        across_ref[g] = ones(((place(jc) > place(jr)) if g == 0 else (place(jc) < place(jr))) | (jr >= SP))
+
+
+def three_parts(a):
+    first = a.astype(BF)
+    rest = a - first.astype(F32)
+    second = rest.astype(BF)
+    return first, second, (rest - second.astype(F32)).astype(BF)
+
+
+def group_max(a, lane):
+    for k in (1, 2, 4, 8):
+        inside = (lane % POS) + k < POS
+        a = jnp.maximum(a, jnp.where(inside, pltpu.roll(a, HD - k, 1), pltpu.roll(a, POS - k, 1)))
+    return a
+
+
+def log_sigmoid(a):
+    return jnp.minimum(a, 0.0) - jnp.log1p(jnp.exp(-jnp.abs(a)))
+
+
+def landed(refs):
+    own, (mirror, twin, s1, s2, s3, far) = list(refs[:ROW]), refs[ROW:]
+    from_mirror, from_twin = [
+        [kept.at[0]] + [s.at[i] for s in (s1, s2, s3)] for i, kept in enumerate((mirror, twin))
+    ]
+    return own + from_twin + [far.at[k] for k in range(ROW)] + from_mirror
+
+
+def rows_mine():
+    row = lax.broadcasted_iota(jnp.int32, (OWN, HD), 0)
+    lane = lax.broadcasted_iota(jnp.int32, (OWN, HD), 1)
+    return row, lane, (lane // POS) == row
+
+
+def two_parts(a):
+    high = a.astype(BF)
+    return jnp.concatenate((high, (a - high.astype(F32)).astype(BF)), axis=0)
+
+
+def read_kernel(*refs):
+    blocks = landed(refs[:10])
+    q_ref, wo_ref, ib_ref, fb_ref, inside_ref, across_ref, keep_ref, send_ref, weight_ref, turned_ref, stab_ref = refs[10:]
+    scale = HD ** -0.5
+    row, lane8, mine = rows_mine()
+    query = q_ref[...]
+    scores = [jnp.where(mine, dot(query, blk[:ROWS, :], ((1,), (1,))), 0.0) for blk in blocks]
+
+    gates = jnp.stack([blk[2 * ROWS :, :].astype(F32) for blk in blocks])
+    part = lambda c: gates[:, c, :] + gates[:, c + 4, :]
+    in_pre = [part(g) + ib_ref[0:1, g : g + 1] for g in range(2)]
+    forget = [log_sigmoid(part(2 + g) + fb_ref[0:1, g : g + 1]) for g in range(2)]
+
     lane = lax.broadcasted_iota(jnp.int32, (1, HD), 1)
     log_weight = []
     total = []
     for g in range(2):
-        order = (r > c) if g == 0 else (r < c)
-        inside = jnp.concatenate((ones(same & order), ones(same)), axis=1)
-        sums = sum(dot(p, inside) for p in three_parts(forget[g]))
+        sums = sum(dot(p, inside_ref[g]) for p in three_parts(forget[g]))
         block = sums[:, HD:]
-        across = ones(((place(jc) > place(jr)) if g == 0 else (place(jc) < place(jr))) | (jr >= SP))
-        outside = sum(dot(across, p) for p in three_parts(block))
+        outside = sum(dot(across_ref[g], p) for p in three_parts(block))
         log_weight.append(in_pre[g] + sums[:, :HD] + outside[:SP])
         total.append(outside[SP : SP + 1])
     stab = [
@@ -297,13 +305,16 @@
         prompt, w_key.reshape(D, HD), w_value.reshape(D, HD), w_in_gate.reshape(2, D), w_forget_gate.reshape(2, D)
     )
     mirror = shift(mirror, 3, 0)
-    twin = run(second_kernel, block(ROW), (later, w, gates))
+    cross = run(third_kernel, (block(),) * ROW, (later, w, gates))
+    cross = [cross[0]] + [shift(cross[k], 0, k) for k in hops]
+    twin = run(twin_kernel, block(ROW), (later, w, gates))
     twin = shift(twin, 1, 0)
-    made = run(third_kernel, (block(),) * (2 * ROW), (later, w, gates))
-    cross = [made[0]] + [shift(made[k], 0, k) for k in hops]
-    own = [made[ROW]] + [shift(made[ROW + k], 0, k) for k in hops]
     far = run(gather_kernel, block(ROW), cross, 4)
     far = shift(far, 2, 0)
+    masks = (pltpu.VMEM((2, HD, 2 * HD), BF), pltpu.VMEM((2, 2 * SP, SP), BF))
+    *own, inside, outside = run(own_kernel, (block(),) * ROW + masks, (later, w, gates))
+    masks = (inside, outside)
+    own = [own[0]] + [shift(own[k], 0, k) for k in hops]
     side = run(legs_kernel, (block(2),) * 3, (mirror, twin), 4)
     side = [shift(blocks, 0, k) for k, blocks in zip(hops, side)]
     blocks = (*own, mirror, twin, *side, far)
@@ -312,7 +323,8 @@
         read_kernel,
         (half, half, pltpu.VMEM((2 * SP, HD), F32), pltpu.VMEM((HD, 2 * SP), F32),
          jax.ShapeDtypeStruct((2, 1, OWN), F32)),
-        (*blocks, query.reshape(OWN, HD), w_out.reshape(HD, D), in_bias.reshape(1, 2), forget_bias.reshape(1, 2)),
+        (*blocks, query.reshape(OWN, HD), w_out.reshape(HD, D), in_bias.reshape(1, 2), forget_bias.reshape(1, 2),
+         *masks),
     )
     got = across(send, "tp_1", 1)
     values, norm = run(

time: 48.8 us -> 49 us (level)
    pallas_call x9 -> x10, Pallas kernels: 6.58 us -> 6.92 us  [run(): pl.pallas_call(kernel, in_specs=[VM] * len(args), out_specs=specs, out_sh...]
  transfers between devices with their start and end apart: 16 -> 16, of which waited for: 6 -> 6; matrix products, arithmetic and copies ran while one was open for 0% -> 0% of each run, Pallas kernels for 7% -> 8%
where the time goes in v9:
time: 49 us; the launch traced here: 48.9 us
  starting transfers between devices  26.3 us (54%)
  waiting for transfers between devices  12.5 us (26%)
  Pallas kernels  9.42 us (19%)
  between operations  0.74 us (2%)
    ppermute x12, starting transfers between devices, shift(): return lax.ppermute(array, 'sp', pairs)  20.6 us
    ppermute x12, waiting for transfers between devices, shift(): return lax.ppermute(array, 'sp', pairs)  11.3 us
    pallas_call x10, Pallas kernels, run(): pl.pallas_call(kernel, in_specs=[VM] * len(args), out_specs=specs, out_sh...  6.92 us
    ppermute x4, starting transfers between devices, across(): lax.ppermute(array, axis, [(i, (i + hop) % size) for i in range(size)])  5.66 us
    pallas_call x1, Pallas kernels, project_near(): pl.pallas_call(near_kernel, in_specs=[ANY] * 5, out_specs=[VM] * 4, out_s...  2.5 us
    ppermute x4, waiting for transfers between devices, across(): lax.ppermute(array, axis, [(i, (i + hop) % size) for i in range(size)])  1.19 us
  transfers between devices with their start and end apart: 16, of which 6 were waited for; matrix products, arithmetic and copies ran while one was open for 0% of the time, Pallas kernels for 8%

profile of v9, /device:TPU:64, one launch (start us, length us, event | category | flops | bytes accessed | tf_op | source)
XLA Modules:
  0.0 48.9 jit_solution(3197919935688005557)
XLA Ops:
  0.6 2.5 %near.1 = (bf16[4,264,128]{2,1,0:T(8,128)(2,1)S(1)}, bf16[1024,256]{1,0:T(8,128)(2,1)S(1)}, bf16[8,1024]{1,0:T(8,128)(2,1)S(1)}, bf16[12,8,16,1024]{3,2,1,0:T(8,128)(2,1)S(1)}) custom-call(bf16[128,16,1024]{2,1,0:T(8,128)(2,1)} %x_ref.1, bf16[1024,128]{1,0:T(8,128)(2,1)} %bitcast.22, bf16[1024,128]{1,0:T(8,128)(2,1)} %bitcast.23, bf16[2,1024]{1,0:T(2,128)(2,1)} %bitcast.24, ...), custom_call_target="tpu_custom_call" | custom-call | tf_op jit(solution)/shard_map/near/pallas_call | solution.py:123
  3.1 0.7 %shard_map.121 = bf16[4,264,128]{2,1,0:T(8,128)(2,1)S(1)} custom-call(bf16[12,8,16,1024]{3,2,1,0:T(8,128)(2,1)S(1)} %get-tuple-element.32.rest_ref, bf16[1024,256]{1,0:T(8,128)(2,1)S(1)} %get-tuple-element.33.w_ref, bf16[8,1024]{1,0:T(8,128)(2,1)S(1)} %get-tuple-element.34.g_ref), custom_call_target="tpu_custom_call" | custom-call | tf_op jit(solution)/shard_map/pallas_call | solution.py:112
  3.8 2.0 %collective-permute-start.4 = (bf16[4,264,128]{2,1,0:T(8,128)(2,1)S(1)}, bf16[4,264,128]{2,1,0:T(8,128)(2,1)S(1)}, u32[]{:S(2)}, u32[]{:S(2)}) collective-permute-start(bf16[4,264,128]{2,1,0:T(8,128)(2,1)S(1)} %shard_map.121), channel_id=1, source_target_pairs={{0,32},{8,40},{16,48},{24,56},{32,0},{40,8},{48,16},{56,24},{64,96... | collective-permute-start | bytes 811016 | tf_op jit(solution)/shard_map/ppermute | solution.py:294
  5.9 0.1 collective-permute-start.3
  6.0 0.7 %shard_map.123 = (bf16[264,128]{1,0:T(8,128)(2,1)S(1)}, bf16[264,128]{1,0:T(8,128)(2,1)S(1)}, bf16[264,128]{1,0:T(8,128)(2,1)S(1)}, bf16[264,128]{1,0:T(8,128)(2,1)S(1)}) custom-call(bf16[12,8,16,1024]{3,2,1,0:T(8,128)(2,1)S(1)} %get-tuple-element.32.rest_ref, bf16[1024,256]{1,0:T(8,128)(2,1)S(1)} %get-tuple-element.33.w_ref, ...), custom_call_target="tpu_custom_call" | custom-call | tf_op jit(solution)/shard_map/pallas_call | solution.py:112
  6.7 1.7 %collective-permute-start.8 = (bf16[264,128]{1,0:T(8,128)(2,1)S(1)}, bf16[264,128]{1,0:T(8,128)(2,1)S(1)}, u32[]{:S(2)}, u32[]{:S(2)}) collective-permute-start(bf16[264,128]{1,0:T(8,128)(2,1)S(1)} %get-tuple-element.44), channel_id=1, source_target_pairs={{0,8},{8,16},{16,24},{24,0},{32,40},{40,48},{48,56},{56,32},{64,72... | collective-permute-start | bytes 202760 | tf_op jit(solution)/shard_map/ppermute | solution.py:294
  8.3 2.9 %collective-permute-start.9 = (bf16[264,128]{1,0:T(8,128)(2,1)S(1)}, bf16[264,128]{1,0:T(8,128)(2,1)S(1)}, u32[]{:S(2)}, u32[]{:S(2)}) collective-permute-start(bf16[264,128]{1,0:T(8,128)(2,1)S(1)} %get-tuple-element.45), channel_id=1, source_target_pairs={{0,16},{8,24},{16,0},{24,8},{32,48},{40,56},{48,32},{56,40},{64,80... | collective-permute-start | bytes 202760 | tf_op jit(solution)/shard_map/ppermute | solution.py:294
  11.2 1.3 %collective-permute-start.10 = (bf16[264,128]{1,0:T(8,128)(2,1)S(1)}, bf16[264,128]{1,0:T(8,128)(2,1)S(1)}, u32[]{:S(2)}, u32[]{:S(2)}) collective-permute-start(bf16[264,128]{1,0:T(8,128)(2,1)S(1)} %get-tuple-element.46), channel_id=1, source_target_pairs={{0,24},{8,0},{16,8},{24,16},{32,56},{40,32},{48,40},{56,48},{64,88... | collective-permute-start | bytes 202760 | tf_op jit(solution)/shard_map/ppermute | solution.py:294
  12.6 0.4 collective-permute-done.8.refs_1_
  13.0 1.3 %collective-permute-done.9.refs_2_ = bf16[264,128]{1,0:T(8,128)(2,1)S(1)} collective-permute-done((bf16[264,128]{1,0:T(8,128)(2,1)S(1)}, bf16[264,128]{1,0:T(8,128)(2,1)S(1)}, u32[]{:S(2)}, u32[]{:S(2)}) %collective-permute-start.9) | collective-permute-done | bytes 67616 | tf_op jit(solution)/shard_map/ppermute | solution.py:294
  14.2 1.3 %collective-permute-done.10.refs_3_ = bf16[264,128]{1,0:T(8,128)(2,1)S(1)} collective-permute-done((bf16[264,128]{1,0:T(8,128)(2,1)S(1)}, bf16[264,128]{1,0:T(8,128)(2,1)S(1)}, u32[]{:S(2)}, u32[]{:S(2)}) %collective-permute-start.10) | collective-permute-done | bytes 67616 | tf_op jit(solution)/shard_map/ppermute | solution.py:294
  15.5 2.5 %collective-permute-start.11 = (bf16[4,264,128]{2,1,0:T(8,128)(2,1)S(1)}, bf16[4,264,128]{2,1,0:T(8,128)(2,1)S(1)}, u32[]{:S(2)}, u32[]{:S(2)}) collective-permute-start(bf16[4,264,128]{2,1,0:T(8,128)(2,1)S(1)} %shard_map.124), channel_id=1, source_target_pairs={{0,64},{8,72},{16,80},{24,88},{32,96},{40,104},{48,112},{56,120},{... | collective-permute-start | bytes 811016 | tf_op jit(solution)/shard_map/ppermute | solution.py:294
  18.1 0.7 %shard_map.120 = (bf16[264,128]{1,0:T(8,128)(2,1)S(1)}, bf16[264,128]{1,0:T(8,128)(2,1)S(1)}, bf16[264,128]{1,0:T(8,128)(2,1)S(1)}, bf16[264,128]{1,0:T(8,128)(2...) custom-call(bf16[12,8,16,1024]{3,2,1,0:T(8,128)(2,1)S(1)} %get-tuple-element.32.rest_ref, ...), custom_call_target="tpu_custom_call" | custom-call | tf_op jit(solution)/shard_map/pallas_call | solution.py:112
  18.8 0.4 collective-permute-start
  19.2 3.7 %collective-permute-start.1 = (bf16[264,128]{1,0:T(8,128)(2,1)S(1)}, bf16[264,128]{1,0:T(8,128)(2,1)S(1)}, u32[]{:S(2)}, u32[]{:S(2)}) collective-permute-start(bf16[264,128]{1,0:T(8,128)(2,1)S(1)} %get-tuple-element.37), channel_id=1, source_target_pairs={{0,16},{8,24},{16,0},{24,8},{32,48},{40,56},{48,32},{56,40},{64,80... | collective-permute-start | bytes 202760 | tf_op jit(solution)/shard_map/ppermute | solution.py:294
  22.9 4.0 %collective-permute-done.3.a_ref.refs_4_ = bf16[4,264,128]{2,1,0:T(8,128)(2,1)S(1)} collective-permute-done((bf16[4,264,128]{2,1,0:T(8,128)(2,1)S(1)}, bf16[4,264,128]{2,1,0:T(8,128)(2,1)S(1)}, u32[]{:S(2)}, u32[]{:S(2)}) %collective-permute-start.3) | collective-permute-done | bytes 270368 | tf_op jit(solution)/shard_map/ppermute | solution.py:294
  26.9 1.7 %collective-permute-start.5 = (bf16[2,264,128]{2,1,0:T(8,128)(2,1)S(1)}, bf16[2,264,128]{2,1,0:T(8,128)(2,1)S(1)}, u32[]{:S(2)}, u32[]{:S(2)}) collective-permute-start(bf16[2,264,128]{2,1,0:T(8,128)(2,1)S(1)} %get-tuple-element.40), channel_id=1, source_target_pairs={{0,8},{8,16},{16,24},{24,0},{32,40},{40,48},{48,56},{56,32},{64,72... | collective-permute-start | bytes 405512 | tf_op jit(solution)/shard_map/ppermute | solution.py:294
  28.6 2.9 %collective-permute-start.6 = (bf16[2,264,128]{2,1,0:T(8,128)(2,1)S(1)}, bf16[2,264,128]{2,1,0:T(8,128)(2,1)S(1)}, u32[]{:S(2)}, u32[]{:S(2)}) collective-permute-start(bf16[2,264,128]{2,1,0:T(8,128)(2,1)S(1)} %get-tuple-element.41), channel_id=1, source_target_pairs={{0,16},{8,24},{16,0},{24,8},{32,48},{40,56},{48,32},{56,40},{64,80... | collective-permute-start | bytes 405512 | tf_op jit(solution)/shard_map/ppermute | solution.py:294
  31.5 0.0 collective-permute-done.refs_1_
  31.5 1.3 %collective-permute-start.7 = (bf16[2,264,128]{2,1,0:T(8,128)(2,1)S(1)}, bf16[2,264,128]{2,1,0:T(8,128)(2,1)S(1)}, u32[]{:S(2)}, u32[]{:S(2)}) collective-permute-start(bf16[2,264,128]{2,1,0:T(8,128)(2,1)S(1)} %get-tuple-element.42), channel_id=1, source_target_pairs={{0,24},{8,0},{16,8},{24,16},{32,56},{40,32},{48,40},{56,48},{64,88... | collective-permute-start | bytes 405512 | tf_op jit(solution)/shard_map/ppermute | solution.py:294
  32.8 0.1 collective-permute-start.2
  32.9 4.3 %collective-permute-done.2.refs_3_ = bf16[264,128]{1,0:T(8,128)(2,1)S(1)} collective-permute-done((bf16[264,128]{1,0:T(8,128)(2,1)S(1)}, bf16[264,128]{1,0:T(8,128)(2,1)S(1)}, u32[]{:S(2)}, u32[]{:S(2)}) %collective-permute-start.2) | collective-permute-done | bytes 67616 | tf_op jit(solution)/shard_map/ppermute | solution.py:294
  37.2 0.0 collective-permute-done.11.refs_9_
  37.2 0.0 collective-permute-done.5.refs_6_
  37.3 2.0 %shard_map.125 = (f32[4,8,128]{2,1,0:T(8,128)S(1)}, f32[4,8,128]{2,1,0:T(8,128)S(1)}, f32[32,128]{1,0:T(8,128)S(1)}, f32[128,32]{1,0:T(8,128)S(1)}, f32[2,1,8]{2,1,0:T(1,128)}) custom-call(bf16[264,128]{1,0:T(8,128)(2,1)S(1)} %get-tuple-element.35.refs_0_, bf16[264,128]{1,0:T(8,128)(2,1)S(1)} %collective-permute-done.refs_1_, ...), custom_call_target="tpu_custom_call" | custom-call | tf_op jit(solution)/shard_map/pallas_call | solution.py:112
  39.2 1.2 %collective-permute-done.12.got_ref = f32[4,8,128]{2,1,0:T(8,128)S(1)} collective-permute-done((f32[4,8,128]{2,1,0:T(8,128)S(1)}, f32[4,8,128]{2,1,0:T(8,128)S(1)}, u32[]{:S(2)}, u32[]{:S(2)}) %collective-permute-start.12) | collective-permute-done | bytes 16416 | tf_op jit(solution)/shard_map/ppermute | solution.py:299
  40.4 1.5 %collective-permute-start.13 = (f32[8,128]{1,0:T(8,128)S(1)}, f32[8,128]{1,0:T(8,128)S(1)}, u32[]{:S(2)}, u32[]{:S(2)}) collective-permute-start(f32[8,128]{1,0:T(8,128)S(1)} %get-tuple-element.57), channel_id=1, source_target_pairs={{0,2},{2,4},{4,6},{6,0},{1,3},{3,5},{5,7},{7,1},{8,10},{10,12},{12... | collective-permute-start | bytes 12296 | tf_op jit(solution)/shard_map/ppermute | solution.py:299
  41.9 2.7 %collective-permute-start.14 = (f32[8,128]{1,0:T(8,128)S(1)}, f32[8,128]{1,0:T(8,128)S(1)}, u32[]{:S(2)}, u32[]{:S(2)}) collective-permute-start(f32[8,128]{1,0:T(8,128)S(1)} %get-tuple-element.58), channel_id=1, source_target_pairs={{0,4},{2,6},{4,0},{6,2},{1,5},{3,7},{5,1},{7,3},{8,12},{10,14},{12... | collective-permute-start | bytes 12296 | tf_op jit(solution)/shard_map/ppermute | solution.py:299
  44.6 1.4 %collective-permute-start.15 = (f32[8,128]{1,0:T(8,128)S(1)}, f32[8,128]{1,0:T(8,128)S(1)}, u32[]{:S(2)}, u32[]{:S(2)}) collective-permute-start(f32[8,128]{1,0:T(8,128)S(1)} %get-tuple-element.59), channel_id=1, source_target_pairs={{0,6},{2,0},{4,2},{6,4},{1,7},{3,1},{5,3},{7,5},{8,14},{10,8},{12,... | collective-permute-start | bytes 12296 | tf_op jit(solution)/shard_map/ppermute | solution.py:299
  46.1 1.1 %shard_map.126 = (bf16[16,128,256]{2,1,0:T(8,128)(2,1)S(1)}, f32[16,128]{1,0:T(8,128)}) custom-call(bf16[264,128]{1,0:T(8,128)(2,1)S(1)} %get-tuple-element.35.refs_0_, bf16[264,128]{1,0:T(8,128)(2,1)S(1)} %collective-permute-done.refs_1_, bf16[264,128]{1,0:T(8,128)(2,1)S(1)} %collective-permute-done.1.refs_2_, ...), custom_call_target="tpu_custom_call" | custom-call | tf_op jit(solution)/shard_map/pallas_call | solution.py:112
  47.2 1.2 %shard_map.127 = bf16[2,8,128,128]{3,2,1,0:T(8,128)(2,1)} custom-call(bf16[264,128]{1,0:T(8,128)(2,1)S(1)} %get-tuple-element.35.refs_0_, bf16[264,128]{1,0:T(8,128)(2,1)S(1)} %collective-permute-done.refs_1_, bf16[264,128]{1,0:T(8,128)(2,1)S(1)} %collective-permute-done.1.refs_2_, bf16[264,128]{1,0:T(8,128)(2,1)S(1)} %collective-permute-done.2.refs_3_, ...), custom_call_target="tpu_custom_call" | custom-call | tf_op jit(solution)/shard_map/pallas_call | solution.py:112
  48.3 0.6 %shard_map.129 = bf16[8,128]{1,0:T(8,128)(2,1)} custom-call(f32[8,128]{1,0:T(8,128)S(1)} %get-tuple-element.56.a_ref, f32[8,128]{1,0:T(8,128)S(1)} %collective-permute-done.13.b_ref, f32[8,128]{1,0:T(8,128)S(1)} %collective-permute-done.14.c_ref, f32[8,128]{1,0:T(8,128)S(1)} %collective-permute-done.15.d_ref), custom_call_target="tpu_custom_call" | custom-call | tf_op jit(solution)/shard_map/pallas_call | solution.py:112
  (19 shorter events, 0.1 us)
Async XLA Ops:
  3.8 19.0 %collective-permute-start.4 = (bf16[4,264,128]{2,1,0:T(8,128)(2,1)S(1)}, bf16[4,264,128]{2,1,0:T(8,128)(2,1)S(1)}, u32[]{:S(2)}, u32[]{:S(2)}) collective-permute-start(bf16[4,264,128]{2,1,0:T(8,128)(2,1)S(1)} %shard_map.121), channel_id=1, source_target_pairs={{0,32},{8,40},{16,48},{24,56},{32,0},{40,8},{48,16},{56,24},{64,96... | collective-permute-start | bytes 811016 | tf_op jit(solution)/shard_map/ppermute | solution.py:294
  5.8 31.4 %copy-start = (bf16[1,128,1024]{2,1,0:T(8,128)(2,1)S(1)}, bf16[1,128,1024]{2,1,0:T(8,128)(2,1)}, u32[]{:S(2)}) copy-start(bf16[1,128,1024]{2,1,0:T(8,128)(2,1)} %param.17) | copy-start | bytes 786436
  5.8 31.4 %copy-start.1 = (bf16[8,1,128]{2,0,1:T(8,128)(2,1)S(1)}, bf16[8,1,128]{2,0,1:T(8,128)(2,1)}, u32[]{:S(2)}) copy-start(bf16[8,1,128]{2,0,1:T(8,128)(2,1)} %param.16) | copy-start | bytes 6148
  5.8 31.4 %copy-start.2 = (f32[2,1]{0,1:T(1,128)S(1)}, f32[2,1]{0,1:T(1,128)}, u32[]{:S(2)}) copy-start(f32[2,1]{0,1:T(1,128)} %param.14) | copy-start | bytes 28
  5.9 31.4 %copy-start.3 = (f32[2,1]{0,1:T(1,128)S(1)}, f32[2,1]{0,1:T(1,128)}, u32[]{:S(2)}) copy-start(f32[2,1]{0,1:T(1,128)} %param.15) | copy-start | bytes 28
  5.9 21.0 %collective-permute-start.3 = (bf16[4,264,128]{2,1,0:T(8,128)(2,1)S(1)}, bf16[4,264,128]{2,1,0:T(8,128)(2,1)S(1)}, u32[]{:S(2)}, u32[]{:S(2)}) collective-permute-start(bf16[4,264,128]{2,1,0:T(8,128)(2,1)S(1)} %get-tuple-element.39), channel_id=1, source_target_pairs={{0,96},{8,104},{16,112},{24,120},{32,64},{40,72},{48,80},{56,88},{... | collective-permute-start | bytes 811016 | tf_op jit(solution)/shard_map/ppermute | solution.py:294
  6.7 6.3 %collective-permute-start.8 = (bf16[264,128]{1,0:T(8,128)(2,1)S(1)}, bf16[264,128]{1,0:T(8,128)(2,1)S(1)}, u32[]{:S(2)}, u32[]{:S(2)}) collective-permute-start(bf16[264,128]{1,0:T(8,128)(2,1)S(1)} %get-tuple-element.44), channel_id=1, source_target_pairs={{0,8},{8,16},{16,24},{24,0},{32,40},{40,48},{48,56},{56,32},{64,72... | collective-permute-start | bytes 202760 | tf_op jit(solution)/shard_map/ppermute | solution.py:294
  8.3 5.9 %collective-permute-start.9 = (bf16[264,128]{1,0:T(8,128)(2,1)S(1)}, bf16[264,128]{1,0:T(8,128)(2,1)S(1)}, u32[]{:S(2)}, u32[]{:S(2)}) collective-permute-start(bf16[264,128]{1,0:T(8,128)(2,1)S(1)} %get-tuple-element.45), channel_id=1, source_target_pairs={{0,16},{8,24},{16,0},{24,8},{32,48},{40,56},{48,32},{56,40},{64,80... | collective-permute-start | bytes 202760 | tf_op jit(solution)/shard_map/ppermute | solution.py:294
  11.2 4.3 %collective-permute-start.10 = (bf16[264,128]{1,0:T(8,128)(2,1)S(1)}, bf16[264,128]{1,0:T(8,128)(2,1)S(1)}, u32[]{:S(2)}, u32[]{:S(2)}) collective-permute-start(bf16[264,128]{1,0:T(8,128)(2,1)S(1)} %get-tuple-element.46), channel_id=1, source_target_pairs={{0,24},{8,0},{16,8},{24,16},{32,56},{40,32},{48,40},{56,48},{64,88... | collective-permute-start | bytes 202760 | tf_op jit(solution)/shard_map/ppermute | solution.py:294
  15.5 21.7 %collective-permute-start.11 = (bf16[4,264,128]{2,1,0:T(8,128)(2,1)S(1)}, bf16[4,264,128]{2,1,0:T(8,128)(2,1)S(1)}, u32[]{:S(2)}, u32[]{:S(2)}) collective-permute-start(bf16[4,264,128]{2,1,0:T(8,128)(2,1)S(1)} %shard_map.124), channel_id=1, source_target_pairs={{0,64},{8,72},{16,80},{24,88},{32,96},{40,104},{48,112},{56,120},{... | collective-permute-start | bytes 811016 | tf_op jit(solution)/shard_map/ppermute | solution.py:294
  18.8 12.7 %collective-permute-start = (bf16[264,128]{1,0:T(8,128)(2,1)S(1)}, bf16[264,128]{1,0:T(8,128)(2,1)S(1)}, u32[]{:S(2)}, u32[]{:S(2)}) collective-permute-start(bf16[264,128]{1,0:T(8,128)(2,1)S(1)} %get-tuple-element.36), channel_id=1, source_target_pairs={{0,8},{8,16},{16,24},{24,0},{32,40},{40,48},{48,56},{56,32},{64,72... | collective-permute-start | bytes 202760 | tf_op jit(solution)/shard_map/ppermute | solution.py:294
  19.2 13.6 %collective-permute-start.1 = (bf16[264,128]{1,0:T(8,128)(2,1)S(1)}, bf16[264,128]{1,0:T(8,128)(2,1)S(1)}, u32[]{:S(2)}, u32[]{:S(2)}) collective-permute-start(bf16[264,128]{1,0:T(8,128)(2,1)S(1)} %get-tuple-element.37), channel_id=1, source_target_pairs={{0,16},{8,24},{16,0},{24,8},{32,48},{40,56},{48,32},{56,40},{64,80... | collective-permute-start | bytes 202760 | tf_op jit(solution)/shard_map/ppermute | solution.py:294
  26.9 10.3 %collective-permute-start.5 = (bf16[2,264,128]{2,1,0:T(8,128)(2,1)S(1)}, bf16[2,264,128]{2,1,0:T(8,128)(2,1)S(1)}, u32[]{:S(2)}, u32[]{:S(2)}) collective-permute-start(bf16[2,264,128]{2,1,0:T(8,128)(2,1)S(1)} %get-tuple-element.40), channel_id=1, source_target_pairs={{0,8},{8,16},{16,24},{24,0},{32,40},{40,48},{48,56},{56,32},{64,72... | collective-permute-start | bytes 405512 | tf_op jit(solution)/shard_map/ppermute | solution.py:294
  28.6 8.7 %collective-permute-start.6 = (bf16[2,264,128]{2,1,0:T(8,128)(2,1)S(1)}, bf16[2,264,128]{2,1,0:T(8,128)(2,1)S(1)}, u32[]{:S(2)}, u32[]{:S(2)}) collective-permute-start(bf16[2,264,128]{2,1,0:T(8,128)(2,1)S(1)} %get-tuple-element.41), channel_id=1, source_target_pairs={{0,16},{8,24},{16,0},{24,8},{32,48},{40,56},{48,32},{56,40},{64,80... | collective-permute-start | bytes 405512 | tf_op jit(solution)/shard_map/ppermute | solution.py:294
  31.5 5.8 %collective-permute-start.7 = (bf16[2,264,128]{2,1,0:T(8,128)(2,1)S(1)}, bf16[2,264,128]{2,1,0:T(8,128)(2,1)S(1)}, u32[]{:S(2)}, u32[]{:S(2)}) collective-permute-start(bf16[2,264,128]{2,1,0:T(8,128)(2,1)S(1)} %get-tuple-element.42), channel_id=1, source_target_pairs={{0,24},{8,0},{16,8},{24,16},{32,56},{40,32},{48,40},{56,48},{64,88... | collective-permute-start | bytes 405512 | tf_op jit(solution)/shard_map/ppermute | solution.py:294
  32.8 4.4 %collective-permute-start.2 = (bf16[264,128]{1,0:T(8,128)(2,1)S(1)}, bf16[264,128]{1,0:T(8,128)(2,1)S(1)}, u32[]{:S(2)}, u32[]{:S(2)}) collective-permute-start(bf16[264,128]{1,0:T(8,128)(2,1)S(1)} %get-tuple-element.38), channel_id=1, source_target_pairs={{0,24},{8,0},{16,8},{24,16},{32,56},{40,32},{48,40},{56,48},{64,88... | collective-permute-start | bytes 202760 | tf_op jit(solution)/shard_map/ppermute | solution.py:294
  39.2 1.2 %collective-permute-start.12 = (f32[4,8,128]{2,1,0:T(8,128)S(1)}, f32[4,8,128]{2,1,0:T(8,128)S(1)}, u32[]{:S(2)}, u32[]{:S(2)}) collective-permute-start(f32[4,8,128]{2,1,0:T(8,128)S(1)} %get-tuple-element.55), channel_id=1, source_target_pairs={{0,1},{1,0},{2,3},{3,2},{4,5},{5,4},{6,7},{7,6},{8,9},{9,8},{10,11... | collective-permute-start | bytes 49160 | tf_op jit(solution)/shard_map/ppermute | solution.py:299
  40.4 7.9 %collective-permute-start.13 = (f32[8,128]{1,0:T(8,128)S(1)}, f32[8,128]{1,0:T(8,128)S(1)}, u32[]{:S(2)}, u32[]{:S(2)}) collective-permute-start(f32[8,128]{1,0:T(8,128)S(1)} %get-tuple-element.57), channel_id=1, source_target_pairs={{0,2},{2,4},{4,6},{6,0},{1,3},{3,5},{5,7},{7,1},{8,10},{10,12},{12... | collective-permute-start | bytes 12296 | tf_op jit(solution)/shard_map/ppermute | solution.py:299
  41.9 6.4 %collective-permute-start.14 = (f32[8,128]{1,0:T(8,128)S(1)}, f32[8,128]{1,0:T(8,128)S(1)}, u32[]{:S(2)}, u32[]{:S(2)}) collective-permute-start(f32[8,128]{1,0:T(8,128)S(1)} %get-tuple-element.58), channel_id=1, source_target_pairs={{0,4},{2,6},{4,0},{6,2},{1,5},{3,7},{5,1},{7,3},{8,12},{10,14},{12... | collective-permute-start | bytes 12296 | tf_op jit(solution)/shard_map/ppermute | solution.py:299
  44.6 3.7 %collective-permute-start.15 = (f32[8,128]{1,0:T(8,128)S(1)}, f32[8,128]{1,0:T(8,128)S(1)}, u32[]{:S(2)}, u32[]{:S(2)}) collective-permute-start(f32[8,128]{1,0:T(8,128)S(1)} %get-tuple-element.59), channel_id=1, source_target_pairs={{0,6},{2,0},{4,2},{6,4},{1,7},{3,1},{5,3},{7,5},{8,14},{10,8},{12,... | collective-permute-start | bytes 12296 | tf_op jit(solution)/shard_map/ppermute | solution.py:299

commit v10 on v5

--- a/solution.py
+++ b/solution.py
@@ -82,9 +82,12 @@
     project_blocks(rest_ref, 0, w_ref[...], g_ref[...], [twin_ref.at[k] for k in range(ROW)])
 
 
-def third_kernel(rest_ref, w_ref, g_ref, c1_ref, c2_ref, c3_ref, far_ref, own0_ref, own3_ref):
-    project_blocks(rest_ref, ROW, w_ref[...], g_ref[...], [far_ref, c1_ref.at[0], c2_ref.at[0], c3_ref])
-    project_blocks(rest_ref, 2 * ROW, w_ref[...], g_ref[...], [own0_ref, c1_ref.at[1], c2_ref.at[1], own3_ref])
+def third_kernel(rest_ref, w_ref, g_ref, *outs):
+    project_blocks(rest_ref, ROW, w_ref[...], g_ref[...], outs)
+
+
+def own_kernel(rest_ref, w_ref, g_ref, *outs):
+    project_blocks(rest_ref, 2 * ROW, w_ref[...], g_ref[...], outs)
 
 
 ANY = pl.BlockSpec(memory_space=pl.ANY)
@@ -132,11 +135,9 @@
     )(*[pltpu.with_memory_space_constraint(a, pltpu.HBM) for a in args])
 
 
-def gather_kernel(a_ref, b_ref, c_ref, d_ref, out_ref):
-    out_ref[0] = a_ref[...]
-    out_ref[1] = b_ref[0]
-    out_ref[2] = c_ref[0]
-    out_ref[3] = d_ref[...]
+def gather_kernel(*refs):
+    for i in range(ROW):
+        refs[ROW][i] = refs[i][...]
 
 
 def legs_kernel(a_ref, b_ref, own3_ref, *outs):
@@ -165,8 +166,8 @@
 
 
 def landed(refs):
-    own0, c1, c2, mirror, twin, s1, s2, s3, far = refs
-    own = [own0, c1.at[1], c2.at[1], s3.at[2]]
+    own0, o1, o2, mirror, twin, s1, s2, s3, far = refs
+    own = [own0, o1, o2, s3.at[2]]
     from_mirror, from_twin = [
         [kept.at[0]] + [s.at[i] for s in (s1, s2, s3)] for i, kept in enumerate((mirror, twin))
     ]
@@ -303,15 +304,15 @@
     mirror = shift(mirror, 3, 0)
     twin = run(second_kernel, block(ROW), (later, w, gates))
     twin = shift(twin, 1, 0)
-    *cross, far, own0, own3 = run(
-        third_kernel, (block(2), block(2), block(), block(), block(), block()), (later, w, gates)
-    )
-    cross = [shift(blocks, 0, k) for k, blocks in zip(hops, cross)]
-    far = run(gather_kernel, block(ROW), (far, *cross), 4)
+    cross = run(third_kernel, (block(),) * ROW, (later, w, gates))
+    cross = [cross[0]] + [shift(cross[k], 0, k) for k in hops]
+    far = run(gather_kernel, block(ROW), cross, 4)
     far = shift(far, 2, 0)
+    *own, own3 = run(own_kernel, (block(),) * ROW, (later, w, gates))
+    own = [own[0]] + [shift(own[k], 0, k) for k in (1, 2)]
     side = run(legs_kernel, (block(2), block(2), block(3)), (mirror, twin, own3), 4)
     side = [shift(blocks, 0, k) for k, blocks in zip(hops, side)]
-    blocks = (own0, cross[0], cross[1], mirror, twin, *side, far)
+    blocks = (*own, mirror, twin, *side, far)
     half = pltpu.VMEM((TPX, OWN, HD), F32)
     keep, send, weight, turned, stab = run(
         read_kernel,

time: 49.2 us -> 54.3 us (1.10)
  waiting for transfers between devices: 17.3 us -> 20.2 us
  starting transfers between devices: 22 us -> 24 us
    ppermute x9 -> x11, waiting for transfers between devices: 16.1 us -> 19 us  [shift(): return lax.ppermute(array, 'sp', pairs)]
    ppermute x9 -> x11, starting transfers between devices: 16.4 us -> 18.3 us  [shift(): return lax.ppermute(array, 'sp', pairs)]
    pallas_call x9 -> x10, Pallas kernels: 6.57 us -> 6.75 us  [run(): pl.pallas_call(kernel, in_specs=[VM] * len(args), out_specs=specs, out_sh...]
  transfers between devices with their start and end apart: 13 -> 15, of which waited for: 5 -> 7; matrix products, arithmetic and copies ran while one was open for 0% -> 0% of each run, Pallas kernels for 7% -> 7%
where the time goes in v10:
time: 54.3 us; the launch traced here: 54.2 us
  starting transfers between devices  24 us (44%)
  waiting for transfers between devices  20.2 us (37%)
  Pallas kernels  9.25 us (17%)
  between operations  0.75 us (1%)
    ppermute x11, waiting for transfers between devices, shift(): return lax.ppermute(array, 'sp', pairs)  19 us
    ppermute x11, starting transfers between devices, shift(): return lax.ppermute(array, 'sp', pairs)  18.3 us
    pallas_call x10, Pallas kernels, run(): pl.pallas_call(kernel, in_specs=[VM] * len(args), out_specs=specs, out_sh...  6.75 us
    ppermute x4, starting transfers between devices, across(): lax.ppermute(array, axis, [(i, (i + hop) % size) for i in range(size)])  5.66 us
    pallas_call x1, Pallas kernels, project_near(): pl.pallas_call(near_kernel, in_specs=[ANY] * 5, out_specs=[VM] * 4, out_s...  2.5 us
    ppermute x4, waiting for transfers between devices, across(): lax.ppermute(array, axis, [(i, (i + hop) % size) for i in range(size)])  1.19 us
  transfers between devices with their start and end apart: 15, of which 7 were waited for; matrix products, arithmetic and copies ran while one was open for 0% of the time, Pallas kernels for 7%

profile of v10, /device:TPU:64, one launch (start us, length us, event | category | flops | bytes accessed | tf_op | source)
XLA Modules:
  0.0 54.2 jit_solution(8584984678847076698)
XLA Ops:
  0.6 2.5 %near.1 = (bf16[4,264,128]{2,1,0:T(8,128)(2,1)S(1)}, bf16[1024,256]{1,0:T(8,128)(2,1)S(1)}, bf16[8,1024]{1,0:T(8,128)(2,1)S(1)}, bf16[12,8,16,1024]{3,2,1,0:T(8,128)(2,1)S(1)}) custom-call(bf16[128,16,1024]{2,1,0:T(8,128)(2,1)} %x_ref.1, bf16[1024,128]{1,0:T(8,128)(2,1)} %bitcast.22, bf16[1024,128]{1,0:T(8,128)(2,1)} %bitcast.23, bf16[2,1024]{1,0:T(2,128)(2,1)} %bitcast.24, ...), custom_call_target="tpu_custom_call" | custom-call | tf_op jit(solution)/shard_map/near/pallas_call | solution.py:122
  3.1 0.7 %shard_map.121 = bf16[4,264,128]{2,1,0:T(8,128)(2,1)S(1)} custom-call(bf16[12,8,16,1024]{3,2,1,0:T(8,128)(2,1)S(1)} %get-tuple-element.30.rest_ref, bf16[1024,256]{1,0:T(8,128)(2,1)S(1)} %get-tuple-element.31.w_ref, bf16[8,1024]{1,0:T(8,128)(2,1)S(1)} %get-tuple-element.32.g_ref), custom_call_target="tpu_custom_call" | custom-call | tf_op jit(solution)/shard_map/pallas_call | solution.py:111
  3.8 2.0 %collective-permute-start.3 = (bf16[4,264,128]{2,1,0:T(8,128)(2,1)S(1)}, bf16[4,264,128]{2,1,0:T(8,128)(2,1)S(1)}, u32[]{:S(2)}, u32[]{:S(2)}) collective-permute-start(bf16[4,264,128]{2,1,0:T(8,128)(2,1)S(1)} %shard_map.121), channel_id=1, source_target_pairs={{0,32},{8,40},{16,48},{24,56},{32,0},{40,8},{48,16},{56,24},{64,96... | collective-permute-start | bytes 811016 | tf_op jit(solution)/shard_map/ppermute | solution.py:291
  5.9 0.1 collective-permute-start.2
  6.0 0.7 %shard_map.123 = (bf16[264,128]{1,0:T(8,128)(2,1)S(1)}, bf16[264,128]{1,0:T(8,128)(2,1)S(1)}, bf16[264,128]{1,0:T(8,128)(2,1)S(1)}, bf16[264,128]{1,0:T(8,128)(2,1)S(1)}) custom-call(bf16[12,8,16,1024]{3,2,1,0:T(8,128)(2,1)S(1)} %get-tuple-element.30.rest_ref, bf16[1024,256]{1,0:T(8,128)(2,1)S(1)} %get-tuple-element.31.w_ref, ...), custom_call_target="tpu_custom_call" | custom-call | tf_op jit(solution)/shard_map/pallas_call | solution.py:111
  6.7 1.7 %collective-permute-start.7 = (bf16[264,128]{1,0:T(8,128)(2,1)S(1)}, bf16[264,128]{1,0:T(8,128)(2,1)S(1)}, u32[]{:S(2)}, u32[]{:S(2)}) collective-permute-start(bf16[264,128]{1,0:T(8,128)(2,1)S(1)} %get-tuple-element.42), channel_id=1, source_target_pairs={{0,8},{8,16},{16,24},{24,0},{32,40},{40,48},{48,56},{56,32},{64,72... | collective-permute-start | bytes 202760 | tf_op jit(solution)/shard_map/ppermute | solution.py:291
  8.3 2.9 %collective-permute-start.8 = (bf16[264,128]{1,0:T(8,128)(2,1)S(1)}, bf16[264,128]{1,0:T(8,128)(2,1)S(1)}, u32[]{:S(2)}, u32[]{:S(2)}) collective-permute-start(bf16[264,128]{1,0:T(8,128)(2,1)S(1)} %get-tuple-element.43), channel_id=1, source_target_pairs={{0,16},{8,24},{16,0},{24,8},{32,48},{40,56},{48,32},{56,40},{64,80... | collective-permute-start | bytes 202760 | tf_op jit(solution)/shard_map/ppermute | solution.py:291
  11.2 1.3 %collective-permute-start.9 = (bf16[264,128]{1,0:T(8,128)(2,1)S(1)}, bf16[264,128]{1,0:T(8,128)(2,1)S(1)}, u32[]{:S(2)}, u32[]{:S(2)}) collective-permute-start(bf16[264,128]{1,0:T(8,128)(2,1)S(1)} %get-tuple-element.44), channel_id=1, source_target_pairs={{0,24},{8,0},{16,8},{24,16},{32,56},{40,32},{48,40},{56,48},{64,88... | collective-permute-start | bytes 202760 | tf_op jit(solution)/shard_map/ppermute | solution.py:291
  12.6 0.4 collective-permute-done.7.refs_1_
  13.0 1.3 %collective-permute-done.8.refs_2_ = bf16[264,128]{1,0:T(8,128)(2,1)S(1)} collective-permute-done((bf16[264,128]{1,0:T(8,128)(2,1)S(1)}, bf16[264,128]{1,0:T(8,128)(2,1)S(1)}, u32[]{:S(2)}, u32[]{:S(2)}) %collective-permute-start.8) | collective-permute-done | bytes 67616 | tf_op jit(solution)/shard_map/ppermute | solution.py:291
  14.2 1.3 %collective-permute-done.9.refs_3_ = bf16[264,128]{1,0:T(8,128)(2,1)S(1)} collective-permute-done((bf16[264,128]{1,0:T(8,128)(2,1)S(1)}, bf16[264,128]{1,0:T(8,128)(2,1)S(1)}, u32[]{:S(2)}, u32[]{:S(2)}) %collective-permute-start.9) | collective-permute-done | bytes 67616 | tf_op jit(solution)/shard_map/ppermute | solution.py:291
  15.5 2.5 %collective-permute-start.10 = (bf16[4,264,128]{2,1,0:T(8,128)(2,1)S(1)}, bf16[4,264,128]{2,1,0:T(8,128)(2,1)S(1)}, u32[]{:S(2)}, u32[]{:S(2)}) collective-permute-start(bf16[4,264,128]{2,1,0:T(8,128)(2,1)S(1)} %shard_map.124), channel_id=1, source_target_pairs={{0,64},{8,72},{16,80},{24,88},{32,96},{40,104},{48,112},{56,120},{... | collective-permute-start | bytes 811016 | tf_op jit(solution)/shard_map/ppermute | solution.py:291
  18.1 0.7 %shard_map.120 = (bf16[264,128]{1,0:T(8,128)(2,1)S(1)}, bf16[264,128]{1,0:T(8,128)(2,1)S(1)}, bf16[264,128]{1,0:T(8,128)(2,1)S(1)}, bf16[264,128]{1,0:T(8,128)(2,1)S(1)}) custom-call(bf16[12,8,16,1024]{3,2,1,0:T(8,128)(2,1)S(1)} %get-tuple-element.30.rest_ref, bf16[1024,256]{1,0:T(8,128)(2,1)S(1)} %get-tuple-element.31.w_ref, ...), custom_call_target="tpu_custom_call" | custom-call | tf_op jit(solution)/shard_map/pallas_call | solution.py:111
  18.8 8.1 %collective-permute-done.2.a_ref.refs_3_ = bf16[4,264,128]{2,1,0:T(8,128)(2,1)S(1)} collective-permute-done((bf16[4,264,128]{2,1,0:T(8,128)(2,1)S(1)}, bf16[4,264,128]{2,1,0:T(8,128)(2,1)S(1)}, u32[]{:S(2)}, u32[]{:S(2)}) %collective-permute-start.2) | collective-permute-done | bytes 270368 | tf_op jit(solution)/shard_map/ppermute | solution.py:291
  26.9 3.1 %collective-permute-start.6 = (bf16[3,264,128]{2,1,0:T(8,128)(2,1)S(1)}, bf16[3,264,128]{2,1,0:T(8,128)(2,1)S(1)}, u32[]{:S(2)}, u32[]{:S(2)}) collective-permute-start(bf16[3,264,128]{2,1,0:T(8,128)(2,1)S(1)} %get-tuple-element.40), channel_id=1, source_target_pairs={{0,24},{8,0},{16,8},{24,16},{32,56},{40,32},{48,40},{56,48},{64,88... | collective-permute-start | bytes 608264 | tf_op jit(solution)/shard_map/ppermute | solution.py:291
  30.0 0.0 collective-permute-start
  30.0 0.6 %collective-permute-start.4 = (bf16[2,264,128]{2,1,0:T(8,128)(2,1)S(1)}, bf16[2,264,128]{2,1,0:T(8,128)(2,1)S(1)}, u32[]{:S(2)}, u32[]{:S(2)}) collective-permute-start(bf16[2,264,128]{2,1,0:T(8,128)(2,1)S(1)} %get-tuple-element.38), channel_id=1, source_target_pairs={{0,8},{8,16},{16,24},{24,0},{32,40},{40,48},{48,56},{56,32},{64,72... | collective-permute-start | bytes 405512 | tf_op jit(solution)/shard_map/ppermute | solution.py:291
  30.6 4.1 %collective-permute-start.5 = (bf16[2,264,128]{2,1,0:T(8,128)(2,1)S(1)}, bf16[2,264,128]{2,1,0:T(8,128)(2,1)S(1)}, u32[]{:S(2)}, u32[]{:S(2)}) collective-permute-start(bf16[2,264,128]{2,1,0:T(8,128)(2,1)S(1)} %get-tuple-element.39), channel_id=1, source_target_pairs={{0,16},{8,24},{16,0},{24,8},{32,48},{40,56},{48,32},{56,40},{64,80... | collective-permute-start | bytes 405512 | tf_op jit(solution)/shard_map/ppermute | solution.py:291
  34.7 2.2 %collective-permute-done.refs_1_ = bf16[264,128]{1,0:T(8,128)(2,1)S(1)} collective-permute-done((bf16[264,128]{1,0:T(8,128)(2,1)S(1)}, bf16[264,128]{1,0:T(8,128)(2,1)S(1)}, u32[]{:S(2)}, u32[]{:S(2)}) %collective-permute-start) | collective-permute-done | bytes 67616 | tf_op jit(solution)/shard_map/ppermute | solution.py:291
  36.9 0.0 collective-permute-start.1
  36.9 5.8 %collective-permute-done.1.refs_2_ = bf16[264,128]{1,0:T(8,128)(2,1)S(1)} collective-permute-done((bf16[264,128]{1,0:T(8,128)(2,1)S(1)}, bf16[264,128]{1,0:T(8,128)(2,1)S(1)}, u32[]{:S(2)}, u32[]{:S(2)}) %collective-permute-start.1) | collective-permute-done | bytes 67616 | tf_op jit(solution)/shard_map/ppermute | solution.py:291
  42.7 0.0 collective-permute-done.4.refs_5_
  42.7 0.0 collective-permute-done.5.refs_6_
  42.7 0.0 collective-permute-done.6.refs_7_
  42.7 1.8 %shard_map.125 = (f32[4,8,128]{2,1,0:T(8,128)S(1)}, f32[4,8,128]{2,1,0:T(8,128)S(1)}, f32[32,128]{1,0:T(8,128)S(1)}, f32[128,32]{1,0:T(8,128)S(1)}, f32[2,1,8]{2,1,0:T(1,128)}) custom-call(bf16[264,128]{1,0:T(8,128)(2,1)S(1)} %get-tuple-element.33.refs_0_, bf16[264,128]{1,0:T(8,128)(2,1)S(1)} %collective-permute-done.refs_1_, ...), custom_call_target="tpu_custom_call" | custom-call | tf_op jit(solution)/shard_map/pallas_call | solution.py:111
  44.5 1.2 %collective-permute-done.11.got_ref = f32[4,8,128]{2,1,0:T(8,128)S(1)} collective-permute-done((f32[4,8,128]{2,1,0:T(8,128)S(1)}, f32[4,8,128]{2,1,0:T(8,128)S(1)}, u32[]{:S(2)}, u32[]{:S(2)}) %collective-permute-start.11) | collective-permute-done | bytes 16416 | tf_op jit(solution)/shard_map/ppermute | solution.py:296
  45.7 1.5 %collective-permute-start.12 = (f32[8,128]{1,0:T(8,128)S(1)}, f32[8,128]{1,0:T(8,128)S(1)}, u32[]{:S(2)}, u32[]{:S(2)}) collective-permute-start(f32[8,128]{1,0:T(8,128)S(1)} %get-tuple-element.53), channel_id=1, source_target_pairs={{0,2},{2,4},{4,6},{6,0},{1,3},{3,5},{5,7},{7,1},{8,10},{10,12},{12... | collective-permute-start | bytes 12296 | tf_op jit(solution)/shard_map/ppermute | solution.py:296
  47.2 2.7 %collective-permute-start.13 = (f32[8,128]{1,0:T(8,128)S(1)}, f32[8,128]{1,0:T(8,128)S(1)}, u32[]{:S(2)}, u32[]{:S(2)}) collective-permute-start(f32[8,128]{1,0:T(8,128)S(1)} %get-tuple-element.54), channel_id=1, source_target_pairs={{0,4},{2,6},{4,0},{6,2},{1,5},{3,7},{5,1},{7,3},{8,12},{10,14},{12... | collective-permute-start | bytes 12296 | tf_op jit(solution)/shard_map/ppermute | solution.py:296
  49.9 1.4 %collective-permute-start.14 = (f32[8,128]{1,0:T(8,128)S(1)}, f32[8,128]{1,0:T(8,128)S(1)}, u32[]{:S(2)}, u32[]{:S(2)}) collective-permute-start(f32[8,128]{1,0:T(8,128)S(1)} %get-tuple-element.55), channel_id=1, source_target_pairs={{0,6},{2,0},{4,2},{6,4},{1,7},{3,1},{5,3},{7,5},{8,14},{10,8},{12,... | collective-permute-start | bytes 12296 | tf_op jit(solution)/shard_map/ppermute | solution.py:296
  51.4 1.1 %shard_map.126 = (bf16[16,128,256]{2,1,0:T(8,128)(2,1)S(1)}, f32[16,128]{1,0:T(8,128)}) custom-call(bf16[264,128]{1,0:T(8,128)(2,1)S(1)} %get-tuple-element.33.refs_0_, bf16[264,128]{1,0:T(8,128)(2,1)S(1)} %collective-permute-done.refs_1_, bf16[264,128]{1,0:T(8,128)(2,1)S(1)} %collective-permute-done.1.refs_2_, ...), custom_call_target="tpu_custom_call" | custom-call | tf_op jit(solution)/shard_map/pallas_call | solution.py:111
  52.4 1.2 %shard_map.127 = bf16[2,8,128,128]{3,2,1,0:T(8,128)(2,1)} custom-call(bf16[264,128]{1,0:T(8,128)(2,1)S(1)} %get-tuple-element.33.refs_0_, bf16[264,128]{1,0:T(8,128)(2,1)S(1)} %collective-permute-done.refs_1_, bf16[264,128]{1,0:T(8,128)(2,1)S(1)} %collective-permute-done.1.refs_2_, bf16[4,264,128]{2,1,0:T(8,128)(2,1)S(1)} %collective-permute-done.2.a_ref.refs_3_, ...), custom_call_target="tpu_custom_call" | custom-call | tf_op jit(solution)/shard_map/pallas_call | solution.py:111
  53.6 0.6 %shard_map.129 = bf16[8,128]{1,0:T(8,128)(2,1)} custom-call(f32[8,128]{1,0:T(8,128)S(1)} %get-tuple-element.52.a_ref, f32[8,128]{1,0:T(8,128)S(1)} %collective-permute-done.12.b_ref, f32[8,128]{1,0:T(8,128)S(1)} %collective-permute-done.13.c_ref, f32[8,128]{1,0:T(8,128)S(1)} %collective-permute-done.14.d_ref), custom_call_target="tpu_custom_call" | custom-call | tf_op jit(solution)/shard_map/pallas_call | solution.py:111
  (17 shorter events, 0.1 us)
Async XLA Ops:
  3.8 14.9 %collective-permute-start.3 = (bf16[4,264,128]{2,1,0:T(8,128)(2,1)S(1)}, bf16[4,264,128]{2,1,0:T(8,128)(2,1)S(1)}, u32[]{:S(2)}, u32[]{:S(2)}) collective-permute-start(bf16[4,264,128]{2,1,0:T(8,128)(2,1)S(1)} %shard_map.121), channel_id=1, source_target_pairs={{0,32},{8,40},{16,48},{24,56},{32,0},{40,8},{48,16},{56,24},{64,96... | collective-permute-start | bytes 811016 | tf_op jit(solution)/shard_map/ppermute | solution.py:291
  5.8 36.8 %copy-start = (bf16[1,128,1024]{2,1,0:T(8,128)(2,1)S(1)}, bf16[1,128,1024]{2,1,0:T(8,128)(2,1)}, u32[]{:S(2)}) copy-start(bf16[1,128,1024]{2,1,0:T(8,128)(2,1)} %param.17) | copy-start | bytes 786436
  5.8 36.8 %copy-start.1 = (bf16[8,1,128]{2,0,1:T(8,128)(2,1)S(1)}, bf16[8,1,128]{2,0,1:T(8,128)(2,1)}, u32[]{:S(2)}) copy-start(bf16[8,1,128]{2,0,1:T(8,128)(2,1)} %param.16) | copy-start | bytes 6148
  5.8 36.9 %copy-start.2 = (f32[2,1]{0,1:T(1,128)S(1)}, f32[2,1]{0,1:T(1,128)}, u32[]{:S(2)}) copy-start(f32[2,1]{0,1:T(1,128)} %param.14) | copy-start | bytes 28
  5.9 36.9 %copy-start.3 = (f32[2,1]{0,1:T(1,128)S(1)}, f32[2,1]{0,1:T(1,128)}, u32[]{:S(2)}) copy-start(f32[2,1]{0,1:T(1,128)} %param.15) | copy-start | bytes 28
  5.9 21.0 %collective-permute-start.2 = (bf16[4,264,128]{2,1,0:T(8,128)(2,1)S(1)}, bf16[4,264,128]{2,1,0:T(8,128)(2,1)S(1)}, u32[]{:S(2)}, u32[]{:S(2)}) collective-permute-start(bf16[4,264,128]{2,1,0:T(8,128)(2,1)S(1)} %get-tuple-element.36), channel_id=1, source_target_pairs={{0,96},{8,104},{16,112},{24,120},{32,64},{40,72},{48,80},{56,88},{... | collective-permute-start | bytes 811016 | tf_op jit(solution)/shard_map/ppermute | solution.py:291
  6.7 6.3 %collective-permute-start.7 = (bf16[264,128]{1,0:T(8,128)(2,1)S(1)}, bf16[264,128]{1,0:T(8,128)(2,1)S(1)}, u32[]{:S(2)}, u32[]{:S(2)}) collective-permute-start(bf16[264,128]{1,0:T(8,128)(2,1)S(1)} %get-tuple-element.42), channel_id=1, source_target_pairs={{0,8},{8,16},{16,24},{24,0},{32,40},{40,48},{48,56},{56,32},{64,72... | collective-permute-start | bytes 202760 | tf_op jit(solution)/shard_map/ppermute | solution.py:291
  8.3 5.9 %collective-permute-start.8 = (bf16[264,128]{1,0:T(8,128)(2,1)S(1)}, bf16[264,128]{1,0:T(8,128)(2,1)S(1)}, u32[]{:S(2)}, u32[]{:S(2)}) collective-permute-start(bf16[264,128]{1,0:T(8,128)(2,1)S(1)} %get-tuple-element.43), channel_id=1, source_target_pairs={{0,16},{8,24},{16,0},{24,8},{32,48},{40,56},{48,32},{56,40},{64,80... | collective-permute-start | bytes 202760 | tf_op jit(solution)/shard_map/ppermute | solution.py:291
  11.2 4.3 %collective-permute-start.9 = (bf16[264,128]{1,0:T(8,128)(2,1)S(1)}, bf16[264,128]{1,0:T(8,128)(2,1)S(1)}, u32[]{:S(2)}, u32[]{:S(2)}) collective-permute-start(bf16[264,128]{1,0:T(8,128)(2,1)S(1)} %get-tuple-element.44), channel_id=1, source_target_pairs={{0,24},{8,0},{16,8},{24,16},{32,56},{40,32},{48,40},{56,48},{64,88... | collective-permute-start | bytes 202760 | tf_op jit(solution)/shard_map/ppermute | solution.py:291
  15.5 27.1 %collective-permute-start.10 = (bf16[4,264,128]{2,1,0:T(8,128)(2,1)S(1)}, bf16[4,264,128]{2,1,0:T(8,128)(2,1)S(1)}, u32[]{:S(2)}, u32[]{:S(2)}) collective-permute-start(bf16[4,264,128]{2,1,0:T(8,128)(2,1)S(1)} %shard_map.124), channel_id=1, source_target_pairs={{0,64},{8,72},{16,80},{24,88},{32,96},{40,104},{48,112},{56,120},{... | collective-permute-start | bytes 811016 | tf_op jit(solution)/shard_map/ppermute | solution.py:291
  26.9 15.8 %collective-permute-start.6 = (bf16[3,264,128]{2,1,0:T(8,128)(2,1)S(1)}, bf16[3,264,128]{2,1,0:T(8,128)(2,1)S(1)}, u32[]{:S(2)}, u32[]{:S(2)}) collective-permute-start(bf16[3,264,128]{2,1,0:T(8,128)(2,1)S(1)} %get-tuple-element.40), channel_id=1, source_target_pairs={{0,24},{8,0},{16,8},{24,16},{32,56},{40,32},{48,40},{56,48},{64,88... | collective-permute-start | bytes 608264 | tf_op jit(solution)/shard_map/ppermute | solution.py:291
  30.0 6.9 %collective-permute-start = (bf16[264,128]{1,0:T(8,128)(2,1)S(1)}, bf16[264,128]{1,0:T(8,128)(2,1)S(1)}, u32[]{:S(2)}, u32[]{:S(2)}) collective-permute-start(bf16[264,128]{1,0:T(8,128)(2,1)S(1)} %get-tuple-element.34), channel_id=1, source_target_pairs={{0,8},{8,16},{16,24},{24,0},{32,40},{40,48},{48,56},{56,32},{64,72... | collective-permute-start | bytes 202760 | tf_op jit(solution)/shard_map/ppermute | solution.py:291
  30.0 12.7 %collective-permute-start.4 = (bf16[2,264,128]{2,1,0:T(8,128)(2,1)S(1)}, bf16[2,264,128]{2,1,0:T(8,128)(2,1)S(1)}, u32[]{:S(2)}, u32[]{:S(2)}) collective-permute-start(bf16[2,264,128]{2,1,0:T(8,128)(2,1)S(1)} %get-tuple-element.38), channel_id=1, source_target_pairs={{0,8},{8,16},{16,24},{24,0},{32,40},{40,48},{48,56},{56,32},{64,72... | collective-permute-start | bytes 405512 | tf_op jit(solution)/shard_map/ppermute | solution.py:291
  30.6 12.1 %collective-permute-start.5 = (bf16[2,264,128]{2,1,0:T(8,128)(2,1)S(1)}, bf16[2,264,128]{2,1,0:T(8,128)(2,1)S(1)}, u32[]{:S(2)}, u32[]{:S(2)}) collective-permute-start(bf16[2,264,128]{2,1,0:T(8,128)(2,1)S(1)} %get-tuple-element.39), channel_id=1, source_target_pairs={{0,16},{8,24},{16,0},{24,8},{32,48},{40,56},{48,32},{56,40},{64,80... | collective-permute-start | bytes 405512 | tf_op jit(solution)/shard_map/ppermute | solution.py:291
  36.9 5.8 %collective-permute-start.1 = (bf16[264,128]{1,0:T(8,128)(2,1)S(1)}, bf16[264,128]{1,0:T(8,128)(2,1)S(1)}, u32[]{:S(2)}, u32[]{:S(2)}) collective-permute-start(bf16[264,128]{1,0:T(8,128)(2,1)S(1)} %get-tuple-element.35), channel_id=1, source_target_pairs={{0,16},{8,24},{16,0},{24,8},{32,48},{40,56},{48,32},{56,40},{64,80... | collective-permute-start | bytes 202760 | tf_op jit(solution)/shard_map/ppermute | solution.py:291
  44.5 1.2 %collective-permute-start.11 = (f32[4,8,128]{2,1,0:T(8,128)S(1)}, f32[4,8,128]{2,1,0:T(8,128)S(1)}, u32[]{:S(2)}, u32[]{:S(2)}) collective-permute-start(f32[4,8,128]{2,1,0:T(8,128)S(1)} %get-tuple-element.51), channel_id=1, source_target_pairs={{0,1},{1,0},{2,3},{3,2},{4,5},{5,4},{6,7},{7,6},{8,9},{9,8},{10,11... | collective-permute-start | bytes 49160 | tf_op jit(solution)/shard_map/ppermute | solution.py:296
  45.7 7.9 %collective-permute-start.12 = (f32[8,128]{1,0:T(8,128)S(1)}, f32[8,128]{1,0:T(8,128)S(1)}, u32[]{:S(2)}, u32[]{:S(2)}) collective-permute-start(f32[8,128]{1,0:T(8,128)S(1)} %get-tuple-element.53), channel_id=1, source_target_pairs={{0,2},{2,4},{4,6},{6,0},{1,3},{3,5},{5,7},{7,1},{8,10},{10,12},{12... | collective-permute-start | bytes 12296 | tf_op jit(solution)/shard_map/ppermute | solution.py:296
  47.2 6.4 %collective-permute-start.13 = (f32[8,128]{1,0:T(8,128)S(1)}, f32[8,128]{1,0:T(8,128)S(1)}, u32[]{:S(2)}, u32[]{:S(2)}) collective-permute-start(f32[8,128]{1,0:T(8,128)S(1)} %get-tuple-element.54), channel_id=1, source_target_pairs={{0,4},{2,6},{4,0},{6,2},{1,5},{3,7},{5,1},{7,3},{8,12},{10,14},{12... | collective-permute-start | bytes 12296 | tf_op jit(solution)/shard_map/ppermute | solution.py:296
  49.9 3.7 %collective-permute-start.14 = (f32[8,128]{1,0:T(8,128)S(1)}, f32[8,128]{1,0:T(8,128)S(1)}, u32[]{:S(2)}, u32[]{:S(2)}) collective-permute-start(f32[8,128]{1,0:T(8,128)S(1)} %get-tuple-element.55), channel_id=1, source_target_pairs={{0,6},{2,0},{4,2},{6,4},{1,7},{3,1},{5,3},{7,5},{8,14},{10,8},{12,... | collective-permute-start | bytes 12296 | tf_op jit(solution)/shard_map/ppermute | solution.py:296

commit v11 on v6

--- a/solution.py
+++ b/solution.py
@@ -83,8 +83,11 @@
 
 
 def third_kernel(rest_ref, w_ref, g_ref, *outs):
-    project_blocks(rest_ref, ROW, w_ref[...], g_ref[...], outs[:ROW])
-    project_blocks(rest_ref, 2 * ROW, w_ref[...], g_ref[...], outs[ROW:])
+    project_blocks(rest_ref, ROW, w_ref[...], g_ref[...], outs)
+
+
+def own_kernel(rest_ref, w_ref, g_ref, *outs):
+    project_blocks(rest_ref, 2 * ROW, w_ref[...], g_ref[...], outs)
 
 
 ANY = pl.BlockSpec(memory_space=pl.ANY)
@@ -137,7 +140,7 @@
         refs[ROW][i] = refs[i][...]
 
 
-def legs_kernel(a_ref, b_ref, *outs):
+def pair_kernel(a_ref, b_ref, *outs):
     for k, out in enumerate(outs):
         out[0] = a_ref[k + 1]
         out[1] = b_ref[k + 1]
@@ -163,9 +166,8 @@
 
 def landed(refs):
     own, (mirror, twin, s1, s2, s3, far) = list(refs[:ROW]), refs[ROW:]
-    from_mirror, from_twin = [
-        [kept.at[0]] + [s.at[i] for s in (s1, s2, s3)] for i, kept in enumerate((mirror, twin))
-    ]
+    from_mirror = [mirror.at[0]] + [s.at[0] for s in (s1, s2, s3)]
+    from_twin = [twin.at[0]] + [s.at[1] for s in (s1, s2, s3)]
     return own + from_twin + [far.at[k] for k in range(ROW)] + from_mirror
 
 
@@ -299,12 +301,13 @@
     mirror = shift(mirror, 3, 0)
     twin = run(second_kernel, block(ROW), (later, w, gates))
     twin = shift(twin, 1, 0)
-    made = run(third_kernel, (block(),) * (2 * ROW), (later, w, gates))
-    cross = [made[0]] + [shift(made[k], 0, k) for k in hops]
-    own = [made[ROW]] + [shift(made[ROW + k], 0, k) for k in hops]
+    cross = run(third_kernel, (block(),) * ROW, (later, w, gates))
+    cross = [cross[0]] + [shift(cross[k], 0, k) for k in hops]
     far = run(gather_kernel, block(ROW), cross, 4)
     far = shift(far, 2, 0)
-    side = run(legs_kernel, (block(2),) * 3, (mirror, twin), 4)
+    own = run(own_kernel, (block(),) * ROW, (later, w, gates))
+    own = [own[0]] + [shift(own[k], 0, k) for k in hops]
+    side = run(pair_kernel, (block(2),) * 3, (mirror, twin), 4)
     side = [shift(blocks, 0, k) for k, blocks in zip(hops, side)]
     blocks = (*own, mirror, twin, *side, far)
     half = pltpu.VMEM((TPX, OWN, HD), F32)

time: 48.8 us -> 48.8 us (level)
    pallas_call x9 -> x10, Pallas kernels: 6.58 us -> 6.73 us  [run(): pl.pallas_call(kernel, in_specs=[VM] * len(args), out_specs=specs, out_sh...]
  transfers between devices with their start and end apart: 16 -> 16, of which waited for: 6 -> 6; matrix products, arithmetic and copies ran while one was open for 0% -> 0% of each run, Pallas kernels for 7% -> 8%
where the time goes in v11:
time: 48.8 us; the launch traced here: 48.7 us
  starting transfers between devices  26.3 us (54%)
  waiting for transfers between devices  12.5 us (26%)
  Pallas kernels  9.24 us (19%)
  between operations  0.74 us (2%)
    ppermute x12, starting transfers between devices, shift(): return lax.ppermute(array, 'sp', pairs)  20.6 us
    ppermute x12, waiting for transfers between devices, shift(): return lax.ppermute(array, 'sp', pairs)  11.3 us
    pallas_call x10, Pallas kernels, run(): pl.pallas_call(kernel, in_specs=[VM] * len(args), out_specs=specs, out_sh...  6.73 us
    ppermute x4, starting transfers between devices, across(): lax.ppermute(array, axis, [(i, (i + hop) % size) for i in range(size)])  5.66 us
    pallas_call x1, Pallas kernels, project_near(): pl.pallas_call(near_kernel, in_specs=[ANY] * 5, out_specs=[VM] * 4, out_s...  2.5 us
    ppermute x4, waiting for transfers between devices, across(): lax.ppermute(array, axis, [(i, (i + hop) % size) for i in range(size)])  1.19 us
  transfers between devices with their start and end apart: 16, of which 6 were waited for; matrix products, arithmetic and copies ran while one was open for 0% of the time, Pallas kernels for 8%

profile of v11, /device:TPU:64, one launch (start us, length us, event | category | flops | bytes accessed | tf_op | source)
XLA Modules:
  0.0 48.7 jit_solution(14251890958006022177)
XLA Ops:
  0.6 2.5 %near.1 = (bf16[4,264,128]{2,1,0:T(8,128)(2,1)S(1)}, bf16[1024,256]{1,0:T(8,128)(2,1)S(1)}, bf16[8,1024]{1,0:T(8,128)(2,1)S(1)}, bf16[12,8,16,1024]{3,2,1,0:T(8,128)(2,1)S(1)}) custom-call(bf16[128,16,1024]{2,1,0:T(8,128)(2,1)} %x_ref.1, bf16[1024,128]{1,0:T(8,128)(2,1)} %bitcast.22, bf16[1024,128]{1,0:T(8,128)(2,1)} %bitcast.23, bf16[2,1024]{1,0:T(2,128)(2,1)} %bitcast.24, ...), custom_call_target="tpu_custom_call" | custom-call | tf_op jit(solution)/shard_map/near/pallas_call | solution.py:122
  3.1 0.7 %shard_map.121 = bf16[4,264,128]{2,1,0:T(8,128)(2,1)S(1)} custom-call(bf16[12,8,16,1024]{3,2,1,0:T(8,128)(2,1)S(1)} %get-tuple-element.30.rest_ref, bf16[1024,256]{1,0:T(8,128)(2,1)S(1)} %get-tuple-element.31.w_ref, bf16[8,1024]{1,0:T(8,128)(2,1)S(1)} %get-tuple-element.32.g_ref), custom_call_target="tpu_custom_call" | custom-call | tf_op jit(solution)/shard_map/pallas_call | solution.py:111
  3.8 2.0 %collective-permute-start.4 = (bf16[4,264,128]{2,1,0:T(8,128)(2,1)S(1)}, bf16[4,264,128]{2,1,0:T(8,128)(2,1)S(1)}, u32[]{:S(2)}, u32[]{:S(2)}) collective-permute-start(bf16[4,264,128]{2,1,0:T(8,128)(2,1)S(1)} %shard_map.121), channel_id=1, source_target_pairs={{0,32},{8,40},{16,48},{24,56},{32,0},{40,8},{48,16},{56,24},{64,96... | collective-permute-start | bytes 811016 | tf_op jit(solution)/shard_map/ppermute | solution.py:288
  5.9 0.1 collective-permute-start.3
  6.0 0.7 %shard_map.123 = (bf16[264,128]{1,0:T(8,128)(2,1)S(1)}, bf16[264,128]{1,0:T(8,128)(2,1)S(1)}, bf16[264,128]{1,0:T(8,128)(2,1)S(1)}, bf16[264,128]{1,0:T(8,128)(2,1)S(1)}) custom-call(bf16[12,8,16,1024]{3,2,1,0:T(8,128)(2,1)S(1)} %get-tuple-element.30.rest_ref, bf16[1024,256]{1,0:T(8,128)(2,1)S(1)} %get-tuple-element.31.w_ref, ...), custom_call_target="tpu_custom_call" | custom-call | tf_op jit(solution)/shard_map/pallas_call | solution.py:111
  6.7 1.7 %collective-permute-start.8 = (bf16[264,128]{1,0:T(8,128)(2,1)S(1)}, bf16[264,128]{1,0:T(8,128)(2,1)S(1)}, u32[]{:S(2)}, u32[]{:S(2)}) collective-permute-start(bf16[264,128]{1,0:T(8,128)(2,1)S(1)} %get-tuple-element.42), channel_id=1, source_target_pairs={{0,8},{8,16},{16,24},{24,0},{32,40},{40,48},{48,56},{56,32},{64,72... | collective-permute-start | bytes 202760 | tf_op jit(solution)/shard_map/ppermute | solution.py:288
  8.3 2.9 %collective-permute-start.9 = (bf16[264,128]{1,0:T(8,128)(2,1)S(1)}, bf16[264,128]{1,0:T(8,128)(2,1)S(1)}, u32[]{:S(2)}, u32[]{:S(2)}) collective-permute-start(bf16[264,128]{1,0:T(8,128)(2,1)S(1)} %get-tuple-element.43), channel_id=1, source_target_pairs={{0,16},{8,24},{16,0},{24,8},{32,48},{40,56},{48,32},{56,40},{64,80... | collective-permute-start | bytes 202760 | tf_op jit(solution)/shard_map/ppermute | solution.py:288
  11.2 1.3 %collective-permute-start.10 = (bf16[264,128]{1,0:T(8,128)(2,1)S(1)}, bf16[264,128]{1,0:T(8,128)(2,1)S(1)}, u32[]{:S(2)}, u32[]{:S(2)}) collective-permute-start(bf16[264,128]{1,0:T(8,128)(2,1)S(1)} %get-tuple-element.44), channel_id=1, source_target_pairs={{0,24},{8,0},{16,8},{24,16},{32,56},{40,32},{48,40},{56,48},{64,88... | collective-permute-start | bytes 202760 | tf_op jit(solution)/shard_map/ppermute | solution.py:288
  12.6 0.4 collective-permute-done.8.refs_1_
  13.0 1.3 %collective-permute-done.9.refs_2_ = bf16[264,128]{1,0:T(8,128)(2,1)S(1)} collective-permute-done((bf16[264,128]{1,0:T(8,128)(2,1)S(1)}, bf16[264,128]{1,0:T(8,128)(2,1)S(1)}, u32[]{:S(2)}, u32[]{:S(2)}) %collective-permute-start.9) | collective-permute-done | bytes 67616 | tf_op jit(solution)/shard_map/ppermute | solution.py:288
  14.2 1.3 %collective-permute-done.10.refs_3_ = bf16[264,128]{1,0:T(8,128)(2,1)S(1)} collective-permute-done((bf16[264,128]{1,0:T(8,128)(2,1)S(1)}, bf16[264,128]{1,0:T(8,128)(2,1)S(1)}, u32[]{:S(2)}, u32[]{:S(2)}) %collective-permute-start.10) | collective-permute-done | bytes 67616 | tf_op jit(solution)/shard_map/ppermute | solution.py:288
  15.5 2.5 %collective-permute-start.11 = (bf16[4,264,128]{2,1,0:T(8,128)(2,1)S(1)}, bf16[4,264,128]{2,1,0:T(8,128)(2,1)S(1)}, u32[]{:S(2)}, u32[]{:S(2)}) collective-permute-start(bf16[4,264,128]{2,1,0:T(8,128)(2,1)S(1)} %shard_map.124), channel_id=1, source_target_pairs={{0,64},{8,72},{16,80},{24,88},{32,96},{40,104},{48,112},{56,120},{... | collective-permute-start | bytes 811016 | tf_op jit(solution)/shard_map/ppermute | solution.py:288
  18.1 0.7 %shard_map.120 = (bf16[264,128]{1,0:T(8,128)(2,1)S(1)}, bf16[264,128]{1,0:T(8,128)(2,1)S(1)}, bf16[264,128]{1,0:T(8,128)(2,1)S(1)}, bf16[264,128]{1,0:T(8,128)(2,1)S(1)}) custom-call(bf16[12,8,16,1024]{3,2,1,0:T(8,128)(2,1)S(1)} %get-tuple-element.30.rest_ref, bf16[1024,256]{1,0:T(8,128)(2,1)S(1)} %get-tuple-element.31.w_ref, ...), custom_call_target="tpu_custom_call" | custom-call | tf_op jit(solution)/shard_map/pallas_call | solution.py:111
  18.8 0.4 collective-permute-start
  19.2 3.7 %collective-permute-start.1 = (bf16[264,128]{1,0:T(8,128)(2,1)S(1)}, bf16[264,128]{1,0:T(8,128)(2,1)S(1)}, u32[]{:S(2)}, u32[]{:S(2)}) collective-permute-start(bf16[264,128]{1,0:T(8,128)(2,1)S(1)} %get-tuple-element.35), channel_id=1, source_target_pairs={{0,16},{8,24},{16,0},{24,8},{32,48},{40,56},{48,32},{56,40},{64,80... | collective-permute-start | bytes 202760 | tf_op jit(solution)/shard_map/ppermute | solution.py:288
  22.9 4.0 %collective-permute-done.3.a_ref.refs_4_ = bf16[4,264,128]{2,1,0:T(8,128)(2,1)S(1)} collective-permute-done((bf16[4,264,128]{2,1,0:T(8,128)(2,1)S(1)}, bf16[4,264,128]{2,1,0:T(8,128)(2,1)S(1)}, u32[]{:S(2)}, u32[]{:S(2)}) %collective-permute-start.3) | collective-permute-done | bytes 270368 | tf_op jit(solution)/shard_map/ppermute | solution.py:288
  26.9 1.7 %collective-permute-start.5 = (bf16[2,264,128]{2,1,0:T(8,128)(2,1)S(1)}, bf16[2,264,128]{2,1,0:T(8,128)(2,1)S(1)}, u32[]{:S(2)}, u32[]{:S(2)}) collective-permute-start(bf16[2,264,128]{2,1,0:T(8,128)(2,1)S(1)} %get-tuple-element.38), channel_id=1, source_target_pairs={{0,8},{8,16},{16,24},{24,0},{32,40},{40,48},{48,56},{56,32},{64,72... | collective-permute-start | bytes 405512 | tf_op jit(solution)/shard_map/ppermute | solution.py:288
  28.6 2.9 %collective-permute-start.6 = (bf16[2,264,128]{2,1,0:T(8,128)(2,1)S(1)}, bf16[2,264,128]{2,1,0:T(8,128)(2,1)S(1)}, u32[]{:S(2)}, u32[]{:S(2)}) collective-permute-start(bf16[2,264,128]{2,1,0:T(8,128)(2,1)S(1)} %get-tuple-element.39), channel_id=1, source_target_pairs={{0,16},{8,24},{16,0},{24,8},{32,48},{40,56},{48,32},{56,40},{64,80... | collective-permute-start | bytes 405512 | tf_op jit(solution)/shard_map/ppermute | solution.py:288
  31.5 0.0 collective-permute-done.refs_1_
  31.5 1.3 %collective-permute-start.7 = (bf16[2,264,128]{2,1,0:T(8,128)(2,1)S(1)}, bf16[2,264,128]{2,1,0:T(8,128)(2,1)S(1)}, u32[]{:S(2)}, u32[]{:S(2)}) collective-permute-start(bf16[2,264,128]{2,1,0:T(8,128)(2,1)S(1)} %get-tuple-element.40), channel_id=1, source_target_pairs={{0,24},{8,0},{16,8},{24,16},{32,56},{40,32},{48,40},{56,48},{64,88... | collective-permute-start | bytes 405512 | tf_op jit(solution)/shard_map/ppermute | solution.py:288
  32.8 0.1 collective-permute-start.2
  32.9 4.3 %collective-permute-done.2.refs_3_ = bf16[264,128]{1,0:T(8,128)(2,1)S(1)} collective-permute-done((bf16[264,128]{1,0:T(8,128)(2,1)S(1)}, bf16[264,128]{1,0:T(8,128)(2,1)S(1)}, u32[]{:S(2)}, u32[]{:S(2)}) %collective-permute-start.2) | collective-permute-done | bytes 67616 | tf_op jit(solution)/shard_map/ppermute | solution.py:288
  37.2 0.0 collective-permute-done.11.refs_9_
  37.2 0.0 collective-permute-done.5.refs_6_
  37.3 1.8 %shard_map.125 = (f32[4,8,128]{2,1,0:T(8,128)S(1)}, f32[4,8,128]{2,1,0:T(8,128)S(1)}, f32[32,128]{1,0:T(8,128)S(1)}, f32[128,32]{1,0:T(8,128)S(1)}, f32[2,1,8]{2,1,0:T(1,128)}) custom-call(bf16[264,128]{1,0:T(8,128)(2,1)S(1)} %get-tuple-element.33.refs_0_, bf16[264,128]{1,0:T(8,128)(2,1)S(1)} %collective-permute-done.refs_1_, ...), custom_call_target="tpu_custom_call" | custom-call | tf_op jit(solution)/shard_map/pallas_call | solution.py:111
  39.1 1.2 %collective-permute-done.12.got_ref = f32[4,8,128]{2,1,0:T(8,128)S(1)} collective-permute-done((f32[4,8,128]{2,1,0:T(8,128)S(1)}, f32[4,8,128]{2,1,0:T(8,128)S(1)}, u32[]{:S(2)}, u32[]{:S(2)}) %collective-permute-start.12) | collective-permute-done | bytes 16416 | tf_op jit(solution)/shard_map/ppermute | solution.py:293
  40.2 1.5 %collective-permute-start.13 = (f32[8,128]{1,0:T(8,128)S(1)}, f32[8,128]{1,0:T(8,128)S(1)}, u32[]{:S(2)}, u32[]{:S(2)}) collective-permute-start(f32[8,128]{1,0:T(8,128)S(1)} %get-tuple-element.53), channel_id=1, source_target_pairs={{0,2},{2,4},{4,6},{6,0},{1,3},{3,5},{5,7},{7,1},{8,10},{10,12},{12... | collective-permute-start | bytes 12296 | tf_op jit(solution)/shard_map/ppermute | solution.py:293
  41.7 2.7 %collective-permute-start.14 = (f32[8,128]{1,0:T(8,128)S(1)}, f32[8,128]{1,0:T(8,128)S(1)}, u32[]{:S(2)}, u32[]{:S(2)}) collective-permute-start(f32[8,128]{1,0:T(8,128)S(1)} %get-tuple-element.54), channel_id=1, source_target_pairs={{0,4},{2,6},{4,0},{6,2},{1,5},{3,7},{5,1},{7,3},{8,12},{10,14},{12... | collective-permute-start | bytes 12296 | tf_op jit(solution)/shard_map/ppermute | solution.py:293
  44.5 1.4 %collective-permute-start.15 = (f32[8,128]{1,0:T(8,128)S(1)}, f32[8,128]{1,0:T(8,128)S(1)}, u32[]{:S(2)}, u32[]{:S(2)}) collective-permute-start(f32[8,128]{1,0:T(8,128)S(1)} %get-tuple-element.55), channel_id=1, source_target_pairs={{0,6},{2,0},{4,2},{6,4},{1,7},{3,1},{5,3},{7,5},{8,14},{10,8},{12,... | collective-permute-start | bytes 12296 | tf_op jit(solution)/shard_map/ppermute | solution.py:293
  45.9 1.1 %shard_map.126 = (bf16[16,128,256]{2,1,0:T(8,128)(2,1)S(1)}, f32[16,128]{1,0:T(8,128)}) custom-call(bf16[264,128]{1,0:T(8,128)(2,1)S(1)} %get-tuple-element.33.refs_0_, bf16[264,128]{1,0:T(8,128)(2,1)S(1)} %collective-permute-done.refs_1_, bf16[264,128]{1,0:T(8,128)(2,1)S(1)} %collective-permute-done.1.refs_2_, ...), custom_call_target="tpu_custom_call" | custom-call | tf_op jit(solution)/shard_map/pallas_call | solution.py:111
  47.0 1.2 %shard_map.127 = bf16[2,8,128,128]{3,2,1,0:T(8,128)(2,1)} custom-call(bf16[264,128]{1,0:T(8,128)(2,1)S(1)} %get-tuple-element.33.refs_0_, bf16[264,128]{1,0:T(8,128)(2,1)S(1)} %collective-permute-done.refs_1_, bf16[264,128]{1,0:T(8,128)(2,1)S(1)} %collective-permute-done.1.refs_2_, bf16[264,128]{1,0:T(8,128)(2,1)S(1)} %collective-permute-done.2.refs_3_, ...), custom_call_target="tpu_custom_call" | custom-call | tf_op jit(solution)/shard_map/pallas_call | solution.py:111
  48.1 0.6 %shard_map.129 = bf16[8,128]{1,0:T(8,128)(2,1)} custom-call(f32[8,128]{1,0:T(8,128)S(1)} %get-tuple-element.52.a_ref, f32[8,128]{1,0:T(8,128)S(1)} %collective-permute-done.13.b_ref, f32[8,128]{1,0:T(8,128)S(1)} %collective-permute-done.14.c_ref, f32[8,128]{1,0:T(8,128)S(1)} %collective-permute-done.15.d_ref), custom_call_target="tpu_custom_call" | custom-call | tf_op jit(solution)/shard_map/pallas_call | solution.py:111
  (19 shorter events, 0.1 us)
Async XLA Ops:
  3.8 19.0 %collective-permute-start.4 = (bf16[4,264,128]{2,1,0:T(8,128)(2,1)S(1)}, bf16[4,264,128]{2,1,0:T(8,128)(2,1)S(1)}, u32[]{:S(2)}, u32[]{:S(2)}) collective-permute-start(bf16[4,264,128]{2,1,0:T(8,128)(2,1)S(1)} %shard_map.121), channel_id=1, source_target_pairs={{0,32},{8,40},{16,48},{24,56},{32,0},{40,8},{48,16},{56,24},{64,96... | collective-permute-start | bytes 811016 | tf_op jit(solution)/shard_map/ppermute | solution.py:288
  5.8 31.4 %copy-start = (bf16[1,128,1024]{2,1,0:T(8,128)(2,1)S(1)}, bf16[1,128,1024]{2,1,0:T(8,128)(2,1)}, u32[]{:S(2)}) copy-start(bf16[1,128,1024]{2,1,0:T(8,128)(2,1)} %param.17) | copy-start | bytes 786436
  5.8 31.4 %copy-start.1 = (bf16[8,1,128]{2,0,1:T(8,128)(2,1)S(1)}, bf16[8,1,128]{2,0,1:T(8,128)(2,1)}, u32[]{:S(2)}) copy-start(bf16[8,1,128]{2,0,1:T(8,128)(2,1)} %param.16) | copy-start | bytes 6148
  5.8 31.4 %copy-start.2 = (f32[2,1]{0,1:T(1,128)S(1)}, f32[2,1]{0,1:T(1,128)}, u32[]{:S(2)}) copy-start(f32[2,1]{0,1:T(1,128)} %param.14) | copy-start | bytes 28
  5.9 31.4 %copy-start.3 = (f32[2,1]{0,1:T(1,128)S(1)}, f32[2,1]{0,1:T(1,128)}, u32[]{:S(2)}) copy-start(f32[2,1]{0,1:T(1,128)} %param.15) | copy-start | bytes 28
  5.9 21.0 %collective-permute-start.3 = (bf16[4,264,128]{2,1,0:T(8,128)(2,1)S(1)}, bf16[4,264,128]{2,1,0:T(8,128)(2,1)S(1)}, u32[]{:S(2)}, u32[]{:S(2)}) collective-permute-start(bf16[4,264,128]{2,1,0:T(8,128)(2,1)S(1)} %get-tuple-element.37), channel_id=1, source_target_pairs={{0,96},{8,104},{16,112},{24,120},{32,64},{40,72},{48,80},{56,88},{... | collective-permute-start | bytes 811016 | tf_op jit(solution)/shard_map/ppermute | solution.py:288
  6.7 6.3 %collective-permute-start.8 = (bf16[264,128]{1,0:T(8,128)(2,1)S(1)}, bf16[264,128]{1,0:T(8,128)(2,1)S(1)}, u32[]{:S(2)}, u32[]{:S(2)}) collective-permute-start(bf16[264,128]{1,0:T(8,128)(2,1)S(1)} %get-tuple-element.42), channel_id=1, source_target_pairs={{0,8},{8,16},{16,24},{24,0},{32,40},{40,48},{48,56},{56,32},{64,72... | collective-permute-start | bytes 202760 | tf_op jit(solution)/shard_map/ppermute | solution.py:288
  8.3 5.9 %collective-permute-start.9 = (bf16[264,128]{1,0:T(8,128)(2,1)S(1)}, bf16[264,128]{1,0:T(8,128)(2,1)S(1)}, u32[]{:S(2)}, u32[]{:S(2)}) collective-permute-start(bf16[264,128]{1,0:T(8,128)(2,1)S(1)} %get-tuple-element.43), channel_id=1, source_target_pairs={{0,16},{8,24},{16,0},{24,8},{32,48},{40,56},{48,32},{56,40},{64,80... | collective-permute-start | bytes 202760 | tf_op jit(solution)/shard_map/ppermute | solution.py:288
  11.2 4.3 %collective-permute-start.10 = (bf16[264,128]{1,0:T(8,128)(2,1)S(1)}, bf16[264,128]{1,0:T(8,128)(2,1)S(1)}, u32[]{:S(2)}, u32[]{:S(2)}) collective-permute-start(bf16[264,128]{1,0:T(8,128)(2,1)S(1)} %get-tuple-element.44), channel_id=1, source_target_pairs={{0,24},{8,0},{16,8},{24,16},{32,56},{40,32},{48,40},{56,48},{64,88... | collective-permute-start | bytes 202760 | tf_op jit(solution)/shard_map/ppermute | solution.py:288
  15.5 21.7 %collective-permute-start.11 = (bf16[4,264,128]{2,1,0:T(8,128)(2,1)S(1)}, bf16[4,264,128]{2,1,0:T(8,128)(2,1)S(1)}, u32[]{:S(2)}, u32[]{:S(2)}) collective-permute-start(bf16[4,264,128]{2,1,0:T(8,128)(2,1)S(1)} %shard_map.124), channel_id=1, source_target_pairs={{0,64},{8,72},{16,80},{24,88},{32,96},{40,104},{48,112},{56,120},{... | collective-permute-start | bytes 811016 | tf_op jit(solution)/shard_map/ppermute | solution.py:288
  18.8 12.7 %collective-permute-start = (bf16[264,128]{1,0:T(8,128)(2,1)S(1)}, bf16[264,128]{1,0:T(8,128)(2,1)S(1)}, u32[]{:S(2)}, u32[]{:S(2)}) collective-permute-start(bf16[264,128]{1,0:T(8,128)(2,1)S(1)} %get-tuple-element.34), channel_id=1, source_target_pairs={{0,8},{8,16},{16,24},{24,0},{32,40},{40,48},{48,56},{56,32},{64,72... | collective-permute-start | bytes 202760 | tf_op jit(solution)/shard_map/ppermute | solution.py:288
  19.2 13.6 %collective-permute-start.1 = (bf16[264,128]{1,0:T(8,128)(2,1)S(1)}, bf16[264,128]{1,0:T(8,128)(2,1)S(1)}, u32[]{:S(2)}, u32[]{:S(2)}) collective-permute-start(bf16[264,128]{1,0:T(8,128)(2,1)S(1)} %get-tuple-element.35), channel_id=1, source_target_pairs={{0,16},{8,24},{16,0},{24,8},{32,48},{40,56},{48,32},{56,40},{64,80... | collective-permute-start | bytes 202760 | tf_op jit(solution)/shard_map/ppermute | solution.py:288
  26.9 10.3 %collective-permute-start.5 = (bf16[2,264,128]{2,1,0:T(8,128)(2,1)S(1)}, bf16[2,264,128]{2,1,0:T(8,128)(2,1)S(1)}, u32[]{:S(2)}, u32[]{:S(2)}) collective-permute-start(bf16[2,264,128]{2,1,0:T(8,128)(2,1)S(1)} %get-tuple-element.38), channel_id=1, source_target_pairs={{0,8},{8,16},{16,24},{24,0},{32,40},{40,48},{48,56},{56,32},{64,72... | collective-permute-start | bytes 405512 | tf_op jit(solution)/shard_map/ppermute | solution.py:288
  28.6 8.7 %collective-permute-start.6 = (bf16[2,264,128]{2,1,0:T(8,128)(2,1)S(1)}, bf16[2,264,128]{2,1,0:T(8,128)(2,1)S(1)}, u32[]{:S(2)}, u32[]{:S(2)}) collective-permute-start(bf16[2,264,128]{2,1,0:T(8,128)(2,1)S(1)} %get-tuple-element.39), channel_id=1, source_target_pairs={{0,16},{8,24},{16,0},{24,8},{32,48},{40,56},{48,32},{56,40},{64,80... | collective-permute-start | bytes 405512 | tf_op jit(solution)/shard_map/ppermute | solution.py:288
  31.5 5.8 %collective-permute-start.7 = (bf16[2,264,128]{2,1,0:T(8,128)(2,1)S(1)}, bf16[2,264,128]{2,1,0:T(8,128)(2,1)S(1)}, u32[]{:S(2)}, u32[]{:S(2)}) collective-permute-start(bf16[2,264,128]{2,1,0:T(8,128)(2,1)S(1)} %get-tuple-element.40), channel_id=1, source_target_pairs={{0,24},{8,0},{16,8},{24,16},{32,56},{40,32},{48,40},{56,48},{64,88... | collective-permute-start | bytes 405512 | tf_op jit(solution)/shard_map/ppermute | solution.py:288
  32.8 4.4 %collective-permute-start.2 = (bf16[264,128]{1,0:T(8,128)(2,1)S(1)}, bf16[264,128]{1,0:T(8,128)(2,1)S(1)}, u32[]{:S(2)}, u32[]{:S(2)}) collective-permute-start(bf16[264,128]{1,0:T(8,128)(2,1)S(1)} %get-tuple-element.36), channel_id=1, source_target_pairs={{0,24},{8,0},{16,8},{24,16},{32,56},{40,32},{48,40},{56,48},{64,88... | collective-permute-start | bytes 202760 | tf_op jit(solution)/shard_map/ppermute | solution.py:288
  39.0 1.2 %collective-permute-start.12 = (f32[4,8,128]{2,1,0:T(8,128)S(1)}, f32[4,8,128]{2,1,0:T(8,128)S(1)}, u32[]{:S(2)}, u32[]{:S(2)}) collective-permute-start(f32[4,8,128]{2,1,0:T(8,128)S(1)} %get-tuple-element.51), channel_id=1, source_target_pairs={{0,1},{1,0},{2,3},{3,2},{4,5},{5,4},{6,7},{7,6},{8,9},{9,8},{10,11... | collective-permute-start | bytes 49160 | tf_op jit(solution)/shard_map/ppermute | solution.py:293
  40.2 7.9 %collective-permute-start.13 = (f32[8,128]{1,0:T(8,128)S(1)}, f32[8,128]{1,0:T(8,128)S(1)}, u32[]{:S(2)}, u32[]{:S(2)}) collective-permute-start(f32[8,128]{1,0:T(8,128)S(1)} %get-tuple-element.53), channel_id=1, source_target_pairs={{0,2},{2,4},{4,6},{6,0},{1,3},{3,5},{5,7},{7,1},{8,10},{10,12},{12... | collective-permute-start | bytes 12296 | tf_op jit(solution)/shard_map/ppermute | solution.py:293
  41.7 6.4 %collective-permute-start.14 = (f32[8,128]{1,0:T(8,128)S(1)}, f32[8,128]{1,0:T(8,128)S(1)}, u32[]{:S(2)}, u32[]{:S(2)}) collective-permute-start(f32[8,128]{1,0:T(8,128)S(1)} %get-tuple-element.54), channel_id=1, source_target_pairs={{0,4},{2,6},{4,0},{6,2},{1,5},{3,7},{5,1},{7,3},{8,12},{10,14},{12... | collective-permute-start | bytes 12296 | tf_op jit(solution)/shard_map/ppermute | solution.py:293
  44.5 3.7 %collective-permute-start.15 = (f32[8,128]{1,0:T(8,128)S(1)}, f32[8,128]{1,0:T(8,128)S(1)}, u32[]{:S(2)}, u32[]{:S(2)}) collective-permute-start(f32[8,128]{1,0:T(8,128)S(1)} %get-tuple-element.55), channel_id=1, source_target_pairs={{0,6},{2,0},{4,2},{6,4},{1,7},{3,1},{5,3},{7,5},{8,14},{10,8},{12,... | collective-permute-start | bytes 12296 | tf_op jit(solution)/shard_map/ppermute | solution.py:293

commit v12 on v11

--- a/solution.py
+++ b/solution.py
@@ -64,7 +64,7 @@
     for copy in (*gate_copies, key_copy, value_copy):
         copy.start()
     copies = take(x_ref, buf_ref, sem_ref, 0, [(3, dy) for dy in range(ROW)])
-    later = take(x_ref, rest_ref, sem_ref, ROW, [(dz, dy) for dz in (1, 2, 0) for dy in range(ROW)])
+    later = take(x_ref, rest_ref, sem_ref, ROW, [(dz, dy) for dz in (1, 2) for dy in range(ROW)])
     for copy in gate_copies:
         copy.wait()
     gates = jnp.concatenate((wi_buf[...].astype(F32), wf_buf[...].astype(F32), jnp.zeros((4, D), F32)), axis=0)
@@ -86,8 +86,11 @@
     project_blocks(rest_ref, ROW, w_ref[...], g_ref[...], outs)
 
 
-def own_kernel(rest_ref, w_ref, g_ref, *outs):
-    project_blocks(rest_ref, 2 * ROW, w_ref[...], g_ref[...], outs)
+def own_kernel(x_ref, w_ref, g_ref, *refs):
+    outs, (buf_ref, sem_ref) = refs[:ROW], refs[ROW:]
+    for copy in take(x_ref, buf_ref, sem_ref, 0, [(0, dy) for dy in range(ROW)]):
+        copy.wait()
+    project_blocks(buf_ref, 0, w_ref[...], g_ref[...], outs)
 
 
 ANY = pl.BlockSpec(memory_space=pl.ANY)
@@ -124,7 +127,7 @@
         in_specs=[ANY] * 5,
         out_specs=[VM] * 4,
         out_shape=(
-            block(ROW), pltpu.VMEM((D, 2 * HD), BF), pltpu.VMEM((8, D), BF), pltpu.VMEM((3 * ROW, OWN, POS, D), BF)
+            block(ROW), pltpu.VMEM((D, 2 * HD), BF), pltpu.VMEM((8, D), BF), pltpu.VMEM((2 * ROW, OWN, POS, D), BF)
         ),
         scratch_shapes=[
             pltpu.VMEM((ROW, OWN, POS, D), BF), pltpu.VMEM((2, D), BF), pltpu.VMEM((2, D), BF),
@@ -135,6 +138,18 @@
     )(*[pltpu.with_memory_space_constraint(a, pltpu.HBM) for a in args])
 
 
+def project_own(prompt, w, gates):
+    return pl.pallas_call(
+        own_kernel,
+        in_specs=[ANY, VM, VM],
+        out_specs=[VM] * ROW,
+        out_shape=(block(),) * ROW,
+        scratch_shapes=[pltpu.VMEM((ROW, OWN, POS, D), BF), pltpu.SemaphoreType.DMA((ROW,))],
+        compiler_params=grant(16),
+        name="own",
+    )(pltpu.with_memory_space_constraint(prompt, pltpu.HBM), vm(w), vm(gates))
+
+
 def gather_kernel(*refs):
     for i in range(ROW):
         refs[ROW][i] = refs[i][...]
@@ -188,7 +203,10 @@
     scale = HD ** -0.5
     row, lane8, mine = rows_mine()
     query = q_ref[...]
-    scores = [jnp.where(mine, dot(query, blk[:ROWS, :], ((1,), (1,))), 0.0) for blk in blocks]
+    scores = []
+    for a, b in zip(blocks[::2], blocks[1::2]):
+        both = dot(query, jnp.concatenate((a[:ROWS, :], b[:ROWS, :]), axis=0), ((1,), (1,)))
+        scores += [jnp.where(mine, both[:, :HD], 0.0), jnp.where(mine, both[:, HD:], 0.0)]
 
     gates = jnp.stack([blk[2 * ROWS :, :].astype(F32) for blk in blocks])
     part = lambda c: gates[:, c, :] + gates[:, c + 4, :]
@@ -224,10 +242,14 @@
 
     shares = jnp.zeros((2 * OWN, HD), F32)
     numerator = jnp.zeros((4 * OWN, HD), F32)
-    for j, blk in enumerate(blocks):
-        share = jnp.concatenate([scores[j] * weight[g * SP + j : g * SP + j + 1] for g in range(2)], axis=0)
-        shares += share
-        numerator += dot(two_parts(share), blk[ROWS : 2 * ROWS, :])
+    for j in range(0, SP, 2):
+        pair = [
+            jnp.concatenate([scores[i] * weight[g * SP + i : g * SP + i + 1] for g in range(2)], axis=0)
+            for i in (j, j + 1)
+        ]
+        shares += pair[0] + pair[1]
+        values = jnp.concatenate([blocks[i][ROWS : 2 * ROWS, :] for i in (j, j + 1)], axis=0)
+        numerator += dot(jnp.concatenate([two_parts(share) for share in pair], axis=1), values)
     numerator = (numerator[: 2 * OWN] + numerator[2 * OWN :]) * scale
     denominator = jnp.sum(shares, axis=1, keepdims=True) * scale
     hidden = jnp.zeros((OWN, HD), F32)
@@ -305,7 +327,7 @@
     cross = [cross[0]] + [shift(cross[k], 0, k) for k in hops]
     far = run(gather_kernel, block(ROW), cross, 4)
     far = shift(far, 2, 0)
-    own = run(own_kernel, (block(),) * ROW, (later, w, gates))
+    own = project_own(prompt, w, gates)
     own = [own[0]] + [shift(own[k], 0, k) for k in hops]
     side = run(pair_kernel, (block(2),) * 3, (mirror, twin), 4)
     side = [shift(blocks, 0, k) for k, blocks in zip(hops, side)]

time: 48.8 us -> 48.6 us (level)
  waiting for transfers between devices: 12.5 us -> 11.2 us
  Pallas kernels: 9.24 us -> 10.2 us
    pallas_call x0 -> x1, Pallas kernels: none -> 1.93 us  [project_own(): pl.pallas_call(own_kernel, in_specs=[ANY, VM, VM], out_specs=[VM] * ROW,...]
    ppermute x12, waiting for transfers between devices: 11.3 us -> 10 us  [shift(): return lax.ppermute(array, 'sp', pairs)]
    pallas_call x10 -> x9, Pallas kernels: 6.73 us -> 5.99 us  [run(): pl.pallas_call(kernel, in_specs=[VM] * len(args), out_specs=specs, out_sh...]
  transfers between devices with their start and end apart: 16 -> 16, of which waited for: 6 -> 6; matrix products, arithmetic and copies ran while one was open for 0% -> 0% of each run, Pallas kernels for 8% -> 10%
where the time goes in v12:
time: 48.6 us; the launch traced here: 48.5 us
  starting transfers between devices  26.3 us (54%)
  waiting for transfers between devices  11.2 us (23%)
  Pallas kernels  10.2 us (21%)
  between operations  0.74 us (2%)
    ppermute x12, starting transfers between devices, shift(): return lax.ppermute(array, 'sp', pairs)  20.6 us
    ppermute x12, waiting for transfers between devices, shift(): return lax.ppermute(array, 'sp', pairs)  10 us
    pallas_call x9, Pallas kernels, run(): pl.pallas_call(kernel, in_specs=[VM] * len(args), out_specs=specs, out_sh...  5.99 us
    ppermute x4, starting transfers between devices, across(): lax.ppermute(array, axis, [(i, (i + hop) % size) for i in range(size)])  5.67 us
    pallas_call x1, Pallas kernels, project_near(): pl.pallas_call(near_kernel, in_specs=[ANY] * 5, out_specs=[VM] * 4, out_s...  2.26 us
    pallas_call x1, Pallas kernels, project_own(): pl.pallas_call(own_kernel, in_specs=[ANY, VM, VM], out_specs=[VM] * ROW,...  1.93 us
    ppermute x4, waiting for transfers between devices, across(): lax.ppermute(array, axis, [(i, (i + hop) % size) for i in range(size)])  1.19 us
  transfers between devices with their start and end apart: 16, of which 6 were waited for; matrix products, arithmetic and copies ran while one was open for 0% of the time, Pallas kernels for 10%

profile of v12, /device:TPU:64, one launch (start us, length us, event | category | flops | bytes accessed | tf_op | source)
XLA Modules:
  0.0 48.5 jit_solution(18380079356582151268)
XLA Ops:
  0.6 2.3 %near.1 = (bf16[4,264,128]{2,1,0:T(8,128)(2,1)S(1)}, bf16[1024,256]{1,0:T(8,128)(2,1)S(1)}, bf16[8,1024]{1,0:T(8,128)(2,1)S(1)}, bf16[8,8,16,1024]{3,2,1,0:T(8,128)(2,1)S(1)}) custom-call(bf16[128,16,1024]{2,1,0:T(8,128)(2,1)} %x_ref.3, bf16[1024,128]{1,0:T(8,128)(2,1)} %bitcast.22, bf16[1024,128]{1,0:T(8,128)(2,1)} %bitcast.23, bf16[2,1024]{1,0:T(2,128)(2,1)} %bitcast.24, ...), custom_call_target="tpu_custom_call" | custom-call | tf_op jit(solution)/shard_map/near/pallas_call | solution.py:125
  2.9 0.7 %shard_map.120 = bf16[4,264,128]{2,1,0:T(8,128)(2,1)S(1)} custom-call(bf16[8,8,16,1024]{3,2,1,0:T(8,128)(2,1)S(1)} %get-tuple-element.37.rest_ref, bf16[1024,256]{1,0:T(8,128)(2,1)S(1)} %get-tuple-element.30.w_ref, bf16[8,1024]{1,0:T(8,128)(2,1)S(1)} %get-tuple-element.31.g_ref), custom_call_target="tpu_custom_call" | custom-call | tf_op jit(solution)/shard_map/pallas_call | solution.py:114
  3.6 2.0 %collective-permute-start.4 = (bf16[4,264,128]{2,1,0:T(8,128)(2,1)S(1)}, bf16[4,264,128]{2,1,0:T(8,128)(2,1)S(1)}, u32[]{:S(2)}, u32[]{:S(2)}) collective-permute-start(bf16[4,264,128]{2,1,0:T(8,128)(2,1)S(1)} %shard_map.120), channel_id=1, source_target_pairs={{0,32},{8,40},{16,48},{24,56},{32,0},{40,8},{48,16},{56,24},{64,96... | collective-permute-start | bytes 811016 | tf_op jit(solution)/shard_map/ppermute | solution.py:310
  5.6 0.1 collective-permute-start.3
  5.7 0.7 %shard_map.122 = (bf16[264,128]{1,0:T(8,128)(2,1)S(1)}, bf16[264,128]{1,0:T(8,128)(2,1)S(1)}, bf16[264,128]{1,0:T(8,128)(2,1)S(1)}, bf16[264,128]{1,0:T(8,128)(2,1)S(1)}) custom-call(bf16[8,8,16,1024]{3,2,1,0:T(8,128)(2,1)S(1)} %get-tuple-element.37.rest_ref, bf16[1024,256]{1,0:T(8,128)(2,1)S(1)} %get-tuple-element.30.w_ref, ...), custom_call_target="tpu_custom_call" | custom-call | tf_op jit(solution)/shard_map/pallas_call | solution.py:114
  6.4 1.7 %collective-permute-start.8 = (bf16[264,128]{1,0:T(8,128)(2,1)S(1)}, bf16[264,128]{1,0:T(8,128)(2,1)S(1)}, u32[]{:S(2)}, u32[]{:S(2)}) collective-permute-start(bf16[264,128]{1,0:T(8,128)(2,1)S(1)} %get-tuple-element.42), channel_id=1, source_target_pairs={{0,8},{8,16},{16,24},{24,0},{32,40},{40,48},{48,56},{56,32},{64,72... | collective-permute-start | bytes 202760 | tf_op jit(solution)/shard_map/ppermute | solution.py:310
  8.1 2.9 %collective-permute-start.9 = (bf16[264,128]{1,0:T(8,128)(2,1)S(1)}, bf16[264,128]{1,0:T(8,128)(2,1)S(1)}, u32[]{:S(2)}, u32[]{:S(2)}) collective-permute-start(bf16[264,128]{1,0:T(8,128)(2,1)S(1)} %get-tuple-element.43), channel_id=1, source_target_pairs={{0,16},{8,24},{16,0},{24,8},{32,48},{40,56},{48,32},{56,40},{64,80... | collective-permute-start | bytes 202760 | tf_op jit(solution)/shard_map/ppermute | solution.py:310
  11.0 1.3 %collective-permute-start.10 = (bf16[264,128]{1,0:T(8,128)(2,1)S(1)}, bf16[264,128]{1,0:T(8,128)(2,1)S(1)}, u32[]{:S(2)}, u32[]{:S(2)}) collective-permute-start(bf16[264,128]{1,0:T(8,128)(2,1)S(1)} %get-tuple-element.44), channel_id=1, source_target_pairs={{0,24},{8,0},{16,8},{24,16},{32,56},{40,32},{48,40},{56,48},{64,88... | collective-permute-start | bytes 202760 | tf_op jit(solution)/shard_map/ppermute | solution.py:310
  12.3 0.4 collective-permute-done.8.refs_1_
  12.7 1.3 %collective-permute-done.9.refs_2_ = bf16[264,128]{1,0:T(8,128)(2,1)S(1)} collective-permute-done((bf16[264,128]{1,0:T(8,128)(2,1)S(1)}, bf16[264,128]{1,0:T(8,128)(2,1)S(1)}, u32[]{:S(2)}, u32[]{:S(2)}) %collective-permute-start.9) | collective-permute-done | bytes 67616 | tf_op jit(solution)/shard_map/ppermute | solution.py:310
  14.0 1.3 %collective-permute-done.10.refs_3_ = bf16[264,128]{1,0:T(8,128)(2,1)S(1)} collective-permute-done((bf16[264,128]{1,0:T(8,128)(2,1)S(1)}, bf16[264,128]{1,0:T(8,128)(2,1)S(1)}, u32[]{:S(2)}, u32[]{:S(2)}) %collective-permute-start.10) | collective-permute-done | bytes 67616 | tf_op jit(solution)/shard_map/ppermute | solution.py:310
  15.3 2.5 %collective-permute-start.11 = (bf16[4,264,128]{2,1,0:T(8,128)(2,1)S(1)}, bf16[4,264,128]{2,1,0:T(8,128)(2,1)S(1)}, u32[]{:S(2)}, u32[]{:S(2)}) collective-permute-start(bf16[4,264,128]{2,1,0:T(8,128)(2,1)S(1)} %shard_map.123), channel_id=1, source_target_pairs={{0,64},{8,72},{16,80},{24,88},{32,96},{40,104},{48,112},{56,120},{... | collective-permute-start | bytes 811016 | tf_op jit(solution)/shard_map/ppermute | solution.py:310
  17.8 1.9 %own.1 = (bf16[264,128]{1,0:T(8,128)(2,1)S(1)}, bf16[264,128]{1,0:T(8,128)(2,1)S(1)}, bf16[264,128]{1,0:T(8,128)(2,1)S(1)}, bf16[264,128]{1,0:T(8,128)(2,1)S(1)}) custom-call(bf16[128,16,1024]{2,1,0:T(8,128)(2,1)} %x_ref.3, bf16[1024,256]{1,0:T(8,128)(2,1)S(1)} %get-tuple-element.30.w_ref, bf16[8,1024]{1,0:T(8,128)(2,1)S(1)} %get-tuple-element.31.g_ref), custom_call_target="tpu_custom_call" | custom-call | tf_op jit(solution)/shard_map/own/pallas_call | solution.py:142
  19.8 0.4 collective-permute-start
  20.2 3.7 %collective-permute-start.1 = (bf16[264,128]{1,0:T(8,128)(2,1)S(1)}, bf16[264,128]{1,0:T(8,128)(2,1)S(1)}, u32[]{:S(2)}, u32[]{:S(2)}) collective-permute-start(bf16[264,128]{1,0:T(8,128)(2,1)S(1)} %get-tuple-element.34), channel_id=1, source_target_pairs={{0,16},{8,24},{16,0},{24,8},{32,48},{40,56},{48,32},{56,40},{64,80... | collective-permute-start | bytes 202760 | tf_op jit(solution)/shard_map/ppermute | solution.py:310
  23.9 0.0 collective-permute-done.4.b_ref.refs_5_
  23.9 2.8 %collective-permute-done.3.a_ref.refs_4_ = bf16[4,264,128]{2,1,0:T(8,128)(2,1)S(1)} collective-permute-done((bf16[4,264,128]{2,1,0:T(8,128)(2,1)S(1)}, bf16[4,264,128]{2,1,0:T(8,128)(2,1)S(1)}, u32[]{:S(2)}, u32[]{:S(2)}) %collective-permute-start.3) | collective-permute-done | bytes 270368 | tf_op jit(solution)/shard_map/ppermute | solution.py:310
  26.7 1.6 %collective-permute-start.5 = (bf16[2,264,128]{2,1,0:T(8,128)(2,1)S(1)}, bf16[2,264,128]{2,1,0:T(8,128)(2,1)S(1)}, u32[]{:S(2)}, u32[]{:S(2)}) collective-permute-start(bf16[2,264,128]{2,1,0:T(8,128)(2,1)S(1)} %get-tuple-element.38), channel_id=1, source_target_pairs={{0,8},{8,16},{16,24},{24,0},{32,40},{40,48},{48,56},{56,32},{64,72... | collective-permute-start | bytes 405512 | tf_op jit(solution)/shard_map/ppermute | solution.py:310
  28.3 2.9 %collective-permute-start.6 = (bf16[2,264,128]{2,1,0:T(8,128)(2,1)S(1)}, bf16[2,264,128]{2,1,0:T(8,128)(2,1)S(1)}, u32[]{:S(2)}, u32[]{:S(2)}) collective-permute-start(bf16[2,264,128]{2,1,0:T(8,128)(2,1)S(1)} %get-tuple-element.39), channel_id=1, source_target_pairs={{0,16},{8,24},{16,0},{24,8},{32,48},{40,56},{48,32},{56,40},{64,80... | collective-permute-start | bytes 405512 | tf_op jit(solution)/shard_map/ppermute | solution.py:310
  31.2 0.0 collective-permute-done.refs_1_
  31.2 1.3 %collective-permute-start.7 = (bf16[2,264,128]{2,1,0:T(8,128)(2,1)S(1)}, bf16[2,264,128]{2,1,0:T(8,128)(2,1)S(1)}, u32[]{:S(2)}, u32[]{:S(2)}) collective-permute-start(bf16[2,264,128]{2,1,0:T(8,128)(2,1)S(1)} %get-tuple-element.40), channel_id=1, source_target_pairs={{0,24},{8,0},{16,8},{24,16},{32,56},{40,32},{48,40},{56,48},{64,88... | collective-permute-start | bytes 405512 | tf_op jit(solution)/shard_map/ppermute | solution.py:310
  32.6 0.0 collective-permute-done.1.refs_2_
  32.6 0.1 collective-permute-start.2
  32.7 4.3 %collective-permute-done.2.refs_3_ = bf16[264,128]{1,0:T(8,128)(2,1)S(1)} collective-permute-done((bf16[264,128]{1,0:T(8,128)(2,1)S(1)}, bf16[264,128]{1,0:T(8,128)(2,1)S(1)}, u32[]{:S(2)}, u32[]{:S(2)}) %collective-permute-start.2) | collective-permute-done | bytes 67616 | tf_op jit(solution)/shard_map/ppermute | solution.py:310
  37.0 1.7 %shard_map.124 = (f32[4,8,128]{2,1,0:T(8,128)S(1)}, f32[4,8,128]{2,1,0:T(8,128)S(1)}, f32[32,128]{1,0:T(8,128)S(1)}, f32[128,32]{1,0:T(8,128)S(1)}, f32[2,1,8]{2,1,0:T(1,128)}) custom-call(bf16[264,128]{1,0:T(8,128)(2,1)S(1)} %get-tuple-element.32.refs_0_, bf16[264,128]{1,0:T(8,128)(2,1)S(1)} %collective-permute-done.refs_1_, ...), custom_call_target="tpu_custom_call" | custom-call | tf_op jit(solution)/shard_map/pallas_call | solution.py:114
  38.8 1.2 %collective-permute-done.12.got_ref = f32[4,8,128]{2,1,0:T(8,128)S(1)} collective-permute-done((f32[4,8,128]{2,1,0:T(8,128)S(1)}, f32[4,8,128]{2,1,0:T(8,128)S(1)}, u32[]{:S(2)}, u32[]{:S(2)}) %collective-permute-start.12) | collective-permute-done | bytes 16416 | tf_op jit(solution)/shard_map/ppermute | solution.py:315
  40.0 1.5 %collective-permute-start.13 = (f32[8,128]{1,0:T(8,128)S(1)}, f32[8,128]{1,0:T(8,128)S(1)}, u32[]{:S(2)}, u32[]{:S(2)}) collective-permute-start(f32[8,128]{1,0:T(8,128)S(1)} %get-tuple-element.53), channel_id=1, source_target_pairs={{0,2},{2,4},{4,6},{6,0},{1,3},{3,5},{5,7},{7,1},{8,10},{10,12},{12... | collective-permute-start | bytes 12296 | tf_op jit(solution)/shard_map/ppermute | solution.py:315
  41.5 2.7 %collective-permute-start.14 = (f32[8,128]{1,0:T(8,128)S(1)}, f32[8,128]{1,0:T(8,128)S(1)}, u32[]{:S(2)}, u32[]{:S(2)}) collective-permute-start(f32[8,128]{1,0:T(8,128)S(1)} %get-tuple-element.54), channel_id=1, source_target_pairs={{0,4},{2,6},{4,0},{6,2},{1,5},{3,7},{5,1},{7,3},{8,12},{10,14},{12... | collective-permute-start | bytes 12296 | tf_op jit(solution)/shard_map/ppermute | solution.py:315
  44.2 1.4 %collective-permute-start.15 = (f32[8,128]{1,0:T(8,128)S(1)}, f32[8,128]{1,0:T(8,128)S(1)}, u32[]{:S(2)}, u32[]{:S(2)}) collective-permute-start(f32[8,128]{1,0:T(8,128)S(1)} %get-tuple-element.55), channel_id=1, source_target_pairs={{0,6},{2,0},{4,2},{6,4},{1,7},{3,1},{5,3},{7,5},{8,14},{10,8},{12,... | collective-permute-start | bytes 12296 | tf_op jit(solution)/shard_map/ppermute | solution.py:315
  45.6 1.1 %shard_map.125 = (bf16[16,128,256]{2,1,0:T(8,128)(2,1)S(1)}, f32[16,128]{1,0:T(8,128)}) custom-call(bf16[264,128]{1,0:T(8,128)(2,1)S(1)} %get-tuple-element.32.refs_0_, bf16[264,128]{1,0:T(8,128)(2,1)S(1)} %collective-permute-done.refs_1_, bf16[264,128]{1,0:T(8,128)(2,1)S(1)} %collective-permute-done.1.refs_2_, ...), custom_call_target="tpu_custom_call" | custom-call | tf_op jit(solution)/shard_map/pallas_call | solution.py:114
  46.7 1.2 %shard_map.126 = bf16[2,8,128,128]{3,2,1,0:T(8,128)(2,1)} custom-call(bf16[264,128]{1,0:T(8,128)(2,1)S(1)} %get-tuple-element.32.refs_0_, bf16[264,128]{1,0:T(8,128)(2,1)S(1)} %collective-permute-done.refs_1_, bf16[264,128]{1,0:T(8,128)(2,1)S(1)} %collective-permute-done.1.refs_2_, bf16[264,128]{1,0:T(8,128)(2,1)S(1)} %collective-permute-done.2.refs_3_, ...), custom_call_target="tpu_custom_call" | custom-call | tf_op jit(solution)/shard_map/pallas_call | solution.py:114
  47.9 0.6 %shard_map.128 = bf16[8,128]{1,0:T(8,128)(2,1)} custom-call(f32[8,128]{1,0:T(8,128)S(1)} %get-tuple-element.52.a_ref, f32[8,128]{1,0:T(8,128)S(1)} %collective-permute-done.13.b_ref, f32[8,128]{1,0:T(8,128)S(1)} %collective-permute-done.14.c_ref, f32[8,128]{1,0:T(8,128)S(1)} %collective-permute-done.15.d_ref), custom_call_target="tpu_custom_call" | custom-call | tf_op jit(solution)/shard_map/pallas_call | solution.py:114
  (19 shorter events, 0.1 us)
Async XLA Ops:
  3.6 20.3 %collective-permute-start.4 = (bf16[4,264,128]{2,1,0:T(8,128)(2,1)S(1)}, bf16[4,264,128]{2,1,0:T(8,128)(2,1)S(1)}, u32[]{:S(2)}, u32[]{:S(2)}) collective-permute-start(bf16[4,264,128]{2,1,0:T(8,128)(2,1)S(1)} %shard_map.120), channel_id=1, source_target_pairs={{0,32},{8,40},{16,48},{24,56},{32,0},{40,8},{48,16},{56,24},{64,96... | collective-permute-start | bytes 811016 | tf_op jit(solution)/shard_map/ppermute | solution.py:310
  5.6 31.4 %copy-start = (bf16[1,128,1024]{2,1,0:T(8,128)(2,1)S(1)}, bf16[1,128,1024]{2,1,0:T(8,128)(2,1)}, u32[]{:S(2)}) copy-start(bf16[1,128,1024]{2,1,0:T(8,128)(2,1)} %param.17) | copy-start | bytes 786436
  5.6 31.4 %copy-start.1 = (bf16[8,1,128]{2,0,1:T(8,128)(2,1)S(1)}, bf16[8,1,128]{2,0,1:T(8,128)(2,1)}, u32[]{:S(2)}) copy-start(bf16[8,1,128]{2,0,1:T(8,128)(2,1)} %param.16) | copy-start | bytes 6148
  5.6 31.4 %copy-start.2 = (f32[2,1]{0,1:T(1,128)S(1)}, f32[2,1]{0,1:T(1,128)}, u32[]{:S(2)}) copy-start(f32[2,1]{0,1:T(1,128)} %param.14) | copy-start | bytes 28
  5.6 31.4 %copy-start.3 = (f32[2,1]{0,1:T(1,128)S(1)}, f32[2,1]{0,1:T(1,128)}, u32[]{:S(2)}) copy-start(f32[2,1]{0,1:T(1,128)} %param.15) | copy-start | bytes 28
  5.6 21.0 %collective-permute-start.3 = (bf16[4,264,128]{2,1,0:T(8,128)(2,1)S(1)}, bf16[4,264,128]{2,1,0:T(8,128)(2,1)S(1)}, u32[]{:S(2)}, u32[]{:S(2)}) collective-permute-start(bf16[4,264,128]{2,1,0:T(8,128)(2,1)S(1)} %get-tuple-element.36), channel_id=1, source_target_pairs={{0,96},{8,104},{16,112},{24,120},{32,64},{40,72},{48,80},{56,88},{... | collective-permute-start | bytes 811016 | tf_op jit(solution)/shard_map/ppermute | solution.py:310
  6.4 6.3 %collective-permute-start.8 = (bf16[264,128]{1,0:T(8,128)(2,1)S(1)}, bf16[264,128]{1,0:T(8,128)(2,1)S(1)}, u32[]{:S(2)}, u32[]{:S(2)}) collective-permute-start(bf16[264,128]{1,0:T(8,128)(2,1)S(1)} %get-tuple-element.42), channel_id=1, source_target_pairs={{0,8},{8,16},{16,24},{24,0},{32,40},{40,48},{48,56},{56,32},{64,72... | collective-permute-start | bytes 202760 | tf_op jit(solution)/shard_map/ppermute | solution.py:310
  8.1 5.9 %collective-permute-start.9 = (bf16[264,128]{1,0:T(8,128)(2,1)S(1)}, bf16[264,128]{1,0:T(8,128)(2,1)S(1)}, u32[]{:S(2)}, u32[]{:S(2)}) collective-permute-start(bf16[264,128]{1,0:T(8,128)(2,1)S(1)} %get-tuple-element.43), channel_id=1, source_target_pairs={{0,16},{8,24},{16,0},{24,8},{32,48},{40,56},{48,32},{56,40},{64,80... | collective-permute-start | bytes 202760 | tf_op jit(solution)/shard_map/ppermute | solution.py:310
  11.0 4.3 %collective-permute-start.10 = (bf16[264,128]{1,0:T(8,128)(2,1)S(1)}, bf16[264,128]{1,0:T(8,128)(2,1)S(1)}, u32[]{:S(2)}, u32[]{:S(2)}) collective-permute-start(bf16[264,128]{1,0:T(8,128)(2,1)S(1)} %get-tuple-element.44), channel_id=1, source_target_pairs={{0,24},{8,0},{16,8},{24,16},{32,56},{40,32},{48,40},{56,48},{64,88... | collective-permute-start | bytes 202760 | tf_op jit(solution)/shard_map/ppermute | solution.py:310
  15.3 21.7 %collective-permute-start.11 = (bf16[4,264,128]{2,1,0:T(8,128)(2,1)S(1)}, bf16[4,264,128]{2,1,0:T(8,128)(2,1)S(1)}, u32[]{:S(2)}, u32[]{:S(2)}) collective-permute-start(bf16[4,264,128]{2,1,0:T(8,128)(2,1)S(1)} %shard_map.123), channel_id=1, source_target_pairs={{0,64},{8,72},{16,80},{24,88},{32,96},{40,104},{48,112},{56,120},{... | collective-permute-start | bytes 811016 | tf_op jit(solution)/shard_map/ppermute | solution.py:310
  19.8 11.5 %collective-permute-start = (bf16[264,128]{1,0:T(8,128)(2,1)S(1)}, bf16[264,128]{1,0:T(8,128)(2,1)S(1)}, u32[]{:S(2)}, u32[]{:S(2)}) collective-permute-start(bf16[264,128]{1,0:T(8,128)(2,1)S(1)} %get-tuple-element.33), channel_id=1, source_target_pairs={{0,8},{8,16},{16,24},{24,0},{32,40},{40,48},{48,56},{56,32},{64,72... | collective-permute-start | bytes 202760 | tf_op jit(solution)/shard_map/ppermute | solution.py:310
  20.2 12.4 %collective-permute-start.1 = (bf16[264,128]{1,0:T(8,128)(2,1)S(1)}, bf16[264,128]{1,0:T(8,128)(2,1)S(1)}, u32[]{:S(2)}, u32[]{:S(2)}) collective-permute-start(bf16[264,128]{1,0:T(8,128)(2,1)S(1)} %get-tuple-element.34), channel_id=1, source_target_pairs={{0,16},{8,24},{16,0},{24,8},{32,48},{40,56},{48,32},{56,40},{64,80... | collective-permute-start | bytes 202760 | tf_op jit(solution)/shard_map/ppermute | solution.py:310
  26.7 10.3 %collective-permute-start.5 = (bf16[2,264,128]{2,1,0:T(8,128)(2,1)S(1)}, bf16[2,264,128]{2,1,0:T(8,128)(2,1)S(1)}, u32[]{:S(2)}, u32[]{:S(2)}) collective-permute-start(bf16[2,264,128]{2,1,0:T(8,128)(2,1)S(1)} %get-tuple-element.38), channel_id=1, source_target_pairs={{0,8},{8,16},{16,24},{24,0},{32,40},{40,48},{48,56},{56,32},{64,72... | collective-permute-start | bytes 405512 | tf_op jit(solution)/shard_map/ppermute | solution.py:310
  28.3 8.7 %collective-permute-start.6 = (bf16[2,264,128]{2,1,0:T(8,128)(2,1)S(1)}, bf16[2,264,128]{2,1,0:T(8,128)(2,1)S(1)}, u32[]{:S(2)}, u32[]{:S(2)}) collective-permute-start(bf16[2,264,128]{2,1,0:T(8,128)(2,1)S(1)} %get-tuple-element.39), channel_id=1, source_target_pairs={{0,16},{8,24},{16,0},{24,8},{32,48},{40,56},{48,32},{56,40},{64,80... | collective-permute-start | bytes 405512 | tf_op jit(solution)/shard_map/ppermute | solution.py:310
  31.2 5.8 %collective-permute-start.7 = (bf16[2,264,128]{2,1,0:T(8,128)(2,1)S(1)}, bf16[2,264,128]{2,1,0:T(8,128)(2,1)S(1)}, u32[]{:S(2)}, u32[]{:S(2)}) collective-permute-start(bf16[2,264,128]{2,1,0:T(8,128)(2,1)S(1)} %get-tuple-element.40), channel_id=1, source_target_pairs={{0,24},{8,0},{16,8},{24,16},{32,56},{40,32},{48,40},{56,48},{64,88... | collective-permute-start | bytes 405512 | tf_op jit(solution)/shard_map/ppermute | solution.py:310
  32.6 4.4 %collective-permute-start.2 = (bf16[264,128]{1,0:T(8,128)(2,1)S(1)}, bf16[264,128]{1,0:T(8,128)(2,1)S(1)}, u32[]{:S(2)}, u32[]{:S(2)}) collective-permute-start(bf16[264,128]{1,0:T(8,128)(2,1)S(1)} %get-tuple-element.35), channel_id=1, source_target_pairs={{0,24},{8,0},{16,8},{24,16},{32,56},{40,32},{48,40},{56,48},{64,88... | collective-permute-start | bytes 202760 | tf_op jit(solution)/shard_map/ppermute | solution.py:310
  38.8 1.2 %collective-permute-start.12 = (f32[4,8,128]{2,1,0:T(8,128)S(1)}, f32[4,8,128]{2,1,0:T(8,128)S(1)}, u32[]{:S(2)}, u32[]{:S(2)}) collective-permute-start(f32[4,8,128]{2,1,0:T(8,128)S(1)} %get-tuple-element.51), channel_id=1, source_target_pairs={{0,1},{1,0},{2,3},{3,2},{4,5},{5,4},{6,7},{7,6},{8,9},{9,8},{10,11... | collective-permute-start | bytes 49160 | tf_op jit(solution)/shard_map/ppermute | solution.py:315
  40.0 7.9 %collective-permute-start.13 = (f32[8,128]{1,0:T(8,128)S(1)}, f32[8,128]{1,0:T(8,128)S(1)}, u32[]{:S(2)}, u32[]{:S(2)}) collective-permute-start(f32[8,128]{1,0:T(8,128)S(1)} %get-tuple-element.53), channel_id=1, source_target_pairs={{0,2},{2,4},{4,6},{6,0},{1,3},{3,5},{5,7},{7,1},{8,10},{10,12},{12... | collective-permute-start | bytes 12296 | tf_op jit(solution)/shard_map/ppermute | solution.py:315
  41.5 6.4 %collective-permute-start.14 = (f32[8,128]{1,0:T(8,128)S(1)}, f32[8,128]{1,0:T(8,128)S(1)}, u32[]{:S(2)}, u32[]{:S(2)}) collective-permute-start(f32[8,128]{1,0:T(8,128)S(1)} %get-tuple-element.54), channel_id=1, source_target_pairs={{0,4},{2,6},{4,0},{6,2},{1,5},{3,7},{5,1},{7,3},{8,12},{10,14},{12... | collective-permute-start | bytes 12296 | tf_op jit(solution)/shard_map/ppermute | solution.py:315
  44.2 3.7 %collective-permute-start.15 = (f32[8,128]{1,0:T(8,128)S(1)}, f32[8,128]{1,0:T(8,128)S(1)}, u32[]{:S(2)}, u32[]{:S(2)}) collective-permute-start(f32[8,128]{1,0:T(8,128)S(1)} %get-tuple-element.55), channel_id=1, source_target_pairs={{0,6},{2,0},{4,2},{6,4},{1,7},{3,1},{5,3},{7,5},{8,14},{10,8},{12,... | collective-permute-start | bytes 12296 | tf_op jit(solution)/shard_map/ppermute | solution.py:315
